TPU v7x, 512 devices: a whole 4x4x16 slice. The times are simulated.
512 devices in a mesh: ep: 128 (over z, x, core), tp: 4 (over y).
Axes of the slice: x: 4, y: 4, z: 16, core: 2. Of those that a mesh axis runs over, the one named last changes fastest.
Arguments:
- tokens: bfloat16 [16384, 2048], P('ep'), may hold values from -6 to 6
- norm_gain: float32 [2048], replicated, may hold values from 0.1 to 1.9
- expert_ids: int32 [16384, 2], P('ep'), may hold values from 0 to 31, all different within a row; in each aligned block of 128 rows (0 to 127, 128 to 255, ...) at most 12 rows name the same one
- gate_weights: float32 [16384, 2], P('ep'), may hold values from 0.2 to 1
- w_gate: bfloat16 [2048, 131072], P(None, ('ep', 'tp')), may hold values from -0.125 to 0.125
- w_up: bfloat16 [2048, 131072], P(None, ('ep', 'tp')), may hold values from -0.125 to 0.125
- w_down: bfloat16 [131072, 2048], P('ep', 'tp'), may hold values from -0.09375 to 0.09375
Outputs:
- moe_out: bfloat16 [16384, 2048], P('ep', 'tp')
Inputs may be any that keep to these rules, and one draw needn't show every extreme that they name: `expert_ids`: each token names 2 different experts; in each aligned block of 128 rows no expert is named by more than 12 rows, a bound that some block reaches.
All inputs are finite; a program needn't handle non-finite values.
Results may differ from a plain program's by a relative error of at most 0.0071.
Values may be sent and summed in bfloat16 or wider, within the bound.
No kernel may reach another device: no remote copies, remote signals or barrier semaphores. Data moves between devices by JAX's collectives and lax.ppermute only.
A program may use at most 64 MiB of HBM per device.

v0:
```python
import jax
import jax.numpy as jnp
from jax import lax
from jax.sharding import Mesh
from jax.sharding import PartitionSpec as P

TOP = 2
EP = ("ep_0", "ep_1", "ep_2")
EP_TP = ("ep_0", "ep_1", "ep_2", "tp")


EPS = 1e-06


def split_up(array, dim, length):
    lengths = array.shape
    parts = array.reshape(*lengths[:dim], length, lengths[dim] // length, *lengths[dim + 1 :])
    return jnp.moveaxis(parts, dim, 0)


def laid_out(parts, dim):
    parts = jnp.moveaxis(parts, 0, dim)
    lengths = parts.shape
    return parts.reshape(*lengths[:dim], lengths[dim] * lengths[dim + 1], *lengths[dim + 2 :])


def turned_blocks(parts, axes, sequence):
    inside = parts.shape[1:]
    out = parts.reshape(*(lax.axis_size(a) for a in axes), *inside)
    for k in sequence:
        out = lax.all_to_all(out, axes[k], k, k, tiled=True)
    return out.reshape(-1, *inside)


def exchange_by_chip(array, groups, sequence, split_dim, concat_dim):
    length = lax.axis_size(groups[0]) * lax.axis_size(groups[1])
    parts = split_up(array, split_dim, length)
    return laid_out(turned_blocks(parts, groups, sequence), concat_dim)


def rms_rows(values, gain):
    widened = values.astype(jnp.float32)
    scale = lax.rsqrt(jnp.mean(widened * widened, axis=-1, keepdims=True) + EPS)
    return (widened * scale * gain).astype(jnp.bfloat16)


def on_device(tokens, norm_gain, expert_ids, gate_weights, w_gate, w_up, w_down):
    ep_count = lax.axis_size(EP)
    tp_count = lax.axis_size("tp")
    row_count = tokens.shape[0]
    group_size = max(1, ep_count // 32)
    expert_count = ep_count // group_size
    share = (row_count * TOP * 5 + 4 * expert_count * tp_count - 1) // (4 * expert_count * tp_count)
    capacity = min(row_count, tp_count * share)
    normed = rms_rows(tokens, norm_gain)
    flat_ids = expert_ids.reshape(-1)
    matches = (flat_ids[:, None] == jnp.arange(expert_count, dtype=jnp.int32)[None, :]).astype(
        jnp.int32
    )
    slot_index = jnp.sum((jnp.cumsum(matches, axis=0) - matches) * matches, axis=1)
    position = flat_ids * capacity + slot_index
    placing = (
        position[:, None] == jnp.arange(expert_count * capacity, dtype=jnp.int32)[None, :]
    ).astype(jnp.float32)
    placing = placing.reshape(row_count, TOP, expert_count * capacity)
    selector = jnp.sum(placing, axis=1).astype(jnp.bfloat16)
    buffers = lax.dot_general(
        selector, normed, (((0,), (0,)), ((), ())), preferred_element_type=jnp.float32
    )
    buffers = buffers.astype(jnp.bfloat16).reshape(expert_count, capacity, -1)
    quarter = capacity // tp_count
    mine = lax.dynamic_slice_in_dim(buffers, lax.axis_index("tp") * quarter, quarter, 1)
    copies = jnp.repeat(mine, group_size, axis=0)
    arrived = exchange_by_chip(copies, (("ep_0", "ep_1"), "ep_2"), (1, 0), 0, 0)
    received = lax.all_gather(arrived, "tp", axis=1, tiled=True)
    sources, slot_count, model_width = received.shape
    flat_rows = received.reshape(sources * slot_count, model_width)
    gate_proj = jnp.dot(flat_rows, w_gate, preferred_element_type=jnp.float32)
    upper = jnp.dot(flat_rows, w_up, preferred_element_type=jnp.float32)
    hidden = (jax.nn.silu(gate_proj) * upper).astype(jnp.bfloat16)
    partial_out = jnp.dot(
        lax.all_gather(hidden, "tp", axis=1, tiled=True), w_down, preferred_element_type=jnp.float32
    ).astype(jnp.bfloat16)
    partial_out = partial_out.reshape(sources, slot_count, w_down.shape[1])
    sources, slot_count, out_width = partial_out.shape
    back = exchange_by_chip(partial_out, (("ep_0", "ep_1"), "ep_2"), (1, 0), 0, 0)
    back = back.reshape(expert_count, group_size, slot_count, out_width).astype(jnp.float32)
    returned = jnp.sum(back, axis=1)
    summed = returned.reshape(expert_count * capacity, -1)
    combine = jnp.sum(placing * gate_weights[:, :, None], axis=1)
    mixed = jnp.dot(
        combine, summed, precision=lax.Precision.HIGHEST, preferred_element_type=jnp.float32
    )
    return mixed.astype(jnp.bfloat16)


def solution(mesh):
    finer = Mesh(mesh.devices.reshape(16, 4, 2, mesh.shape["tp"]), ("ep_0", "ep_1", "ep_2", "tp"))
    placed = (
        P(EP, None),
        P(),
        P(EP, None),
        P(EP, None),
        P(None, EP_TP),
        P(None, EP_TP),
        P(EP, "tp"),
    )
    return jax.shard_map(
        on_device, mesh=finer, in_specs=placed, out_specs=P(EP, "tp"), check_vma=False
    )
```

profile of v0, /device:TPU:6, one launch (start us, length us, event | category | flops | bytes accessed | tf_op | source)
XLA Modules:
  0.0 389.8 jit_solution(7729169001689056819)
XLA Ops:
  6.5 0.0 copy-start
  6.5 0.0 all-gather.3.cloned.1.call-start
  6.5 0.9 copy.81
  7.4 0.1 eq.43
  7.6 0.1 eq.39
  7.7 1.2 fusion.1
  9.0 0.6 reduce-window.6
  9.6 0.2 slice_reduce_fusion
  9.8 0.1 fusion.10
  9.9 0.1 reduce_sum.55
  10.1 0.1 copy.84
  10.1 0.7 multiply_add_fusion
  10.8 0.8 convert_reduce_fusion.1
  11.7 0.0 copy-done.2
  11.7 1.4 convolution_convert_fusion.1
  13.1 1.5 reshape.57
  14.6 2.0 constant_dynamic-slice_fusion
  16.6 0.3 copy.85
  16.9 0.5 broadcast_in_dim.6
  17.4 0.3 broadcast_in_dim.14
  17.7 0.2 broadcast_in_dim.15
  17.8 5.0 %all_to_all.20 = bf16[64,2,1,3,2048]{4,0,3,2,1:T(8,128)(2,1)S(1)} all-to-all(bf16[64,2,1,3,2048]{4,0,3,2,1:T(8,128)(2,1)S(1)} %broadcast_in_dim.15), channel_id=1, replica_groups=mesh['ep_0'=16,'ep_1'=4,'ep_2'=2,'tp'=4] {'ep_2'}, dimensions={1} | all-to-all | bytes 3145728 | tf_op jit(solution)/shard_map/all_to_all | solution.py:31
  22.8 1.6 copy.86
  24.5 96.4 %all_to_all.21 = bf16[64,2,1,3,2048]{4,1,3,2,0:T(2,128)(2,1)S(1)} all-to-all(bf16[64,2,1,3,2048]{4,1,3,2,0:T(2,128)(2,1)S(1)} %copy.86), channel_id=1, replica_groups=mesh['ep_0'=16,'ep_1'=4,'ep_2'=2,'tp'=4] {'ep_0','ep_1'}, dimensions={0} | all-to-all | bytes 3145728 | tf_op jit(solution)/shard_map/all_to_all | solution.py:31
  120.8 1.1 copy.87
  122.0 2.0 reshape_reshape.3
  124.0 0.0 all-gather.3.cloned.1.call-update
  124.0 0.2 all-gather.5.cloned.1.call-start
  124.2 65.0 %all-gather.3.cloned.1.call-done = bf16[128,12,2048]{2,0,1:T(8,128)(2,1)} async-done(((bf16[128,3,2048]{2,0,1:T(8,128)(2,1)}), bf16[128,12,2048]{2,0,1:T(8,128)(2,1)}) %all-gather.3.cloned.1.call-update) | async-done | bytes 6291472 | tf_op jit(solution)/shard_map/all_gather | solution.py:75
  189.2 9.7 %copy.88 = bf16[128,12,2048]{2,1,0:T(8,128)(2,1)} copy(bf16[128,12,2048]{2,0,1:T(8,128)(2,1)} %all-gather.3.cloned.1.call-done) | data formatting | bytes 12582912 | tf_op jit(solution)/shard_map/all_gather | solution.py:75
  198.9 10.8 %reshape.58 = bf16[1536,2048]{1,0:T(8,128)(2,1)} reshape(bf16[128,12,2048]{2,1,0:T(8,128)(2,1)} %copy.88) | data formatting | bytes 12582912 | tf_op jit(solution)/shard_map/reshape | solution.py:77
  209.7 0.0 copy-done.3
  209.7 4.8 %fusion.12 = f32[1536,256]{1,0:T(8,128)S(1)} fusion(bf16[1536,2048]{1,0:T(8,128)(2,1)} %reshape.58, bf16[2048,256]{1,0:T(8,128)(2,1)S(1)} %copy-done.3), kind=kOutput, calls=%fused_computation.30 | convolution fusion | flops 1610612736 | bytes 8912896 | tf_op jit(solution)/shard_map/dot_general | solution.py:78
  214.5 0.0 copy-done.4
  214.5 3.0 fusion
  217.5 0.0 all-gather.5.cloned.1.call-update
  217.5 51.2 %all-gather.5.cloned.1.call-done = bf16[1536,1024]{1,0:T(8,128)(2,1)} async-done(((bf16[1536,256]{1,0:T(8,128)(2,1)}), bf16[1536,1024]{1,0:T(8,128)(2,1)}) %all-gather.5.cloned.1.call-update) | async-done | bytes 3145744 | tf_op jit(solution)/shard_map/all_gather | solution.py:82
  268.7 0.0 copy-done
  268.7 4.8 %convolution_convert_fusion = bf16[1536,512]{1,0:T(8,128)(2,1)} fusion(bf16[1536,1024]{1,0:T(8,128)(2,1)} %all-gather.5.cloned.1.call-done, bf16[1024,512]{1,0:T(8,128)(2,1)S(1)} %copy-done), kind=kOutput, calls=%fused_computation.1 | convolution fusion | flops 1611399168 | bytes 5767168 | tf_op jit(solution)/shard_map/dot_general | solution.py:81
  273.6 2.4 reshape_reshape_reshape.2
  275.9 0.9 copy.89
  276.8 5.0 %all_to_all.22 = bf16[64,2,1,12,512]{4,0,3,2,1:T(8,128)(2,1)S(1)} all-to-all(bf16[64,2,1,12,512]{4,0,3,2,1:T(8,128)(2,1)S(1)} %copy.89), channel_id=1, replica_groups=mesh['ep_0'=16,'ep_1'=4,'ep_2'=2,'tp'=4] {'ep_2'}, dimensions={1} | all-to-all | bytes 3145728 | tf_op jit(solution)/shard_map/all_to_all | solution.py:31
  281.8 1.6 copy.90
  283.4 93.7 %all_to_all.23 = bf16[64,2,1,12,512]{4,1,3,2,0:T(2,128)(2,1)S(1)} all-to-all(bf16[64,2,1,12,512]{4,1,3,2,0:T(2,128)(2,1)S(1)} %copy.90), channel_id=1, replica_groups=mesh['ep_0'=16,'ep_1'=4,'ep_2'=2,'tp'=4] {'ep_0','ep_1'}, dimensions={0} | all-to-all | bytes 3145728 | tf_op jit(solution)/shard_map/all_to_all | solution.py:31
  377.1 4.2 %convert_reduce_fusion = f32[64,12,512]{2,1,0:T(8,128)S(1)} fusion(bf16[64,2,1,12,512]{4,1,3,2,0:T(2,128)(2,1)S(1)} %all_to_all.23), kind=kLoop, calls=%fused_computation | loop fusion | flops 1179648 | bytes 3145728 | tf_op jit(solution)/shard_map/reduce_sum | solution.py:88
  381.3 0.3 bitcast_reduce_fusion
  381.6 0.1 reshape.59
  381.7 1.3 convolution_convert_fusion.2
  (9 shorter events, 0.1 us)
Async XLA Ops:
  6.5 262.2 %copy-start = (bf16[1024,512]{1,0:T(8,128)(2,1)S(1)}, bf16[1024,512]{1,0:T(8,128)(2,1)}, u32[]{:S(2)}) copy-start(bf16[1024,512]{1,0:T(8,128)(2,1)} %param.13) | copy-start | bytes 3145732
  6.5 5.1 %copy-start.2 = (bf16[128,2048]{1,0:T(8,128)(2,1)S(1)}, bf16[128,2048]{1,0:T(8,128)(2,1)}, u32[]{:S(2)}) copy-start(bf16[128,2048]{1,0:T(8,128)(2,1)} %param.7) | copy-start | bytes 1572868
  6.5 182.7 %all-gather.3.cloned.1.call-start = ((), (), s32[]{:S(2)}) async-start(), calls=%async_computation.4 | async-start | bytes 7864320 | tf_op jit(solution)/shard_map/all_gather | solution.py:75
  124.0 144.7 %all-gather.5.cloned.1.call-start = ((), (), s32[]{:S(2)}) async-start(), calls=%async_computation.5 | async-start | bytes 3932160 | tf_op jit(solution)/shard_map/all_gather | solution.py:82
  198.9 10.8 %copy-start.3 = (bf16[2048,256]{1,0:T(8,128)(2,1)S(1)}, bf16[2048,256]{1,0:T(8,128)(2,1)}, u32[]{:S(2)}) copy-start(bf16[2048,256]{1,0:T(8,128)(2,1)} %param.11) | copy-start | bytes 3145732
  209.7 4.8 %copy-start.1 = (bf16[1536,2048]{1,0:T(8,128)(2,1)S(1)}, bf16[1536,2048]{1,0:T(8,128)(2,1)}, u32[]{:S(2)}) copy-start(bf16[1536,2048]{1,0:T(8,128)(2,1)} %reshape.58) | copy-start | bytes 18874372
  209.7 4.9 %copy-start.4 = (bf16[2048,256]{1,0:T(8,128)(2,1)S(1)}, bf16[2048,256]{1,0:T(8,128)(2,1)}, u32[]{:S(2)}) copy-start(bf16[2048,256]{1,0:T(8,128)(2,1)} %param.12) | copy-start | bytes 3145732
Sparse Core Ops, SparseCore 0:
  124.1 65.0 all-gather.2
  217.6 51.0 all-gather.4
where the time goes:
time: 391 us; the launch traced here: 390 us
  blocking collectives  200 us (51%)
  waiting for transfers between devices  116 us (30%)
  local copies, waits for them, and re-layouts  36.5 us (9%)
  matrix products  15.2 us (4%)
  between operations  13.6 us (3%)
  other arithmetic  8.01 us (2%)
    all_to_all x4, blocking collectives, turned_blocks(): out = lax.all_to_all(out, axes[k], k, k, tiled=True)  200 us
    all_gather x1, waiting for transfers between devices, on_device(): received = lax.all_gather(arrived, 'tp', axis=1, tiled=True)  65 us
    all_gather x1, waiting for transfers between devices, on_device(): lax.all_gather(hidden, 'tp', axis=1, tiled=True)  51.2 us
    reshape x1, local copies, waits for them, and re-layouts, on_device(): flat_rows = received.reshape(sources * slot_count, model_width)  10.8 us
    all_gather x1, local copies, waits for them, and re-layouts, on_device(): received = lax.all_gather(arrived, 'tp', axis=1, tiled=True)  9.65 us
  transfers between devices with their start and end apart: 2, of which 2 were waited for; matrix products, arithmetic and copies ran while one was open for 0% of the time, Pallas kernels for 0%

commit v1 on v0

v1 whole, which is shorter than its diff:
```python
import jax
import jax.numpy as jnp
from jax import lax
from jax.sharding import Mesh
from jax.sharding import PartitionSpec as P

EPS = 1e-06
EP = ("z", "xh", "xl", "c")
EP_TP = ("z", "xh", "xl", "c", "y")
EXPERTS = 32
CAP = 12
RING = [(y, (y + 1) % 4) for y in range(4)] + [(4 + y, 4 + (y - 1) % 4) for y in range(4)]
SWAP = [(0, 1), (1, 0)]


def rms_rows(values, gain):
    widened = values.astype(jnp.float32)
    scale = lax.rsqrt(jnp.mean(widened * widened, axis=-1, keepdims=True) + EPS)
    return (widened * scale * gain).astype(jnp.bfloat16)


def ring(block):
    return lax.ppermute(block, ("c", "y"), RING)


def dot32(a, b):
    return jnp.dot(a, b, preferred_element_type=jnp.float32)


def spread(per_expert, width, precision=None):
    expert = lax.broadcasted_iota(jnp.int32, (EXPERTS, EXPERTS * width), 1) // width
    own = lax.broadcasted_iota(jnp.int32, (EXPERTS, EXPERTS * width), 0)
    table = (expert == own).astype(per_expert.dtype)
    return jnp.dot(per_expert, table, precision=precision, preferred_element_type=jnp.float32)


def on_device(tokens, norm_gain, expert_ids, gate_weights, w_gate, w_up, w_down):
    y = lax.axis_index("y")
    turn = 1 - 2 * lax.axis_index("c")
    rows = tokens.shape[0]
    width = tokens.shape[1]
    share = CAP // 4
    normed = rms_rows(tokens, norm_gain)
    experts = jnp.arange(EXPERTS, dtype=jnp.int32)[None, :]
    first = expert_ids[:, 0:1] == experts
    second = expert_ids[:, 1:2] == experts
    named = first | second
    weight = jnp.where(first, gate_weights[:, 0:1], 0.0) + jnp.where(
        second, gate_weights[:, 1:2], 0.0
    )
    earlier = (
        lax.broadcasted_iota(jnp.int32, (rows, rows), 0)
        > lax.broadcasted_iota(jnp.int32, (rows, rows), 1)
    ).astype(jnp.bfloat16)
    rank = dot32(earlier, named.astype(jnp.bfloat16))
    rank = jnp.where(named, rank, -1.0).astype(jnp.bfloat16)
    column = lax.broadcasted_iota(jnp.int32, (1, EXPERTS * share), 1)
    slot = share * y + column % share
    selector = (spread(rank, share) == slot.astype(jnp.float32)).astype(jnp.bfloat16)
    mine = lax.dot_general(
        selector, normed, (((0,), (0,)), ((), ())), preferred_element_type=jnp.float32
    ).astype(jnp.bfloat16)
    mine = mine.reshape(EXPERTS, share * width // 128, 128)
    arrived = lax.all_to_all(mine, ("z", "xh"), 0, 0, tiled=True)
    arrived = arrived.reshape(EXPERTS * share, width)

    other = lax.ppermute(arrived, "xl", SWAP)
    near, far = [arrived], [other]
    for _ in range(3):
        near.append(ring(near[-1]))
        far.append(ring(far[-1]))

    def hidden_of(block):
        gate_proj = dot32(block, w_gate)
        upper = dot32(block, w_up)
        return (jax.nn.silu(gate_proj) * upper).astype(jnp.bfloat16)

    own_hidden, partner_hidden = [], []
    for step in range(4):
        block = jnp.concatenate([near[step], far[step]], 0)
        swapped = lax.ppermute(block, "c", SWAP)
        own_hidden.append(hidden_of(block))
        partner_hidden.append(hidden_of(swapped))
    own = jnp.concatenate(own_hidden, 0)
    partner = jnp.concatenate(partner_hidden, 0)
    block_rows = own.shape[0] // 4
    depth = own.shape[1]
    own_sum = partner_sum = 0.0
    for step in range(4):
        start = ((y - turn * step) % 4) * depth
        down = lax.dynamic_slice_in_dim(w_down, start, depth, 0)
        own_sum += dot32(jnp.roll(own, step * block_rows, 0), down)
        partner_sum += dot32(jnp.roll(partner, -step * block_rows, 0), down)
        if step < 3:
            own, partner = ring(own), ring(partner)
    out_width = w_down.shape[1]
    pieces = (4, 2, EXPERTS * share, out_width)
    own_sum = own_sum.reshape(pieces)
    partner_sum = partner_sum.astype(jnp.bfloat16).reshape(pieces)
    away = own_sum[:, 1] + lax.ppermute(partner_sum[:, 1], "c", SWAP).astype(jnp.float32)
    back = lax.ppermute(away.astype(jnp.bfloat16), "xl", SWAP)
    home = own_sum[:, 0] + lax.ppermute(partner_sum[:, 0], "c", SWAP).astype(jnp.float32)
    home = (home + back.astype(jnp.float32)).astype(jnp.bfloat16)
    home = home.reshape(4, EXPERTS, share, out_width).transpose(1, 0, 2, 3)
    home = home.reshape(EXPERTS, CAP * out_width // 128, 128)
    returned = lax.all_to_all(home, ("z", "xh"), 0, 0, tiled=True)
    returned = returned.reshape(EXPERTS * CAP, out_width).astype(jnp.float32)
    column = lax.broadcasted_iota(jnp.int32, (1, EXPERTS * CAP), 1) % CAP
    slot = share * ((y - turn * (column // share)) % 4) + column % share
    chosen = spread(rank, CAP) == slot.astype(jnp.float32)
    spread_weight = spread(weight, CAP, lax.Precision.HIGHEST)
    combine = jnp.where(chosen, spread_weight, 0.0)
    mixed = jnp.dot(
        combine, returned, precision=lax.Precision.HIGHEST, preferred_element_type=jnp.float32
    )
    return mixed.astype(jnp.bfloat16)


def solution(mesh):
    finer = Mesh(mesh.devices.reshape(16, 2, 2, 2, 4), EP_TP)
    placed = (
        P(EP, None),
        P(),
        P(EP, None),
        P(EP, None),
        P(None, EP_TP),
        P(None, EP_TP),
        P(EP, "y"),
    )
    return jax.shard_map(
        on_device, mesh=finer, in_specs=placed, out_specs=P(EP, "y"), check_vma=False
    )
```

time: 391 us -> 196 us (0.50)
  blocking collectives: 200 us -> 45.3 us
  starting transfers between devices: 0.22 us -> 54.9 us
  waiting for transfers between devices: 116 us -> 74.6 us
  local copies, waits for them, and re-layouts: 36.5 us -> 4.29 us
  between operations: 13.6 us -> 0.79 us
  other arithmetic: 8.01 us -> 3.43 us
    all_to_all x4 -> x1, blocking collectives: 200 us -> 45.3 us  [on_device(): arrived = lax.all_to_all(mine, ('z', 'xh'), 0, 0, tiled=True)]
    all_gather x2 -> x0, waiting for transfers between devices: 116 us -> none  [the longest x1 65 us: on_device(): received = lax.all_gather(arrived, 'tp', axis=1, tiled=True)]
    ppermute x0 -> x20, waiting for transfers between devices: none -> 48.7 us  [the longest x12 35 us: ring(): return lax.ppermute(block, ('c', 'y'), RING)]
    ppermute x0 -> x20, starting transfers between devices: none -> 47.4 us  [the longest x12 29.6 us: ring(): return lax.ppermute(block, ('c', 'y'), RING)]
    all_to_all x0 -> x1, waiting for transfers between devices: none -> 25.8 us  [on_device(): returned = lax.all_to_all(home, ('z', 'xh'), 0, 0, tiled=True)]
    reshape x3 -> x4, local copies, waits for them, and re-layouts: 12.4 us -> 1.68 us  [the longest x1 1.09 us: on_device(): home = home.reshape(EXPERTS, CAP * out_width // 128, 128)]
    all_gather x1 -> x0, local copies, waits for them, and re-layouts: 9.65 us -> none  [on_device(): received = lax.all_gather(arrived, 'tp', axis=1, tiled=True)]
    all_to_all x0 -> x1, starting transfers between devices: none -> 7.51 us  [on_device(): returned = lax.all_to_all(home, ('z', 'xh'), 0, 0, tiled=True)]
  transfers between devices with their start and end apart: 2 -> 21, of which waited for: 2 -> 12; matrix products, arithmetic and copies ran while one was open for 0% -> 6% of each run, Pallas kernels for 0% -> 0%
where the time goes in v1:
time: 196 us; the launch traced here: 195 us
  waiting for transfers between devices  74.6 us (38%)
  starting transfers between devices  54.9 us (28%)
  blocking collectives  45.3 us (23%)
  matrix products  12.2 us (6%)
  local copies, waits for them, and re-layouts  4.29 us (2%)
  other arithmetic  3.43 us (2%)
    all_to_all x1, blocking collectives, on_device(): arrived = lax.all_to_all(mine, ('z', 'xh'), 0, 0, tiled=True)  45.3 us
    ppermute x12, waiting for transfers between devices, ring(): return lax.ppermute(block, ('c', 'y'), RING)  35 us
    ppermute x12, starting transfers between devices, ring(): return lax.ppermute(block, ('c', 'y'), RING)  29.6 us
    all_to_all x1, waiting for transfers between devices, on_device(): returned = lax.all_to_all(home, ('z', 'xh'), 0, 0, tiled=True)  25.8 us
    ppermute x1, waiting for transfers between devices, on_device(): back = lax.ppermute(away.astype(jnp.bfloat16), 'xl', SWAP)  10.2 us
    dot_general x25, matrix products, dot32(): return jnp.dot(a, b, preferred_element_type=jnp.float32)  9.15 us
    ppermute x4, starting transfers between devices, on_device(): swapped = lax.ppermute(block, 'c', SWAP)  7.81 us
    all_to_all x1, starting transfers between devices, on_device(): returned = lax.all_to_all(home, ('z', 'xh'), 0, 0, tiled=True)  7.51 us
  transfers between devices with their start and end apart: 21, of which 12 were waited for; matrix products, arithmetic and copies ran while one was open for 6% of the time, Pallas kernels for 0%

profile of v1, /device:TPU:6, one launch (start us, length us, event | category | flops | bytes accessed | tf_op | source)
XLA Modules:
  0.0 195.5 jit_solution(12355826006361560808)
XLA Ops:
  0.0 0.8 slice_bitcast_fusion.3
  0.8 1.2 fusion.1
  2.2 1.5 convolution_convert_fusion
  4.0 45.3 %all_to_all.10 = bf16[32,48,128]{2,1,0:T(8,128)(2,1)S(1)} all-to-all(bf16[32,48,128]{2,1,0:T(8,128)(2,1)S(1)} %reshape.117), channel_id=1, replica_groups=mesh['z'=16,'xh'=2,'xl'=2,'c'=2,'y'=4] {'z','xh'}, dimensions={0} | all-to-all | bytes 786432 | tf_op jit(solution)/shard_map/all_to_all | solution.py:64
  49.4 2.7 %collective-permute-start = (bf16[96,2048]{1,0:T(8,128)(2,1)S(1)}, bf16[96,2048]{1,0:T(8,128)(2,1)S(1)}, u32[]{:S(2)}, u32[]{:S(2)}) collective-permute-start(bf16[96,2048]{1,0:T(8,128)(2,1)S(1)} %reshape.118), channel_id=1, source_target_pairs={{0,8},{8,0},{1,9},{9,1},{2,10},{10,2},{3,11},{11,3},{4,12},{12,4},... | collective-permute-start | bytes 1179656 | tf_op jit(solution)/shard_map/ppermute | solution.py:67
  52.1 3.5 %collective-permute-start.1 = (bf16[96,2048]{1,0:T(8,128)(2,1)S(1)}, bf16[96,2048]{1,0:T(8,128)(2,1)S(1)}, u32[]{:S(2)}, u32[]{:S(2)}) collective-permute-start(bf16[96,2048]{1,0:T(8,128)(2,1)S(1)} %reshape.118), channel_id=1, source_target_pairs={{0,1},{1,2},{2,3},{3,0},{4,7},{5,4},{6,5},{7,6},{8,9},{9,10},{10,1... | collective-permute-start | bytes 1179656 | tf_op jit(solution)/shard_map/ppermute | solution.py:23
  55.7 3.5 %collective-permute-done = bf16[96,2048]{1,0:T(8,128)(2,1)S(1)} collective-permute-done((bf16[96,2048]{1,0:T(8,128)(2,1)S(1)}, bf16[96,2048]{1,0:T(8,128)(2,1)S(1)}, u32[]{:S(2)}, u32[]{:S(2)}) %collective-permute-start) | collective-permute-done | bytes 393248 | tf_op jit(solution)/shard_map/ppermute | solution.py:67
  59.2 2.1 %collective-permute-start.10 = (bf16[192,2048]{1,0:T(8,128)(2,1)S(1)}, bf16[192,2048]{1,0:T(8,128)(2,1)S(1)}, u32[]{:S(2)}, u32[]{:S(2)}) collective-permute-start(bf16[192,2048]{1,0:T(8,128)(2,1)S(1)} %constant_dynamic-update-slice_fusion), channel_id=1, source_target_pairs={{0,4},{4,0},{1,5},{5,1},{2,6},{6,2},{3,7},{7,3},{8,12},{12,8},{9,1... | collective-permute-start | bytes 2359304 | tf_op jit(solution)/shard_map/ppermute | solution.py:81
  61.3 3.5 %collective-permute-start.2 = (bf16[96,2048]{1,0:T(8,128)(2,1)S(1)}, bf16[96,2048]{1,0:T(8,128)(2,1)S(1)}, u32[]{:S(2)}, u32[]{:S(2)}) collective-permute-start(bf16[96,2048]{1,0:T(8,128)(2,1)S(1)} %collective-permute-done), channel_id=1, source_target_pairs={{0,1},{1,2},{2,3},{3,0},{4,7},{5,4},{6,5},{7,6},{8,9},{9,10},{10,1... | collective-permute-start | bytes 1179656 | tf_op jit(solution)/shard_map/ppermute | solution.py:23
  64.8 0.4 fusion.102
  65.2 3.5 %collective-permute-start.3 = (bf16[96,2048]{1,0:T(8,128)(2,1)S(1)}, bf16[96,2048]{1,0:T(8,128)(2,1)S(1)}, u32[]{:S(2)}, u32[]{:S(2)}) collective-permute-start(bf16[96,2048]{1,0:T(8,128)(2,1)S(1)} %collective-permute-done.1), channel_id=1, source_target_pairs={{0,1},{1,2},{2,3},{3,0},{4,7},{5,4},{6,5},{7,6},{8,9},{9,10},{10,1... | collective-permute-start | bytes 1179656 | tf_op jit(solution)/shard_map/ppermute | solution.py:23
  68.7 0.4 multiply_convert_fusion.7
  69.1 3.0 %collective-permute-done.2 = bf16[96,2048]{1,0:T(8,128)(2,1)S(1)} collective-permute-done((bf16[96,2048]{1,0:T(8,128)(2,1)S(1)}, bf16[96,2048]{1,0:T(8,128)(2,1)S(1)}, u32[]{:S(2)}, u32[]{:S(2)}) %collective-permute-start.2) | collective-permute-done | bytes 393248 | tf_op jit(solution)/shard_map/ppermute | solution.py:23
  72.2 1.9 collective-permute-start.11
  74.1 2.3 %collective-permute-start.4 = (bf16[96,2048]{1,0:T(8,128)(2,1)S(1)}, bf16[96,2048]{1,0:T(8,128)(2,1)S(1)}, u32[]{:S(2)}, u32[]{:S(2)}) collective-permute-start(bf16[96,2048]{1,0:T(8,128)(2,1)S(1)} %collective-permute-done.2), channel_id=1, source_target_pairs={{0,1},{1,2},{2,3},{3,0},{4,7},{5,4},{6,5},{7,6},{8,9},{9,10},{10,1... | collective-permute-start | bytes 1179656 | tf_op jit(solution)/shard_map/ppermute | solution.py:23
  76.8 3.5 %collective-permute-start.5 = (bf16[96,2048]{1,0:T(8,128)(2,1)S(1)}, bf16[96,2048]{1,0:T(8,128)(2,1)S(1)}, u32[]{:S(2)}, u32[]{:S(2)}) collective-permute-start(bf16[96,2048]{1,0:T(8,128)(2,1)S(1)} %collective-permute-done.3), channel_id=1, source_target_pairs={{0,1},{1,2},{2,3},{3,0},{4,7},{5,4},{6,5},{7,6},{8,9},{9,10},{10,1... | collective-permute-start | bytes 1179656 | tf_op jit(solution)/shard_map/ppermute | solution.py:23
  80.3 0.4 multiply_convert_fusion.6
  80.7 4.3 %collective-permute-done.4 = bf16[96,2048]{1,0:T(8,128)(2,1)S(1)} collective-permute-done((bf16[96,2048]{1,0:T(8,128)(2,1)S(1)}, bf16[96,2048]{1,0:T(8,128)(2,1)S(1)}, u32[]{:S(2)}, u32[]{:S(2)}) %collective-permute-start.4) | collective-permute-done | bytes 393248 | tf_op jit(solution)/shard_map/ppermute | solution.py:23
  85.0 1.9 collective-permute-start.12
  87.0 1.9 collective-permute-start.6
  89.3 0.4 fusion.106
  90.1 0.4 multiply_convert_fusion.3
  90.5 7.3 %collective-permute-done.6 = bf16[96,2048]{1,0:T(8,128)(2,1)S(1)} collective-permute-done((bf16[96,2048]{1,0:T(8,128)(2,1)S(1)}, bf16[96,2048]{1,0:T(8,128)(2,1)S(1)}, u32[]{:S(2)}, u32[]{:S(2)}) %collective-permute-start.6) | collective-permute-done | bytes 393248 | tf_op jit(solution)/shard_map/ppermute | solution.py:23
  97.9 1.9 collective-permute-start.13
  100.6 0.8 pad_maximum_fusion
  101.3 1.9 collective-permute-start.7
  105.2 0.4 multiply_convert_fusion
  105.6 1.9 collective-permute-start.14
  107.6 4.8 %collective-permute-done.7 = bf16[768,256]{1,0:T(8,128)(2,1)S(1)} collective-permute-done((bf16[768,256]{1,0:T(8,128)(2,1)}, bf16[768,256]{1,0:T(8,128)(2,1)S(1)}, u32[]{:S(2)}, u32[]{:S(2)}) %collective-permute-start.7) | collective-permute-done | bytes 393248 | tf_op jit(solution)/shard_map/ppermute | solution.py:23
  112.4 1.9 collective-permute-start.8
  115.1 1.5 collective-permute-done.14
  116.6 1.9 collective-permute-start.15
  118.9 4.4 %collective-permute-done.8 = bf16[768,256]{1,0:T(8,128)(2,1)S(1)} collective-permute-done((bf16[768,256]{1,0:T(8,128)(2,1)S(1)}, bf16[768,256]{1,0:T(8,128)(2,1)S(1)}, u32[]{:S(2)}, u32[]{:S(2)}) %collective-permute-start.8) | collective-permute-done | bytes 393248 | tf_op jit(solution)/shard_map/ppermute | solution.py:23
  123.3 1.9 collective-permute-start.9
  125.7 1.8 collective-permute-done.15
  127.5 1.9 collective-permute-start.16
  129.8 4.4 %collective-permute-done.9 = bf16[768,256]{1,0:T(8,128)(2,1)S(1)} collective-permute-done((bf16[768,256]{1,0:T(8,128)(2,1)S(1)}, bf16[768,256]{1,0:T(8,128)(2,1)S(1)}, u32[]{:S(2)}, u32[]{:S(2)}) %collective-permute-start.9) | collective-permute-done | bytes 393248 | tf_op jit(solution)/shard_map/ppermute | solution.py:23
  134.9 3.5 %collective-permute-done.16 = bf16[768,256]{1,0:T(8,128)(2,1)S(1)} collective-permute-done((bf16[768,256]{1,0:T(8,128)(2,1)S(1)}, bf16[768,256]{1,0:T(8,128)(2,1)S(1)}, u32[]{:S(2)}, u32[]{:S(2)}) %collective-permute-start.16) | collective-permute-done | bytes 393248 | tf_op jit(solution)/shard_map/ppermute | solution.py:23
  139.2 1.9 collective-permute-start.18
  142.0 2.6 %collective-permute-start.17 = (bf16[4,96,512]{2,0,1:T(4,128)(2,1)S(1)}, bf16[4,96,512]{2,0,1:T(4,128)(2,1)S(1)}, u32[]{:S(2)}, u32[]{:S(2)}) collective-permute-start(bf16[4,96,512]{2,0,1:T(4,128)(2,1)S(1)} %bitcast.73), channel_id=1, source_target_pairs={{0,4},{4,0},{1,5},{5,1},{2,6},{6,2},{3,7},{7,3},{8,12},{12,8},{9,1... | collective-permute-start | bytes 1179656 | tf_op jit(solution)/shard_map/ppermute | solution.py:102
  144.6 0.6 fusion.5
  145.2 2.8 %collective-permute-start.19 = (bf16[4,96,512]{2,0,1:T(4,128)(2,1)S(1)}, bf16[4,96,512]{2,0,1:T(4,128)(2,1)S(1)}, u32[]{:S(2)}, u32[]{:S(2)}) collective-permute-start(bf16[4,96,512]{2,0,1:T(4,128)(2,1)S(1)} %fusion.5), channel_id=1, source_target_pairs={{0,8},{8,0},{1,9},{9,1},{2,10},{10,2},{3,11},{11,3},{4,12},{12,4},... | collective-permute-start | bytes 1179656 | tf_op jit(solution)/shard_map/ppermute | solution.py:101
  148.0 10.2 %collective-permute-done.19 = bf16[4,96,512]{2,0,1:T(4,128)(2,1)S(1)} collective-permute-done((bf16[4,96,512]{2,0,1:T(4,128)(2,1)S(1)}, bf16[4,96,512]{2,0,1:T(4,128)(2,1)S(1)}, u32[]{:S(2)}, u32[]{:S(2)}) %collective-permute-start.19) | collective-permute-done | bytes 393248 | tf_op jit(solution)/shard_map/ppermute | solution.py:101
  158.2 0.7 fusion.8
  159.1 1.1 reshape.122
  160.2 7.5 %all-to-all-start.1 = ((bf16[32,48,128]{2,1,0:T(8,128)(2,1)}), bf16[32,48,128]{2,1,0:T(8,128)(2,1)S(1)}, u32[]{:S(2)}, u32[]{:S(2)}) async-start(bf16[32,48,128]{2,1,0:T(8,128)(2,1)} %reshape.122), calls=%async_computation.1 | async-start | bytes 786432 | tf_op jit(solution)/shard_map/all_to_all | solution.py:106
  168.4 25.8 %all-to-all-done.1 = bf16[32,48,128]{2,1,0:T(8,128)(2,1)S(1)} async-done(((bf16[32,48,128]{2,1,0:T(8,128)(2,1)}), bf16[32,48,128]{2,1,0:T(8,128)(2,1)S(1)}, u32[]{:S(2)}, u32[]{:S(2)}) %all-to-all-start.1) | async-done | bytes 393248 | tf_op jit(solution)/shard_map/all_to_all | solution.py:106
  194.4 1.0 convolution_convert_fusion.1
  (77 shorter events, 9.9 us)
Async XLA Ops:
  0.0 114.3 %copy-start = (bf16[1024,512]{1,0:T(8,128)(2,1)S(1)}, bf16[1024,512]{1,0:T(8,128)(2,1)}, u32[]{:S(2)}) copy-start(bf16[1024,512]{1,0:T(8,128)(2,1)} %param.13) | copy-start | bytes 3145732
  3.9 60.8 %copy-start.1 = (bf16[2048,256]{1,0:T(8,128)(2,1)S(1)}, bf16[2048,256]{1,0:T(8,128)(2,1)}, u32[]{:S(2)}) copy-start(bf16[2048,256]{1,0:T(8,128)(2,1)} %param.11) | copy-start | bytes 3145732
  49.4 9.8 %collective-permute-start = (bf16[96,2048]{1,0:T(8,128)(2,1)S(1)}, bf16[96,2048]{1,0:T(8,128)(2,1)S(1)}, u32[]{:S(2)}, u32[]{:S(2)}) collective-permute-start(bf16[96,2048]{1,0:T(8,128)(2,1)S(1)} %reshape.118), channel_id=1, source_target_pairs={{0,8},{8,0},{1,9},{9,1},{2,10},{10,2},{3,11},{11,3},{4,12},{12,4},... | collective-permute-start | bytes 1179656 | tf_op jit(solution)/shard_map/ppermute | solution.py:67
  52.1 13.0 %collective-permute-start.1 = (bf16[96,2048]{1,0:T(8,128)(2,1)S(1)}, bf16[96,2048]{1,0:T(8,128)(2,1)S(1)}, u32[]{:S(2)}, u32[]{:S(2)}) collective-permute-start(bf16[96,2048]{1,0:T(8,128)(2,1)S(1)} %reshape.118), channel_id=1, source_target_pairs={{0,1},{1,2},{2,3},{3,0},{4,7},{5,4},{6,5},{7,6},{8,9},{9,10},{10,1... | collective-permute-start | bytes 1179656 | tf_op jit(solution)/shard_map/ppermute | solution.py:23
  59.2 9.5 %copy-start.4 = (bf16[2048,256]{1,0:T(8,128)(2,1)S(1)}, bf16[2048,256]{1,0:T(8,128)(2,1)}, u32[]{:S(2)}) copy-start(bf16[2048,256]{1,0:T(8,128)(2,1)} %param.12) | copy-start | bytes 3145732
  59.2 30.1 %collective-permute-start.10 = (bf16[192,2048]{1,0:T(8,128)(2,1)S(1)}, bf16[192,2048]{1,0:T(8,128)(2,1)S(1)}, u32[]{:S(2)}, u32[]{:S(2)}) collective-permute-start(bf16[192,2048]{1,0:T(8,128)(2,1)S(1)} %constant_dynamic-update-slice_fusion), channel_id=1, source_target_pairs={{0,4},{4,0},{1,5},{5,1},{2,6},{6,2},{3,7},{7,3},{8,12},{12,8},{9,1... | collective-permute-start | bytes 2359304 | tf_op jit(solution)/shard_map/ppermute | solution.py:81
  61.3 10.9 %collective-permute-start.2 = (bf16[96,2048]{1,0:T(8,128)(2,1)S(1)}, bf16[96,2048]{1,0:T(8,128)(2,1)S(1)}, u32[]{:S(2)}, u32[]{:S(2)}) collective-permute-start(bf16[96,2048]{1,0:T(8,128)(2,1)S(1)} %collective-permute-done), channel_id=1, source_target_pairs={{0,1},{1,2},{2,3},{3,0},{4,7},{5,4},{6,5},{7,6},{8,9},{9,10},{10,1... | collective-permute-start | bytes 1179656 | tf_op jit(solution)/shard_map/ppermute | solution.py:23
  65.2 11.6 %collective-permute-start.3 = (bf16[96,2048]{1,0:T(8,128)(2,1)S(1)}, bf16[96,2048]{1,0:T(8,128)(2,1)S(1)}, u32[]{:S(2)}, u32[]{:S(2)}) collective-permute-start(bf16[96,2048]{1,0:T(8,128)(2,1)S(1)} %collective-permute-done.1), channel_id=1, source_target_pairs={{0,1},{1,2},{2,3},{3,0},{4,7},{5,4},{6,5},{7,6},{8,9},{9,10},{10,1... | collective-permute-start | bytes 1179656 | tf_op jit(solution)/shard_map/ppermute | solution.py:23
  72.2 31.1 %collective-permute-start.11 = (bf16[192,2048]{1,0:T(8,128)(2,1)S(1)}, bf16[192,2048]{1,0:T(8,128)(2,1)S(1)}, u32[]{:S(2)}, u32[]{:S(2)}) collective-permute-start(bf16[192,2048]{1,0:T(8,128)(2,1)S(1)} %constant_dynamic-update-slice_fusion.2), channel_id=1, source_target_pairs={{0,4},{4,0},{1,5},{5,1},{2,6},{6,2},{3,7},{7,3},{8,12},{12,8},{9,1... | collective-permute-start | bytes 2359304 | tf_op jit(solution)/shard_map/ppermute | solution.py:81
  74.1 10.9 %collective-permute-start.4 = (bf16[96,2048]{1,0:T(8,128)(2,1)S(1)}, bf16[96,2048]{1,0:T(8,128)(2,1)S(1)}, u32[]{:S(2)}, u32[]{:S(2)}) collective-permute-start(bf16[96,2048]{1,0:T(8,128)(2,1)S(1)} %collective-permute-done.2), channel_id=1, source_target_pairs={{0,1},{1,2},{2,3},{3,0},{4,7},{5,4},{6,5},{7,6},{8,9},{9,10},{10,1... | collective-permute-start | bytes 1179656 | tf_op jit(solution)/shard_map/ppermute | solution.py:23
  76.8 13.3 %collective-permute-start.5 = (bf16[96,2048]{1,0:T(8,128)(2,1)S(1)}, bf16[96,2048]{1,0:T(8,128)(2,1)S(1)}, u32[]{:S(2)}, u32[]{:S(2)}) collective-permute-start(bf16[96,2048]{1,0:T(8,128)(2,1)S(1)} %collective-permute-done.3), channel_id=1, source_target_pairs={{0,1},{1,2},{2,3},{3,0},{4,7},{5,4},{6,5},{7,6},{8,9},{9,10},{10,1... | collective-permute-start | bytes 1179656 | tf_op jit(solution)/shard_map/ppermute | solution.py:23
  85.0 19.0 %collective-permute-start.12 = (bf16[192,2048]{1,0:T(8,128)(2,1)S(1)}, bf16[192,2048]{1,0:T(8,128)(2,1)S(1)}, u32[]{:S(2)}, u32[]{:S(2)}) collective-permute-start(bf16[192,2048]{1,0:T(8,128)(2,1)S(1)} %constant_dynamic-update-slice_fusion.4), channel_id=1, source_target_pairs={{0,4},{4,0},{1,5},{5,1},{2,6},{6,2},{3,7},{7,3},{8,12},{12,8},{9,1... | collective-permute-start | bytes 2359304 | tf_op jit(solution)/shard_map/ppermute | solution.py:81
  87.0 10.9 %collective-permute-start.6 = (bf16[96,2048]{1,0:T(8,128)(2,1)S(1)}, bf16[96,2048]{1,0:T(8,128)(2,1)S(1)}, u32[]{:S(2)}, u32[]{:S(2)}) collective-permute-start(bf16[96,2048]{1,0:T(8,128)(2,1)S(1)} %collective-permute-done.4), channel_id=1, source_target_pairs={{0,1},{1,2},{2,3},{3,0},{4,7},{5,4},{6,5},{7,6},{8,9},{9,10},{10,1... | collective-permute-start | bytes 1179656 | tf_op jit(solution)/shard_map/ppermute | solution.py:23
  97.9 6.9 %collective-permute-start.13 = (bf16[192,2048]{1,0:T(8,128)(2,1)S(1)}, bf16[192,2048]{1,0:T(8,128)(2,1)S(1)}, u32[]{:S(2)}, u32[]{:S(2)}) collective-permute-start(bf16[192,2048]{1,0:T(8,128)(2,1)S(1)} %constant_dynamic-update-slice_fusion.6), channel_id=1, source_target_pairs={{0,4},{4,0},{1,5},{5,1},{2,6},{6,2},{3,7},{7,3},{8,12},{12,8},{9,1... | collective-permute-start | bytes 2359304 | tf_op jit(solution)/shard_map/ppermute | solution.py:81
  101.3 11.1 %collective-permute-start.7 = (bf16[768,256]{1,0:T(8,128)(2,1)}, bf16[768,256]{1,0:T(8,128)(2,1)S(1)}, u32[]{:S(2)}, u32[]{:S(2)}) collective-permute-start(bf16[768,256]{1,0:T(8,128)(2,1)} %pad_maximum_fusion), channel_id=1, source_target_pairs={{0,1},{1,2},{2,3},{3,0},{4,7},{5,4},{6,5},{7,6},{8,9},{9,10},{10,1... | collective-permute-start | bytes 1179656 | tf_op jit(solution)/shard_map/ppermute | solution.py:23
  105.6 11.0 %collective-permute-start.14 = (bf16[768,256]{1,0:T(8,128)(2,1)S(1)}, bf16[768,256]{1,0:T(8,128)(2,1)S(1)}, u32[]{:S(2)}, u32[]{:S(2)}) collective-permute-start(bf16[768,256]{1,0:T(8,128)(2,1)S(1)} %pad_maximum_fusion.1), channel_id=1, source_target_pairs={{0,1},{1,2},{2,3},{3,0},{4,7},{5,4},{6,5},{7,6},{8,9},{9,10},{10,1... | collective-permute-start | bytes 1179656 | tf_op jit(solution)/shard_map/ppermute | solution.py:23
  112.4 10.9 %collective-permute-start.8 = (bf16[768,256]{1,0:T(8,128)(2,1)S(1)}, bf16[768,256]{1,0:T(8,128)(2,1)S(1)}, u32[]{:S(2)}, u32[]{:S(2)}) collective-permute-start(bf16[768,256]{1,0:T(8,128)(2,1)S(1)} %collective-permute-done.7), channel_id=1, source_target_pairs={{0,1},{1,2},{2,3},{3,0},{4,7},{5,4},{6,5},{7,6},{8,9},{9,10},{10,1... | collective-permute-start | bytes 1179656 | tf_op jit(solution)/shard_map/ppermute | solution.py:23
  116.6 10.9 %collective-permute-start.15 = (bf16[768,256]{1,0:T(8,128)(2,1)S(1)}, bf16[768,256]{1,0:T(8,128)(2,1)S(1)}, u32[]{:S(2)}, u32[]{:S(2)}) collective-permute-start(bf16[768,256]{1,0:T(8,128)(2,1)S(1)} %collective-permute-done.14), channel_id=1, source_target_pairs={{0,1},{1,2},{2,3},{3,0},{4,7},{5,4},{6,5},{7,6},{8,9},{9,10},{10,1... | collective-permute-start | bytes 1179656 | tf_op jit(solution)/shard_map/ppermute | solution.py:23
  123.3 10.9 %collective-permute-start.9 = (bf16[768,256]{1,0:T(8,128)(2,1)S(1)}, bf16[768,256]{1,0:T(8,128)(2,1)S(1)}, u32[]{:S(2)}, u32[]{:S(2)}) collective-permute-start(bf16[768,256]{1,0:T(8,128)(2,1)S(1)} %collective-permute-done.8), channel_id=1, source_target_pairs={{0,1},{1,2},{2,3},{3,0},{4,7},{5,4},{6,5},{7,6},{8,9},{9,10},{10,1... | collective-permute-start | bytes 1179656 | tf_op jit(solution)/shard_map/ppermute | solution.py:23
  127.5 10.9 %collective-permute-start.16 = (bf16[768,256]{1,0:T(8,128)(2,1)S(1)}, bf16[768,256]{1,0:T(8,128)(2,1)S(1)}, u32[]{:S(2)}, u32[]{:S(2)}) collective-permute-start(bf16[768,256]{1,0:T(8,128)(2,1)S(1)} %collective-permute-done.15), channel_id=1, source_target_pairs={{0,1},{1,2},{2,3},{3,0},{4,7},{5,4},{6,5},{7,6},{8,9},{9,10},{10,1... | collective-permute-start | bytes 1179656 | tf_op jit(solution)/shard_map/ppermute | solution.py:23
  134.2 0.7 copy-start.2
  138.8 2.3 %slice-start = ((bf16[768,256]{1,0:T(8,128)(2,1)}), bf16[192,256]{1,0:T(8,128)(2,1)S(1)}, s32[]{:S(2)}) async-start(bf16[768,256]{1,0:T(8,128)(2,1)} %copy-done.2), calls=%async_computation.2 | async-start | bytes 196608 | tf_op jit(solution)/shard_map/jit(_roll_static)/slice | solution.py:92
  138.8 2.3 %slice-start.1 = ((bf16[768,256]{1,0:T(8,128)(2,1)}), bf16[576,256]{1,0:T(8,128)(2,1)S(1)}, s32[]{:S(2)}) async-start(bf16[768,256]{1,0:T(8,128)(2,1)} %copy-done.2), calls=%async_computation.3 | async-start | bytes 589824 | tf_op jit(solution)/shard_map/jit(_roll_static)/slice | solution.py:92
  139.2 5.4 %collective-permute-start.18 = (bf16[4,96,512]{2,0,1:T(4,128)(2,1)S(1)}, bf16[4,96,512]{2,0,1:T(4,128)(2,1)S(1)}, u32[]{:S(2)}, u32[]{:S(2)}) collective-permute-start(bf16[4,96,512]{2,0,1:T(4,128)(2,1)S(1)} %bitcast.72), channel_id=1, source_target_pairs={{0,4},{4,0},{1,5},{5,1},{2,6},{6,2},{3,7},{7,3},{8,12},{12,8},{9,1... | collective-permute-start | bytes 1179656 | tf_op jit(solution)/shard_map/ppermute | solution.py:100
  142.0 6.0 %collective-permute-start.17 = (bf16[4,96,512]{2,0,1:T(4,128)(2,1)S(1)}, bf16[4,96,512]{2,0,1:T(4,128)(2,1)S(1)}, u32[]{:S(2)}, u32[]{:S(2)}) collective-permute-start(bf16[4,96,512]{2,0,1:T(4,128)(2,1)S(1)} %bitcast.73), channel_id=1, source_target_pairs={{0,4},{4,0},{1,5},{5,1},{2,6},{6,2},{3,7},{7,3},{8,12},{12,8},{9,1... | collective-permute-start | bytes 1179656 | tf_op jit(solution)/shard_map/ppermute | solution.py:102
  145.2 12.9 %collective-permute-start.19 = (bf16[4,96,512]{2,0,1:T(4,128)(2,1)S(1)}, bf16[4,96,512]{2,0,1:T(4,128)(2,1)S(1)}, u32[]{:S(2)}, u32[]{:S(2)}) collective-permute-start(bf16[4,96,512]{2,0,1:T(4,128)(2,1)S(1)} %fusion.5), channel_id=1, source_target_pairs={{0,8},{8,0},{1,9},{9,1},{2,10},{10,2},{3,11},{11,3},{4,12},{12,4},... | collective-permute-start | bytes 1179656 | tf_op jit(solution)/shard_map/ppermute | solution.py:101
  158.9 8.9 %copy-start.3 = (f32[128,2]{0,1:T(2,128)S(1)}, f32[128,2]{0,1:T(2,128)}, u32[]{:S(2)}) copy-start(f32[128,2]{0,1:T(2,128)} %param.10) | copy-start | bytes 3076
  160.2 34.0 %all-to-all-start.1 = ((bf16[32,48,128]{2,1,0:T(8,128)(2,1)}), bf16[32,48,128]{2,1,0:T(8,128)(2,1)S(1)}, u32[]{:S(2)}, u32[]{:S(2)}) async-start(bf16[32,48,128]{2,1,0:T(8,128)(2,1)} %reshape.122), calls=%async_computation.1 | async-start | bytes 786432 | tf_op jit(solution)/shard_map/all_to_all | solution.py:106

commit v2 on v1

v2 whole, which is shorter than its diff:
```python
import jax
import jax.numpy as jnp
from jax import lax
from jax.sharding import Mesh
from jax.sharding import PartitionSpec as P

EPS = 1e-06
EP = ("z", "xh", "xl", "c")
EP_TP = ("z", "xh", "xl", "c", "y")
EXPERTS = 32
CAP = 12
RING = [(y, (y + 1) % 4) for y in range(4)] + [(4 + y, 4 + (y - 1) % 4) for y in range(4)]
SWAP = [(0, 1), (1, 0)]


def rms_rows(values, gain):
    widened = values.astype(jnp.float32)
    scale = lax.rsqrt(jnp.mean(widened * widened, axis=-1, keepdims=True) + EPS)
    return (widened * scale * gain).astype(jnp.bfloat16)


def ring(block):
    return lax.ppermute(block, ("c", "y"), RING)


def dot32(a, b):
    return jnp.dot(a, b, preferred_element_type=jnp.float32)


def spread(per_expert, width, precision=None):
    expert = lax.broadcasted_iota(jnp.int32, (EXPERTS, EXPERTS * width), 1) // width
    own = lax.broadcasted_iota(jnp.int32, (EXPERTS, EXPERTS * width), 0)
    table = (expert == own).astype(per_expert.dtype)
    return jnp.dot(per_expert, table, precision=precision, preferred_element_type=jnp.float32)


def on_device(tokens, norm_gain, expert_ids, gate_weights, w_gate, w_up, w_down):
    y = lax.axis_index("y")
    turn = 1 - 2 * lax.axis_index("c")
    rows = tokens.shape[0]
    width = tokens.shape[1]
    share = CAP // 4
    block_rows = EXPERTS * share
    normed = rms_rows(tokens, norm_gain)
    experts = jnp.arange(EXPERTS, dtype=jnp.int32)[None, :]
    first = expert_ids[:, 0:1] == experts
    second = expert_ids[:, 1:2] == experts
    named = first | second
    weight = jnp.where(first, gate_weights[:, 0:1], 0.0) + jnp.where(
        second, gate_weights[:, 1:2], 0.0
    )
    earlier = (
        lax.broadcasted_iota(jnp.int32, (rows, rows), 0)
        > lax.broadcasted_iota(jnp.int32, (rows, rows), 1)
    ).astype(jnp.bfloat16)
    rank = dot32(earlier, named.astype(jnp.bfloat16))
    rank = jnp.where(named, rank, -1.0).astype(jnp.bfloat16)
    column = lax.broadcasted_iota(jnp.int32, (1, block_rows), 1)
    slot = share * y + column % share
    selector = (spread(rank, share) == slot.astype(jnp.float32)).astype(jnp.bfloat16)

    cuts = (0, width // 2, width)
    near, far = [], []
    for low, high in zip(cuts[:-1], cuts[1:]):
        mine = lax.dot_general(
            selector,
            normed[:, low:high],
            (((0,), (0,)), ((), ())),
            preferred_element_type=jnp.float32,
        ).astype(jnp.bfloat16)
        mine = mine.reshape(EXPERTS, share * (high - low) // 128, 128)
        arrived = lax.all_to_all(mine, ("z", "xh"), 0, 0, tiled=True)
        near.append(arrived.reshape(block_rows, high - low))

    gates = (w_gate, lax.ppermute(w_gate, "c", SWAP))
    uppers = (w_up, lax.ppermute(w_up, "c", SWAP))
    downs = (w_down, lax.ppermute(w_down, "c", SWAP))

    sums = [[0.0] * 4 for _ in range(4)]
    for part, (low, high) in enumerate(zip(cuts[:-1], cuts[1:])):
        block = jnp.concatenate([near[part], lax.ppermute(near[part], "xl", SWAP)], 0)
        for step in range(4):
            for i, matrix in enumerate(gates + uppers):
                sums[step][i] += dot32(block, matrix[low:high])
            if step < 3:
                block = ring(block)
    hidden = []
    for g0, g1, u0, u1 in sums:
        parts = [(jax.nn.silu(g) * u).astype(jnp.bfloat16) for g, u in ((g0, u0), (g1, u1))]
        hidden.append(jnp.concatenate(parts, 1))
    hidden = jnp.concatenate(hidden, 0)
    depth = w_gate.shape[1]
    out_width = w_down.shape[1]

    column = lax.broadcasted_iota(jnp.int32, (1, EXPERTS * CAP // 2), 1)
    spread_rank = spread(rank, CAP // 2)
    spread_weight = spread(weight, CAP // 2, lax.Precision.HIGHEST)
    mixed = 0.0
    for half in range(2):
        pieces = []
        for side in range(2):
            for q in (2 * half, 2 * half + 1):
                start = ((turn * (y - q)) & 3) * (2 * block_rows) + side * block_rows
                pieces.append(lax.dynamic_slice_in_dim(hidden, start, block_rows, 0))
        block = jnp.concatenate(pieces, 0)
        total = 0.0
        for step in range(4):
            start = ((y - turn * step) & 3) * depth
            for core in range(2):
                down = lax.dynamic_slice_in_dim(downs[core], start, depth, 0)
                total += dot32(block[:, core * depth : (core + 1) * depth], down)
            if step < 3:
                block = ring(block)
        home, away = total[: 2 * block_rows], total[2 * block_rows :]
        back = lax.ppermute(away.astype(jnp.bfloat16), "xl", SWAP)
        home = (home + back.astype(jnp.float32)).astype(jnp.bfloat16)
        home = home.reshape(2, EXPERTS, share, out_width).transpose(1, 0, 2, 3)
        home = home.reshape(EXPERTS, 2 * share * out_width // 128, 128)
        returned = lax.all_to_all(home, ("z", "xh"), 0, 0, tiled=True)
        returned = returned.reshape(EXPERTS * CAP // 2, out_width).astype(jnp.float32)
        slot = column % (CAP // 2) + half * (CAP // 2)
        combine = jnp.where(spread_rank == slot.astype(jnp.float32), spread_weight, 0.0)
        mixed += jnp.dot(
            combine, returned, precision=lax.Precision.HIGHEST, preferred_element_type=jnp.float32
        )
    return mixed.astype(jnp.bfloat16)


def solution(mesh):
    finer = Mesh(mesh.devices.reshape(16, 2, 2, 2, 4), EP_TP)
    placed = (
        P(EP, None),
        P(),
        P(EP, None),
        P(EP, None),
        P(None, EP_TP),
        P(None, EP_TP),
        P(EP, "y"),
    )
    return jax.shard_map(
        on_device, mesh=finer, in_specs=placed, out_specs=P(EP, "y"), check_vma=False
    )
```

time: 196 us -> 214 us (1.092)
  blocking collectives: 45.3 us -> 0 us
  starting transfers between devices: 54.9 us -> 89.3 us
  matrix products: 12.2 us -> 32.6 us
  waiting for transfers between devices: 74.6 us -> 78.2 us
  local copies, waits for them, and re-layouts: 4.29 us -> 7.73 us
    all_to_all x1 -> x0, blocking collectives: 45.3 us -> none  [on_device(): arrived = lax.all_to_all(mine, ('z', 'xh'), 0, 0, tiled=True)]
    all_to_all x0 -> x2, waiting for transfers between devices: none -> 25.7 us  [on_device(): arrived = lax.all_to_all(mine, ('z', 'xh'), 0, 0, tiled=True)]
    all_to_all x0 -> x2, starting transfers between devices: none -> 23.3 us  [on_device(): arrived = lax.all_to_all(mine, ('z', 'xh'), 0, 0, tiled=True)]
    dot_general x25 -> x49, matrix products: 9.15 us -> 30 us  [dot32(): return jnp.dot(a, b, preferred_element_type=jnp.float32)]
    all_to_all x1 -> x2, starting transfers between devices: 7.51 us -> 20.2 us  [on_device(): returned = lax.all_to_all(home, ('z', 'xh'), 0, 0, tiled=True)]
    ppermute x12, waiting for transfers between devices: 35 us -> 24.3 us  [ring(): return lax.ppermute(block, ('c', 'y'), RING)]
    all_to_all x1 -> x2, waiting for transfers between devices: 25.8 us -> 19.3 us  [on_device(): returned = lax.all_to_all(home, ('z', 'xh'), 0, 0, tiled=True)]
    ppermute x7 -> x5, waiting for transfers between devices: 3.53 us -> 0.01 us  [the longest x2 0.01 us: on_device(): lax.ppermute(near[part], 'xl', SWAP)]
  transfers between devices with their start and end apart: 21 -> 23, of which waited for: 12 -> 15; matrix products, arithmetic and copies ran while one was open for 6% -> 18% of each run, Pallas kernels for 0% -> 0%
where the time goes in v2:
time: 214 us; the launch traced here: 212 us
  starting transfers between devices  89.3 us (42%)
  waiting for transfers between devices  78.2 us (37%)
  matrix products  32.6 us (15%)
  local copies, waits for them, and re-layouts  7.73 us (4%)
  other arithmetic  3.31 us (2%)
    dot_general x49, matrix products, dot32(): return jnp.dot(a, b, preferred_element_type=jnp.float32)  30 us
    ppermute x12, starting transfers between devices, ring(): return lax.ppermute(block, ('c', 'y'), RING)  28 us
    all_to_all x2, waiting for transfers between devices, on_device(): arrived = lax.all_to_all(mine, ('z', 'xh'), 0, 0, tiled=True)  25.7 us
    ppermute x12, waiting for transfers between devices, ring(): return lax.ppermute(block, ('c', 'y'), RING)  24.3 us
    all_to_all x2, starting transfers between devices, on_device(): arrived = lax.all_to_all(mine, ('z', 'xh'), 0, 0, tiled=True)  23.3 us
    all_to_all x2, starting transfers between devices, on_device(): returned = lax.all_to_all(home, ('z', 'xh'), 0, 0, tiled=True)  20.2 us
    all_to_all x2, waiting for transfers between devices, on_device(): returned = lax.all_to_all(home, ('z', 'xh'), 0, 0, tiled=True)  19.3 us
    ppermute x2, waiting for transfers between devices, on_device(): back = lax.ppermute(away.astype(jnp.bfloat16), 'xl', SWAP)  8.87 us
  transfers between devices with their start and end apart: 23, of which 15 were waited for; matrix products, arithmetic and copies ran while one was open for 18% of the time, Pallas kernels for 0%

profile of v2, /device:TPU:6, one launch (start us, length us, event | category | flops | bytes accessed | tf_op | source)
XLA Modules:
  0.0 212.1 jit_solution(13833154848097795672)
XLA Ops:
  0.8 1.2 fusion.8
  2.2 1.3 fusion.10
  4.7 18.2 %all-to-all-start.1 = ((bf16[32,24,128]{2,1,0:T(8,128)(2,1)}), bf16[32,24,128]{2,1,0:T(8,128)(2,1)S(1)}, u32[]{:S(2)}, u32[]{:S(2)}) async-start(bf16[32,24,128]{2,1,0:T(8,128)(2,1)} %reshape.82), calls=%async_computation.1 | async-start | bytes 393216 | tf_op jit(solution)/shard_map/all_to_all | solution.py:72
  23.9 17.8 %all-to-all-done.1 = bf16[32,24,128]{2,1,0:T(8,128)(2,1)S(1)} async-done(((bf16[32,24,128]{2,1,0:T(8,128)(2,1)}), bf16[32,24,128]{2,1,0:T(8,128)(2,1)S(1)}, u32[]{:S(2)}, u32[]{:S(2)}) %all-to-all-start.1) | async-done | bytes 196640 | tf_op jit(solution)/shard_map/all_to_all | solution.py:72
  41.7 5.1 %all-to-all-start = ((bf16[32,24,128]{2,1,0:T(8,128)(2,1)}), bf16[32,24,128]{2,1,0:T(8,128)(2,1)S(1)}, u32[]{:S(2)}, u32[]{:S(2)}) async-start(bf16[32,24,128]{2,1,0:T(8,128)(2,1)} %reshape.80), calls=%async_computation | async-start | bytes 393216 | tf_op jit(solution)/shard_map/all_to_all | solution.py:72
  46.8 1.9 collective-permute-start.2
  48.7 2.4 %collective-permute-start.3 = (bf16[2048,256]{1,0:T(8,128)(2,1)}, bf16[2048,256]{1,0:T(8,128)(2,1)}, u32[]{:S(2)}, u32[]{:S(2)}) collective-permute-start(bf16[2048,256]{1,0:T(8,128)(2,1)} %param.12), channel_id=1, source_target_pairs={{0,4},{4,0},{1,5},{5,1},{2,6},{6,2},{3,7},{7,3},{8,12},{12,8},{9,1... | collective-permute-start | bytes 3145736 | tf_op jit(solution)/shard_map/ppermute | solution.py:76
  51.1 1.9 collective-permute-start.10
  54.5 2.7 %collective-permute-start.1 = (bf16[96,1024]{1,0:T(8,128)(2,1)}, bf16[96,1024]{1,0:T(8,128)(2,1)}, u32[]{:S(2)}, u32[]{:S(2)}) collective-permute-start(bf16[96,1024]{1,0:T(8,128)(2,1)} %reshape.83), channel_id=1, source_target_pairs={{0,8},{8,0},{1,9},{9,1},{2,10},{10,2},{3,11},{11,3},{4,12},{12,4},... | collective-permute-start | bytes 589832 | tf_op jit(solution)/shard_map/ppermute | solution.py:81
  57.2 7.9 %all-to-all-done = bf16[32,24,128]{2,1,0:T(8,128)(2,1)S(1)} async-done(((bf16[32,24,128]{2,1,0:T(8,128)(2,1)}), bf16[32,24,128]{2,1,0:T(8,128)(2,1)S(1)}, u32[]{:S(2)}, u32[]{:S(2)}) %all-to-all-start) | async-done | bytes 196640 | tf_op jit(solution)/shard_map/all_to_all | solution.py:72
  65.2 2.6 %collective-permute-start = (bf16[96,1024]{1,0:T(8,128)(2,1)S(1)}, bf16[96,1024]{1,0:T(8,128)(2,1)S(1)}, u32[]{:S(2)}, u32[]{:S(2)}) collective-permute-start(bf16[96,1024]{1,0:T(8,128)(2,1)S(1)} %reshape.81), channel_id=1, source_target_pairs={{0,8},{8,0},{1,9},{9,1},{2,10},{10,2},{3,11},{11,3},{4,12},{12,4},... | collective-permute-start | bytes 589832 | tf_op jit(solution)/shard_map/ppermute | solution.py:81
  69.8 3.5 %collective-permute-start.5 = (bf16[192,1024]{1,0:T(8,128)(2,1)S(1)}, bf16[192,1024]{1,0:T(8,128)(2,1)S(1)}, u32[]{:S(2)}, u32[]{:S(2)}) collective-permute-start(bf16[192,1024]{1,0:T(8,128)(2,1)S(1)} %constant_dynamic-update-slice_fusion.2), channel_id=1, source_target_pairs={{0,1},{1,2},{2,3},{3,0},{4,7},{5,4},{6,5},{7,6},{8,9},{9,10},{10,1... | collective-permute-start | bytes 1179656 | tf_op jit(solution)/shard_map/ppermute | solution.py:23
  73.9 3.5 %collective-permute-start.4 = (bf16[192,1024]{1,0:T(8,128)(2,1)S(1)}, bf16[192,1024]{1,0:T(8,128)(2,1)S(1)}, u32[]{:S(2)}, u32[]{:S(2)}) collective-permute-start(bf16[192,1024]{1,0:T(8,128)(2,1)S(1)} %constant_dynamic-update-slice_fusion), channel_id=1, source_target_pairs={{0,1},{1,2},{2,3},{3,0},{4,7},{5,4},{6,5},{7,6},{8,9},{9,10},{10,1... | collective-permute-start | bytes 1179656 | tf_op jit(solution)/shard_map/ppermute | solution.py:23
  78.5 1.3 fusion.19
  79.8 1.3 multiply_convert_fusion.6
  81.5 3.2 %collective-permute-start.7 = (bf16[192,1024]{1,0:T(8,128)(2,1)S(1)}, bf16[192,1024]{1,0:T(8,128)(2,1)S(1)}, u32[]{:S(2)}, u32[]{:S(2)}) collective-permute-start(bf16[192,1024]{1,0:T(8,128)(2,1)S(1)} %collective-permute-done.5), channel_id=1, source_target_pairs={{0,1},{1,2},{2,3},{3,0},{4,7},{5,4},{6,5},{7,6},{8,9},{9,10},{10,1... | collective-permute-start | bytes 1179656 | tf_op jit(solution)/shard_map/ppermute | solution.py:23
  84.7 1.3 fusion.17
  86.3 2.3 %collective-permute-start.6 = (bf16[192,1024]{1,0:T(8,128)(2,1)S(1)}, bf16[192,1024]{1,0:T(8,128)(2,1)S(1)}, u32[]{:S(2)}, u32[]{:S(2)}) collective-permute-start(bf16[192,1024]{1,0:T(8,128)(2,1)S(1)} %collective-permute-done.4), channel_id=1, source_target_pairs={{0,1},{1,2},{2,3},{3,0},{4,7},{5,4},{6,5},{7,6},{8,9},{9,10},{10,1... | collective-permute-start | bytes 1179656 | tf_op jit(solution)/shard_map/ppermute | solution.py:23
  89.2 1.3 multiply_convert_fusion.4
  91.1 1.3 collective-permute-done.7
  92.6 2.0 collective-permute-start.9
  95.2 2.0 collective-permute-done.6
  97.2 1.9 collective-permute-start.8
  99.9 1.3 fusion.15
  101.2 1.3 multiply_convert_fusion.2
  104.3 3.7 %collective-permute-done.8 = bf16[192,1024]{1,0:T(8,128)(2,1)S(1)} collective-permute-done((bf16[192,1024]{1,0:T(8,128)(2,1)S(1)}, bf16[192,1024]{1,0:T(8,128)(2,1)S(1)}, u32[]{:S(2)}, u32[]{:S(2)}) %collective-permute-start.8) | collective-permute-done | bytes 393248 | tf_op jit(solution)/shard_map/ppermute | solution.py:23
  108.9 1.3 fusion.13
  110.2 1.3 multiply_convert_fusion
  111.7 1.9 collective-permute-start.15
  113.7 2.1 collective-permute-start.11
  117.5 1.2 convolution_add_fusion.7
  118.7 3.9 %collective-permute-done.15 = bf16[384,512]{1,0:T(8,128)(2,1)S(1)} collective-permute-done((bf16[384,512]{1,0:T(8,128)(2,1)S(1)}, bf16[384,512]{1,0:T(8,128)(2,1)S(1)}, u32[]{:S(2)}, u32[]{:S(2)}) %collective-permute-start.15) | collective-permute-done | bytes 393248 | tf_op jit(solution)/shard_map/ppermute | solution.py:23
  122.6 1.9 collective-permute-start.16
  126.8 1.9 collective-permute-start.12
  130.5 3.0 %collective-permute-done.16 = bf16[384,512]{1,0:T(8,128)(2,1)S(1)} collective-permute-done((bf16[384,512]{1,0:T(8,128)(2,1)S(1)}, bf16[384,512]{1,0:T(8,128)(2,1)S(1)}, u32[]{:S(2)}, u32[]{:S(2)}) %collective-permute-start.16) | collective-permute-done | bytes 393248 | tf_op jit(solution)/shard_map/ppermute | solution.py:23
  133.4 1.9 collective-permute-start.17
  135.4 1.2 fusion.69
  137.7 1.9 collective-permute-start.13
  141.1 7.5 %collective-permute-done.13 = bf16[384,512]{1,0:T(8,128)(2,1)S(1)} collective-permute-done((bf16[384,512]{1,0:T(8,128)(2,1)S(1)}, bf16[384,512]{1,0:T(8,128)(2,1)S(1)}, u32[]{:S(2)}, u32[]{:S(2)}) %collective-permute-start.13) | collective-permute-done | bytes 393248 | tf_op jit(solution)/shard_map/ppermute | solution.py:23
  150.1 3.4 %collective-permute-start.14 = (bf16[192,512]{1,0:T(8,128)(2,1)S(1)}, bf16[192,512]{1,0:T(8,128)(2,1)S(1)}, u32[]{:S(2)}, u32[]{:S(2)}) collective-permute-start(bf16[192,512]{1,0:T(8,128)(2,1)S(1)} %slice.301), channel_id=1, source_target_pairs={{0,8},{8,0},{1,9},{9,1},{2,10},{10,2},{3,11},{11,3},{4,12},{12,4},... | collective-permute-start | bytes 589832 | tf_op jit(solution)/shard_map/ppermute | solution.py:115
  153.8 3.9 %collective-permute-done.14 = bf16[192,512]{1,0:T(8,128)(2,1)S(1)} collective-permute-done((bf16[192,512]{1,0:T(8,128)(2,1)S(1)}, bf16[192,512]{1,0:T(8,128)(2,1)S(1)}, u32[]{:S(2)}, u32[]{:S(2)}) %collective-permute-start.14) | collective-permute-done | bytes 196640 | tf_op jit(solution)/shard_map/ppermute | solution.py:115
  158.8 10.2 %all-to-all-start.2 = ((bf16[32,24,128]{2,1,0:T(8,128)(2,1)}), bf16[32,24,128]{2,1,0:T(8,128)(2,1)S(1)}, u32[]{:S(2)}, u32[]{:S(2)}) async-start(bf16[32,24,128]{2,1,0:T(8,128)(2,1)} %reshape.85), calls=%async_computation.2 | async-start | bytes 393216 | tf_op jit(solution)/shard_map/all_to_all | solution.py:119
  169.0 1.3 fusion.63
  171.5 2.7 %collective-permute-start.18 = (bf16[192,512]{1,0:T(8,128)(2,1)S(1)}, bf16[192,512]{1,0:T(8,128)(2,1)S(1)}, u32[]{:S(2)}, u32[]{:S(2)}) collective-permute-start(bf16[192,512]{1,0:T(8,128)(2,1)S(1)} %slice.300), channel_id=1, source_target_pairs={{0,8},{8,0},{1,9},{9,1},{2,10},{10,2},{3,11},{11,3},{4,12},{12,4},... | collective-permute-start | bytes 589832 | tf_op jit(solution)/shard_map/ppermute | solution.py:115
  174.3 5.0 %collective-permute-done.18 = bf16[192,512]{1,0:T(8,128)(2,1)S(1)} collective-permute-done((bf16[192,512]{1,0:T(8,128)(2,1)S(1)}, bf16[192,512]{1,0:T(8,128)(2,1)S(1)}, u32[]{:S(2)}, u32[]{:S(2)}) %collective-permute-start.18) | collective-permute-done | bytes 196640 | tf_op jit(solution)/shard_map/ppermute | solution.py:115
  180.4 4.5 %all-to-all-done.2 = bf16[32,24,128]{2,1,0:T(8,128)(2,1)S(1)} async-done(((bf16[32,24,128]{2,1,0:T(8,128)(2,1)}), bf16[32,24,128]{2,1,0:T(8,128)(2,1)S(1)}, u32[]{:S(2)}, u32[]{:S(2)}) %all-to-all-start.2) | async-done | bytes 196640 | tf_op jit(solution)/shard_map/all_to_all | solution.py:119
  184.9 10.0 %all-to-all-start.3 = ((bf16[32,24,128]{2,1,0:T(8,128)(2,1)}), bf16[32,24,128]{2,1,0:T(8,128)(2,1)S(1)}, u32[]{:S(2)}, u32[]{:S(2)}) async-start(bf16[32,24,128]{2,1,0:T(8,128)(2,1)} %reshape.88), calls=%async_computation.3 | async-start | bytes 393216 | tf_op jit(solution)/shard_map/all_to_all | solution.py:119
  196.0 14.9 %all-to-all-done.3 = bf16[32,24,128]{2,1,0:T(8,128)(2,1)S(1)} async-done(((bf16[32,24,128]{2,1,0:T(8,128)(2,1)}), bf16[32,24,128]{2,1,0:T(8,128)(2,1)S(1)}, u32[]{:S(2)}, u32[]{:S(2)}) %all-to-all-start.3) | async-done | bytes 196640 | tf_op jit(solution)/shard_map/all_to_all | solution.py:119
  (109 shorter events, 30.0 us)
Async XLA Ops:
  0.8 2.6 %copy-start.5 = (s32[128]{0:T(128)}, s32[128]{0:T(128)S(1)}, u32[]{:S(2)}) copy-start(s32[128]{0:T(128)S(1)} %get-tuple-element.15) | copy-start | bytes 1540
  0.8 2.7 %copy-start.7 = (s32[128]{0:T(128)}, s32[128]{0:T(128)S(1)}, u32[]{:S(2)}) copy-start(s32[128]{0:T(128)S(1)} %get-tuple-element.16) | copy-start | bytes 1540
  3.7 47.4 %copy-start.1 = (bf16[1024,512]{1,0:T(8,128)(2,1)S(1)}, bf16[1024,512]{1,0:T(8,128)(2,1)}, u32[]{:S(2)}) copy-start(bf16[1024,512]{1,0:T(8,128)(2,1)} %param.13) | copy-start | bytes 3145732
  3.9 42.9 %copy-start = (bf16[2048,256]{1,0:T(8,128)(2,1)S(1)}, bf16[2048,256]{1,0:T(8,128)(2,1)}, u32[]{:S(2)}) copy-start(bf16[2048,256]{1,0:T(8,128)(2,1)} %param.11) | copy-start | bytes 3145732
  4.7 37.0 %all-to-all-start.1 = ((bf16[32,24,128]{2,1,0:T(8,128)(2,1)}), bf16[32,24,128]{2,1,0:T(8,128)(2,1)S(1)}, u32[]{:S(2)}, u32[]{:S(2)}) async-start(bf16[32,24,128]{2,1,0:T(8,128)(2,1)} %reshape.82), calls=%async_computation.1 | async-start | bytes 393216 | tf_op jit(solution)/shard_map/all_to_all | solution.py:72
  41.7 23.4 %all-to-all-start = ((bf16[32,24,128]{2,1,0:T(8,128)(2,1)}), bf16[32,24,128]{2,1,0:T(8,128)(2,1)S(1)}, u32[]{:S(2)}, u32[]{:S(2)}) async-start(bf16[32,24,128]{2,1,0:T(8,128)(2,1)} %reshape.80), calls=%async_computation | async-start | bytes 393216 | tf_op jit(solution)/shard_map/all_to_all | solution.py:72
  46.8 31.2 %collective-permute-start.2 = (bf16[2048,256]{1,0:T(8,128)(2,1)S(1)}, bf16[2048,256]{1,0:T(8,128)(2,1)S(1)}, u32[]{:S(2)}, u32[]{:S(2)}) collective-permute-start(bf16[2048,256]{1,0:T(8,128)(2,1)S(1)} %copy-done), channel_id=1, source_target_pairs={{0,4},{4,0},{1,5},{5,1},{2,6},{6,2},{3,7},{7,3},{8,12},{12,8},{9,1... | collective-permute-start | bytes 3145736 | tf_op jit(solution)/shard_map/ppermute | solution.py:75
  48.7 29.8 %collective-permute-start.3 = (bf16[2048,256]{1,0:T(8,128)(2,1)}, bf16[2048,256]{1,0:T(8,128)(2,1)}, u32[]{:S(2)}, u32[]{:S(2)}) collective-permute-start(bf16[2048,256]{1,0:T(8,128)(2,1)} %param.12), channel_id=1, source_target_pairs={{0,4},{4,0},{1,5},{5,1},{2,6},{6,2},{3,7},{7,3},{8,12},{12,8},{9,1... | collective-permute-start | bytes 3145736 | tf_op jit(solution)/shard_map/ppermute | solution.py:76
  51.1 64.9 %collective-permute-start.10 = (bf16[1024,512]{1,0:T(8,128)(2,1)S(1)}, bf16[1024,512]{1,0:T(8,128)(2,1)}, u32[]{:S(2)}, u32[]{:S(2)}) collective-permute-start(bf16[1024,512]{1,0:T(8,128)(2,1)S(1)} %copy-done.1), channel_id=1, source_target_pairs={{0,4},{4,0},{1,5},{5,1},{2,6},{6,2},{3,7},{7,3},{8,12},{12,8},{9,1... | collective-permute-start | bytes 3145736 | tf_op jit(solution)/shard_map/ppermute | solution.py:77
  54.5 14.3 %collective-permute-start.1 = (bf16[96,1024]{1,0:T(8,128)(2,1)}, bf16[96,1024]{1,0:T(8,128)(2,1)}, u32[]{:S(2)}, u32[]{:S(2)}) collective-permute-start(bf16[96,1024]{1,0:T(8,128)(2,1)} %reshape.83), channel_id=1, source_target_pairs={{0,8},{8,0},{1,9},{9,1},{2,10},{10,2},{3,11},{11,3},{4,12},{12,4},... | collective-permute-start | bytes 589832 | tf_op jit(solution)/shard_map/ppermute | solution.py:81
  65.2 8.7 %collective-permute-start = (bf16[96,1024]{1,0:T(8,128)(2,1)S(1)}, bf16[96,1024]{1,0:T(8,128)(2,1)S(1)}, u32[]{:S(2)}, u32[]{:S(2)}) collective-permute-start(bf16[96,1024]{1,0:T(8,128)(2,1)S(1)} %reshape.81), channel_id=1, source_target_pairs={{0,8},{8,0},{1,9},{9,1},{2,10},{10,2},{3,11},{11,3},{4,12},{12,4},... | collective-permute-start | bytes 589832 | tf_op jit(solution)/shard_map/ppermute | solution.py:81
  68.7 4.8 %copy-start.2 = (bf16[2048,256]{1,0:T(8,128)(2,1)S(1)}, bf16[2048,256]{1,0:T(8,128)(2,1)}, u32[]{:S(2)}) copy-start(bf16[2048,256]{1,0:T(8,128)(2,1)} %param.12) | copy-start | bytes 3145732
  69.8 11.4 %collective-permute-start.5 = (bf16[192,1024]{1,0:T(8,128)(2,1)S(1)}, bf16[192,1024]{1,0:T(8,128)(2,1)S(1)}, u32[]{:S(2)}, u32[]{:S(2)}) collective-permute-start(bf16[192,1024]{1,0:T(8,128)(2,1)S(1)} %constant_dynamic-update-slice_fusion.2), channel_id=1, source_target_pairs={{0,1},{1,2},{2,3},{3,0},{4,7},{5,4},{6,5},{7,6},{8,9},{9,10},{10,1... | collective-permute-start | bytes 1179656 | tf_op jit(solution)/shard_map/ppermute | solution.py:23
  73.9 12.4 %collective-permute-start.4 = (bf16[192,1024]{1,0:T(8,128)(2,1)S(1)}, bf16[192,1024]{1,0:T(8,128)(2,1)S(1)}, u32[]{:S(2)}, u32[]{:S(2)}) collective-permute-start(bf16[192,1024]{1,0:T(8,128)(2,1)S(1)} %constant_dynamic-update-slice_fusion), channel_id=1, source_target_pairs={{0,1},{1,2},{2,3},{3,0},{4,7},{5,4},{6,5},{7,6},{8,9},{9,10},{10,1... | collective-permute-start | bytes 1179656 | tf_op jit(solution)/shard_map/ppermute | solution.py:23
  81.5 10.9 %collective-permute-start.7 = (bf16[192,1024]{1,0:T(8,128)(2,1)S(1)}, bf16[192,1024]{1,0:T(8,128)(2,1)S(1)}, u32[]{:S(2)}, u32[]{:S(2)}) collective-permute-start(bf16[192,1024]{1,0:T(8,128)(2,1)S(1)} %collective-permute-done.5), channel_id=1, source_target_pairs={{0,1},{1,2},{2,3},{3,0},{4,7},{5,4},{6,5},{7,6},{8,9},{9,10},{10,1... | collective-permute-start | bytes 1179656 | tf_op jit(solution)/shard_map/ppermute | solution.py:23
  86.3 10.9 %collective-permute-start.6 = (bf16[192,1024]{1,0:T(8,128)(2,1)S(1)}, bf16[192,1024]{1,0:T(8,128)(2,1)S(1)}, u32[]{:S(2)}, u32[]{:S(2)}) collective-permute-start(bf16[192,1024]{1,0:T(8,128)(2,1)S(1)} %collective-permute-done.4), channel_id=1, source_target_pairs={{0,1},{1,2},{2,3},{3,0},{4,7},{5,4},{6,5},{7,6},{8,9},{9,10},{10,1... | collective-permute-start | bytes 1179656 | tf_op jit(solution)/shard_map/ppermute | solution.py:23
  92.6 10.9 %collective-permute-start.9 = (bf16[192,1024]{1,0:T(8,128)(2,1)S(1)}, bf16[192,1024]{1,0:T(8,128)(2,1)S(1)}, u32[]{:S(2)}, u32[]{:S(2)}) collective-permute-start(bf16[192,1024]{1,0:T(8,128)(2,1)S(1)} %collective-permute-done.7), channel_id=1, source_target_pairs={{0,1},{1,2},{2,3},{3,0},{4,7},{5,4},{6,5},{7,6},{8,9},{9,10},{10,1... | collective-permute-start | bytes 1179656 | tf_op jit(solution)/shard_map/ppermute | solution.py:23
  97.2 10.9 %collective-permute-start.8 = (bf16[192,1024]{1,0:T(8,128)(2,1)S(1)}, bf16[192,1024]{1,0:T(8,128)(2,1)S(1)}, u32[]{:S(2)}, u32[]{:S(2)}) collective-permute-start(bf16[192,1024]{1,0:T(8,128)(2,1)S(1)} %collective-permute-done.6), channel_id=1, source_target_pairs={{0,1},{1,2},{2,3},{3,0},{4,7},{5,4},{6,5},{7,6},{8,9},{9,10},{10,1... | collective-permute-start | bytes 1179656 | tf_op jit(solution)/shard_map/ppermute | solution.py:23
  111.7 10.9 %collective-permute-start.15 = (bf16[384,512]{1,0:T(8,128)(2,1)S(1)}, bf16[384,512]{1,0:T(8,128)(2,1)S(1)}, u32[]{:S(2)}, u32[]{:S(2)}) collective-permute-start(bf16[384,512]{1,0:T(8,128)(2,1)S(1)} %pad_maximum_fusion.1), channel_id=1, source_target_pairs={{0,1},{1,2},{2,3},{3,0},{4,7},{5,4},{6,5},{7,6},{8,9},{9,10},{10,1... | collective-permute-start | bytes 1179656 | tf_op jit(solution)/shard_map/ppermute | solution.py:23
  113.7 13.1 %collective-permute-start.11 = (bf16[384,512]{1,0:T(8,128)(2,1)S(1)}, bf16[384,512]{1,0:T(8,128)(2,1)S(1)}, u32[]{:S(2)}, u32[]{:S(2)}) collective-permute-start(bf16[384,512]{1,0:T(8,128)(2,1)S(1)} %pad_maximum_fusion), channel_id=1, source_target_pairs={{0,1},{1,2},{2,3},{3,0},{4,7},{5,4},{6,5},{7,6},{8,9},{9,10},{10,1... | collective-permute-start | bytes 1179656 | tf_op jit(solution)/shard_map/ppermute | solution.py:23
  122.6 10.9 %collective-permute-start.16 = (bf16[384,512]{1,0:T(8,128)(2,1)S(1)}, bf16[384,512]{1,0:T(8,128)(2,1)S(1)}, u32[]{:S(2)}, u32[]{:S(2)}) collective-permute-start(bf16[384,512]{1,0:T(8,128)(2,1)S(1)} %collective-permute-done.15), channel_id=1, source_target_pairs={{0,1},{1,2},{2,3},{3,0},{4,7},{5,4},{6,5},{7,6},{8,9},{9,10},{10,1... | collective-permute-start | bytes 1179656 | tf_op jit(solution)/shard_map/ppermute | solution.py:23
  126.8 10.9 %collective-permute-start.12 = (bf16[384,512]{1,0:T(8,128)(2,1)S(1)}, bf16[384,512]{1,0:T(8,128)(2,1)S(1)}, u32[]{:S(2)}, u32[]{:S(2)}) collective-permute-start(bf16[384,512]{1,0:T(8,128)(2,1)S(1)} %collective-permute-done.11), channel_id=1, source_target_pairs={{0,1},{1,2},{2,3},{3,0},{4,7},{5,4},{6,5},{7,6},{8,9},{9,10},{10,1... | collective-permute-start | bytes 1179656 | tf_op jit(solution)/shard_map/ppermute | solution.py:23
  133.4 35.5 %collective-permute-start.17 = (bf16[384,512]{1,0:T(8,128)(2,1)S(1)}, bf16[384,512]{1,0:T(8,128)(2,1)}, u32[]{:S(2)}, u32[]{:S(2)}) collective-permute-start(bf16[384,512]{1,0:T(8,128)(2,1)S(1)} %collective-permute-done.16), channel_id=1, source_target_pairs={{0,1},{1,2},{2,3},{3,0},{4,7},{5,4},{6,5},{7,6},{8,9},{9,10},{10,1... | collective-permute-start | bytes 1179656 | tf_op jit(solution)/shard_map/ppermute | solution.py:23
  137.7 10.9 %collective-permute-start.13 = (bf16[384,512]{1,0:T(8,128)(2,1)S(1)}, bf16[384,512]{1,0:T(8,128)(2,1)S(1)}, u32[]{:S(2)}, u32[]{:S(2)}) collective-permute-start(bf16[384,512]{1,0:T(8,128)(2,1)S(1)} %collective-permute-done.12), channel_id=1, source_target_pairs={{0,1},{1,2},{2,3},{3,0},{4,7},{5,4},{6,5},{7,6},{8,9},{9,10},{10,1... | collective-permute-start | bytes 1179656 | tf_op jit(solution)/shard_map/ppermute | solution.py:23
  150.1 7.6 %collective-permute-start.14 = (bf16[192,512]{1,0:T(8,128)(2,1)S(1)}, bf16[192,512]{1,0:T(8,128)(2,1)S(1)}, u32[]{:S(2)}, u32[]{:S(2)}) collective-permute-start(bf16[192,512]{1,0:T(8,128)(2,1)S(1)} %slice.301), channel_id=1, source_target_pairs={{0,8},{8,0},{1,9},{9,1},{2,10},{10,2},{3,11},{11,3},{4,12},{12,4},... | collective-permute-start | bytes 589832 | tf_op jit(solution)/shard_map/ppermute | solution.py:115
  158.8 26.1 %all-to-all-start.2 = ((bf16[32,24,128]{2,1,0:T(8,128)(2,1)}), bf16[32,24,128]{2,1,0:T(8,128)(2,1)S(1)}, u32[]{:S(2)}, u32[]{:S(2)}) async-start(bf16[32,24,128]{2,1,0:T(8,128)(2,1)} %reshape.85), calls=%async_computation.2 | async-start | bytes 393216 | tf_op jit(solution)/shard_map/all_to_all | solution.py:119
  170.3 4.0 %copy-start.9 = (f32[128,2]{0,1:T(2,128)S(1)}, f32[128,2]{0,1:T(2,128)}, u32[]{:S(2)}) copy-start(f32[128,2]{0,1:T(2,128)} %param.10) | copy-start | bytes 3076
  171.5 7.8 %collective-permute-start.18 = (bf16[192,512]{1,0:T(8,128)(2,1)S(1)}, bf16[192,512]{1,0:T(8,128)(2,1)S(1)}, u32[]{:S(2)}, u32[]{:S(2)}) collective-permute-start(bf16[192,512]{1,0:T(8,128)(2,1)S(1)} %slice.300), channel_id=1, source_target_pairs={{0,8},{8,0},{1,9},{9,1},{2,10},{10,2},{3,11},{11,3},{4,12},{12,4},... | collective-permute-start | bytes 589832 | tf_op jit(solution)/shard_map/ppermute | solution.py:115
  179.3 15.6 %copy-start.6 = (s32[128]{0:T(128)S(1)}, s32[128]{0:T(128)}, u32[]{:S(2)}) copy-start(s32[128]{0:T(128)} %copy-done.5) | copy-start | bytes 1540
  179.3 15.6 %copy-start.8 = (s32[128]{0:T(128)S(1)}, s32[128]{0:T(128)}, u32[]{:S(2)}) copy-start(s32[128]{0:T(128)} %copy-done.7) | copy-start | bytes 1540
  179.5 16.2 %copy-start.4 = (f32[192]{0:T(256)S(1)}, f32[192]{0:T(256)}, u32[]{:S(2)}) copy-start(f32[192]{0:T(256)} %get-tuple-element.18) | copy-start | bytes 2308
  180.4 30.6 %copy-start.3 = (f32[192]{0:T(256)S(1)}, f32[192]{0:T(256)}, u32[]{:S(2)}) copy-start(f32[192]{0:T(256)} %get-tuple-element.17) | copy-start | bytes 2308
  184.9 26.0 %all-to-all-start.3 = ((bf16[32,24,128]{2,1,0:T(8,128)(2,1)}), bf16[32,24,128]{2,1,0:T(8,128)(2,1)S(1)}, u32[]{:S(2)}, u32[]{:S(2)}) async-start(bf16[32,24,128]{2,1,0:T(8,128)(2,1)} %reshape.88), calls=%async_computation.3 | async-start | bytes 393216 | tf_op jit(solution)/shard_map/all_to_all | solution.py:119

commit v3 on v1

v3 whole, which is shorter than its diff:
```python
import jax
import jax.numpy as jnp
from jax import lax
from jax.sharding import Mesh
from jax.sharding import PartitionSpec as P


EPS = 1e-06
EP = ("z", "xh", "xl", "c")
EP_TP = ("z", "xh", "xl", "c", "y")
CAP = 12
SWAP = [(0, 1), (1, 0)]


def rms_rows(values, gain):
    widened = values.astype(jnp.float32)
    scale = lax.rsqrt(jnp.mean(widened * widened, axis=-1, keepdims=True) + EPS)
    return (widened * scale * gain).astype(jnp.bfloat16)


def shift(block, by=1):
    up = [(y, (y + by) % 4) for y in range(4)]
    down = [(4 + y, 4 + (y - by) % 4) for y in range(4)]
    return lax.ppermute(block, ("c", "y"), up + down)


def swap(block, axis):
    return lax.ppermute(block, axis, SWAP)


def dot32(a, b):
    return jnp.dot(a, b, preferred_element_type=jnp.float32)


def spread(per_expert, width, precision=None):
    count = per_expert.shape[1]
    expert = lax.broadcasted_iota(jnp.int32, (count, count * width), 1) // width
    own = lax.broadcasted_iota(jnp.int32, (count, count * width), 0)
    table = (expert == own).astype(per_expert.dtype)
    return jnp.dot(per_expert, table, precision=precision, preferred_element_type=jnp.float32)


def layer(tokens, norm_gain, expert_ids, gate_weights, w_gate, w_up, w_down):
    y = lax.axis_index("y")
    turn = 1 - 2 * lax.axis_index("c")
    rows = tokens.shape[0]
    width = tokens.shape[1]
    share = CAP // 4
    expert_count = lax.axis_size(("z", "xh"))
    block_rows = expert_count * share
    depth = w_gate.shape[1]
    out_width = w_down.shape[1]

    gate_x = swap(w_gate, "xl")
    up_x = swap(w_up, "xl")

    normed = rms_rows(tokens, norm_gain)
    experts = jnp.arange(expert_count, dtype=jnp.int32)[None, :]
    first = expert_ids[:, 0:1] == experts
    second = expert_ids[:, 1:2] == experts
    named = first | second
    weight = jnp.where(first, gate_weights[:, 0:1], 0.0) + jnp.where(
        second, gate_weights[:, 1:2], 0.0
    )
    earlier = (
        lax.broadcasted_iota(jnp.int32, (rows, rows), 0)
        > lax.broadcasted_iota(jnp.int32, (rows, rows), 1)
    ).astype(jnp.bfloat16)
    rank = dot32(earlier, named.astype(jnp.bfloat16))
    rank = jnp.where(named, rank, -1.0).astype(jnp.bfloat16)
    column = lax.broadcasted_iota(jnp.int32, (1, block_rows), 1)
    slot = share * y + column % share
    selector = (spread(rank, share) == slot.astype(jnp.float32)).astype(jnp.bfloat16)
    mine = lax.dot_general(
        selector, normed, (((0,), (0,)), ((), ())), preferred_element_type=jnp.float32
    ).astype(jnp.bfloat16)
    mine = mine.reshape(expert_count, share * width // 128, 128)
    arrived = lax.all_to_all(mine, ("z", "xh"), 0, 0, tiled=True)
    near = arrived.reshape(block_rows, width)

    cut = []
    for k in range(4):
        start = ((y + turn * k) & 3) * depth
        cut.append(lax.dynamic_slice_in_dim(w_down, start, depth, 0))
    for k in (1, 2, 3):
        cut[k] = shift(cut[k], k)
    down_o = (jnp.stack([cut[1], cut[3]]), jnp.stack([cut[2], cut[0]]))
    down_x = (swap(down_o[0], "xl"), swap(down_o[1], "xl"))
    gate_c = swap(w_gate, "c")
    up_c = swap(w_up, "c")
    down_c = (swap(down_o[0], "c"), swap(down_o[1], "c"))
    gate_d = swap(gate_x, "c")
    up_d = swap(up_x, "c")
    down_d = (swap(down_x[0], "c"), swap(down_x[1], "c"))

    halves = [near[: block_rows // 2], near[block_rows // 2 :]]
    gathered = list(halves)
    for _ in range(3):
        halves = [shift(halves[0]), shift(halves[1])]
        gathered += halves
    order = (0, 2, 1, 3)
    gathered = jnp.concatenate([gathered[2 * k + i] for k in order for i in range(2)], 0)

    gates = (w_gate, gate_c, gate_x, gate_d)
    uppers = (w_up, up_c, up_x, up_d)
    hidden = []
    for gate, up in zip(gates, uppers):
        gate_proj = dot32(gathered, gate)
        upper = dot32(gathered, up)
        hidden.append((jax.nn.silu(gate_proj) * upper).astype(jnp.bfloat16))

    def pick(pair, k):
        return pair[0][k // 2] if k % 2 else pair[1][0 if k else 1]

    half_rows = 2 * block_rows

    def partial(k):
        total = 0.0
        for matrix, pair, at in zip(
            hidden, (down_o, down_c, down_x, down_d), (k, (-k) % 4, k, (-k) % 4)
        ):
            total += dot32(matrix, pick(pair, at))
        return total

    total = partial(1)
    for step in (1, 2, 3):
        away = total.astype(jnp.bfloat16)
        back = [shift(away[:half_rows]), shift(away[half_rows:])]
        turned = [back[1][block_rows:], back[1][:block_rows], back[0]]
        total = partial((step + 1) % 4) + jnp.concatenate(turned, 0).astype(jnp.float32)
    home = total.astype(jnp.bfloat16)
    home = home.reshape(4, expert_count, share, out_width).transpose(1, 0, 2, 3)
    home = home.reshape(expert_count, CAP * out_width // 128, 128)
    returned = lax.all_to_all(home, ("z", "xh"), 0, 0, tiled=True)
    returned = returned.reshape(expert_count * CAP, out_width).astype(jnp.float32)
    column = lax.broadcasted_iota(jnp.int32, (1, expert_count * CAP), 1) % CAP
    place = column // share
    behind = 2 * (place % 2) + place // 2
    slot = share * ((y - turn * behind) & 3) + column % share
    chosen = spread(rank, CAP) == slot.astype(jnp.float32)
    combine = jnp.where(chosen, spread(weight, CAP, lax.Precision.HIGHEST), 0.0)
    mixed = jnp.dot(
        combine, returned, precision=lax.Precision.HIGHEST, preferred_element_type=jnp.float32
    )
    return mixed.astype(jnp.bfloat16)


def mapped(mesh):
    finer = Mesh(mesh.devices.reshape(-1, 2, 2, 2, 4), EP_TP)
    placed = (
        P(EP, None),
        P(),
        P(EP, None),
        P(EP, None),
        P(None, EP_TP),
        P(None, EP_TP),
        P(EP, "y"),
    )
    return jax.shard_map(layer, mesh=finer, in_specs=placed, out_specs=P(EP, "y"), check_vma=False)


def solution(mesh):
    return mapped(mesh)
```

time: 196 us -> 206 us (1.051)
  blocking collectives: 45.3 us -> 0 us
  starting transfers between devices: 54.9 us -> 92.8 us
  waiting for transfers between devices: 74.6 us -> 87.7 us
  matrix products: 12.2 us -> 15.7 us
    all_to_all x1 -> x0, blocking collectives: 45.3 us -> none  [on_device(): arrived = lax.all_to_all(mine, ('z', 'xh'), 0, 0, tiled=True)]
    ppermute x20 -> x27, starting transfers between devices: 47.4 us -> 68.3 us  [the longest x15 40.2 us: shift(): return lax.ppermute(block, ('c', 'y'), up + down)]
    all_to_all x1 -> x2, starting transfers between devices: 7.51 us -> 24.5 us  [the longest x1 18.2 us: layer(): arrived = lax.all_to_all(mine, ('z', 'xh'), 0, 0, tiled=True)]
    ppermute x20 -> x27, waiting for transfers between devices: 48.7 us -> 56.6 us  [the longest x15 41.9 us: shift(): return lax.ppermute(block, ('c', 'y'), up + down)]
    all_to_all x1 -> x2, waiting for transfers between devices: 25.8 us -> 31.1 us  [the longest x1 22.8 us: layer(): returned = lax.all_to_all(home, ('z', 'xh'), 0, 0, tiled=True)]
    dot_general x25, matrix products: 9.15 us -> 12.6 us  [dot32(): return jnp.dot(a, b, preferred_element_type=jnp.float32)]
  transfers between devices with their start and end apart: 21 -> 29, of which waited for: 12 -> 14; matrix products, arithmetic and copies ran while one was open for 6% -> 7% of each run, Pallas kernels for 0% -> 0%
where the time goes in v3:
time: 206 us; the launch traced here: 204 us
  starting transfers between devices  92.8 us (45%)
  waiting for transfers between devices  87.7 us (43%)
  matrix products  15.7 us (8%)
  local copies, waits for them, and re-layouts  4.7 us (2%)
  other arithmetic  2.29 us (1%)
    ppermute x15, waiting for transfers between devices, shift(): return lax.ppermute(block, ('c', 'y'), up + down)  41.9 us
    ppermute x15, starting transfers between devices, shift(): return lax.ppermute(block, ('c', 'y'), up + down)  40.2 us
    ppermute x12, starting transfers between devices, swap(): return lax.ppermute(block, axis, SWAP)  28.1 us
    all_to_all x1, waiting for transfers between devices, layer(): returned = lax.all_to_all(home, ('z', 'xh'), 0, 0, tiled=True)  22.8 us
    all_to_all x1, starting transfers between devices, layer(): arrived = lax.all_to_all(mine, ('z', 'xh'), 0, 0, tiled=True)  18.2 us
    ppermute x12, waiting for transfers between devices, swap(): return lax.ppermute(block, axis, SWAP)  14.7 us
    dot_general x25, matrix products, dot32(): return jnp.dot(a, b, preferred_element_type=jnp.float32)  12.6 us
    all_to_all x1, waiting for transfers between devices, layer(): arrived = lax.all_to_all(mine, ('z', 'xh'), 0, 0, tiled=True)  8.29 us
  transfers between devices with their start and end apart: 29, of which 14 were waited for; matrix products, arithmetic and copies ran while one was open for 7% of the time, Pallas kernels for 0%

profile of v3, /device:TPU:6, one launch (start us, length us, event | category | flops | bytes accessed | tf_op | source)
XLA Modules:
  0.0 204.1 jit_solution(13170161862806607033)
XLA Ops:
  0.8 1.3 fusion.11
  2.3 1.5 convolution_convert_fusion
  4.8 18.2 %all-to-all-start = ((bf16[32,48,128]{2,1,0:T(8,128)(2,1)}), bf16[32,48,128]{2,1,0:T(8,128)(2,1)S(1)}, u32[]{:S(2)}, u32[]{:S(2)}) async-start(bf16[32,48,128]{2,1,0:T(8,128)(2,1)} %reshape.150), calls=%async_computation | async-start | bytes 786432 | tf_op jit(solution)/shard_map/all_to_all | solution.py:78
  23.1 5.1 %collective-permute-start.8 = (bf16[256,512]{1,0:T(8,128)(2,1)S(1)}, bf16[256,512]{1,0:T(8,128)(2,1)S(1)}, u32[]{:S(2)}, u32[]{:S(2)}) collective-permute-start(bf16[256,512]{1,0:T(8,128)(2,1)S(1)} %get-tuple-element.7), channel_id=1, source_target_pairs={{0,2},{1,3},{2,0},{3,1},{4,6},{5,7},{6,4},{7,5},{8,10},{9,11},{10,... | collective-permute-start | bytes 786440 | tf_op jit(solution)/shard_map/ppermute | solution.py:24
  28.2 3.0 %collective-permute-start.16 = (bf16[256,512]{1,0:T(8,128)(2,1)S(1)}, bf16[256,512]{1,0:T(8,128)(2,1)S(1)}, u32[]{:S(2)}, u32[]{:S(2)}) collective-permute-start(bf16[256,512]{1,0:T(8,128)(2,1)S(1)} %get-tuple-element.8), channel_id=1, source_target_pairs={{0,3},{1,0},{2,1},{3,2},{4,5},{5,6},{6,7},{7,4},{8,11},{9,8},{10,9... | collective-permute-start | bytes 786440 | tf_op jit(solution)/shard_map/ppermute | solution.py:24
  31.2 2.9 %collective-permute-start.17 = (bf16[256,512]{1,0:T(8,128)(2,1)S(1)}, bf16[256,512]{1,0:T(8,128)(2,1)S(1)}, u32[]{:S(2)}, u32[]{:S(2)}) collective-permute-start(bf16[256,512]{1,0:T(8,128)(2,1)S(1)} %get-tuple-element.5), channel_id=1, source_target_pairs={{0,1},{1,2},{2,3},{3,0},{4,7},{5,4},{6,5},{7,6},{8,9},{9,10},{10,1... | collective-permute-start | bytes 786440 | tf_op jit(solution)/shard_map/ppermute | solution.py:24
  34.1 1.9 collective-permute-start.6
  36.0 2.7 %collective-permute-start.10 = (bf16[2048,256]{1,0:T(8,128)(2,1)}, bf16[2048,256]{1,0:T(8,128)(2,1)}, u32[]{:S(2)}, u32[]{:S(2)}) collective-permute-start(bf16[2048,256]{1,0:T(8,128)(2,1)} %param.11), channel_id=1, source_target_pairs={{0,8},{8,0},{1,9},{9,1},{2,10},{10,2},{3,11},{11,3},{4,12},{12,4},... | collective-permute-start | bytes 3145736 | tf_op jit(solution)/shard_map/ppermute | solution.py:28
  38.8 2.1 %collective-permute-start.7 = (bf16[2048,256]{1,0:T(8,128)(2,1)}, bf16[2048,256]{1,0:T(8,128)(2,1)}, u32[]{:S(2)}, u32[]{:S(2)}) collective-permute-start(bf16[2048,256]{1,0:T(8,128)(2,1)} %param.12), channel_id=1, source_target_pairs={{0,4},{4,0},{1,5},{5,1},{2,6},{6,2},{3,7},{7,3},{8,12},{12,8},{9,1... | collective-permute-start | bytes 3145736 | tf_op jit(solution)/shard_map/ppermute | solution.py:28
  41.8 8.3 %all-to-all-done = bf16[32,48,128]{2,1,0:T(8,128)(2,1)S(1)} async-done(((bf16[32,48,128]{2,1,0:T(8,128)(2,1)}), bf16[32,48,128]{2,1,0:T(8,128)(2,1)S(1)}, u32[]{:S(2)}, u32[]{:S(2)}) %all-to-all-start) | async-done | bytes 393248 | tf_op jit(solution)/shard_map/all_to_all | solution.py:78
  50.3 3.5 %collective-permute-start = (bf16[48,2048]{1,0:T(8,128)(2,1)S(1)}, bf16[48,2048]{1,0:T(8,128)(2,1)S(1)}, u32[]{:S(2)}, u32[]{:S(2)}) collective-permute-start(bf16[48,2048]{1,0:T(8,128)(2,1)S(1)} %slice.101), channel_id=1, source_target_pairs={{0,1},{1,2},{2,3},{3,0},{4,7},{5,4},{6,5},{7,6},{8,9},{9,10},{10,1... | collective-permute-start | bytes 589832 | tf_op jit(solution)/shard_map/ppermute | solution.py:24
  53.8 3.5 %collective-permute-start.2 = (bf16[48,2048]{1,0:T(8,128)(2,1)S(1)}, bf16[48,2048]{1,0:T(8,128)(2,1)S(1)}, u32[]{:S(2)}, u32[]{:S(2)}) collective-permute-start(bf16[48,2048]{1,0:T(8,128)(2,1)S(1)} %slice.103), channel_id=1, source_target_pairs={{0,1},{1,2},{2,3},{3,0},{4,7},{5,4},{6,5},{7,6},{8,9},{9,10},{10,1... | collective-permute-start | bytes 589832 | tf_op jit(solution)/shard_map/ppermute | solution.py:24
  57.3 1.8 collective-permute-done
  59.1 2.3 %collective-permute-start.1 = (bf16[48,2048]{1,0:T(8,128)(2,1)S(1)}, bf16[48,2048]{1,0:T(8,128)(2,1)S(1)}, u32[]{:S(2)}, u32[]{:S(2)}) collective-permute-start(bf16[48,2048]{1,0:T(8,128)(2,1)S(1)} %collective-permute-done), channel_id=1, source_target_pairs={{0,1},{1,2},{2,3},{3,0},{4,7},{5,4},{6,5},{7,6},{8,9},{9,10},{10,1... | collective-permute-start | bytes 589832 | tf_op jit(solution)/shard_map/ppermute | solution.py:24
  61.4 1.2 collective-permute-done.2
  62.6 2.7 %collective-permute-start.11 = (bf16[2048,256]{1,0:T(8,128)(2,1)}, bf16[2048,256]{1,0:T(8,128)(2,1)S(1)}, u32[]{:S(2)}, u32[]{:S(2)}) collective-permute-start(bf16[2048,256]{1,0:T(8,128)(2,1)} %param.12), channel_id=1, source_target_pairs={{0,8},{8,0},{1,9},{9,1},{2,10},{10,2},{3,11},{11,3},{4,12},{12,4},... | collective-permute-start | bytes 3145736 | tf_op jit(solution)/shard_map/ppermute | solution.py:28
  65.3 2.5 %collective-permute-done.1 = bf16[48,2048]{1,0:T(8,128)(2,1)S(1)} collective-permute-done((bf16[48,2048]{1,0:T(8,128)(2,1)S(1)}, bf16[48,2048]{1,0:T(8,128)(2,1)S(1)}, u32[]{:S(2)}, u32[]{:S(2)}) %collective-permute-start.1) | collective-permute-done | bytes 196640 | tf_op jit(solution)/shard_map/ppermute | solution.py:24
  67.9 1.9 collective-permute-start.3
  69.8 6.8 %collective-permute-done.3 = bf16[48,2048]{1,0:T(8,128)(2,1)S(1)} collective-permute-done((bf16[48,2048]{1,0:T(8,128)(2,1)S(1)}, bf16[48,2048]{1,0:T(8,128)(2,1)S(1)}, u32[]{:S(2)}, u32[]{:S(2)}) %collective-permute-start.3) | collective-permute-done | bytes 196640 | tf_op jit(solution)/shard_map/ppermute | solution.py:24
  76.6 1.9 collective-permute-start.4
  78.6 6.8 %collective-permute-done.4 = bf16[48,2048]{1,0:T(8,128)(2,1)S(1)} collective-permute-done((bf16[48,2048]{1,0:T(8,128)(2,1)S(1)}, bf16[48,2048]{1,0:T(8,128)(2,1)S(1)}, u32[]{:S(2)}, u32[]{:S(2)}) %collective-permute-start.4) | collective-permute-done | bytes 196640 | tf_op jit(solution)/shard_map/ppermute | solution.py:24
  85.4 1.9 collective-permute-start.5
  87.3 6.8 %collective-permute-done.5 = bf16[48,2048]{1,0:T(8,128)(2,1)S(1)} collective-permute-done((bf16[48,2048]{1,0:T(8,128)(2,1)S(1)}, bf16[48,2048]{1,0:T(8,128)(2,1)S(1)}, u32[]{:S(2)}, u32[]{:S(2)}) %collective-permute-start.5) | collective-permute-done | bytes 196640 | tf_op jit(solution)/shard_map/ppermute | solution.py:24
  94.1 1.9 collective-permute-start.9
  96.1 2.9 %collective-permute-start.12 = (bf16[2,256,512]{2,1,0:T(8,128)(2,1)S(1)}, bf16[2,256,512]{2,1,0:T(8,128)(2,1)S(1)}, u32[]{:S(2)}, u32[]{:S(2)}) collective-permute-start(bf16[2,256,512]{2,1,0:T(8,128)(2,1)S(1)} %pad_maximum_fusion), channel_id=1, source_target_pairs={{0,8},{8,0},{1,9},{9,1},{2,10},{10,2},{3,11},{11,3},{4,12},{12,4},... | collective-permute-start | bytes 1572872 | tf_op jit(solution)/shard_map/ppermute | solution.py:28
  99.0 1.8 fusion.81
  100.8 3.2 %collective-permute-start.19 = (bf16[2,256,512]{2,1,0:T(8,128)(2,1)S(1)}, bf16[2,256,512]{2,1,0:T(8,128)(2,1)S(1)}, u32[]{:S(2)}, u32[]{:S(2)}) collective-permute-start(bf16[2,256,512]{2,1,0:T(8,128)(2,1)S(1)} %copy-done.1), channel_id=1, source_target_pairs={{0,8},{8,0},{1,9},{9,1},{2,10},{10,2},{3,11},{11,3},{4,12},{12,4},... | collective-permute-start | bytes 1572872 | tf_op jit(solution)/shard_map/ppermute | solution.py:28
  105.3 1.9 collective-permute-start.13
  107.2 1.8 fusion.80
  109.0 14.7 %collective-permute-done.19 = bf16[2,256,512]{2,1,0:T(8,128)(2,1)S(1)} collective-permute-done((bf16[2,256,512]{2,1,0:T(8,128)(2,1)S(1)}, bf16[2,256,512]{2,1,0:T(8,128)(2,1)S(1)}, u32[]{:S(2)}, u32[]{:S(2)}) %collective-permute-start.19) | collective-permute-done | bytes 524320 | tf_op jit(solution)/shard_map/ppermute | solution.py:28
  123.7 1.9 collective-permute-start.18
  125.9 2.4 %collective-permute-start.20 = (bf16[2,256,512]{2,1,0:T(8,128)(2,1)S(1)}, bf16[2,256,512]{2,1,0:T(8,128)(2,1)S(1)}, u32[]{:S(2)}, u32[]{:S(2)}) collective-permute-start(bf16[2,256,512]{2,1,0:T(8,128)(2,1)S(1)} %collective-permute-done.19), channel_id=1, source_target_pairs={{0,4},{4,0},{1,5},{5,1},{2,6},{6,2},{3,7},{7,3},{8,12},{12,8},{9,1... | collective-permute-start | bytes 1572872 | tf_op jit(solution)/shard_map/ppermute | solution.py:28
  128.3 1.9 collective-permute-start.15
  130.2 1.8 multiply_convert_fusion.2
  132.1 2.4 %collective-permute-start.14 = (bf16[2048,256]{1,0:T(8,128)(2,1)S(1)}, bf16[2048,256]{1,0:T(8,128)(2,1)S(1)}, u32[]{:S(2)}, u32[]{:S(2)}) collective-permute-start(bf16[2048,256]{1,0:T(8,128)(2,1)S(1)} %collective-permute-done.11), channel_id=1, source_target_pairs={{0,4},{4,0},{1,5},{5,1},{2,6},{6,2},{3,7},{7,3},{8,12},{12,8},{9,1... | collective-permute-start | bytes 3145736 | tf_op jit(solution)/shard_map/ppermute | solution.py:28
  137.7 1.9 collective-permute-start.22
  139.7 1.9 collective-permute-start.21
  143.5 5.1 %collective-permute-done.21 = bf16[192,512]{1,0:T(8,128)(2,1)S(1)} collective-permute-done((bf16[192,512]{1,0:T(8,128)(2,1)S(1)}, bf16[192,512]{1,0:T(8,128)(2,1)S(1)}, u32[]{:S(2)}, u32[]{:S(2)}) %collective-permute-start.21) | collective-permute-done | bytes 196640 | tf_op jit(solution)/shard_map/ppermute | solution.py:24
  148.9 1.9 collective-permute-start.23
  151.1 2.7 %collective-permute-start.24 = (bf16[192,512]{1,0:T(8,128)(2,1)S(1)}, bf16[192,512]{1,0:T(8,128)(2,1)S(1)}, u32[]{:S(2)}, u32[]{:S(2)}) collective-permute-start(bf16[192,512]{1,0:T(8,128)(2,1)S(1)} %get-tuple-element.12), channel_id=1, source_target_pairs={{0,1},{1,2},{2,3},{3,0},{4,7},{5,4},{6,5},{7,6},{8,9},{9,10},{10,1... | collective-permute-start | bytes 589832 | tf_op jit(solution)/shard_map/ppermute | solution.py:24
  153.8 3.9 %collective-permute-done.23 = bf16[192,512]{1,0:T(8,128)(2,1)S(1)} collective-permute-done((bf16[192,512]{1,0:T(8,128)(2,1)S(1)}, bf16[192,512]{1,0:T(8,128)(2,1)S(1)}, u32[]{:S(2)}, u32[]{:S(2)}) %collective-permute-start.23) | collective-permute-done | bytes 196640 | tf_op jit(solution)/shard_map/ppermute | solution.py:24
  157.7 2.2 %collective-permute-done.24 = bf16[192,512]{1,0:T(8,128)(2,1)S(1)} collective-permute-done((bf16[192,512]{1,0:T(8,128)(2,1)S(1)}, bf16[192,512]{1,0:T(8,128)(2,1)S(1)}, u32[]{:S(2)}, u32[]{:S(2)}) %collective-permute-start.24) | collective-permute-done | bytes 196640 | tf_op jit(solution)/shard_map/ppermute | solution.py:24
  160.2 1.9 collective-permute-start.25
  162.4 3.9 %collective-permute-start.26 = (bf16[192,512]{1,0:T(8,128)(2,1)S(1)}, bf16[192,512]{1,0:T(8,128)(2,1)S(1)}, u32[]{:S(2)}, u32[]{:S(2)}) collective-permute-start(bf16[192,512]{1,0:T(8,128)(2,1)S(1)} %get-tuple-element.10), channel_id=1, source_target_pairs={{0,1},{1,2},{2,3},{3,0},{4,7},{5,4},{6,5},{7,6},{8,9},{9,10},{10,1... | collective-permute-start | bytes 589832 | tf_op jit(solution)/shard_map/ppermute | solution.py:24
  166.4 2.6 %collective-permute-done.25 = bf16[192,512]{1,0:T(8,128)(2,1)S(1)} collective-permute-done((bf16[192,512]{1,0:T(8,128)(2,1)S(1)}, bf16[192,512]{1,0:T(8,128)(2,1)S(1)}, u32[]{:S(2)}, u32[]{:S(2)}) %collective-permute-start.25) | collective-permute-done | bytes 196640 | tf_op jit(solution)/shard_map/ppermute | solution.py:24
  169.0 2.2 %collective-permute-done.26 = bf16[192,512]{1,0:T(8,128)(2,1)S(1)} collective-permute-done((bf16[192,512]{1,0:T(8,128)(2,1)S(1)}, bf16[192,512]{1,0:T(8,128)(2,1)S(1)}, u32[]{:S(2)}, u32[]{:S(2)}) %collective-permute-start.26) | collective-permute-done | bytes 196640 | tf_op jit(solution)/shard_map/ppermute | solution.py:24
  173.1 6.3 %all-to-all-start.1 = ((bf16[32,48,128]{2,1,0:T(8,128)(2,1)}), bf16[32,48,128]{2,1,0:T(8,128)(2,1)S(1)}, u32[]{:S(2)}, u32[]{:S(2)}) async-start(bf16[32,48,128]{2,1,0:T(8,128)(2,1)} %reshape.152), calls=%async_computation.1 | async-start | bytes 786432 | tf_op jit(solution)/shard_map/all_to_all | solution.py:134
  180.0 22.8 %all-to-all-done.1 = bf16[32,48,128]{2,1,0:T(8,128)(2,1)S(1)} async-done(((bf16[32,48,128]{2,1,0:T(8,128)(2,1)}), bf16[32,48,128]{2,1,0:T(8,128)(2,1)S(1)}, u32[]{:S(2)}, u32[]{:S(2)}) %all-to-all-start.1) | async-done | bytes 393248 | tf_op jit(solution)/shard_map/all_to_all | solution.py:134
  (84 shorter events, 14.5 us)
Async XLA Ops:
  0.8 22.2 %copy-start = (bf16[1024,512]{1,0:T(8,128)(2,1)S(1)}, bf16[1024,512]{1,0:T(8,128)(2,1)}, u32[]{:S(2)}) copy-start(bf16[1024,512]{1,0:T(8,128)(2,1)} %param.13) | copy-start | bytes 3145732
  4.8 45.3 %all-to-all-start = ((bf16[32,48,128]{2,1,0:T(8,128)(2,1)}), bf16[32,48,128]{2,1,0:T(8,128)(2,1)S(1)}, u32[]{:S(2)}, u32[]{:S(2)}) async-start(bf16[32,48,128]{2,1,0:T(8,128)(2,1)} %reshape.150), calls=%async_computation | async-start | bytes 786432 | tf_op jit(solution)/shard_map/all_to_all | solution.py:78
  23.1 15.7 %collective-permute-start.8 = (bf16[256,512]{1,0:T(8,128)(2,1)S(1)}, bf16[256,512]{1,0:T(8,128)(2,1)S(1)}, u32[]{:S(2)}, u32[]{:S(2)}) collective-permute-start(bf16[256,512]{1,0:T(8,128)(2,1)S(1)} %get-tuple-element.7), channel_id=1, source_target_pairs={{0,2},{1,3},{2,0},{3,1},{4,6},{5,7},{6,4},{7,5},{8,10},{9,11},{10,... | collective-permute-start | bytes 786440 | tf_op jit(solution)/shard_map/ppermute | solution.py:24
  28.2 12.7 %collective-permute-start.16 = (bf16[256,512]{1,0:T(8,128)(2,1)S(1)}, bf16[256,512]{1,0:T(8,128)(2,1)S(1)}, u32[]{:S(2)}, u32[]{:S(2)}) collective-permute-start(bf16[256,512]{1,0:T(8,128)(2,1)S(1)} %get-tuple-element.8), channel_id=1, source_target_pairs={{0,3},{1,0},{2,1},{3,2},{4,5},{5,6},{6,7},{7,4},{8,11},{9,8},{10,9... | collective-permute-start | bytes 786440 | tf_op jit(solution)/shard_map/ppermute | solution.py:24
  31.2 9.8 %collective-permute-start.17 = (bf16[256,512]{1,0:T(8,128)(2,1)S(1)}, bf16[256,512]{1,0:T(8,128)(2,1)S(1)}, u32[]{:S(2)}, u32[]{:S(2)}) collective-permute-start(bf16[256,512]{1,0:T(8,128)(2,1)S(1)} %get-tuple-element.5), channel_id=1, source_target_pairs={{0,1},{1,2},{2,3},{3,0},{4,7},{5,4},{6,5},{7,6},{8,9},{9,10},{10,1... | collective-permute-start | bytes 786440 | tf_op jit(solution)/shard_map/ppermute | solution.py:24
  34.1 71.2 %collective-permute-start.6 = (bf16[2048,256]{1,0:T(8,128)(2,1)}, bf16[2048,256]{1,0:T(8,128)(2,1)}, u32[]{:S(2)}, u32[]{:S(2)}) collective-permute-start(bf16[2048,256]{1,0:T(8,128)(2,1)} %param.11), channel_id=1, source_target_pairs={{0,4},{4,0},{1,5},{5,1},{2,6},{6,2},{3,7},{7,3},{8,12},{12,8},{9,1... | collective-permute-start | bytes 3145736 | tf_op jit(solution)/shard_map/ppermute | solution.py:28
  36.0 60.1 %collective-permute-start.10 = (bf16[2048,256]{1,0:T(8,128)(2,1)}, bf16[2048,256]{1,0:T(8,128)(2,1)}, u32[]{:S(2)}, u32[]{:S(2)}) collective-permute-start(bf16[2048,256]{1,0:T(8,128)(2,1)} %param.11), channel_id=1, source_target_pairs={{0,8},{8,0},{1,9},{9,1},{2,10},{10,2},{3,11},{11,3},{4,12},{12,4},... | collective-permute-start | bytes 3145736 | tf_op jit(solution)/shard_map/ppermute | solution.py:28
  38.8 89.5 %collective-permute-start.7 = (bf16[2048,256]{1,0:T(8,128)(2,1)}, bf16[2048,256]{1,0:T(8,128)(2,1)}, u32[]{:S(2)}, u32[]{:S(2)}) collective-permute-start(bf16[2048,256]{1,0:T(8,128)(2,1)} %param.12), channel_id=1, source_target_pairs={{0,4},{4,0},{1,5},{5,1},{2,6},{6,2},{3,7},{7,3},{8,12},{12,8},{9,1... | collective-permute-start | bytes 3145736 | tf_op jit(solution)/shard_map/ppermute | solution.py:28
  50.3 8.8 %collective-permute-start = (bf16[48,2048]{1,0:T(8,128)(2,1)S(1)}, bf16[48,2048]{1,0:T(8,128)(2,1)S(1)}, u32[]{:S(2)}, u32[]{:S(2)}) collective-permute-start(bf16[48,2048]{1,0:T(8,128)(2,1)S(1)} %slice.101), channel_id=1, source_target_pairs={{0,1},{1,2},{2,3},{3,0},{4,7},{5,4},{6,5},{7,6},{8,9},{9,10},{10,1... | collective-permute-start | bytes 589832 | tf_op jit(solution)/shard_map/ppermute | solution.py:24
  53.8 8.8 %collective-permute-start.2 = (bf16[48,2048]{1,0:T(8,128)(2,1)S(1)}, bf16[48,2048]{1,0:T(8,128)(2,1)S(1)}, u32[]{:S(2)}, u32[]{:S(2)}) collective-permute-start(bf16[48,2048]{1,0:T(8,128)(2,1)S(1)} %slice.103), channel_id=1, source_target_pairs={{0,1},{1,2},{2,3},{3,0},{4,7},{5,4},{6,5},{7,6},{8,9},{9,10},{10,1... | collective-permute-start | bytes 589832 | tf_op jit(solution)/shard_map/ppermute | solution.py:24
  59.1 8.8 %collective-permute-start.1 = (bf16[48,2048]{1,0:T(8,128)(2,1)S(1)}, bf16[48,2048]{1,0:T(8,128)(2,1)S(1)}, u32[]{:S(2)}, u32[]{:S(2)}) collective-permute-start(bf16[48,2048]{1,0:T(8,128)(2,1)S(1)} %collective-permute-done), channel_id=1, source_target_pairs={{0,1},{1,2},{2,3},{3,0},{4,7},{5,4},{6,5},{7,6},{8,9},{9,10},{10,1... | collective-permute-start | bytes 589832 | tf_op jit(solution)/shard_map/ppermute | solution.py:24
  62.6 38.2 %collective-permute-start.11 = (bf16[2048,256]{1,0:T(8,128)(2,1)}, bf16[2048,256]{1,0:T(8,128)(2,1)S(1)}, u32[]{:S(2)}, u32[]{:S(2)}) collective-permute-start(bf16[2048,256]{1,0:T(8,128)(2,1)} %param.12), channel_id=1, source_target_pairs={{0,8},{8,0},{1,9},{9,1},{2,10},{10,2},{3,11},{11,3},{4,12},{12,4},... | collective-permute-start | bytes 3145736 | tf_op jit(solution)/shard_map/ppermute | solution.py:28
  67.9 8.8 %collective-permute-start.3 = (bf16[48,2048]{1,0:T(8,128)(2,1)S(1)}, bf16[48,2048]{1,0:T(8,128)(2,1)S(1)}, u32[]{:S(2)}, u32[]{:S(2)}) collective-permute-start(bf16[48,2048]{1,0:T(8,128)(2,1)S(1)} %collective-permute-done.2), channel_id=1, source_target_pairs={{0,1},{1,2},{2,3},{3,0},{4,7},{5,4},{6,5},{7,6},{8,9},{9,10},{10,1... | collective-permute-start | bytes 589832 | tf_op jit(solution)/shard_map/ppermute | solution.py:24
  76.6 8.8 %collective-permute-start.4 = (bf16[48,2048]{1,0:T(8,128)(2,1)S(1)}, bf16[48,2048]{1,0:T(8,128)(2,1)S(1)}, u32[]{:S(2)}, u32[]{:S(2)}) collective-permute-start(bf16[48,2048]{1,0:T(8,128)(2,1)S(1)} %collective-permute-done.1), channel_id=1, source_target_pairs={{0,1},{1,2},{2,3},{3,0},{4,7},{5,4},{6,5},{7,6},{8,9},{9,10},{10,1... | collective-permute-start | bytes 589832 | tf_op jit(solution)/shard_map/ppermute | solution.py:24
  85.4 8.8 %collective-permute-start.5 = (bf16[48,2048]{1,0:T(8,128)(2,1)S(1)}, bf16[48,2048]{1,0:T(8,128)(2,1)S(1)}, u32[]{:S(2)}, u32[]{:S(2)}) collective-permute-start(bf16[48,2048]{1,0:T(8,128)(2,1)S(1)} %collective-permute-done.3), channel_id=1, source_target_pairs={{0,1},{1,2},{2,3},{3,0},{4,7},{5,4},{6,5},{7,6},{8,9},{9,10},{10,1... | collective-permute-start | bytes 589832 | tf_op jit(solution)/shard_map/ppermute | solution.py:24
  94.1 48.2 %collective-permute-start.9 = (bf16[2,256,512]{2,1,0:T(8,128)(2,1)S(1)}, bf16[2,256,512]{2,1,0:T(8,128)(2,1)S(1)}, u32[]{:S(2)}, u32[]{:S(2)}) collective-permute-start(bf16[2,256,512]{2,1,0:T(8,128)(2,1)S(1)} %pad_maximum_fusion), channel_id=1, source_target_pairs={{0,4},{4,0},{1,5},{5,1},{2,6},{6,2},{3,7},{7,3},{8,12},{12,8},{9,1... | collective-permute-start | bytes 1572872 | tf_op jit(solution)/shard_map/ppermute | solution.py:28
  96.1 4.7 %copy-start.1 = (bf16[2,256,512]{2,1,0:T(8,128)(2,1)S(1)}, bf16[2,256,512]{2,1,0:T(8,128)(2,1)}, u32[]{:S(2)}) copy-start(bf16[2,256,512]{2,1,0:T(8,128)(2,1)} %pad_maximum_fusion.1) | copy-start | bytes 1572868
  96.1 29.8 %collective-permute-start.12 = (bf16[2,256,512]{2,1,0:T(8,128)(2,1)S(1)}, bf16[2,256,512]{2,1,0:T(8,128)(2,1)S(1)}, u32[]{:S(2)}, u32[]{:S(2)}) collective-permute-start(bf16[2,256,512]{2,1,0:T(8,128)(2,1)S(1)} %pad_maximum_fusion), channel_id=1, source_target_pairs={{0,8},{8,0},{1,9},{9,1},{2,10},{10,2},{3,11},{11,3},{4,12},{12,4},... | collective-permute-start | bytes 1572872 | tf_op jit(solution)/shard_map/ppermute | solution.py:28
  100.8 3.9 %copy-start.3 = (bf16[2048,256]{1,0:T(8,128)(2,1)S(1)}, bf16[2048,256]{1,0:T(8,128)(2,1)}, u32[]{:S(2)}) copy-start(bf16[2048,256]{1,0:T(8,128)(2,1)} %param.11) | copy-start | bytes 3145732
  100.8 22.9 %collective-permute-start.19 = (bf16[2,256,512]{2,1,0:T(8,128)(2,1)S(1)}, bf16[2,256,512]{2,1,0:T(8,128)(2,1)S(1)}, u32[]{:S(2)}, u32[]{:S(2)}) collective-permute-start(bf16[2,256,512]{2,1,0:T(8,128)(2,1)S(1)} %copy-done.1), channel_id=1, source_target_pairs={{0,8},{8,0},{1,9},{9,1},{2,10},{10,2},{3,11},{11,3},{4,12},{12,4},... | collective-permute-start | bytes 1572872 | tf_op jit(solution)/shard_map/ppermute | solution.py:28
  105.3 29.5 %collective-permute-start.13 = (bf16[2048,256]{1,0:T(8,128)(2,1)}, bf16[2048,256]{1,0:T(8,128)(2,1)S(1)}, u32[]{:S(2)}, u32[]{:S(2)}) collective-permute-start(bf16[2048,256]{1,0:T(8,128)(2,1)} %collective-permute-done.10), channel_id=1, source_target_pairs={{0,4},{4,0},{1,5},{5,1},{2,6},{6,2},{3,7},{7,3},{8,12},{12,8},{9,1... | collective-permute-start | bytes 3145736 | tf_op jit(solution)/shard_map/ppermute | solution.py:28
  123.7 8.4 %collective-permute-start.18 = (bf16[2,256,512]{2,1,0:T(8,128)(2,1)S(1)}, bf16[2,256,512]{2,1,0:T(8,128)(2,1)S(1)}, u32[]{:S(2)}, u32[]{:S(2)}) collective-permute-start(bf16[2,256,512]{2,1,0:T(8,128)(2,1)S(1)} %copy-done.1), channel_id=1, source_target_pairs={{0,4},{4,0},{1,5},{5,1},{2,6},{6,2},{3,7},{7,3},{8,12},{12,8},{9,1... | collective-permute-start | bytes 1572872 | tf_op jit(solution)/shard_map/ppermute | solution.py:28
  125.9 11.5 %collective-permute-start.20 = (bf16[2,256,512]{2,1,0:T(8,128)(2,1)S(1)}, bf16[2,256,512]{2,1,0:T(8,128)(2,1)S(1)}, u32[]{:S(2)}, u32[]{:S(2)}) collective-permute-start(bf16[2,256,512]{2,1,0:T(8,128)(2,1)S(1)} %collective-permute-done.19), channel_id=1, source_target_pairs={{0,4},{4,0},{1,5},{5,1},{2,6},{6,2},{3,7},{7,3},{8,12},{12,8},{9,1... | collective-permute-start | bytes 1572872 | tf_op jit(solution)/shard_map/ppermute | solution.py:28
  128.3 20.3 %collective-permute-start.15 = (bf16[2,256,512]{2,1,0:T(8,128)(2,1)S(1)}, bf16[2,256,512]{2,1,0:T(8,128)(2,1)S(1)}, u32[]{:S(2)}, u32[]{:S(2)}) collective-permute-start(bf16[2,256,512]{2,1,0:T(8,128)(2,1)S(1)} %collective-permute-done.12), channel_id=1, source_target_pairs={{0,4},{4,0},{1,5},{5,1},{2,6},{6,2},{3,7},{7,3},{8,12},{12,8},{9,1... | collective-permute-start | bytes 1572872 | tf_op jit(solution)/shard_map/ppermute | solution.py:28
  132.1 4.7 %collective-permute-start.14 = (bf16[2048,256]{1,0:T(8,128)(2,1)S(1)}, bf16[2048,256]{1,0:T(8,128)(2,1)S(1)}, u32[]{:S(2)}, u32[]{:S(2)}) collective-permute-start(bf16[2048,256]{1,0:T(8,128)(2,1)S(1)} %collective-permute-done.11), channel_id=1, source_target_pairs={{0,4},{4,0},{1,5},{5,1},{2,6},{6,2},{3,7},{7,3},{8,12},{12,8},{9,1... | collective-permute-start | bytes 3145736 | tf_op jit(solution)/shard_map/ppermute | solution.py:28
  134.7 1.2 copy-start.4
  137.7 10.9 %collective-permute-start.22 = (bf16[192,512]{1,0:T(8,128)(2,1)S(1)}, bf16[192,512]{1,0:T(8,128)(2,1)S(1)}, u32[]{:S(2)}, u32[]{:S(2)}) collective-permute-start(bf16[192,512]{1,0:T(8,128)(2,1)S(1)} %get-tuple-element.14), channel_id=1, source_target_pairs={{0,1},{1,2},{2,3},{3,0},{4,7},{5,4},{6,5},{7,6},{8,9},{9,10},{10,1... | collective-permute-start | bytes 589832 | tf_op jit(solution)/shard_map/ppermute | solution.py:24
  139.7 9.0 %collective-permute-start.21 = (bf16[192,512]{1,0:T(8,128)(2,1)S(1)}, bf16[192,512]{1,0:T(8,128)(2,1)S(1)}, u32[]{:S(2)}, u32[]{:S(2)}) collective-permute-start(bf16[192,512]{1,0:T(8,128)(2,1)S(1)} %get-tuple-element.13), channel_id=1, source_target_pairs={{0,1},{1,2},{2,3},{3,0},{4,7},{5,4},{6,5},{7,6},{8,9},{9,10},{10,1... | collective-permute-start | bytes 589832 | tf_op jit(solution)/shard_map/ppermute | solution.py:24
  148.9 8.8 %collective-permute-start.23 = (bf16[192,512]{1,0:T(8,128)(2,1)S(1)}, bf16[192,512]{1,0:T(8,128)(2,1)S(1)}, u32[]{:S(2)}, u32[]{:S(2)}) collective-permute-start(bf16[192,512]{1,0:T(8,128)(2,1)S(1)} %get-tuple-element.11), channel_id=1, source_target_pairs={{0,1},{1,2},{2,3},{3,0},{4,7},{5,4},{6,5},{7,6},{8,9},{9,10},{10,1... | collective-permute-start | bytes 589832 | tf_op jit(solution)/shard_map/ppermute | solution.py:24
  151.1 8.8 %collective-permute-start.24 = (bf16[192,512]{1,0:T(8,128)(2,1)S(1)}, bf16[192,512]{1,0:T(8,128)(2,1)S(1)}, u32[]{:S(2)}, u32[]{:S(2)}) collective-permute-start(bf16[192,512]{1,0:T(8,128)(2,1)S(1)} %get-tuple-element.12), channel_id=1, source_target_pairs={{0,1},{1,2},{2,3},{3,0},{4,7},{5,4},{6,5},{7,6},{8,9},{9,10},{10,1... | collective-permute-start | bytes 589832 | tf_op jit(solution)/shard_map/ppermute | solution.py:24
  160.2 8.8 %collective-permute-start.25 = (bf16[192,512]{1,0:T(8,128)(2,1)S(1)}, bf16[192,512]{1,0:T(8,128)(2,1)S(1)}, u32[]{:S(2)}, u32[]{:S(2)}) collective-permute-start(bf16[192,512]{1,0:T(8,128)(2,1)S(1)} %get-tuple-element.9), channel_id=1, source_target_pairs={{0,1},{1,2},{2,3},{3,0},{4,7},{5,4},{6,5},{7,6},{8,9},{9,10},{10,1... | collective-permute-start | bytes 589832 | tf_op jit(solution)/shard_map/ppermute | solution.py:24
  162.4 8.8 %collective-permute-start.26 = (bf16[192,512]{1,0:T(8,128)(2,1)S(1)}, bf16[192,512]{1,0:T(8,128)(2,1)S(1)}, u32[]{:S(2)}, u32[]{:S(2)}) collective-permute-start(bf16[192,512]{1,0:T(8,128)(2,1)S(1)} %get-tuple-element.10), channel_id=1, source_target_pairs={{0,1},{1,2},{2,3},{3,0},{4,7},{5,4},{6,5},{7,6},{8,9},{9,10},{10,1... | collective-permute-start | bytes 589832 | tf_op jit(solution)/shard_map/ppermute | solution.py:24
  171.7 7.8 %copy-start.2 = (f32[128,2]{0,1:T(2,128)S(1)}, f32[128,2]{0,1:T(2,128)}, u32[]{:S(2)}) copy-start(f32[128,2]{0,1:T(2,128)} %param.10) | copy-start | bytes 3076
  173.1 29.7 %all-to-all-start.1 = ((bf16[32,48,128]{2,1,0:T(8,128)(2,1)}), bf16[32,48,128]{2,1,0:T(8,128)(2,1)S(1)}, u32[]{:S(2)}, u32[]{:S(2)}) async-start(bf16[32,48,128]{2,1,0:T(8,128)(2,1)} %reshape.152), calls=%async_computation.1 | async-start | bytes 786432 | tf_op jit(solution)/shard_map/all_to_all | solution.py:134

commit v4 on v3

--- a/solution.py
+++ b/solution.py
@@ -93,26 +93,22 @@
     up_d = swap(up_x, "c")
     down_d = (swap(down_x[0], "c"), swap(down_x[1], "c"))
 
-    halves = [near[: block_rows // 2], near[block_rows // 2 :]]
-    gathered = list(halves)
+    blocks = [near]
     for _ in range(3):
-        halves = [shift(halves[0]), shift(halves[1])]
-        gathered += halves
-    order = (0, 2, 1, 3)
-    gathered = jnp.concatenate([gathered[2 * k + i] for k in order for i in range(2)], 0)
+        blocks.append(shift(blocks[-1]))
 
-    gates = (w_gate, gate_c, gate_x, gate_d)
-    uppers = (w_up, up_c, up_x, up_d)
     hidden = []
-    for gate, up in zip(gates, uppers):
-        gate_proj = dot32(gathered, gate)
-        upper = dot32(gathered, up)
-        hidden.append((jax.nn.silu(gate_proj) * upper).astype(jnp.bfloat16))
+    for gate, up in zip((w_gate, gate_c, gate_x, gate_d), (w_up, up_c, up_x, up_d)):
+        parts = []
+        for low in (0, 2):
+            rows_now = jnp.concatenate(blocks[low : low + 2], 0)
+            gate_proj = dot32(rows_now, gate)
+            upper = dot32(rows_now, up)
+            parts.append((jax.nn.silu(gate_proj) * upper).astype(jnp.bfloat16))
+        hidden.append(jnp.concatenate(parts, 0))
 
     def pick(pair, k):
         return pair[0][k // 2] if k % 2 else pair[1][0 if k else 1]
-
-    half_rows = 2 * block_rows
 
     def partial(k):
         total = 0.0
@@ -124,19 +120,15 @@
 
     total = partial(1)
     for step in (1, 2, 3):
-        away = total.astype(jnp.bfloat16)
-        back = [shift(away[:half_rows]), shift(away[half_rows:])]
-        turned = [back[1][block_rows:], back[1][:block_rows], back[0]]
-        total = partial((step + 1) % 4) + jnp.concatenate(turned, 0).astype(jnp.float32)
+        back = jnp.roll(shift(total.astype(jnp.bfloat16)), block_rows, 0)
+        total = partial((step + 1) % 4) + back.astype(jnp.float32)
     home = total.astype(jnp.bfloat16)
     home = home.reshape(4, expert_count, share, out_width).transpose(1, 0, 2, 3)
     home = home.reshape(expert_count, CAP * out_width // 128, 128)
     returned = lax.all_to_all(home, ("z", "xh"), 0, 0, tiled=True)
     returned = returned.reshape(expert_count * CAP, out_width).astype(jnp.float32)
     column = lax.broadcasted_iota(jnp.int32, (1, expert_count * CAP), 1) % CAP
-    place = column // share
-    behind = 2 * (place % 2) + place // 2
-    slot = share * ((y - turn * behind) & 3) + column % share
+    slot = share * ((y - turn * (column // share)) & 3) + column % share
     chosen = spread(rank, CAP) == slot.astype(jnp.float32)
     combine = jnp.where(chosen, spread(weight, CAP, lax.Precision.HIGHEST), 0.0)
     mixed = jnp.dot(
@@ -156,7 +148,9 @@
         P(None, EP_TP),
         P(EP, "y"),
     )
-    return jax.shard_map(layer, mesh=finer, in_specs=placed, out_specs=P(EP, "y"), check_vma=False)
+    return jax.shard_map(
+        layer, mesh=finer, in_specs=placed, out_specs=P(EP, "y"), check_vma=False
+    )
 
 
 def solution(mesh):

time: 206 us -> 195 us (0.947)
  starting transfers between devices: 92.8 us -> 82.2 us
  waiting for transfers between devices: 87.7 us -> 83 us
  local copies, waits for them, and re-layouts: 4.7 us -> 7.72 us
    ppermute x15 -> x9, starting transfers between devices: 40.2 us -> 25.3 us  [shift(): return lax.ppermute(block, ('c', 'y'), up + down)]
    ppermute x15 -> x9, waiting for transfers between devices: 41.9 us -> 29.6 us  [shift(): return lax.ppermute(block, ('c', 'y'), up + down)]
    ppermute x12, waiting for transfers between devices: 14.7 us -> 21.9 us  [swap(): return lax.ppermute(block, axis, SWAP)]
    ppermute x12, starting transfers between devices: 28.1 us -> 31.5 us  [swap(): return lax.ppermute(block, axis, SWAP)]
    all_to_all x1, waiting for transfers between devices: 8.29 us -> 10.4 us  [layer(): arrived = lax.all_to_all(mine, ('z', 'xh'), 0, 0, tiled=True)]
    dot_general x25 -> x33, matrix products: 12.6 us -> 14.1 us  [dot32(): return jnp.dot(a, b, preferred_element_type=jnp.float32)]
  transfers between devices with their start and end apart: 29 -> 23, of which waited for: 14 -> 9; matrix products, arithmetic and copies ran while one was open for 7% -> 9% of each run, Pallas kernels for 0% -> 0%
where the time goes in v4:
time: 195 us; the launch traced here: 193 us
  waiting for transfers between devices  83 us (43%)
  starting transfers between devices  82.2 us (42%)
  matrix products  16.2 us (8%)
  local copies, waits for them, and re-layouts  7.72 us (4%)
  other arithmetic  3.48 us (2%)
    ppermute x12, starting transfers between devices, swap(): return lax.ppermute(block, axis, SWAP)  31.5 us
    ppermute x9, waiting for transfers between devices, shift(): return lax.ppermute(block, ('c', 'y'), up + down)  29.6 us
    ppermute x9, starting transfers between devices, shift(): return lax.ppermute(block, ('c', 'y'), up + down)  25.3 us
    ppermute x12, waiting for transfers between devices, swap(): return lax.ppermute(block, axis, SWAP)  21.9 us
    all_to_all x1, waiting for transfers between devices, layer(): returned = lax.all_to_all(home, ('z', 'xh'), 0, 0, tiled=True)  21.1 us
    all_to_all x1, starting transfers between devices, layer(): arrived = lax.all_to_all(mine, ('z', 'xh'), 0, 0, tiled=True)  18.2 us
    dot_general x33, matrix products, dot32(): return jnp.dot(a, b, preferred_element_type=jnp.float32)  14.1 us
    all_to_all x1, waiting for transfers between devices, layer(): arrived = lax.all_to_all(mine, ('z', 'xh'), 0, 0, tiled=True)  10.4 us
  transfers between devices with their start and end apart: 23, of which 9 were waited for; matrix products, arithmetic and copies ran while one was open for 9% of the time, Pallas kernels for 0%

profile of v4, /device:TPU:6, one launch (start us, length us, event | category | flops | bytes accessed | tf_op | source)
XLA Modules:
  0.0 193.2 jit_solution(17748920220387343477)
XLA Ops:
  0.0 0.8 slice_bitcast_fusion.27
  0.8 1.2 fusion.11
  2.2 0.6 copy-done.7
  3.2 0.9 reshape.96
  4.2 18.2 %all-to-all-start = ((bf16[32,48,128]{2,1,0:T(8,128)(2,1)}), bf16[32,48,128]{2,1,0:T(8,128)(2,1)S(1)}, u32[]{:S(2)}, u32[]{:S(2)}) async-start(bf16[32,48,128]{2,1,0:T(8,128)(2,1)} %reshape.96), calls=%async_computation | async-start | bytes 786432 | tf_op jit(solution)/shard_map/all_to_all | solution.py:78
  22.4 2.7 %collective-permute-start.7 = (bf16[2048,256]{1,0:T(8,128)(2,1)S(1)}, bf16[2048,256]{1,0:T(8,128)(2,1)S(1)}, u32[]{:S(2)}, u32[]{:S(2)}) collective-permute-start(bf16[2048,256]{1,0:T(8,128)(2,1)S(1)} %copy-done), channel_id=1, source_target_pairs={{0,8},{8,0},{1,9},{9,1},{2,10},{10,2},{3,11},{11,3},{4,12},{12,4},... | collective-permute-start | bytes 3145736 | tf_op jit(solution)/shard_map/ppermute | solution.py:28
  25.2 1.0 constant_dynamic-slice_fusion
  26.2 4.9 %collective-permute-start.13 = (bf16[256,512]{1,0:T(8,128)(2,1)}, bf16[256,512]{1,0:T(8,128)(2,1)}, u32[]{:S(2)}, u32[]{:S(2)}) collective-permute-start(bf16[256,512]{1,0:T(8,128)(2,1)} %get-tuple-element.8), channel_id=1, source_target_pairs={{0,3},{1,0},{2,1},{3,2},{4,5},{5,6},{6,7},{7,4},{8,11},{9,8},{10,9... | collective-permute-start | bytes 786440 | tf_op jit(solution)/shard_map/ppermute | solution.py:24
  31.1 1.9 collective-permute-start.14
  33.0 4.1 %collective-permute-start.5 = (bf16[256,512]{1,0:T(8,128)(2,1)}, bf16[256,512]{1,0:T(8,128)(2,1)}, u32[]{:S(2)}, u32[]{:S(2)}) collective-permute-start(bf16[256,512]{1,0:T(8,128)(2,1)} %get-tuple-element.7), channel_id=1, source_target_pairs={{0,2},{1,3},{2,0},{3,1},{4,6},{5,7},{6,4},{7,5},{8,10},{9,11},{10,... | collective-permute-start | bytes 786440 | tf_op jit(solution)/shard_map/ppermute | solution.py:24
  37.2 1.9 collective-permute-start.3
  39.1 10.4 %all-to-all-done = bf16[32,48,128]{2,1,0:T(8,128)(2,1)S(1)} async-done(((bf16[32,48,128]{2,1,0:T(8,128)(2,1)}), bf16[32,48,128]{2,1,0:T(8,128)(2,1)S(1)}, u32[]{:S(2)}, u32[]{:S(2)}) %all-to-all-start) | async-done | bytes 393248 | tf_op jit(solution)/shard_map/all_to_all | solution.py:78
  49.5 0.9 reshape.97
  50.4 1.9 collective-permute-start.4
  52.4 3.5 %collective-permute-start = (bf16[96,2048]{1,0:T(8,128)(2,1)}, bf16[96,2048]{1,0:T(8,128)(2,1)S(1)}, u32[]{:S(2)}, u32[]{:S(2)}) collective-permute-start(bf16[96,2048]{1,0:T(8,128)(2,1)} %reshape.97), channel_id=1, source_target_pairs={{0,1},{1,2},{2,3},{3,0},{4,7},{5,4},{6,5},{7,6},{8,9},{9,10},{10,1... | collective-permute-start | bytes 1179656 | tf_op jit(solution)/shard_map/ppermute | solution.py:24
  55.9 1.1 pad_maximum_fusion.1
  57.0 2.7 %collective-permute-start.8 = (bf16[2048,256]{1,0:T(8,128)(2,1)}, bf16[2048,256]{1,0:T(8,128)(2,1)S(1)}, u32[]{:S(2)}, u32[]{:S(2)}) collective-permute-start(bf16[2048,256]{1,0:T(8,128)(2,1)} %param.12), channel_id=1, source_target_pairs={{0,8},{8,0},{1,9},{9,1},{2,10},{10,2},{3,11},{11,3},{4,12},{12,4},... | collective-permute-start | bytes 3145736 | tf_op jit(solution)/shard_map/ppermute | solution.py:28
  59.8 1.1 pad_maximum_fusion
  60.9 3.1 %collective-permute-start.16 = (bf16[2,256,512]{2,1,0:T(8,128)(2,1)S(1)}, bf16[2,256,512]{2,1,0:T(8,128)(2,1)S(1)}, u32[]{:S(2)}, u32[]{:S(2)}) collective-permute-start(bf16[2,256,512]{2,1,0:T(8,128)(2,1)S(1)} %pad_maximum_fusion.1), channel_id=1, source_target_pairs={{0,8},{8,0},{1,9},{9,1},{2,10},{10,2},{3,11},{11,3},{4,12},{12,4},... | collective-permute-start | bytes 1572872 | tf_op jit(solution)/shard_map/ppermute | solution.py:28
  64.0 3.0 %collective-permute-start.10 = (bf16[2048,256]{1,0:T(8,128)(2,1)S(1)}, bf16[2048,256]{1,0:T(8,128)(2,1)S(1)}, u32[]{:S(2)}, u32[]{:S(2)}) collective-permute-start(bf16[2048,256]{1,0:T(8,128)(2,1)S(1)} %collective-permute-done.7), channel_id=1, source_target_pairs={{0,4},{4,0},{1,5},{5,1},{2,6},{6,2},{3,7},{7,3},{8,12},{12,8},{9,1... | collective-permute-start | bytes 3145736 | tf_op jit(solution)/shard_map/ppermute | solution.py:28
  67.4 0.8 copy-done.6
  69.1 2.7 %collective-permute-start.9 = (bf16[2,256,512]{2,1,0:T(8,128)(2,1)S(1)}, bf16[2,256,512]{2,1,0:T(8,128)(2,1)S(1)}, u32[]{:S(2)}, u32[]{:S(2)}) collective-permute-start(bf16[2,256,512]{2,1,0:T(8,128)(2,1)S(1)} %pad_maximum_fusion), channel_id=1, source_target_pairs={{0,8},{8,0},{1,9},{9,1},{2,10},{10,2},{3,11},{11,3},{4,12},{12,4},... | collective-permute-start | bytes 1572872 | tf_op jit(solution)/shard_map/ppermute | solution.py:28
  71.8 12.6 %collective-permute-done.8 = bf16[2048,256]{1,0:T(8,128)(2,1)S(1)} collective-permute-done((bf16[2048,256]{1,0:T(8,128)(2,1)}, bf16[2048,256]{1,0:T(8,128)(2,1)S(1)}, u32[]{:S(2)}, u32[]{:S(2)}) %collective-permute-start.8) | collective-permute-done | bytes 1048608 | tf_op jit(solution)/shard_map/ppermute | solution.py:28
  84.5 3.4 %collective-permute-start.11 = (bf16[2048,256]{1,0:T(8,128)(2,1)S(1)}, bf16[2048,256]{1,0:T(8,128)(2,1)S(1)}, u32[]{:S(2)}, u32[]{:S(2)}) collective-permute-start(bf16[2048,256]{1,0:T(8,128)(2,1)S(1)} %collective-permute-done.8), channel_id=1, source_target_pairs={{0,4},{4,0},{1,5},{5,1},{2,6},{6,2},{3,7},{7,3},{8,12},{12,8},{9,1... | collective-permute-start | bytes 3145736 | tf_op jit(solution)/shard_map/ppermute | solution.py:28
  88.6 2.7 %collective-permute-start.1 = (bf16[96,2048]{1,0:T(8,128)(2,1)S(1)}, bf16[96,2048]{1,0:T(8,128)(2,1)S(1)}, u32[]{:S(2)}, u32[]{:S(2)}) collective-permute-start(bf16[96,2048]{1,0:T(8,128)(2,1)S(1)} %collective-permute-done), channel_id=1, source_target_pairs={{0,1},{1,2},{2,3},{3,0},{4,7},{5,4},{6,5},{7,6},{8,9},{9,10},{10,1... | collective-permute-start | bytes 1179656 | tf_op jit(solution)/shard_map/ppermute | solution.py:24
  91.7 2.2 %collective-permute-start.15 = (bf16[2,256,512]{2,1,0:T(8,128)(2,1)S(1)}, bf16[2,256,512]{2,1,0:T(8,128)(2,1)S(1)}, u32[]{:S(2)}, u32[]{:S(2)}) collective-permute-start(bf16[2,256,512]{2,1,0:T(8,128)(2,1)S(1)} %pad_maximum_fusion.1), channel_id=1, source_target_pairs={{0,4},{4,0},{1,5},{5,1},{2,6},{6,2},{3,7},{7,3},{8,12},{12,8},{9,1... | collective-permute-start | bytes 1572872 | tf_op jit(solution)/shard_map/ppermute | solution.py:28
  94.3 1.4 collective-permute-done.16
  95.7 3.4 %collective-permute-start.6 = (bf16[2,256,512]{2,1,0:T(8,128)(2,1)S(1)}, bf16[2,256,512]{2,1,0:T(8,128)(2,1)S(1)}, u32[]{:S(2)}, u32[]{:S(2)}) collective-permute-start(bf16[2,256,512]{2,1,0:T(8,128)(2,1)S(1)} %pad_maximum_fusion), channel_id=1, source_target_pairs={{0,4},{4,0},{1,5},{5,1},{2,6},{6,2},{3,7},{7,3},{8,12},{12,8},{9,1... | collective-permute-start | bytes 1572872 | tf_op jit(solution)/shard_map/ppermute | solution.py:28
  99.1 7.8 %collective-permute-done.9 = bf16[2,256,512]{2,1,0:T(8,128)(2,1)S(1)} collective-permute-done((bf16[2,256,512]{2,1,0:T(8,128)(2,1)S(1)}, bf16[2,256,512]{2,1,0:T(8,128)(2,1)S(1)}, u32[]{:S(2)}, u32[]{:S(2)}) %collective-permute-start.9) | collective-permute-done | bytes 524320 | tf_op jit(solution)/shard_map/ppermute | solution.py:28
  106.9 2.4 %collective-permute-start.17 = (bf16[2,256,512]{2,1,0:T(8,128)(2,1)S(1)}, bf16[2,256,512]{2,1,0:T(8,128)(2,1)S(1)}, u32[]{:S(2)}, u32[]{:S(2)}) collective-permute-start(bf16[2,256,512]{2,1,0:T(8,128)(2,1)S(1)} %collective-permute-done.16), channel_id=1, source_target_pairs={{0,4},{4,0},{1,5},{5,1},{2,6},{6,2},{3,7},{7,3},{8,12},{12,8},{9,1... | collective-permute-start | bytes 1572872 | tf_op jit(solution)/shard_map/ppermute | solution.py:28
  109.3 1.9 collective-permute-start.12
  111.3 2.3 %collective-permute-start.2 = (bf16[96,2048]{1,0:T(8,128)(2,1)S(1)}, bf16[96,2048]{1,0:T(8,128)(2,1)S(1)}, u32[]{:S(2)}, u32[]{:S(2)}) collective-permute-start(bf16[96,2048]{1,0:T(8,128)(2,1)S(1)} %collective-permute-done.1), channel_id=1, source_target_pairs={{0,1},{1,2},{2,3},{3,0},{4,7},{5,4},{6,5},{7,6},{8,9},{9,10},{10,1... | collective-permute-start | bytes 1179656 | tf_op jit(solution)/shard_map/ppermute | solution.py:24
  114.0 8.2 %collective-permute-done.2 = bf16[96,2048]{1,0:T(8,128)(2,1)S(1)} collective-permute-done((bf16[96,2048]{1,0:T(8,128)(2,1)S(1)}, bf16[96,2048]{1,0:T(8,128)(2,1)S(1)}, u32[]{:S(2)}, u32[]{:S(2)}) %collective-permute-start.2) | collective-permute-done | bytes 393248 | tf_op jit(solution)/shard_map/ppermute | solution.py:24
  125.8 1.2 fusion
  127.3 1.9 collective-permute-start.18
  130.3 1.2 fusion.2
  131.5 6.7 %collective-permute-done.18 = bf16[384,512]{1,0:T(8,128)(2,1)S(1)} collective-permute-done((bf16[384,512]{1,0:T(8,128)(2,1)S(1)}, bf16[384,512]{1,0:T(8,128)(2,1)S(1)}, u32[]{:S(2)}, u32[]{:S(2)}) %collective-permute-start.18) | collective-permute-done | bytes 393248 | tf_op jit(solution)/shard_map/ppermute | solution.py:24
  138.5 1.9 collective-permute-start.19
  140.4 1.2 fusion.23
  141.7 1.2 fusion.4
  142.9 6.5 %collective-permute-done.19 = bf16[384,512]{1,0:T(8,128)(2,1)S(1)} collective-permute-done((bf16[384,512]{1,0:T(8,128)(2,1)S(1)}, bf16[384,512]{1,0:T(8,128)(2,1)S(1)}, u32[]{:S(2)}, u32[]{:S(2)}) %collective-permute-start.19) | collective-permute-done | bytes 393248 | tf_op jit(solution)/shard_map/ppermute | solution.py:24
  149.7 2.1 %collective-permute-start.20 = (bf16[384,512]{1,0:T(8,128)(2,1)S(1)}, bf16[384,512]{1,0:T(8,128)(2,1)S(1)}, u32[]{:S(2)}, u32[]{:S(2)}) collective-permute-start(bf16[384,512]{1,0:T(8,128)(2,1)S(1)} %fusion.7), channel_id=1, source_target_pairs={{0,1},{1,2},{2,3},{3,0},{4,7},{5,4},{6,5},{7,6},{8,9},{9,10},{10,1... | collective-permute-start | bytes 1179656 | tf_op jit(solution)/shard_map/ppermute | solution.py:24
  152.3 8.2 %collective-permute-done.20 = bf16[384,512]{1,0:T(8,128)(2,1)S(1)} collective-permute-done((bf16[384,512]{1,0:T(8,128)(2,1)S(1)}, bf16[384,512]{1,0:T(8,128)(2,1)S(1)}, u32[]{:S(2)}, u32[]{:S(2)}) %collective-permute-start.20) | collective-permute-done | bytes 393248 | tf_op jit(solution)/shard_map/ppermute | solution.py:24
  161.4 1.1 reshape.99
  162.5 7.2 %all-to-all-start.1 = ((bf16[32,48,128]{2,1,0:T(8,128)(2,1)}), bf16[32,48,128]{2,1,0:T(8,128)(2,1)S(1)}, u32[]{:S(2)}, u32[]{:S(2)}) async-start(bf16[32,48,128]{2,1,0:T(8,128)(2,1)} %reshape.99), calls=%async_computation.1 | async-start | bytes 786432 | tf_op jit(solution)/shard_map/all_to_all | solution.py:128
  169.7 0.7 copy-done.5
  170.9 21.1 %all-to-all-done.1 = bf16[32,48,128]{2,1,0:T(8,128)(2,1)S(1)} async-done(((bf16[32,48,128]{2,1,0:T(8,128)(2,1)}), bf16[32,48,128]{2,1,0:T(8,128)(2,1)S(1)}, u32[]{:S(2)}, u32[]{:S(2)}) %all-to-all-start.1) | async-done | bytes 393248 | tf_op jit(solution)/shard_map/all_to_all | solution.py:128
  192.2 1.0 convolution_convert_fusion.1
  (80 shorter events, 11.4 us)
Async XLA Ops:
  0.0 2.2 %copy-start.4 = (bf16[128,2048]{1,0:T(8,128)(2,1)S(1)}, bf16[128,2048]{1,0:T(8,128)(2,1)}, u32[]{:S(2)}) copy-start(bf16[128,2048]{1,0:T(8,128)(2,1)} %param.7) | copy-start | bytes 1572868
  2.0 0.7 copy-start.7
  2.7 19.6 %copy-start = (bf16[2048,256]{1,0:T(8,128)(2,1)S(1)}, bf16[2048,256]{1,0:T(8,128)(2,1)}, u32[]{:S(2)}) copy-start(bf16[2048,256]{1,0:T(8,128)(2,1)} %param.11) | copy-start | bytes 3145732
  3.2 21.9 %copy-start.1 = (bf16[1024,512]{1,0:T(8,128)(2,1)S(1)}, bf16[1024,512]{1,0:T(8,128)(2,1)}, u32[]{:S(2)}) copy-start(bf16[1024,512]{1,0:T(8,128)(2,1)} %param.13) | copy-start | bytes 3145732
  4.2 45.3 %all-to-all-start = ((bf16[32,48,128]{2,1,0:T(8,128)(2,1)}), bf16[32,48,128]{2,1,0:T(8,128)(2,1)S(1)}, u32[]{:S(2)}, u32[]{:S(2)}) async-start(bf16[32,48,128]{2,1,0:T(8,128)(2,1)} %reshape.96), calls=%async_computation | async-start | bytes 786432 | tf_op jit(solution)/shard_map/all_to_all | solution.py:78
  22.4 38.5 %collective-permute-start.7 = (bf16[2048,256]{1,0:T(8,128)(2,1)S(1)}, bf16[2048,256]{1,0:T(8,128)(2,1)S(1)}, u32[]{:S(2)}, u32[]{:S(2)}) collective-permute-start(bf16[2048,256]{1,0:T(8,128)(2,1)S(1)} %copy-done), channel_id=1, source_target_pairs={{0,8},{8,0},{1,9},{9,1},{2,10},{10,2},{3,11},{11,3},{4,12},{12,4},... | collective-permute-start | bytes 3145736 | tf_op jit(solution)/shard_map/ppermute | solution.py:28
  26.2 24.2 %collective-permute-start.13 = (bf16[256,512]{1,0:T(8,128)(2,1)}, bf16[256,512]{1,0:T(8,128)(2,1)}, u32[]{:S(2)}, u32[]{:S(2)}) collective-permute-start(bf16[256,512]{1,0:T(8,128)(2,1)} %get-tuple-element.8), channel_id=1, source_target_pairs={{0,3},{1,0},{2,1},{3,2},{4,5},{5,6},{6,7},{7,4},{8,11},{9,8},{10,9... | collective-permute-start | bytes 786440 | tf_op jit(solution)/shard_map/ppermute | solution.py:24
  31.1 21.2 %collective-permute-start.14 = (bf16[256,512]{1,0:T(8,128)(2,1)}, bf16[256,512]{1,0:T(8,128)(2,1)}, u32[]{:S(2)}, u32[]{:S(2)}) collective-permute-start(bf16[256,512]{1,0:T(8,128)(2,1)} %get-tuple-element.5), channel_id=1, source_target_pairs={{0,1},{1,2},{2,3},{3,0},{4,7},{5,4},{6,5},{7,6},{8,9},{9,10},{10,1... | collective-permute-start | bytes 786440 | tf_op jit(solution)/shard_map/ppermute | solution.py:24
  33.0 24.0 %collective-permute-start.5 = (bf16[256,512]{1,0:T(8,128)(2,1)}, bf16[256,512]{1,0:T(8,128)(2,1)}, u32[]{:S(2)}, u32[]{:S(2)}) collective-permute-start(bf16[256,512]{1,0:T(8,128)(2,1)} %get-tuple-element.7), channel_id=1, source_target_pairs={{0,2},{1,3},{2,0},{3,1},{4,6},{5,7},{6,4},{7,5},{8,10},{9,11},{10,... | collective-permute-start | bytes 786440 | tf_op jit(solution)/shard_map/ppermute | solution.py:24
  37.2 31.9 %collective-permute-start.3 = (bf16[2048,256]{1,0:T(8,128)(2,1)S(1)}, bf16[2048,256]{1,0:T(8,128)(2,1)S(1)}, u32[]{:S(2)}, u32[]{:S(2)}) collective-permute-start(bf16[2048,256]{1,0:T(8,128)(2,1)S(1)} %copy-done), channel_id=1, source_target_pairs={{0,4},{4,0},{1,5},{5,1},{2,6},{6,2},{3,7},{7,3},{8,12},{12,8},{9,1... | collective-permute-start | bytes 3145736 | tf_op jit(solution)/shard_map/ppermute | solution.py:28
  50.4 38.2 %collective-permute-start.4 = (bf16[2048,256]{1,0:T(8,128)(2,1)}, bf16[2048,256]{1,0:T(8,128)(2,1)S(1)}, u32[]{:S(2)}, u32[]{:S(2)}) collective-permute-start(bf16[2048,256]{1,0:T(8,128)(2,1)} %param.12), channel_id=1, source_target_pairs={{0,4},{4,0},{1,5},{5,1},{2,6},{6,2},{3,7},{7,3},{8,12},{12,8},{9,1... | collective-permute-start | bytes 3145736 | tf_op jit(solution)/shard_map/ppermute | solution.py:28
  52.4 11.6 %collective-permute-start = (bf16[96,2048]{1,0:T(8,128)(2,1)}, bf16[96,2048]{1,0:T(8,128)(2,1)S(1)}, u32[]{:S(2)}, u32[]{:S(2)}) collective-permute-start(bf16[96,2048]{1,0:T(8,128)(2,1)} %reshape.97), channel_id=1, source_target_pairs={{0,1},{1,2},{2,3},{3,0},{4,7},{5,4},{6,5},{7,6},{8,9},{9,10},{10,1... | collective-permute-start | bytes 1179656 | tf_op jit(solution)/shard_map/ppermute | solution.py:24
  55.9 3.9 %copy-start.3 = (bf16[1,256,512]{2,1,0:T(8,128)(2,1)S(1)}, bf16[1,256,512]{2,1,0:T(8,128)(2,1)}, u32[]{:S(2)}) copy-start(bf16[1,256,512]{2,1,0:T(8,128)(2,1)} %get-tuple-element.6) | copy-start | bytes 786436
  57.0 27.4 %collective-permute-start.8 = (bf16[2048,256]{1,0:T(8,128)(2,1)}, bf16[2048,256]{1,0:T(8,128)(2,1)S(1)}, u32[]{:S(2)}, u32[]{:S(2)}) collective-permute-start(bf16[2048,256]{1,0:T(8,128)(2,1)} %param.12), channel_id=1, source_target_pairs={{0,8},{8,0},{1,9},{9,1},{2,10},{10,2},{3,11},{11,3},{4,12},{12,4},... | collective-permute-start | bytes 3145736 | tf_op jit(solution)/shard_map/ppermute | solution.py:28
  59.8 1.1 copy-start.2
  60.9 34.8 %collective-permute-start.16 = (bf16[2,256,512]{2,1,0:T(8,128)(2,1)S(1)}, bf16[2,256,512]{2,1,0:T(8,128)(2,1)S(1)}, u32[]{:S(2)}, u32[]{:S(2)}) collective-permute-start(bf16[2,256,512]{2,1,0:T(8,128)(2,1)S(1)} %pad_maximum_fusion.1), channel_id=1, source_target_pairs={{0,8},{8,0},{1,9},{9,1},{2,10},{10,2},{3,11},{11,3},{4,12},{12,4},... | collective-permute-start | bytes 1572872 | tf_op jit(solution)/shard_map/ppermute | solution.py:28
  64.0 27.7 %collective-permute-start.10 = (bf16[2048,256]{1,0:T(8,128)(2,1)S(1)}, bf16[2048,256]{1,0:T(8,128)(2,1)S(1)}, u32[]{:S(2)}, u32[]{:S(2)}) collective-permute-start(bf16[2048,256]{1,0:T(8,128)(2,1)S(1)} %collective-permute-done.7), channel_id=1, source_target_pairs={{0,4},{4,0},{1,5},{5,1},{2,6},{6,2},{3,7},{7,3},{8,12},{12,8},{9,1... | collective-permute-start | bytes 3145736 | tf_op jit(solution)/shard_map/ppermute | solution.py:28
  67.0 1.2 copy-start.6
  69.1 37.9 %collective-permute-start.9 = (bf16[2,256,512]{2,1,0:T(8,128)(2,1)S(1)}, bf16[2,256,512]{2,1,0:T(8,128)(2,1)S(1)}, u32[]{:S(2)}, u32[]{:S(2)}) collective-permute-start(bf16[2,256,512]{2,1,0:T(8,128)(2,1)S(1)} %pad_maximum_fusion), channel_id=1, source_target_pairs={{0,8},{8,0},{1,9},{9,1},{2,10},{10,2},{3,11},{11,3},{4,12},{12,4},... | collective-permute-start | bytes 1572872 | tf_op jit(solution)/shard_map/ppermute | solution.py:28
  84.5 24.9 %collective-permute-start.11 = (bf16[2048,256]{1,0:T(8,128)(2,1)S(1)}, bf16[2048,256]{1,0:T(8,128)(2,1)S(1)}, u32[]{:S(2)}, u32[]{:S(2)}) collective-permute-start(bf16[2048,256]{1,0:T(8,128)(2,1)S(1)} %collective-permute-done.8), channel_id=1, source_target_pairs={{0,4},{4,0},{1,5},{5,1},{2,6},{6,2},{3,7},{7,3},{8,12},{12,8},{9,1... | collective-permute-start | bytes 3145736 | tf_op jit(solution)/shard_map/ppermute | solution.py:28
  88.6 22.7 %collective-permute-start.1 = (bf16[96,2048]{1,0:T(8,128)(2,1)S(1)}, bf16[96,2048]{1,0:T(8,128)(2,1)S(1)}, u32[]{:S(2)}, u32[]{:S(2)}) collective-permute-start(bf16[96,2048]{1,0:T(8,128)(2,1)S(1)} %collective-permute-done), channel_id=1, source_target_pairs={{0,1},{1,2},{2,3},{3,0},{4,7},{5,4},{6,5},{7,6},{8,9},{9,10},{10,1... | collective-permute-start | bytes 1179656 | tf_op jit(solution)/shard_map/ppermute | solution.py:24
  91.7 33.8 %collective-permute-start.15 = (bf16[2,256,512]{2,1,0:T(8,128)(2,1)S(1)}, bf16[2,256,512]{2,1,0:T(8,128)(2,1)S(1)}, u32[]{:S(2)}, u32[]{:S(2)}) collective-permute-start(bf16[2,256,512]{2,1,0:T(8,128)(2,1)S(1)} %pad_maximum_fusion.1), channel_id=1, source_target_pairs={{0,4},{4,0},{1,5},{5,1},{2,6},{6,2},{3,7},{7,3},{8,12},{12,8},{9,1... | collective-permute-start | bytes 1572872 | tf_op jit(solution)/shard_map/ppermute | solution.py:28
  95.7 34.3 %collective-permute-start.6 = (bf16[2,256,512]{2,1,0:T(8,128)(2,1)S(1)}, bf16[2,256,512]{2,1,0:T(8,128)(2,1)S(1)}, u32[]{:S(2)}, u32[]{:S(2)}) collective-permute-start(bf16[2,256,512]{2,1,0:T(8,128)(2,1)S(1)} %pad_maximum_fusion), channel_id=1, source_target_pairs={{0,4},{4,0},{1,5},{5,1},{2,6},{6,2},{3,7},{7,3},{8,12},{12,8},{9,1... | collective-permute-start | bytes 1572872 | tf_op jit(solution)/shard_map/ppermute | solution.py:28
  106.9 20.1 %collective-permute-start.17 = (bf16[2,256,512]{2,1,0:T(8,128)(2,1)S(1)}, bf16[2,256,512]{2,1,0:T(8,128)(2,1)S(1)}, u32[]{:S(2)}, u32[]{:S(2)}) collective-permute-start(bf16[2,256,512]{2,1,0:T(8,128)(2,1)S(1)} %collective-permute-done.16), channel_id=1, source_target_pairs={{0,4},{4,0},{1,5},{5,1},{2,6},{6,2},{3,7},{7,3},{8,12},{12,8},{9,1... | collective-permute-start | bytes 1572872 | tf_op jit(solution)/shard_map/ppermute | solution.py:28
  109.3 28.9 %collective-permute-start.12 = (bf16[2,256,512]{2,1,0:T(8,128)(2,1)S(1)}, bf16[2,256,512]{2,1,0:T(8,128)(2,1)S(1)}, u32[]{:S(2)}, u32[]{:S(2)}) collective-permute-start(bf16[2,256,512]{2,1,0:T(8,128)(2,1)S(1)} %collective-permute-done.9), channel_id=1, source_target_pairs={{0,4},{4,0},{1,5},{5,1},{2,6},{6,2},{3,7},{7,3},{8,12},{12,8},{9,1... | collective-permute-start | bytes 1572872 | tf_op jit(solution)/shard_map/ppermute | solution.py:28
  111.3 10.9 %collective-permute-start.2 = (bf16[96,2048]{1,0:T(8,128)(2,1)S(1)}, bf16[96,2048]{1,0:T(8,128)(2,1)S(1)}, u32[]{:S(2)}, u32[]{:S(2)}) collective-permute-start(bf16[96,2048]{1,0:T(8,128)(2,1)S(1)} %collective-permute-done.1), channel_id=1, source_target_pairs={{0,1},{1,2},{2,3},{3,0},{4,7},{5,4},{6,5},{7,6},{8,9},{9,10},{10,1... | collective-permute-start | bytes 1179656 | tf_op jit(solution)/shard_map/ppermute | solution.py:24
  127.3 10.9 %collective-permute-start.18 = (bf16[384,512]{1,0:T(8,128)(2,1)S(1)}, bf16[384,512]{1,0:T(8,128)(2,1)S(1)}, u32[]{:S(2)}, u32[]{:S(2)}) collective-permute-start(bf16[384,512]{1,0:T(8,128)(2,1)S(1)} %fusion.9), channel_id=1, source_target_pairs={{0,1},{1,2},{2,3},{3,0},{4,7},{5,4},{6,5},{7,6},{8,9},{9,10},{10,1... | collective-permute-start | bytes 1179656 | tf_op jit(solution)/shard_map/ppermute | solution.py:24
  138.5 10.9 %collective-permute-start.19 = (bf16[384,512]{1,0:T(8,128)(2,1)S(1)}, bf16[384,512]{1,0:T(8,128)(2,1)S(1)}, u32[]{:S(2)}, u32[]{:S(2)}) collective-permute-start(bf16[384,512]{1,0:T(8,128)(2,1)S(1)} %fusion.8), channel_id=1, source_target_pairs={{0,1},{1,2},{2,3},{3,0},{4,7},{5,4},{6,5},{7,6},{8,9},{9,10},{10,1... | collective-permute-start | bytes 1179656 | tf_op jit(solution)/shard_map/ppermute | solution.py:24
  149.7 10.9 %collective-permute-start.20 = (bf16[384,512]{1,0:T(8,128)(2,1)S(1)}, bf16[384,512]{1,0:T(8,128)(2,1)S(1)}, u32[]{:S(2)}, u32[]{:S(2)}) collective-permute-start(bf16[384,512]{1,0:T(8,128)(2,1)S(1)} %fusion.7), channel_id=1, source_target_pairs={{0,1},{1,2},{2,3},{3,0},{4,7},{5,4},{6,5},{7,6},{8,9},{9,10},{10,1... | collective-permute-start | bytes 1179656 | tf_op jit(solution)/shard_map/ppermute | solution.py:24
  162.5 29.5 %all-to-all-start.1 = ((bf16[32,48,128]{2,1,0:T(8,128)(2,1)}), bf16[32,48,128]{2,1,0:T(8,128)(2,1)S(1)}, u32[]{:S(2)}, u32[]{:S(2)}) async-start(bf16[32,48,128]{2,1,0:T(8,128)(2,1)} %reshape.99), calls=%async_computation.1 | async-start | bytes 786432 | tf_op jit(solution)/shard_map/all_to_all | solution.py:128
  169.7 0.7 copy-start.5

commit v5 on v4

--- a/solution.py
+++ b/solution.py
@@ -1,6 +1,8 @@
 import jax
 import jax.numpy as jnp
 from jax import lax
+from jax.experimental import pallas as pl
+from jax.experimental.pallas import tpu as pltpu
 from jax.sharding import Mesh
 from jax.sharding import PartitionSpec as P
 
@@ -10,6 +12,7 @@
 EP_TP = ("z", "xh", "xl", "c", "y")
 CAP = 12
 SWAP = [(0, 1), (1, 0)]
+TILE = 512
 
 
 def rms_rows(values, gain):
@@ -40,6 +43,50 @@
     return jnp.dot(per_expert, table, precision=precision, preferred_element_type=jnp.float32)
 
 
+def hidden_kernel(rows_ref, gate_ref, up_ref, out_ref, gate_sum, up_sum):
+    step = pl.program_id(0)
+
+    @pl.when(step == 0)
+    def _():
+        gate_sum[...] = jnp.zeros_like(gate_sum)
+        up_sum[...] = jnp.zeros_like(up_sum)
+
+    tile = gate_ref.shape[0]
+    rows = rows_ref[:, pl.ds(pl.multiple_of(step * tile, tile), tile)]
+    gate_sum[...] += dot32(rows, gate_ref[...])
+    up_sum[...] += dot32(rows, up_ref[...])
+
+    @pl.when(step == pl.num_programs(0) - 1)
+    def _():
+        out_ref[...] = (jax.nn.silu(gate_sum[...]) * up_sum[...]).astype(out_ref.dtype)
+
+
+def hidden_of(rows, weights):
+    count, width = rows.shape
+    depth = weights.shape[1]
+    tile = min(TILE, width)
+    steps = width // tile
+    return pl.pallas_call(
+        hidden_kernel,
+        grid=(steps,),
+        in_specs=[
+            pl.BlockSpec(memory_space=pltpu.VMEM),
+            pl.BlockSpec((tile, depth), lambda k: (k, 0)),
+            pl.BlockSpec((tile, depth), lambda k: (steps + k, 0)),
+        ],
+        out_specs=pl.BlockSpec(memory_space=pltpu.VMEM),
+        out_shape=jax.ShapeDtypeStruct((count, depth), jnp.bfloat16),
+        scratch_shapes=[pltpu.VMEM((count, depth), jnp.float32)] * 2,
+        cost_estimate=pl.CostEstimate(
+            flops=4 * count * width * depth,
+            bytes_accessed=2 * (count * width + 2 * width * depth + count * depth),
+            transcendentals=count * depth,
+        ),
+        compiler_params=pltpu.CompilerParams(dimension_semantics=("arbitrary",)),
+        name="hidden",
+    )(rows, weights, weights)
+
+
 def layer(tokens, norm_gain, expert_ids, gate_weights, w_gate, w_up, w_down):
     y = lax.axis_index("y")
     turn = 1 - 2 * lax.axis_index("c")
@@ -51,8 +98,13 @@
     depth = w_gate.shape[1]
     out_width = w_down.shape[1]
 
-    gate_x = swap(w_gate, "xl")
-    up_x = swap(w_up, "xl")
+    weights_o = jnp.concatenate([w_gate, w_up], 0)
+    weights_x = swap(weights_o, "xl")
+    down_x = swap(w_down, "xl")
+    weights_c = swap(weights_o, "c")
+    down_c = swap(w_down, "c")
+    weights_d = swap(weights_x, "c")
+    down_d = swap(down_x, "c")
 
     normed = rms_rows(tokens, norm_gain)
     experts = jnp.arange(expert_count, dtype=jnp.int32)[None, :]
@@ -78,50 +130,33 @@
     arrived = lax.all_to_all(mine, ("z", "xh"), 0, 0, tiled=True)
     near = arrived.reshape(block_rows, width)
 
-    cut = []
-    for k in range(4):
-        start = ((y + turn * k) & 3) * depth
-        cut.append(lax.dynamic_slice_in_dim(w_down, start, depth, 0))
-    for k in (1, 2, 3):
-        cut[k] = shift(cut[k], k)
-    down_o = (jnp.stack([cut[1], cut[3]]), jnp.stack([cut[2], cut[0]]))
-    down_x = (swap(down_o[0], "xl"), swap(down_o[1], "xl"))
-    gate_c = swap(w_gate, "c")
-    up_c = swap(w_up, "c")
-    down_c = (swap(down_o[0], "c"), swap(down_o[1], "c"))
-    gate_d = swap(gate_x, "c")
-    up_d = swap(up_x, "c")
-    down_d = (swap(down_x[0], "c"), swap(down_x[1], "c"))
-
     blocks = [near]
     for _ in range(3):
         blocks.append(shift(blocks[-1]))
 
-    hidden = []
-    for gate, up in zip((w_gate, gate_c, gate_x, gate_d), (w_up, up_c, up_x, up_d)):
-        parts = []
-        for low in (0, 2):
-            rows_now = jnp.concatenate(blocks[low : low + 2], 0)
-            gate_proj = dot32(rows_now, gate)
-            upper = dot32(rows_now, up)
-            parts.append((jax.nn.silu(gate_proj) * upper).astype(jnp.bfloat16))
-        hidden.append(jnp.concatenate(parts, 0))
+    gathered = jnp.concatenate(blocks, 0)
 
-    def pick(pair, k):
-        return pair[0][k // 2] if k % 2 else pair[1][0 if k else 1]
+    near_pair = (hidden_of(gathered, weights_o), hidden_of(gathered, weights_c))
+    far_pair = (hidden_of(gathered, weights_x), hidden_of(gathered, weights_d))
+    near_steps = [jnp.concatenate(near_pair, 1)]
+    far_steps = [jnp.concatenate(far_pair, 1)]
+    for _ in range(3):
+        near_steps.append(shift(near_steps[-1]))
+        far_steps.append(shift(far_steps[-1]))
+    for step in (0, 1):
+        far_steps[step], _ = lax.optimization_barrier((far_steps[step], near_steps[2]))
 
-    def partial(k):
+    def down_of(steps, side, matrix):
         total = 0.0
-        for matrix, pair, at in zip(
-            hidden, (down_o, down_c, down_x, down_d), (k, (-k) % 4, k, (-k) % 4)
-        ):
-            total += dot32(matrix, pick(pair, at))
+        for step in range(4):
+            start = ((y - turn * step) & 3) * depth
+            turned = jnp.roll(steps[step], step * block_rows, 0)
+            down = lax.dynamic_slice_in_dim(matrix, start, depth, 0)
+            total += dot32(turned[:, side * depth : (side + 1) * depth], down)
         return total
 
-    total = partial(1)
-    for step in (1, 2, 3):
-        back = jnp.roll(shift(total.astype(jnp.bfloat16)), block_rows, 0)
-        total = partial((step + 1) % 4) + back.astype(jnp.float32)
+    total = down_of(near_steps, 0, w_down) + down_of(near_steps, 1, down_c)
+    total += down_of(far_steps, 0, down_x) + down_of(far_steps, 1, down_d)
     home = total.astype(jnp.bfloat16)
     home = home.reshape(4, expert_count, share, out_width).transpose(1, 0, 2, 3)
     home = home.reshape(expert_count, CAP * out_width // 128, 128)

time: 195 us -> 210 us (1.077)
  Pallas kernels: 0 us -> 18.6 us
  starting transfers between devices: 82.2 us -> 64.2 us
  waiting for transfers between devices: 83 us -> 91.3 us
  matrix products: 16.2 us -> 22.7 us
    pallas_call x0 -> x4, Pallas kernels: none -> 18.6 us  [hidden_of(): pl.pallas_call(hidden_kernel, grid=(steps,), in_specs=[pl.BlockSpec(memor...]
    ppermute x12 -> x6, starting transfers between devices: 31.5 us -> 13.3 us  [swap(): return lax.ppermute(block, axis, SWAP)]
    ppermute x12 -> x6, waiting for transfers between devices: 21.9 us -> 5.04 us  [swap(): return lax.ppermute(block, axis, SWAP)]
    ppermute x9, waiting for transfers between devices: 29.6 us -> 45.6 us  [shift(): return lax.ppermute(block, ('c', 'y'), up + down)]
    all_to_all x1, waiting for transfers between devices: 10.4 us -> 20.3 us  [layer(): arrived = lax.all_to_all(mine, ('z', 'xh'), 0, 0, tiled=True)]
    all_to_all x1, starting transfers between devices: 7.16 us -> 13.3 us  [layer(): returned = lax.all_to_all(home, ('z', 'xh'), 0, 0, tiled=True)]
    ppermute x9, starting transfers between devices: 25.3 us -> 19.3 us  [shift(): return lax.ppermute(block, ('c', 'y'), up + down)]
    dot_general x33 -> x17, matrix products: 14.1 us -> 19.7 us  [dot32(): return jnp.dot(a, b, preferred_element_type=jnp.float32)]
  transfers between devices with their start and end apart: 23 -> 17, of which waited for: 9 -> 11; matrix products, arithmetic and copies ran while one was open for 9% -> 9% of each run, Pallas kernels for 0% -> 9%
where the time goes in v5:
time: 210 us; the launch traced here: 208 us
  waiting for transfers between devices  91.3 us (43%)
  starting transfers between devices  64.2 us (31%)
  matrix products  22.7 us (11%)
  Pallas kernels  18.6 us (9%)
  local copies, waits for them, and re-layouts  7.34 us (3%)
  other arithmetic  3.3 us (2%)
    ppermute x9, waiting for transfers between devices, shift(): return lax.ppermute(block, ('c', 'y'), up + down)  45.6 us
    all_to_all x1, waiting for transfers between devices, layer(): returned = lax.all_to_all(home, ('z', 'xh'), 0, 0, tiled=True)  20.4 us
    all_to_all x1, waiting for transfers between devices, layer(): arrived = lax.all_to_all(mine, ('z', 'xh'), 0, 0, tiled=True)  20.3 us
    dot_general x17, matrix products, dot32(): return jnp.dot(a, b, preferred_element_type=jnp.float32)  19.7 us
    ppermute x9, starting transfers between devices, shift(): return lax.ppermute(block, ('c', 'y'), up + down)  19.3 us
    pallas_call x4, Pallas kernels, hidden_of(): pl.pallas_call(hidden_kernel, grid=(steps,), in_specs=[pl.BlockSpec(memor...  18.6 us
    all_to_all x1, starting transfers between devices, layer(): arrived = lax.all_to_all(mine, ('z', 'xh'), 0, 0, tiled=True)  18.3 us
    ppermute x6, starting transfers between devices, swap(): return lax.ppermute(block, axis, SWAP)  13.3 us
  transfers between devices with their start and end apart: 17, of which 11 were waited for; matrix products, arithmetic and copies ran while one was open for 9% of the time, Pallas kernels for 9%

profile of v5, /device:TPU:6, one launch (start us, length us, event | category | flops | bytes accessed | tf_op | source)
XLA Modules:
  0.0 207.9 jit_solution(14704390752936814597)
XLA Ops:
  0.8 1.3 fusion.12
  2.3 1.5 convolution_convert_fusion
  4.7 18.3 %all-to-all-start = ((bf16[32,48,128]{2,1,0:T(8,128)(2,1)}), bf16[32,48,128]{2,1,0:T(8,128)(2,1)S(1)}, u32[]{:S(2)}, u32[]{:S(2)}) async-start(bf16[32,48,128]{2,1,0:T(8,128)(2,1)} %reshape.96), calls=%async_computation | async-start | bytes 786432 | tf_op jit(solution)/shard_map/all_to_all | solution.py:130
  25.3 2.7 %collective-permute-start.8 = (bf16[4096,256]{1,0:T(8,128)(2,1)}, bf16[4096,256]{1,0:T(8,128)(2,1)}, u32[]{:S(2)}, u32[]{:S(2)}) collective-permute-start(bf16[4096,256]{1,0:T(8,128)(2,1)} %constant_dynamic-update-slice_fusion.4.gate_ref.up_ref), channel_id=1, source_target_pairs={{0,8},{8,0},{1,9},{9,1},{2,10},{10,2},{3,11},{11,3},{4,12},{12,4},... | collective-permute-start | bytes 6291464 | tf_op jit(solution)/shard_map/ppermute | solution.py:31
  28.0 1.9 collective-permute-start.3
  29.9 20.3 %all-to-all-done = bf16[32,48,128]{2,1,0:T(8,128)(2,1)S(1)} async-done(((bf16[32,48,128]{2,1,0:T(8,128)(2,1)}), bf16[32,48,128]{2,1,0:T(8,128)(2,1)S(1)}, u32[]{:S(2)}, u32[]{:S(2)}) %all-to-all-start) | async-done | bytes 393248 | tf_op jit(solution)/shard_map/all_to_all | solution.py:130
  50.4 3.5 %collective-permute-start = (bf16[96,2048]{1,0:T(8,128)(2,1)S(1)}, bf16[96,2048]{1,0:T(8,128)(2,1)S(1)}, u32[]{:S(2)}, u32[]{:S(2)}) collective-permute-start(bf16[96,2048]{1,0:T(8,128)(2,1)S(1)} %reshape.97), channel_id=1, source_target_pairs={{0,1},{1,2},{2,3},{3,0},{4,7},{5,4},{6,5},{7,6},{8,9},{9,10},{10,1... | collective-permute-start | bytes 1179656 | tf_op jit(solution)/shard_map/ppermute | solution.py:27
  53.9 7.4 %collective-permute-done = bf16[96,2048]{1,0:T(8,128)(2,1)S(1)} collective-permute-done((bf16[96,2048]{1,0:T(8,128)(2,1)S(1)}, bf16[96,2048]{1,0:T(8,128)(2,1)S(1)}, u32[]{:S(2)}, u32[]{:S(2)}) %collective-permute-start) | collective-permute-done | bytes 393248 | tf_op jit(solution)/shard_map/ppermute | solution.py:27
  61.3 2.3 %collective-permute-start.1 = (bf16[96,2048]{1,0:T(8,128)(2,1)S(1)}, bf16[96,2048]{1,0:T(8,128)(2,1)S(1)}, u32[]{:S(2)}, u32[]{:S(2)}) collective-permute-start(bf16[96,2048]{1,0:T(8,128)(2,1)S(1)} %collective-permute-done), channel_id=1, source_target_pairs={{0,1},{1,2},{2,3},{3,0},{4,7},{5,4},{6,5},{7,6},{8,9},{9,10},{10,1... | collective-permute-start | bytes 1179656 | tf_op jit(solution)/shard_map/ppermute | solution.py:27
  63.5 1.9 collective-permute-start.7
  65.5 2.7 %collective-permute-start.10 = (bf16[1024,512]{1,0:T(8,128)(2,1)}, bf16[1024,512]{1,0:T(8,128)(2,1)}, u32[]{:S(2)}, u32[]{:S(2)}) collective-permute-start(bf16[1024,512]{1,0:T(8,128)(2,1)} %param.13), channel_id=1, source_target_pairs={{0,8},{8,0},{1,9},{9,1},{2,10},{10,2},{3,11},{11,3},{4,12},{12,4},... | collective-permute-start | bytes 3145736 | tf_op jit(solution)/shard_map/ppermute | solution.py:31
  68.2 3.9 %collective-permute-done.1 = bf16[96,2048]{1,0:T(8,128)(2,1)S(1)} collective-permute-done((bf16[96,2048]{1,0:T(8,128)(2,1)S(1)}, bf16[96,2048]{1,0:T(8,128)(2,1)S(1)}, u32[]{:S(2)}, u32[]{:S(2)}) %collective-permute-start.1) | collective-permute-done | bytes 393248 | tf_op jit(solution)/shard_map/ppermute | solution.py:27
  72.1 1.9 collective-permute-start.2
  74.1 5.0 %collective-permute-done.8.gate_ref.up_ref = bf16[4096,256]{1,0:T(8,128)(2,1)} collective-permute-done((bf16[4096,256]{1,0:T(8,128)(2,1)}, bf16[4096,256]{1,0:T(8,128)(2,1)}, u32[]{:S(2)}, u32[]{:S(2)}) %collective-permute-start.8) | collective-permute-done | bytes 2097184 | tf_op jit(solution)/shard_map/ppermute | solution.py:31
  79.1 1.9 collective-permute-start.9
  81.1 1.9 collective-permute-done.2
  84.2 4.6 %hidden.4 = bf16[384,256]{1,0:T(8,128)(2,1)} custom-call(bf16[384,2048]{1,0:T(8,128)(2,1)} %copy-done, bf16[4096,256]{1,0:T(8,128)(2,1)} %constant_dynamic-update-slice_fusion.4.gate_ref.up_ref, bf16[4096,256]{1,0:T(8,128)(2,1)} %constant_dynamic-update-slice_fusion.4.gate_ref.up_ref), custom_call_target="tpu_custom_call" | custom-call | flops 805306368 | bytes 3866624 | tf_op jit(solution)/shard_map/hidden/pallas_call | solution.py:69
  88.8 4.7 %hidden.5 = bf16[384,256]{1,0:T(8,128)(2,1)} custom-call(bf16[384,2048]{1,0:T(8,128)(2,1)} %copy-done, bf16[4096,256]{1,0:T(8,128)(2,1)} %collective-permute-done.3.gate_ref.up_ref, bf16[4096,256]{1,0:T(8,128)(2,1)} %collective-permute-done.3.gate_ref.up_ref), custom_call_target="tpu_custom_call" | custom-call | flops 805306368 | bytes 3866624 | tf_op jit(solution)/shard_map/hidden/pallas_call | solution.py:69
  94.5 1.9 collective-permute-start.4
  96.4 9.0 %collective-permute-done.4 = bf16[384,512]{1,0:T(8,128)(2,1)S(1)} collective-permute-done((bf16[384,512]{1,0:T(8,128)(2,1)S(1)}, bf16[384,512]{1,0:T(8,128)(2,1)S(1)}, u32[]{:S(2)}, u32[]{:S(2)}) %collective-permute-start.4) | collective-permute-done | bytes 393248 | tf_op jit(solution)/shard_map/ppermute | solution.py:27
  105.3 1.9 collective-permute-start.5
  107.3 2.1 collective-permute-start.14
  109.4 4.6 %hidden.6 = bf16[384,256]{1,0:T(8,128)(2,1)} custom-call(bf16[384,2048]{1,0:T(8,128)(2,1)} %copy-done, bf16[4096,256]{1,0:T(8,128)(2,1)} %collective-permute-done.8.gate_ref.up_ref, bf16[4096,256]{1,0:T(8,128)(2,1)} %collective-permute-done.8.gate_ref.up_ref), custom_call_target="tpu_custom_call" | custom-call | flops 805306368 | bytes 3866624 | tf_op jit(solution)/shard_map/hidden/pallas_call | solution.py:69
  115.2 1.2 fusion.36
  116.5 1.9 collective-permute-start.6
  118.4 1.2 fusion.40
  119.7 1.2 fusion.34
  120.9 1.2 fusion.9
  122.1 5.3 %collective-permute-done.6 = bf16[384,512]{1,0:T(8,128)(2,1)S(1)} collective-permute-done((bf16[384,512]{1,0:T(8,128)(2,1)S(1)}, bf16[384,512]{1,0:T(8,128)(2,1)S(1)}, u32[]{:S(2)}, u32[]{:S(2)}) %collective-permute-start.6) | collective-permute-done | bytes 393248 | tf_op jit(solution)/shard_map/ppermute | solution.py:27
  127.4 4.7 %hidden.7 = bf16[384,256]{1,0:T(8,128)(2,1)} custom-call(bf16[384,2048]{1,0:T(8,128)(2,1)} %copy-done, bf16[4096,256]{1,0:T(8,128)(2,1)} %collective-permute-done.9.gate_ref.up_ref, bf16[4096,256]{1,0:T(8,128)(2,1)} %collective-permute-done.9.gate_ref.up_ref), custom_call_target="tpu_custom_call" | custom-call | flops 805306368 | bytes 3866624 | tf_op jit(solution)/shard_map/hidden/pallas_call | solution.py:69
  133.1 2.1 collective-permute-start.11
  135.1 1.2 fusion.32
  136.3 1.2 convolution_add_fusion.3
  137.6 6.5 %collective-permute-done.11 = bf16[384,512]{1,0:T(8,128)(2,1)S(1)} collective-permute-done((bf16[384,512]{1,0:T(8,128)(2,1)S(1)}, bf16[384,512]{1,0:T(8,128)(2,1)S(1)}, u32[]{:S(2)}, u32[]{:S(2)}) %collective-permute-start.11) | collective-permute-done | bytes 393248 | tf_op jit(solution)/shard_map/ppermute | solution.py:27
  144.1 1.9 collective-permute-start.12
  146.0 1.2 fusion.8
  147.3 1.2 fusion.29
  149.7 5.2 %collective-permute-done.12 = bf16[384,512]{1,0:T(8,128)(2,1)S(1)} collective-permute-done((bf16[384,512]{1,0:T(8,128)(2,1)S(1)}, bf16[384,512]{1,0:T(8,128)(2,1)S(1)}, u32[]{:S(2)}, u32[]{:S(2)}) %collective-permute-start.12) | collective-permute-done | bytes 393248 | tf_op jit(solution)/shard_map/ppermute | solution.py:27
  154.9 1.9 collective-permute-start.13
  156.9 1.2 fusion.27
  158.1 1.2 fusion.20
  159.3 6.5 %collective-permute-done.13 = bf16[384,512]{1,0:T(8,128)(2,1)S(1)} collective-permute-done((bf16[384,512]{1,0:T(8,128)(2,1)S(1)}, bf16[384,512]{1,0:T(8,128)(2,1)S(1)}, u32[]{:S(2)}, u32[]{:S(2)}) %collective-permute-start.13) | collective-permute-done | bytes 393248 | tf_op jit(solution)/shard_map/ppermute | solution.py:27
  165.8 1.2 fusion.25
  167.1 1.2 fusion.18
  168.3 1.2 fusion.5
  169.5 1.3 fusion.10
  172.4 13.3 %all-to-all-start.1 = ((bf16[32,48,128]{2,1,0:T(8,128)(2,1)}), bf16[32,48,128]{2,1,0:T(8,128)(2,1)S(1)}, u32[]{:S(2)}, u32[]{:S(2)}) async-start(bf16[32,48,128]{2,1,0:T(8,128)(2,1)} %reshape.99), calls=%async_computation.1 | async-start | bytes 786432 | tf_op jit(solution)/shard_map/all_to_all | solution.py:163
  186.3 20.4 %all-to-all-done.1 = bf16[32,48,128]{2,1,0:T(8,128)(2,1)S(1)} async-done(((bf16[32,48,128]{2,1,0:T(8,128)(2,1)}), bf16[32,48,128]{2,1,0:T(8,128)(2,1)S(1)}, u32[]{:S(2)}, u32[]{:S(2)}) %all-to-all-start.1) | async-done | bytes 393248 | tf_op jit(solution)/shard_map/all_to_all | solution.py:163
  (59 shorter events, 13.4 us)
Async XLA Ops:
  0.8 22.3 %copy-start.3 = (bf16[2048,256]{1,0:T(8,128)(2,1)S(1)}, bf16[2048,256]{1,0:T(8,128)(2,1)}, u32[]{:S(2)}) copy-start(bf16[2048,256]{1,0:T(8,128)(2,1)} %param.11) | copy-start | bytes 3145732
  4.7 19.4 %copy-start.4 = (bf16[2048,256]{1,0:T(8,128)(2,1)S(1)}, bf16[2048,256]{1,0:T(8,128)(2,1)}, u32[]{:S(2)}) copy-start(bf16[2048,256]{1,0:T(8,128)(2,1)} %param.12) | copy-start | bytes 3145732
  4.7 45.5 %all-to-all-start = ((bf16[32,48,128]{2,1,0:T(8,128)(2,1)}), bf16[32,48,128]{2,1,0:T(8,128)(2,1)S(1)}, u32[]{:S(2)}, u32[]{:S(2)}) async-start(bf16[32,48,128]{2,1,0:T(8,128)(2,1)} %reshape.96), calls=%async_computation | async-start | bytes 786432 | tf_op jit(solution)/shard_map/all_to_all | solution.py:130
  25.3 53.8 %collective-permute-start.8 = (bf16[4096,256]{1,0:T(8,128)(2,1)}, bf16[4096,256]{1,0:T(8,128)(2,1)}, u32[]{:S(2)}, u32[]{:S(2)}) collective-permute-start(bf16[4096,256]{1,0:T(8,128)(2,1)} %constant_dynamic-update-slice_fusion.4.gate_ref.up_ref), channel_id=1, source_target_pairs={{0,8},{8,0},{1,9},{9,1},{2,10},{10,2},{3,11},{11,3},{4,12},{12,4},... | collective-permute-start | bytes 6291464 | tf_op jit(solution)/shard_map/ppermute | solution.py:31
  28.0 60.8 %collective-permute-start.3 = (bf16[4096,256]{1,0:T(8,128)(2,1)}, bf16[4096,256]{1,0:T(8,128)(2,1)}, u32[]{:S(2)}, u32[]{:S(2)}) collective-permute-start(bf16[4096,256]{1,0:T(8,128)(2,1)} %constant_dynamic-update-slice_fusion.4.gate_ref.up_ref), channel_id=1, source_target_pairs={{0,4},{4,0},{1,5},{5,1},{2,6},{6,2},{3,7},{7,3},{8,12},{12,8},{9,1... | collective-permute-start | bytes 6291464 | tf_op jit(solution)/shard_map/ppermute | solution.py:31
  50.4 10.9 %collective-permute-start = (bf16[96,2048]{1,0:T(8,128)(2,1)S(1)}, bf16[96,2048]{1,0:T(8,128)(2,1)S(1)}, u32[]{:S(2)}, u32[]{:S(2)}) collective-permute-start(bf16[96,2048]{1,0:T(8,128)(2,1)S(1)} %reshape.97), channel_id=1, source_target_pairs={{0,1},{1,2},{2,3},{3,0},{4,7},{5,4},{6,5},{7,6},{8,9},{9,10},{10,1... | collective-permute-start | bytes 1179656 | tf_op jit(solution)/shard_map/ppermute | solution.py:27
  61.3 10.9 %collective-permute-start.1 = (bf16[96,2048]{1,0:T(8,128)(2,1)S(1)}, bf16[96,2048]{1,0:T(8,128)(2,1)S(1)}, u32[]{:S(2)}, u32[]{:S(2)}) collective-permute-start(bf16[96,2048]{1,0:T(8,128)(2,1)S(1)} %collective-permute-done), channel_id=1, source_target_pairs={{0,1},{1,2},{2,3},{3,0},{4,7},{5,4},{6,5},{7,6},{8,9},{9,10},{10,1... | collective-permute-start | bytes 1179656 | tf_op jit(solution)/shard_map/ppermute | solution.py:27
  63.5 51.7 %collective-permute-start.7 = (bf16[1024,512]{1,0:T(8,128)(2,1)}, bf16[1024,512]{1,0:T(8,128)(2,1)}, u32[]{:S(2)}, u32[]{:S(2)}) collective-permute-start(bf16[1024,512]{1,0:T(8,128)(2,1)} %param.13), channel_id=1, source_target_pairs={{0,4},{4,0},{1,5},{5,1},{2,6},{6,2},{3,7},{7,3},{8,12},{12,8},{9,1... | collective-permute-start | bytes 3145736 | tf_op jit(solution)/shard_map/ppermute | solution.py:31
  65.5 41.8 %collective-permute-start.10 = (bf16[1024,512]{1,0:T(8,128)(2,1)}, bf16[1024,512]{1,0:T(8,128)(2,1)}, u32[]{:S(2)}, u32[]{:S(2)}) collective-permute-start(bf16[1024,512]{1,0:T(8,128)(2,1)} %param.13), channel_id=1, source_target_pairs={{0,8},{8,0},{1,9},{9,1},{2,10},{10,2},{3,11},{11,3},{4,12},{12,4},... | collective-permute-start | bytes 3145736 | tf_op jit(solution)/shard_map/ppermute | solution.py:31
  72.1 10.9 %collective-permute-start.2 = (bf16[96,2048]{1,0:T(8,128)(2,1)S(1)}, bf16[96,2048]{1,0:T(8,128)(2,1)S(1)}, u32[]{:S(2)}, u32[]{:S(2)}) collective-permute-start(bf16[96,2048]{1,0:T(8,128)(2,1)S(1)} %collective-permute-done.1), channel_id=1, source_target_pairs={{0,1},{1,2},{2,3},{3,0},{4,7},{5,4},{6,5},{7,6},{8,9},{9,10},{10,1... | collective-permute-start | bytes 1179656 | tf_op jit(solution)/shard_map/ppermute | solution.py:27
  79.1 48.3 %collective-permute-start.9 = (bf16[4096,256]{1,0:T(8,128)(2,1)}, bf16[4096,256]{1,0:T(8,128)(2,1)}, u32[]{:S(2)}, u32[]{:S(2)}) collective-permute-start(bf16[4096,256]{1,0:T(8,128)(2,1)} %collective-permute-done.8.gate_ref.up_ref), channel_id=1, source_target_pairs={{0,4},{4,0},{1,5},{5,1},{2,6},{6,2},{3,7},{7,3},{8,12},{12,8},{9,1... | collective-permute-start | bytes 6291464 | tf_op jit(solution)/shard_map/ppermute | solution.py:31
  83.0 1.2 copy-start
  88.8 4.7 %copy-start.2 = (bf16[384,256]{1,0:T(8,128)(2,1)S(1)}, bf16[384,256]{1,0:T(8,128)(2,1)}, u32[]{:S(2)}) copy-start(bf16[384,256]{1,0:T(8,128)(2,1)} %hidden.4) | copy-start | bytes 589828
  94.5 10.9 %collective-permute-start.4 = (bf16[384,512]{1,0:T(8,128)(2,1)S(1)}, bf16[384,512]{1,0:T(8,128)(2,1)S(1)}, u32[]{:S(2)}, u32[]{:S(2)}) collective-permute-start(bf16[384,512]{1,0:T(8,128)(2,1)S(1)} %pad_maximum_fusion), channel_id=1, source_target_pairs={{0,1},{1,2},{2,3},{3,0},{4,7},{5,4},{6,5},{7,6},{8,9},{9,10},{10,1... | collective-permute-start | bytes 1179656 | tf_op jit(solution)/shard_map/ppermute | solution.py:27
  105.3 11.1 %collective-permute-start.5 = (bf16[384,512]{1,0:T(8,128)(2,1)S(1)}, bf16[384,512]{1,0:T(8,128)(2,1)S(1)}, u32[]{:S(2)}, u32[]{:S(2)}) collective-permute-start(bf16[384,512]{1,0:T(8,128)(2,1)S(1)} %collective-permute-done.4), channel_id=1, source_target_pairs={{0,1},{1,2},{2,3},{3,0},{4,7},{5,4},{6,5},{7,6},{8,9},{9,10},{10,1... | collective-permute-start | bytes 1179656 | tf_op jit(solution)/shard_map/ppermute | solution.py:27
  107.3 41.2 %collective-permute-start.14 = (bf16[1024,512]{1,0:T(8,128)(2,1)}, bf16[1024,512]{1,0:T(8,128)(2,1)}, u32[]{:S(2)}, u32[]{:S(2)}) collective-permute-start(bf16[1024,512]{1,0:T(8,128)(2,1)} %collective-permute-done.10), channel_id=1, source_target_pairs={{0,4},{4,0},{1,5},{5,1},{2,6},{6,2},{3,7},{7,3},{8,12},{12,8},{9,1... | collective-permute-start | bytes 3145736 | tf_op jit(solution)/shard_map/ppermute | solution.py:31
  116.5 10.9 %collective-permute-start.6 = (bf16[384,512]{1,0:T(8,128)(2,1)S(1)}, bf16[384,512]{1,0:T(8,128)(2,1)S(1)}, u32[]{:S(2)}, u32[]{:S(2)}) collective-permute-start(bf16[384,512]{1,0:T(8,128)(2,1)S(1)} %collective-permute-done.5), channel_id=1, source_target_pairs={{0,1},{1,2},{2,3},{3,0},{4,7},{5,4},{6,5},{7,6},{8,9},{9,10},{10,1... | collective-permute-start | bytes 1179656 | tf_op jit(solution)/shard_map/ppermute | solution.py:27
  127.4 4.7 %copy-start.5 = (bf16[384,256]{1,0:T(8,128)(2,1)S(1)}, bf16[384,256]{1,0:T(8,128)(2,1)}, u32[]{:S(2)}) copy-start(bf16[384,256]{1,0:T(8,128)(2,1)} %hidden.6) | copy-start | bytes 589828
  133.0 12.9 %copy-start.1 = (bf16[384,256]{1,0:T(8,128)(2,1)S(1)}, bf16[384,256]{1,0:T(8,128)(2,1)}, u32[]{:S(2)}) copy-start(bf16[384,256]{1,0:T(8,128)(2,1)} %hidden.5) | copy-start | bytes 589828
  133.1 11.0 %collective-permute-start.11 = (bf16[384,512]{1,0:T(8,128)(2,1)S(1)}, bf16[384,512]{1,0:T(8,128)(2,1)S(1)}, u32[]{:S(2)}, u32[]{:S(2)}) collective-permute-start(bf16[384,512]{1,0:T(8,128)(2,1)S(1)} %pad_maximum_fusion.1), channel_id=1, source_target_pairs={{0,1},{1,2},{2,3},{3,0},{4,7},{5,4},{6,5},{7,6},{8,9},{9,10},{10,1... | collective-permute-start | bytes 1179656 | tf_op jit(solution)/shard_map/ppermute | solution.py:27
  144.1 10.9 %collective-permute-start.12 = (bf16[384,512]{1,0:T(8,128)(2,1)S(1)}, bf16[384,512]{1,0:T(8,128)(2,1)S(1)}, u32[]{:S(2)}, u32[]{:S(2)}) collective-permute-start(bf16[384,512]{1,0:T(8,128)(2,1)S(1)} %collective-permute-done.11), channel_id=1, source_target_pairs={{0,1},{1,2},{2,3},{3,0},{4,7},{5,4},{6,5},{7,6},{8,9},{9,10},{10,1... | collective-permute-start | bytes 1179656 | tf_op jit(solution)/shard_map/ppermute | solution.py:27
  154.9 10.9 %collective-permute-start.13 = (bf16[384,512]{1,0:T(8,128)(2,1)S(1)}, bf16[384,512]{1,0:T(8,128)(2,1)S(1)}, u32[]{:S(2)}, u32[]{:S(2)}) collective-permute-start(bf16[384,512]{1,0:T(8,128)(2,1)S(1)} %collective-permute-done.12), channel_id=1, source_target_pairs={{0,1},{1,2},{2,3},{3,0},{4,7},{5,4},{6,5},{7,6},{8,9},{9,10},{10,1... | collective-permute-start | bytes 1179656 | tf_op jit(solution)/shard_map/ppermute | solution.py:27
  171.0 14.7 %copy-start.6 = (f32[128,2]{0,1:T(2,128)S(1)}, f32[128,2]{0,1:T(2,128)}, u32[]{:S(2)}) copy-start(f32[128,2]{0,1:T(2,128)} %param.10) | copy-start | bytes 3076
  172.4 34.3 %all-to-all-start.1 = ((bf16[32,48,128]{2,1,0:T(8,128)(2,1)}), bf16[32,48,128]{2,1,0:T(8,128)(2,1)S(1)}, u32[]{:S(2)}, u32[]{:S(2)}) async-start(bf16[32,48,128]{2,1,0:T(8,128)(2,1)} %reshape.99), calls=%async_computation.1 | async-start | bytes 786432 | tf_op jit(solution)/shard_map/all_to_all | solution.py:163

commit v6 on v4

--- a/solution.py
+++ b/solution.py
@@ -1,6 +1,10 @@
+import functools
+
 import jax
 import jax.numpy as jnp
 from jax import lax
+from jax.experimental import pallas as pl
+from jax.experimental.pallas import tpu as pltpu
 from jax.sharding import Mesh
 from jax.sharding import PartitionSpec as P
 
@@ -18,10 +22,8 @@
     return (widened * scale * gain).astype(jnp.bfloat16)
 
 
-def shift(block, by=1):
-    up = [(y, (y + by) % 4) for y in range(4)]
-    down = [(4 + y, 4 + (y - by) % 4) for y in range(4)]
-    return lax.ppermute(block, ("c", "y"), up + down)
+def shift(block, by):
+    return lax.ppermute(block, "y", [(y, (y + by) % 4) for y in range(4)])
 
 
 def swap(block, axis):
@@ -40,9 +42,100 @@
     return jnp.dot(per_expert, table, precision=precision, preferred_element_type=jnp.float32)
 
 
+def expert_kernel(*refs):
+    rows_ref, gates, uppers, downs = refs[0], refs[1:5], refs[5:9], refs[9:13]
+    hidden_ref, part_ref, wide, tall, sems = refs[13:]
+    depth = wide.shape[2]
+    copies = []
+    for i in range(4):
+        copies.append(pltpu.make_async_copy(gates[i], wide.at[2 * i], sems.at[3 * i]))
+        copies.append(pltpu.make_async_copy(uppers[i], wide.at[2 * i + 1], sems.at[3 * i + 1]))
+        copies.append(pltpu.make_async_copy(downs[i].at[2], tall.at[i], sems.at[3 * i + 2]))
+    for copy in copies:
+        copy.start()
+    total = jnp.zeros(part_ref.shape, jnp.float32)
+    for i in range(4):
+        copies[3 * i].wait()
+        gate_proj = dot32(rows_ref[...], wide[2 * i])
+        copies[3 * i + 1].wait()
+        upper = dot32(rows_ref[...], wide[2 * i + 1])
+        piece = (jax.nn.silu(gate_proj) * upper).astype(jnp.bfloat16)
+        hidden_ref[:, i * depth : (i + 1) * depth] = piece
+        copies[3 * i + 2].wait()
+        total += dot32(piece, tall[i])
+    part_ref[...] = total.astype(part_ref.dtype)
+
+
+def run_experts(rows_in, gates, uppers, downs):
+    count, width = rows_in.shape
+    depth = gates[0].shape[1]
+    _, _, out_width = downs[0].shape
+    return pl.pallas_call(
+        expert_kernel,
+        in_specs=[pl.BlockSpec(memory_space=pltpu.VMEM)]
+        + [pl.BlockSpec(memory_space=pl.ANY)] * 12,
+        out_specs=[pl.BlockSpec(memory_space=pltpu.VMEM)] * 2,
+        out_shape=[
+            jax.ShapeDtypeStruct((count, 4 * depth), jnp.bfloat16),
+            jax.ShapeDtypeStruct((count, out_width), jnp.bfloat16),
+        ],
+        scratch_shapes=[
+            pltpu.VMEM((8, width, depth), jnp.bfloat16),
+            pltpu.VMEM((4, depth, out_width), jnp.bfloat16),
+            pltpu.SemaphoreType.DMA((12,)),
+        ],
+        cost_estimate=pl.CostEstimate(
+            flops=16 * count * width * depth,
+            bytes_accessed=16 * width * depth,
+            transcendentals=4 * count * depth,
+        ),
+        compiler_params=pltpu.CompilerParams(vmem_limit_bytes=40 << 20),
+        name="experts",
+    )(rows_in, *gates, *uppers, *downs)
+
+
+def down_kernel(picks, hidden_ref, *refs):
+    downs, outs, (tall, sems) = refs[:4], refs[4 : 4 + len(picks)], refs[4 + len(picks) :]
+    depth = tall.shape[1]
+    copies = [
+        pltpu.make_async_copy(downs[i].at[k], tall.at[4 * n + i], sems.at[4 * n + i])
+        for n, k in enumerate(picks)
+        for i in range(4)
+    ]
+    for copy in copies:
+        copy.start()
+    for n, out in enumerate(outs):
+        total = jnp.zeros(out.shape, jnp.float32)
+        for i in range(4):
+            copies[4 * n + i].wait()
+            total += dot32(hidden_ref[:, i * depth : (i + 1) * depth], tall[4 * n + i])
+        out[...] = total
+
+
+def run_down(hidden, downs, picks):
+    count = hidden.shape[0]
+    _, depth, out_width = downs[0].shape
+    return pl.pallas_call(
+        functools.partial(down_kernel, picks),
+        in_specs=[pl.BlockSpec(memory_space=pltpu.VMEM)] + [pl.BlockSpec(memory_space=pl.ANY)] * 4,
+        out_specs=[pl.BlockSpec(memory_space=pltpu.VMEM)] * len(picks),
+        out_shape=[jax.ShapeDtypeStruct((count, out_width), jnp.float32)] * len(picks),
+        scratch_shapes=[
+            pltpu.VMEM((4 * len(picks), depth, out_width), jnp.bfloat16),
+            pltpu.SemaphoreType.DMA((4 * len(picks),)),
+        ],
+        cost_estimate=pl.CostEstimate(
+            flops=8 * len(picks) * count * depth * out_width,
+            bytes_accessed=8 * len(picks) * depth * out_width,
+            transcendentals=0,
+        ),
+        compiler_params=pltpu.CompilerParams(vmem_limit_bytes=40 << 20),
+        name="down",
+    )(hidden, *downs)
+
+
 def layer(tokens, norm_gain, expert_ids, gate_weights, w_gate, w_up, w_down):
     y = lax.axis_index("y")
-    turn = 1 - 2 * lax.axis_index("c")
     rows = tokens.shape[0]
     width = tokens.shape[1]
     share = CAP // 4
@@ -80,56 +173,51 @@
 
     cut = []
     for k in range(4):
-        start = ((y + turn * k) & 3) * depth
+        start = ((y - k) & 3) * depth
         cut.append(lax.dynamic_slice_in_dim(w_down, start, depth, 0))
     for k in (1, 2, 3):
-        cut[k] = shift(cut[k], k)
-    down_o = (jnp.stack([cut[1], cut[3]]), jnp.stack([cut[2], cut[0]]))
-    down_x = (swap(down_o[0], "xl"), swap(down_o[1], "xl"))
+        cut[k] = shift(cut[k], -k)
+    down_o = jnp.stack(cut)
+    down_x = swap(down_o, "xl")
     gate_c = swap(w_gate, "c")
     up_c = swap(w_up, "c")
-    down_c = (swap(down_o[0], "c"), swap(down_o[1], "c"))
+    down_c = swap(down_o, "c")
     gate_d = swap(gate_x, "c")
     up_d = swap(up_x, "c")
-    down_d = (swap(down_x[0], "c"), swap(down_x[1], "c"))
-
-    blocks = [near]
-    for _ in range(3):
-        blocks.append(shift(blocks[-1]))
-
-    hidden = []
-    for gate, up in zip((w_gate, gate_c, gate_x, gate_d), (w_up, up_c, up_x, up_d)):
-        parts = []
-        for low in (0, 2):
-            rows_now = jnp.concatenate(blocks[low : low + 2], 0)
-            gate_proj = dot32(rows_now, gate)
-            upper = dot32(rows_now, up)
-            parts.append((jax.nn.silu(gate_proj) * upper).astype(jnp.bfloat16))
-        hidden.append(jnp.concatenate(parts, 0))
-
-    def pick(pair, k):
-        return pair[0][k // 2] if k % 2 else pair[1][0 if k else 1]
-
-    def partial(k):
-        total = 0.0
-        for matrix, pair, at in zip(
-            hidden, (down_o, down_c, down_x, down_d), (k, (-k) % 4, k, (-k) % 4)
-        ):
-            total += dot32(matrix, pick(pair, at))
-        return total
-
-    total = partial(1)
-    for step in (1, 2, 3):
-        back = jnp.roll(shift(total.astype(jnp.bfloat16)), block_rows, 0)
-        total = partial((step + 1) % 4) + back.astype(jnp.float32)
+    down_d = swap(down_x, "c")
+
+    half = block_rows // 2
+    below = shift(near, 1)
+    above = shift(near, -1)
+    gathered = jnp.zeros((4, block_rows, width), jnp.bfloat16)
+    for block, ahead in ((near, 0), (below, 3), (above, 1)):
+        gathered = lax.dynamic_update_slice(gathered, block[None], ((y + ahead) & 3, 0, 0))
+    for block, low in ((shift(below[:half], 1), 0), (shift(above[half:], -1), half)):
+        gathered = lax.dynamic_update_slice(gathered, block[None], ((y + 2) & 3, low, 0))
+    gathered = gathered.reshape(4 * block_rows, width)
+
+    gates, uppers = (w_gate, gate_c, gate_x, gate_d), (w_up, up_c, up_x, up_d)
+    downs = (down_o, down_c, down_x, down_d)
+    hidden, away = run_experts(gathered, gates, uppers, downs)
+    middle = 2 * block_rows
+    first = shift(away[:middle], 1)
+    second = shift(away[middle:], -1)
+    upward, downward = run_down(hidden, downs, (1, 3))
+    upward = jnp.concatenate([upward[:middle] + first.astype(jnp.float32), upward[middle:]], 0)
+    downward = jnp.concatenate(
+        [downward[:middle], downward[middle:] + second.astype(jnp.float32)], 0
+    )
+    first = shift(upward.astype(jnp.bfloat16), 1)
+    second = shift(downward.astype(jnp.bfloat16), -1)
+    (total,) = run_down(hidden, downs, (0,))
+    total = total + first.astype(jnp.float32) + second.astype(jnp.float32)
     home = total.astype(jnp.bfloat16)
     home = home.reshape(4, expert_count, share, out_width).transpose(1, 0, 2, 3)
     home = home.reshape(expert_count, CAP * out_width // 128, 128)
     returned = lax.all_to_all(home, ("z", "xh"), 0, 0, tiled=True)
     returned = returned.reshape(expert_count * CAP, out_width).astype(jnp.float32)
     column = lax.broadcasted_iota(jnp.int32, (1, expert_count * CAP), 1) % CAP
-    slot = share * ((y - turn * (column // share)) & 3) + column % share
-    chosen = spread(rank, CAP) == slot.astype(jnp.float32)
+    chosen = spread(rank, CAP) == column.astype(jnp.float32)
     combine = jnp.where(chosen, spread(weight, CAP, lax.Precision.HIGHEST), 0.0)
     mixed = jnp.dot(
         combine, returned, precision=lax.Precision.HIGHEST, preferred_element_type=jnp.float32
@@ -148,9 +236,7 @@
         P(None, EP_TP),
         P(EP, "y"),
     )
-    return jax.shard_map(
-        layer, mesh=finer, in_specs=placed, out_specs=P(EP, "y"), check_vma=False
-    )
+    return jax.shard_map(layer, mesh=finer, in_specs=placed, out_specs=P(EP, "y"), check_vma=False)
 
 
 def solution(mesh):

time: 195 us -> 188 us (0.964)
  matrix products: 16.2 us -> 3.23 us
  Pallas kernels: 0 us -> 12.7 us
  waiting for transfers between devices: 83 us -> 72.8 us
  local copies, waits for them, and re-layouts: 7.72 us -> 10.5 us
    dot_general x33 -> x1, matrix products: 14.1 us -> 0.14 us  [dot32(): return jnp.dot(a, b, preferred_element_type=jnp.float32)]
    ppermute x9 -> x11, waiting for transfers between devices: 29.6 us -> 16 us  [shift(): return lax.ppermute(block, 'y', [(y, (y + by) % 4) for y in range(4)])]
    ppermute x9 -> x11, starting transfers between devices: 25.3 us -> 38.5 us  [shift(): return lax.ppermute(block, 'y', [(y, (y + by) % 4) for y in range(4)])]
    pallas_call x0 -> x3, Pallas kernels: none -> 12.7 us  [the longest x1 10.2 us: run_experts(): pl.pallas_call(expert_kernel, in_specs=[pl.BlockSpec(memory_space=pltpu.V...]
    ppermute x12 -> x9, starting transfers between devices: 31.5 us -> 21.1 us  [swap(): return lax.ppermute(block, axis, SWAP)]
    ppermute x12 -> x9, waiting for transfers between devices: 21.9 us -> 17.9 us  [swap(): return lax.ppermute(block, axis, SWAP)]
    all_to_all x1, waiting for transfers between devices: 21.1 us -> 24.9 us  [layer(): returned = lax.all_to_all(home, ('z', 'xh'), 0, 0, tiled=True)]
    all_to_all x1, waiting for transfers between devices: 10.4 us -> 13.9 us  [layer(): arrived = lax.all_to_all(mine, ('z', 'xh'), 0, 0, tiled=True)]
  transfers between devices with their start and end apart: 23 -> 22, of which waited for: 9 -> 9; matrix products, arithmetic and copies ran while one was open for 9% -> 4% of each run, Pallas kernels for 0% -> 1%
where the time goes in v6:
time: 188 us; the launch traced here: 186 us
  starting transfers between devices  83 us (44%)
  waiting for transfers between devices  72.8 us (39%)
  Pallas kernels  12.7 us (7%)
  local copies, waits for them, and re-layouts  10.5 us (6%)
  matrix products  3.23 us (2%)
  other arithmetic  2.98 us (2%)
    ppermute x11, starting transfers between devices, shift(): return lax.ppermute(block, 'y', [(y, (y + by) % 4) for y in range(4)])  38.5 us
    all_to_all x1, waiting for transfers between devices, layer(): returned = lax.all_to_all(home, ('z', 'xh'), 0, 0, tiled=True)  24.9 us
    ppermute x9, starting transfers between devices, swap(): return lax.ppermute(block, axis, SWAP)  21.1 us
    all_to_all x1, starting transfers between devices, layer(): arrived = lax.all_to_all(mine, ('z', 'xh'), 0, 0, tiled=True)  18.2 us
    ppermute x9, waiting for transfers between devices, swap(): return lax.ppermute(block, axis, SWAP)  17.9 us
    ppermute x11, waiting for transfers between devices, shift(): return lax.ppermute(block, 'y', [(y, (y + by) % 4) for y in range(4)])  16 us
    all_to_all x1, waiting for transfers between devices, layer(): arrived = lax.all_to_all(mine, ('z', 'xh'), 0, 0, tiled=True)  13.9 us
    pallas_call x1, Pallas kernels, run_experts(): pl.pallas_call(expert_kernel, in_specs=[pl.BlockSpec(memory_space=pltpu.V...  10.2 us
  transfers between devices with their start and end apart: 22, of which 9 were waited for; matrix products, arithmetic and copies ran while one was open for 4% of the time, Pallas kernels for 1%

profile of v6, /device:TPU:6, one launch (start us, length us, event | category | flops | bytes accessed | tf_op | source)
XLA Modules:
  0.0 185.7 jit_solution(9937840374944344486)
XLA Ops:
  0.0 0.8 slice_bitcast_fusion.3
  0.8 1.4 fusion.1
  2.3 1.5 convolution_convert_fusion
  3.9 0.9 reshape.63
  4.8 18.2 %all-to-all-start = ((bf16[32,48,128]{2,1,0:T(8,128)(2,1)}), bf16[32,48,128]{2,1,0:T(8,128)(2,1)S(1)}, u32[]{:S(2)}, u32[]{:S(2)}) async-start(bf16[32,48,128]{2,1,0:T(8,128)(2,1)} %reshape.63), calls=%async_computation | async-start | bytes 786432 | tf_op jit(solution)/shard_map/all_to_all | solution.py:171
  23.0 2.7 %collective-permute-start.5 = (bf16[2048,256]{1,0:T(8,128)(2,1)S(1)}, bf16[2048,256]{1,0:T(8,128)(2,1)}, u32[]{:S(2)}, u32[]{:S(2)}) collective-permute-start(bf16[2048,256]{1,0:T(8,128)(2,1)S(1)} %copy-done), channel_id=1, source_target_pairs={{0,8},{8,0},{1,9},{9,1},{2,10},{10,2},{3,11},{11,3},{4,12},{12,4},... | collective-permute-start | bytes 3145736 | tf_op jit(solution)/shard_map/ppermute | solution.py:30
  25.9 4.9 %collective-permute-start.10 = (bf16[256,512]{1,0:T(8,128)(2,1)S(1)}, bf16[256,512]{1,0:T(8,128)(2,1)S(1)}, u32[]{:S(2)}, u32[]{:S(2)}) collective-permute-start(bf16[256,512]{1,0:T(8,128)(2,1)S(1)} %get-tuple-element.14), channel_id=1, source_target_pairs={{0,3},{1,0},{2,1},{3,2},{4,7},{5,4},{6,5},{7,6},{8,11},{9,8},{10,9... | collective-permute-start | bytes 786440 | tf_op jit(solution)/shard_map/ppermute | solution.py:26
  30.8 2.5 %collective-permute-start.11 = (bf16[256,512]{1,0:T(8,128)(2,1)S(1)}, bf16[256,512]{1,0:T(8,128)(2,1)}, u32[]{:S(2)}, u32[]{:S(2)}) collective-permute-start(bf16[256,512]{1,0:T(8,128)(2,1)S(1)} %get-tuple-element.16), channel_id=1, source_target_pairs={{0,2},{1,3},{2,0},{3,1},{4,6},{5,7},{6,4},{7,5},{8,10},{9,11},{10,... | collective-permute-start | bytes 786440 | tf_op jit(solution)/shard_map/ppermute | solution.py:26
  33.4 2.9 %collective-permute-start.12 = (bf16[256,512]{1,0:T(8,128)(2,1)S(1)}, bf16[256,512]{1,0:T(8,128)(2,1)}, u32[]{:S(2)}, u32[]{:S(2)}) collective-permute-start(bf16[256,512]{1,0:T(8,128)(2,1)S(1)} %get-tuple-element.15), channel_id=1, source_target_pairs={{0,1},{1,2},{2,3},{3,0},{4,5},{5,6},{6,7},{7,4},{8,9},{9,10},{10,1... | collective-permute-start | bytes 786440 | tf_op jit(solution)/shard_map/ppermute | solution.py:26
  36.2 13.9 %all-to-all-done = bf16[32,48,128]{2,1,0:T(8,128)(2,1)S(1)} async-done(((bf16[32,48,128]{2,1,0:T(8,128)(2,1)}), bf16[32,48,128]{2,1,0:T(8,128)(2,1)S(1)}, u32[]{:S(2)}, u32[]{:S(2)}) %all-to-all-start) | async-done | bytes 393248 | tf_op jit(solution)/shard_map/all_to_all | solution.py:171
  50.1 0.9 reshape.64
  51.1 3.5 %collective-permute-start = (bf16[96,2048]{1,0:T(8,128)(2,1)}, bf16[96,2048]{1,0:T(8,128)(2,1)}, u32[]{:S(2)}, u32[]{:S(2)}) collective-permute-start(bf16[96,2048]{1,0:T(8,128)(2,1)} %reshape.64), channel_id=1, source_target_pairs={{0,1},{1,2},{2,3},{3,0},{4,5},{5,6},{6,7},{7,4},{8,9},{9,10},{10,1... | collective-permute-start | bytes 1179656 | tf_op jit(solution)/shard_map/ppermute | solution.py:26
  54.6 1.9 %collective-permute-start.4 = (bf16[2048,256]{1,0:T(8,128)(2,1)S(1)}, bf16[2048,256]{1,0:T(8,128)(2,1)}, u32[]{:S(2)}, u32[]{:S(2)}) collective-permute-start(bf16[2048,256]{1,0:T(8,128)(2,1)S(1)} %copy-done), channel_id=1, source_target_pairs={{0,4},{4,0},{1,5},{5,1},{2,6},{6,2},{3,7},{7,3},{8,12},{12,8},{9,1... | collective-permute-start | bytes 3145736 | tf_op jit(solution)/shard_map/ppermute | solution.py:30
  56.5 2.7 %collective-permute-start.8 = (bf16[2048,256]{1,0:T(8,128)(2,1)}, bf16[2048,256]{1,0:T(8,128)(2,1)}, u32[]{:S(2)}, u32[]{:S(2)}) collective-permute-start(bf16[2048,256]{1,0:T(8,128)(2,1)} %refs_5_.1), channel_id=1, source_target_pairs={{0,8},{8,0},{1,9},{9,1},{2,10},{10,2},{3,11},{11,3},{4,12},{12,4},... | collective-permute-start | bytes 3145736 | tf_op jit(solution)/shard_map/ppermute | solution.py:30
  59.3 1.2 pad_maximum_fusion.refs_9_.refs_0_
  60.5 3.1 %collective-permute-start.14 = (bf16[4,256,512]{2,1,0:T(8,128)(2,1)S(1)}, bf16[4,256,512]{2,1,0:T(8,128)(2,1)S(1)}, u32[]{:S(2)}, u32[]{:S(2)}) collective-permute-start(bf16[4,256,512]{2,1,0:T(8,128)(2,1)S(1)} %pad_maximum_fusion.refs_9_.refs_0_), channel_id=1, source_target_pairs={{0,8},{8,0},{1,9},{9,1},{2,10},{10,2},{3,11},{11,3},{4,12},{12,4},... | collective-permute-start | bytes 3145736 | tf_op jit(solution)/shard_map/ppermute | solution.py:30
  63.6 3.6 %collective-permute-start.1 = (bf16[96,2048]{1,0:T(8,128)(2,1)}, bf16[96,2048]{1,0:T(8,128)(2,1)}, u32[]{:S(2)}, u32[]{:S(2)}) collective-permute-start(bf16[96,2048]{1,0:T(8,128)(2,1)} %reshape.64), channel_id=1, source_target_pairs={{0,3},{1,0},{2,1},{3,2},{4,7},{5,4},{6,5},{7,6},{8,11},{9,8},{10,9... | collective-permute-start | bytes 1179656 | tf_op jit(solution)/shard_map/ppermute | solution.py:26
  67.2 0.9 broadcast_in_dim_reshape.3
  68.3 0.8 copy-done.2
  69.2 0.9 slice.50
  70.1 6.7 %collective-permute-done.1 = bf16[96,2048]{1,0:T(8,128)(2,1)} collective-permute-done((bf16[96,2048]{1,0:T(8,128)(2,1)}, bf16[96,2048]{1,0:T(8,128)(2,1)}, u32[]{:S(2)}, u32[]{:S(2)}) %collective-permute-start.1) | collective-permute-done | bytes 393248 | tf_op jit(solution)/shard_map/ppermute | solution.py:26
  76.8 3.5 %collective-permute-start.2 = (bf16[48,2048]{1,0:T(8,128)(2,1)S(1)}, bf16[48,2048]{1,0:T(8,128)(2,1)S(1)}, u32[]{:S(2)}, u32[]{:S(2)}) collective-permute-start(bf16[48,2048]{1,0:T(8,128)(2,1)S(1)} %slice.50), channel_id=1, source_target_pairs={{0,1},{1,2},{2,3},{3,0},{4,5},{5,6},{6,7},{7,4},{8,9},{9,10},{10,1... | collective-permute-start | bytes 589832 | tf_op jit(solution)/shard_map/ppermute | solution.py:26
  80.3 0.9 slice.51
  81.2 3.6 %collective-permute-start.3 = (bf16[48,2048]{1,0:T(8,128)(2,1)S(1)}, bf16[48,2048]{1,0:T(8,128)(2,1)S(1)}, u32[]{:S(2)}, u32[]{:S(2)}) collective-permute-start(bf16[48,2048]{1,0:T(8,128)(2,1)S(1)} %slice.51), channel_id=1, source_target_pairs={{0,3},{1,0},{2,1},{3,2},{4,7},{5,4},{6,5},{7,6},{8,11},{9,8},{10,9... | collective-permute-start | bytes 589832 | tf_op jit(solution)/shard_map/ppermute | solution.py:26
  84.8 1.0 bitcast_dynamic-update-slice_fusion.1
  85.9 1.9 %collective-permute-start.7 = (bf16[2048,256]{1,0:T(8,128)(2,1)}, bf16[2048,256]{1,0:T(8,128)(2,1)S(1)}, u32[]{:S(2)}, u32[]{:S(2)}) collective-permute-start(bf16[2048,256]{1,0:T(8,128)(2,1)} %refs_5_.1), channel_id=1, source_target_pairs={{0,4},{4,0},{1,5},{5,1},{2,6},{6,2},{3,7},{7,3},{8,12},{12,8},{9,1... | collective-permute-start | bytes 3145736 | tf_op jit(solution)/shard_map/ppermute | solution.py:30
  87.8 2.4 %collective-permute-start.13 = (bf16[4,256,512]{2,1,0:T(8,128)(2,1)S(1)}, bf16[4,256,512]{2,1,0:T(8,128)(2,1)S(1)}, u32[]{:S(2)}, u32[]{:S(2)}) collective-permute-start(bf16[4,256,512]{2,1,0:T(8,128)(2,1)S(1)} %pad_maximum_fusion.refs_9_.refs_0_), channel_id=1, source_target_pairs={{0,4},{4,0},{1,5},{5,1},{2,6},{6,2},{3,7},{7,3},{8,12},{12,8},{9,1... | collective-permute-start | bytes 3145736 | tf_op jit(solution)/shard_map/ppermute | solution.py:30
  90.2 16.4 %collective-permute-done.14.refs_11_.refs_2_ = bf16[4,256,512]{2,1,0:T(8,128)(2,1)S(1)} collective-permute-done((bf16[4,256,512]{2,1,0:T(8,128)(2,1)S(1)}, bf16[4,256,512]{2,1,0:T(8,128)(2,1)S(1)}, u32[]{:S(2)}, u32[]{:S(2)}) %collective-permute-start.14) | collective-permute-done | bytes 1048608 | tf_op jit(solution)/shard_map/ppermute | solution.py:30
  106.6 1.9 %collective-permute-start.6 = (bf16[2048,256]{1,0:T(8,128)(2,1)}, bf16[2048,256]{1,0:T(8,128)(2,1)S(1)}, u32[]{:S(2)}, u32[]{:S(2)}) collective-permute-start(bf16[2048,256]{1,0:T(8,128)(2,1)} %collective-permute-done.5.refs_3_), channel_id=1, source_target_pairs={{0,4},{4,0},{1,5},{5,1},{2,6},{6,2},{3,7},{7,3},{8,12},{12,8},{9,1... | collective-permute-start | bytes 3145736 | tf_op jit(solution)/shard_map/ppermute | solution.py:30
  108.6 2.4 %collective-permute-start.9 = (bf16[2048,256]{1,0:T(8,128)(2,1)}, bf16[2048,256]{1,0:T(8,128)(2,1)S(1)}, u32[]{:S(2)}, u32[]{:S(2)}) collective-permute-start(bf16[2048,256]{1,0:T(8,128)(2,1)} %collective-permute-done.8.refs_7_), channel_id=1, source_target_pairs={{0,4},{4,0},{1,5},{5,1},{2,6},{6,2},{3,7},{7,3},{8,12},{12,8},{9,1... | collective-permute-start | bytes 3145736 | tf_op jit(solution)/shard_map/ppermute | solution.py:30
  111.0 1.9 %collective-permute-start.15 = (bf16[4,256,512]{2,1,0:T(8,128)(2,1)S(1)}, bf16[4,256,512]{2,1,0:T(8,128)(2,1)S(1)}, u32[]{:S(2)}, u32[]{:S(2)}) collective-permute-start(bf16[4,256,512]{2,1,0:T(8,128)(2,1)S(1)} %collective-permute-done.14.refs_11_.refs_2_), channel_id=1, source_target_pairs={{0,4},{4,0},{1,5},{5,1},{2,6},{6,2},{3,7},{7,3},{8,12},{12,8},{9,1... | collective-permute-start | bytes 3145736 | tf_op jit(solution)/shard_map/ppermute | solution.py:30
  112.9 1.0 bitcast_dynamic-update-slice_fusion
  114.1 1.5 collective-permute-done.15.refs_12_.refs_3_
  115.6 10.2 %experts.1 = (bf16[384,1024]{1,0:T(8,128)(2,1)S(1)}, bf16[384,512]{1,0:T(8,128)(2,1)S(1)}) custom-call(bf16[384,2048]{1,0:T(8,128)(2,1)} %bitcast.27, bf16[2048,256]{1,0:T(8,128)(2,1)S(1)} %copy-done, bf16[2048,256]{1,0:T(8,128)(2,1)} %collective-permute-done.4.refs_2_, bf16[2048,256]{1,0:T(8,128)(2,1)} %collective-permute-done.5.refs_3_, ...), custom_call_target="tpu_custom_call" | custom-call | flops 3221225472 | bytes 8388608 | tf_op jit(solution)/shard_map/experts/pallas_call | solution.py:73
  125.8 3.5 %collective-permute-start.16 = (bf16[192,512]{1,0:T(8,128)(2,1)S(1)}, bf16[192,512]{1,0:T(8,128)(2,1)S(1)}, u32[]{:S(2)}, u32[]{:S(2)}) collective-permute-start(bf16[192,512]{1,0:T(8,128)(2,1)S(1)} %get-tuple-element.17), channel_id=1, source_target_pairs={{0,1},{1,2},{2,3},{3,0},{4,5},{5,6},{6,7},{7,4},{8,9},{9,10},{10,1... | collective-permute-start | bytes 589832 | tf_op jit(solution)/shard_map/ppermute | solution.py:26
  129.3 1.6 down.3
  131.0 3.6 %collective-permute-start.18 = (bf16[192,512]{1,0:T(8,128)(2,1)S(1)}, bf16[192,512]{1,0:T(8,128)(2,1)S(1)}, u32[]{:S(2)}, u32[]{:S(2)}) collective-permute-start(bf16[192,512]{1,0:T(8,128)(2,1)S(1)} %get-tuple-element.18), channel_id=1, source_target_pairs={{0,3},{1,0},{2,1},{3,2},{4,7},{5,4},{6,5},{7,6},{8,11},{9,8},{10,9... | collective-permute-start | bytes 589832 | tf_op jit(solution)/shard_map/ppermute | solution.py:26
  134.6 1.3 collective-permute-done.16
  136.0 2.3 %collective-permute-start.17 = (bf16[384,512]{1,0:T(8,128)(2,1)S(1)}, bf16[384,512]{1,0:T(8,128)(2,1)S(1)}, u32[]{:S(2)}, u32[]{:S(2)}) collective-permute-start(bf16[384,512]{1,0:T(8,128)(2,1)S(1)} %pad_maximum_fusion.1), channel_id=1, source_target_pairs={{0,1},{1,2},{2,3},{3,0},{4,5},{5,6},{6,7},{7,4},{8,9},{9,10},{10,1... | collective-permute-start | bytes 1179656 | tf_op jit(solution)/shard_map/ppermute | solution.py:26
  138.2 1.3 collective-permute-done.18
  139.6 4.8 %collective-permute-start.19 = (bf16[384,512]{1,0:T(8,128)(2,1)S(1)}, bf16[384,512]{1,0:T(8,128)(2,1)S(1)}, u32[]{:S(2)}, u32[]{:S(2)}) collective-permute-start(bf16[384,512]{1,0:T(8,128)(2,1)S(1)} %pad_maximum_fusion.2), channel_id=1, source_target_pairs={{0,3},{1,0},{2,1},{3,2},{4,7},{5,4},{6,5},{7,6},{8,11},{9,8},{10,9... | collective-permute-start | bytes 1179656 | tf_op jit(solution)/shard_map/ppermute | solution.py:26
  144.4 0.8 down.2
  145.2 4.1 %collective-permute-done.17 = bf16[384,512]{1,0:T(8,128)(2,1)S(1)} collective-permute-done((bf16[384,512]{1,0:T(8,128)(2,1)S(1)}, bf16[384,512]{1,0:T(8,128)(2,1)S(1)}, u32[]{:S(2)}, u32[]{:S(2)}) %collective-permute-start.17) | collective-permute-done | bytes 393248 | tf_op jit(solution)/shard_map/ppermute | solution.py:26
  149.4 2.6 %collective-permute-done.19 = bf16[384,512]{1,0:T(8,128)(2,1)S(1)} collective-permute-done((bf16[384,512]{1,0:T(8,128)(2,1)S(1)}, bf16[384,512]{1,0:T(8,128)(2,1)S(1)}, u32[]{:S(2)}, u32[]{:S(2)}) %collective-permute-start.19) | collective-permute-done | bytes 393248 | tf_op jit(solution)/shard_map/ppermute | solution.py:26
  152.6 1.1 reshape.67
  153.7 5.2 %all-to-all-start.1 = ((bf16[32,48,128]{2,1,0:T(8,128)(2,1)}), bf16[32,48,128]{2,1,0:T(8,128)(2,1)S(1)}, u32[]{:S(2)}, u32[]{:S(2)}) async-start(bf16[32,48,128]{2,1,0:T(8,128)(2,1)} %reshape.67), calls=%async_computation.1 | async-start | bytes 786432 | tf_op jit(solution)/shard_map/all_to_all | solution.py:217
  159.5 24.9 %all-to-all-done.1 = bf16[32,48,128]{2,1,0:T(8,128)(2,1)S(1)} async-done(((bf16[32,48,128]{2,1,0:T(8,128)(2,1)}), bf16[32,48,128]{2,1,0:T(8,128)(2,1)S(1)}, u32[]{:S(2)}, u32[]{:S(2)}) %all-to-all-start.1) | async-done | bytes 393248 | tf_op jit(solution)/shard_map/all_to_all | solution.py:217
  184.7 1.0 convolution_convert_fusion.1
  (51 shorter events, 2.2 us)
Async XLA Ops:
  0.8 22.2 %copy-start = (bf16[2048,256]{1,0:T(8,128)(2,1)S(1)}, bf16[2048,256]{1,0:T(8,128)(2,1)}, u32[]{:S(2)}) copy-start(bf16[2048,256]{1,0:T(8,128)(2,1)} %refs_1_.1) | copy-start | bytes 3145732
  0.8 25.0 %copy-start.3 = (bf16[1024,512]{1,0:T(8,128)(2,1)S(1)}, bf16[1024,512]{1,0:T(8,128)(2,1)}, u32[]{:S(2)}) copy-start(bf16[1024,512]{1,0:T(8,128)(2,1)} %param.13) | copy-start | bytes 3145732
  4.8 45.3 %all-to-all-start = ((bf16[32,48,128]{2,1,0:T(8,128)(2,1)}), bf16[32,48,128]{2,1,0:T(8,128)(2,1)S(1)}, u32[]{:S(2)}, u32[]{:S(2)}) async-start(bf16[32,48,128]{2,1,0:T(8,128)(2,1)} %reshape.63), calls=%async_computation | async-start | bytes 786432 | tf_op jit(solution)/shard_map/all_to_all | solution.py:171
  23.0 58.2 %collective-permute-start.5 = (bf16[2048,256]{1,0:T(8,128)(2,1)S(1)}, bf16[2048,256]{1,0:T(8,128)(2,1)}, u32[]{:S(2)}, u32[]{:S(2)}) collective-permute-start(bf16[2048,256]{1,0:T(8,128)(2,1)S(1)} %copy-done), channel_id=1, source_target_pairs={{0,8},{8,0},{1,9},{9,1},{2,10},{10,2},{3,11},{11,3},{4,12},{12,4},... | collective-permute-start | bytes 3145736 | tf_op jit(solution)/shard_map/ppermute | solution.py:30
  25.9 28.7 %collective-permute-start.10 = (bf16[256,512]{1,0:T(8,128)(2,1)S(1)}, bf16[256,512]{1,0:T(8,128)(2,1)S(1)}, u32[]{:S(2)}, u32[]{:S(2)}) collective-permute-start(bf16[256,512]{1,0:T(8,128)(2,1)S(1)} %get-tuple-element.14), channel_id=1, source_target_pairs={{0,3},{1,0},{2,1},{3,2},{4,7},{5,4},{6,5},{7,6},{8,11},{9,8},{10,9... | collective-permute-start | bytes 786440 | tf_op jit(solution)/shard_map/ppermute | solution.py:26
  30.8 25.7 %collective-permute-start.11 = (bf16[256,512]{1,0:T(8,128)(2,1)S(1)}, bf16[256,512]{1,0:T(8,128)(2,1)}, u32[]{:S(2)}, u32[]{:S(2)}) collective-permute-start(bf16[256,512]{1,0:T(8,128)(2,1)S(1)} %get-tuple-element.16), channel_id=1, source_target_pairs={{0,2},{1,3},{2,0},{3,1},{4,6},{5,7},{6,4},{7,5},{8,10},{9,11},{10,... | collective-permute-start | bytes 786440 | tf_op jit(solution)/shard_map/ppermute | solution.py:26
  33.4 25.9 %collective-permute-start.12 = (bf16[256,512]{1,0:T(8,128)(2,1)S(1)}, bf16[256,512]{1,0:T(8,128)(2,1)}, u32[]{:S(2)}, u32[]{:S(2)}) collective-permute-start(bf16[256,512]{1,0:T(8,128)(2,1)S(1)} %get-tuple-element.15), channel_id=1, source_target_pairs={{0,1},{1,2},{2,3},{3,0},{4,5},{5,6},{6,7},{7,4},{8,9},{9,10},{10,1... | collective-permute-start | bytes 786440 | tf_op jit(solution)/shard_map/ppermute | solution.py:26
  51.1 12.6 %collective-permute-start = (bf16[96,2048]{1,0:T(8,128)(2,1)}, bf16[96,2048]{1,0:T(8,128)(2,1)}, u32[]{:S(2)}, u32[]{:S(2)}) collective-permute-start(bf16[96,2048]{1,0:T(8,128)(2,1)} %reshape.64), channel_id=1, source_target_pairs={{0,1},{1,2},{2,3},{3,0},{4,5},{5,6},{6,7},{7,4},{8,9},{9,10},{10,1... | collective-permute-start | bytes 1179656 | tf_op jit(solution)/shard_map/ppermute | solution.py:26
  54.6 4.7 %copy-start.4 = (bf16[256,512]{1,0:T(8,128)(2,1)}, bf16[256,512]{1,0:T(8,128)(2,1)S(1)}, u32[]{:S(2)}) copy-start(bf16[256,512]{1,0:T(8,128)(2,1)S(1)} %collective-permute-done.10) | copy-start | bytes 786436
  54.6 33.2 %collective-permute-start.4 = (bf16[2048,256]{1,0:T(8,128)(2,1)S(1)}, bf16[2048,256]{1,0:T(8,128)(2,1)}, u32[]{:S(2)}, u32[]{:S(2)}) collective-permute-start(bf16[2048,256]{1,0:T(8,128)(2,1)S(1)} %copy-done), channel_id=1, source_target_pairs={{0,4},{4,0},{1,5},{5,1},{2,6},{6,2},{3,7},{7,3},{8,12},{12,8},{9,1... | collective-permute-start | bytes 3145736 | tf_op jit(solution)/shard_map/ppermute | solution.py:30
  56.5 29.4 %collective-permute-start.8 = (bf16[2048,256]{1,0:T(8,128)(2,1)}, bf16[2048,256]{1,0:T(8,128)(2,1)}, u32[]{:S(2)}, u32[]{:S(2)}) collective-permute-start(bf16[2048,256]{1,0:T(8,128)(2,1)} %refs_5_.1), channel_id=1, source_target_pairs={{0,8},{8,0},{1,9},{9,1},{2,10},{10,2},{3,11},{11,3},{4,12},{12,4},... | collective-permute-start | bytes 3145736 | tf_op jit(solution)/shard_map/ppermute | solution.py:30
  60.5 46.1 %collective-permute-start.14 = (bf16[4,256,512]{2,1,0:T(8,128)(2,1)S(1)}, bf16[4,256,512]{2,1,0:T(8,128)(2,1)S(1)}, u32[]{:S(2)}, u32[]{:S(2)}) collective-permute-start(bf16[4,256,512]{2,1,0:T(8,128)(2,1)S(1)} %pad_maximum_fusion.refs_9_.refs_0_), channel_id=1, source_target_pairs={{0,8},{8,0},{1,9},{9,1},{2,10},{10,2},{3,11},{11,3},{4,12},{12,4},... | collective-permute-start | bytes 3145736 | tf_op jit(solution)/shard_map/ppermute | solution.py:30
  63.6 13.2 %collective-permute-start.1 = (bf16[96,2048]{1,0:T(8,128)(2,1)}, bf16[96,2048]{1,0:T(8,128)(2,1)}, u32[]{:S(2)}, u32[]{:S(2)}) collective-permute-start(bf16[96,2048]{1,0:T(8,128)(2,1)} %reshape.64), channel_id=1, source_target_pairs={{0,3},{1,0},{2,1},{3,2},{4,7},{5,4},{6,5},{7,6},{8,11},{9,8},{10,9... | collective-permute-start | bytes 1179656 | tf_op jit(solution)/shard_map/ppermute | solution.py:26
  68.1 1.0 copy-start.2
  76.8 31.8 %collective-permute-start.2 = (bf16[48,2048]{1,0:T(8,128)(2,1)S(1)}, bf16[48,2048]{1,0:T(8,128)(2,1)S(1)}, u32[]{:S(2)}, u32[]{:S(2)}) collective-permute-start(bf16[48,2048]{1,0:T(8,128)(2,1)S(1)} %slice.50), channel_id=1, source_target_pairs={{0,1},{1,2},{2,3},{3,0},{4,5},{5,6},{6,7},{7,4},{8,9},{9,10},{10,1... | collective-permute-start | bytes 589832 | tf_op jit(solution)/shard_map/ppermute | solution.py:26
  81.2 29.7 %collective-permute-start.3 = (bf16[48,2048]{1,0:T(8,128)(2,1)S(1)}, bf16[48,2048]{1,0:T(8,128)(2,1)S(1)}, u32[]{:S(2)}, u32[]{:S(2)}) collective-permute-start(bf16[48,2048]{1,0:T(8,128)(2,1)S(1)} %slice.51), channel_id=1, source_target_pairs={{0,3},{1,0},{2,1},{3,2},{4,7},{5,4},{6,5},{7,6},{8,11},{9,8},{10,9... | collective-permute-start | bytes 589832 | tf_op jit(solution)/shard_map/ppermute | solution.py:26
  85.9 28.2 %collective-permute-start.7 = (bf16[2048,256]{1,0:T(8,128)(2,1)}, bf16[2048,256]{1,0:T(8,128)(2,1)S(1)}, u32[]{:S(2)}, u32[]{:S(2)}) collective-permute-start(bf16[2048,256]{1,0:T(8,128)(2,1)} %refs_5_.1), channel_id=1, source_target_pairs={{0,4},{4,0},{1,5},{5,1},{2,6},{6,2},{3,7},{7,3},{8,12},{12,8},{9,1... | collective-permute-start | bytes 3145736 | tf_op jit(solution)/shard_map/ppermute | solution.py:30
  87.8 26.2 %collective-permute-start.13 = (bf16[4,256,512]{2,1,0:T(8,128)(2,1)S(1)}, bf16[4,256,512]{2,1,0:T(8,128)(2,1)S(1)}, u32[]{:S(2)}, u32[]{:S(2)}) collective-permute-start(bf16[4,256,512]{2,1,0:T(8,128)(2,1)S(1)} %pad_maximum_fusion.refs_9_.refs_0_), channel_id=1, source_target_pairs={{0,4},{4,0},{1,5},{5,1},{2,6},{6,2},{3,7},{7,3},{8,12},{12,8},{9,1... | collective-permute-start | bytes 3145736 | tf_op jit(solution)/shard_map/ppermute | solution.py:30
  106.6 7.4 %collective-permute-start.6 = (bf16[2048,256]{1,0:T(8,128)(2,1)}, bf16[2048,256]{1,0:T(8,128)(2,1)S(1)}, u32[]{:S(2)}, u32[]{:S(2)}) collective-permute-start(bf16[2048,256]{1,0:T(8,128)(2,1)} %collective-permute-done.5.refs_3_), channel_id=1, source_target_pairs={{0,4},{4,0},{1,5},{5,1},{2,6},{6,2},{3,7},{7,3},{8,12},{12,8},{9,1... | collective-permute-start | bytes 3145736 | tf_op jit(solution)/shard_map/ppermute | solution.py:30
  108.6 5.5 %collective-permute-start.9 = (bf16[2048,256]{1,0:T(8,128)(2,1)}, bf16[2048,256]{1,0:T(8,128)(2,1)S(1)}, u32[]{:S(2)}, u32[]{:S(2)}) collective-permute-start(bf16[2048,256]{1,0:T(8,128)(2,1)} %collective-permute-done.8.refs_7_), channel_id=1, source_target_pairs={{0,4},{4,0},{1,5},{5,1},{2,6},{6,2},{3,7},{7,3},{8,12},{12,8},{9,1... | collective-permute-start | bytes 3145736 | tf_op jit(solution)/shard_map/ppermute | solution.py:30
  111.0 4.6 %collective-permute-start.15 = (bf16[4,256,512]{2,1,0:T(8,128)(2,1)S(1)}, bf16[4,256,512]{2,1,0:T(8,128)(2,1)S(1)}, u32[]{:S(2)}, u32[]{:S(2)}) collective-permute-start(bf16[4,256,512]{2,1,0:T(8,128)(2,1)S(1)} %collective-permute-done.14.refs_11_.refs_2_), channel_id=1, source_target_pairs={{0,4},{4,0},{1,5},{5,1},{2,6},{6,2},{3,7},{7,3},{8,12},{12,8},{9,1... | collective-permute-start | bytes 3145736 | tf_op jit(solution)/shard_map/ppermute | solution.py:30
  114.0 1.5 copy-start.1
  125.8 10.1 %collective-permute-start.16 = (bf16[192,512]{1,0:T(8,128)(2,1)S(1)}, bf16[192,512]{1,0:T(8,128)(2,1)S(1)}, u32[]{:S(2)}, u32[]{:S(2)}) collective-permute-start(bf16[192,512]{1,0:T(8,128)(2,1)S(1)} %get-tuple-element.17), channel_id=1, source_target_pairs={{0,1},{1,2},{2,3},{3,0},{4,5},{5,6},{6,7},{7,4},{8,9},{9,10},{10,1... | collective-permute-start | bytes 589832 | tf_op jit(solution)/shard_map/ppermute | solution.py:26
  131.0 8.6 %collective-permute-start.18 = (bf16[192,512]{1,0:T(8,128)(2,1)S(1)}, bf16[192,512]{1,0:T(8,128)(2,1)S(1)}, u32[]{:S(2)}, u32[]{:S(2)}) collective-permute-start(bf16[192,512]{1,0:T(8,128)(2,1)S(1)} %get-tuple-element.18), channel_id=1, source_target_pairs={{0,3},{1,0},{2,1},{3,2},{4,7},{5,4},{6,5},{7,6},{8,11},{9,8},{10,9... | collective-permute-start | bytes 589832 | tf_op jit(solution)/shard_map/ppermute | solution.py:26
  136.0 13.4 %collective-permute-start.17 = (bf16[384,512]{1,0:T(8,128)(2,1)S(1)}, bf16[384,512]{1,0:T(8,128)(2,1)S(1)}, u32[]{:S(2)}, u32[]{:S(2)}) collective-permute-start(bf16[384,512]{1,0:T(8,128)(2,1)S(1)} %pad_maximum_fusion.1), channel_id=1, source_target_pairs={{0,1},{1,2},{2,3},{3,0},{4,5},{5,6},{6,7},{7,4},{8,9},{9,10},{10,1... | collective-permute-start | bytes 1179656 | tf_op jit(solution)/shard_map/ppermute | solution.py:26
  139.6 12.3 %collective-permute-start.19 = (bf16[384,512]{1,0:T(8,128)(2,1)S(1)}, bf16[384,512]{1,0:T(8,128)(2,1)S(1)}, u32[]{:S(2)}, u32[]{:S(2)}) collective-permute-start(bf16[384,512]{1,0:T(8,128)(2,1)S(1)} %pad_maximum_fusion.2), channel_id=1, source_target_pairs={{0,3},{1,0},{2,1},{3,2},{4,7},{5,4},{6,5},{7,6},{8,11},{9,8},{10,9... | collective-permute-start | bytes 1179656 | tf_op jit(solution)/shard_map/ppermute | solution.py:26
  152.4 6.6 %copy-start.5 = (f32[128,2]{0,1:T(2,128)S(1)}, f32[128,2]{0,1:T(2,128)}, u32[]{:S(2)}) copy-start(f32[128,2]{0,1:T(2,128)} %param.10) | copy-start | bytes 3076
  153.7 30.7 %all-to-all-start.1 = ((bf16[32,48,128]{2,1,0:T(8,128)(2,1)}), bf16[32,48,128]{2,1,0:T(8,128)(2,1)S(1)}, u32[]{:S(2)}, u32[]{:S(2)}) async-start(bf16[32,48,128]{2,1,0:T(8,128)(2,1)} %reshape.67), calls=%async_computation.1 | async-start | bytes 786432 | tf_op jit(solution)/shard_map/all_to_all | solution.py:217

commit v7 on v6

--- a/solution.py
+++ b/solution.py
@@ -26,6 +26,12 @@
     return lax.ppermute(block, "y", [(y, (y + by) % 4) for y in range(4)])
 
 
+def turn(block):
+    up = [(y, (y + 1) % 4) for y in range(4)]
+    down = [(4 + y, 4 + (y - 1) % 4) for y in range(4)]
+    return lax.ppermute(block, ("c", "y"), up + down)
+
+
 def swap(block, axis):
     return lax.ppermute(block, axis, SWAP)
 
@@ -42,23 +48,29 @@
     return jnp.dot(per_expert, table, precision=precision, preferred_element_type=jnp.float32)
 
 
-def expert_kernel(*refs):
-    rows_ref, gates, uppers, downs = refs[0], refs[1:5], refs[5:9], refs[9:13]
-    hidden_ref, part_ref, wide, tall, sems = refs[13:]
+def expert_kernel(at_ref, *refs):
+    blocks, gates, uppers, downs = refs[0:4], refs[4:8], refs[8:12], refs[12:16]
+    hidden_ref, part_ref, rows, wide, tall, sems, row_sems = refs[16:]
     depth = wide.shape[2]
-    copies = []
+    count = blocks[0].shape[0]
+    moves, copies = [], []
+    for i in range(4):
+        place = pl.ds(pl.multiple_of(((at_ref[0] + i) & 3) * count, 16), count)
+        moves.append(pltpu.make_async_copy(blocks[i], rows.at[place], row_sems.at[i]))
     for i in range(4):
         copies.append(pltpu.make_async_copy(gates[i], wide.at[2 * i], sems.at[3 * i]))
         copies.append(pltpu.make_async_copy(uppers[i], wide.at[2 * i + 1], sems.at[3 * i + 1]))
         copies.append(pltpu.make_async_copy(downs[i].at[2], tall.at[i], sems.at[3 * i + 2]))
-    for copy in copies:
+    for copy in moves + copies:
         copy.start()
+    for move in moves:
+        move.wait()
     total = jnp.zeros(part_ref.shape, jnp.float32)
     for i in range(4):
         copies[3 * i].wait()
-        gate_proj = dot32(rows_ref[...], wide[2 * i])
+        gate_proj = dot32(rows[...], wide[2 * i])
         copies[3 * i + 1].wait()
-        upper = dot32(rows_ref[...], wide[2 * i + 1])
+        upper = dot32(rows[...], wide[2 * i + 1])
         piece = (jax.nn.silu(gate_proj) * upper).astype(jnp.bfloat16)
         hidden_ref[:, i * depth : (i + 1) * depth] = piece
         copies[3 * i + 2].wait()
@@ -66,32 +78,34 @@
     part_ref[...] = total.astype(part_ref.dtype)
 
 
-def run_experts(rows_in, gates, uppers, downs):
-    count, width = rows_in.shape
+def run_experts(at, blocks, gates, uppers, downs):
+    count, width = 4 * blocks[0].shape[0], blocks[0].shape[1]
     depth = gates[0].shape[1]
     _, _, out_width = downs[0].shape
     return pl.pallas_call(
         expert_kernel,
-        in_specs=[pl.BlockSpec(memory_space=pltpu.VMEM)]
-        + [pl.BlockSpec(memory_space=pl.ANY)] * 12,
+        in_specs=[pl.BlockSpec(memory_space=pltpu.SMEM)]
+        + [pl.BlockSpec(memory_space=pl.ANY)] * 16,
         out_specs=[pl.BlockSpec(memory_space=pltpu.VMEM)] * 2,
         out_shape=[
             jax.ShapeDtypeStruct((count, 4 * depth), jnp.bfloat16),
             jax.ShapeDtypeStruct((count, out_width), jnp.bfloat16),
         ],
         scratch_shapes=[
+            pltpu.VMEM((count, width), jnp.bfloat16),
             pltpu.VMEM((8, width, depth), jnp.bfloat16),
             pltpu.VMEM((4, depth, out_width), jnp.bfloat16),
             pltpu.SemaphoreType.DMA((12,)),
+            pltpu.SemaphoreType.DMA((4,)),
         ],
         cost_estimate=pl.CostEstimate(
             flops=16 * count * width * depth,
             bytes_accessed=16 * width * depth,
             transcendentals=4 * count * depth,
         ),
-        compiler_params=pltpu.CompilerParams(vmem_limit_bytes=40 << 20),
+        compiler_params=pltpu.CompilerParams(vmem_limit_bytes=20 << 20),
         name="experts",
-    )(rows_in, *gates, *uppers, *downs)
+    )(at, *blocks, *gates, *uppers, *downs)
 
 
 def down_kernel(picks, hidden_ref, *refs):
@@ -129,7 +143,7 @@
             bytes_accessed=8 * len(picks) * depth * out_width,
             transcendentals=0,
         ),
-        compiler_params=pltpu.CompilerParams(vmem_limit_bytes=40 << 20),
+        compiler_params=pltpu.CompilerParams(vmem_limit_bytes=12 << 20),
         name="down",
     )(hidden, *downs)
 
@@ -186,27 +200,18 @@
     up_d = swap(up_x, "c")
     down_d = swap(down_x, "c")
 
-    half = block_rows // 2
+    lower_core = lax.axis_index("c") == 0
     below = shift(near, 1)
     above = shift(near, -1)
-    gathered = jnp.zeros((4, block_rows, width), jnp.bfloat16)
-    for block, ahead in ((near, 0), (below, 3), (above, 1)):
-        gathered = lax.dynamic_update_slice(gathered, block[None], ((y + ahead) & 3, 0, 0))
-    for block, low in ((shift(below[:half], 1), 0), (shift(above[half:], -1), half)):
-        gathered = lax.dynamic_update_slice(gathered, block[None], ((y + 2) & 3, low, 0))
-    gathered = gathered.reshape(4 * block_rows, width)
-
+    across = turn(jnp.where(lower_core, below, above))
+    blocks = (near, above, across, below)
     gates, uppers = (w_gate, gate_c, gate_x, gate_d), (w_up, up_c, up_x, up_d)
     downs = (down_o, down_c, down_x, down_d)
-    hidden, away = run_experts(gathered, gates, uppers, downs)
-    middle = 2 * block_rows
-    first = shift(away[:middle], 1)
-    second = shift(away[middle:], -1)
+    hidden, away = run_experts(y[None].astype(jnp.int32), blocks, gates, uppers, downs)
+    middle = turn(away).astype(jnp.float32)
     upward, downward = run_down(hidden, downs, (1, 3))
-    upward = jnp.concatenate([upward[:middle] + first.astype(jnp.float32), upward[middle:]], 0)
-    downward = jnp.concatenate(
-        [downward[:middle], downward[middle:] + second.astype(jnp.float32)], 0
-    )
+    upward += jnp.where(lower_core, middle, 0.0)
+    downward += jnp.where(lower_core, 0.0, middle)
     first = shift(upward.astype(jnp.bfloat16), 1)
     second = shift(downward.astype(jnp.bfloat16), -1)
     (total,) = run_down(hidden, downs, (0,))

time: 188 us -> 204 us (1.085)
  waiting for transfers between devices: 72.8 us -> 88.9 us
  local copies, waits for them, and re-layouts: 10.5 us -> 7.98 us
    ppermute x9, waiting for transfers between devices: 17.9 us -> 44 us  [swap(): return lax.ppermute(block, axis, SWAP)]
    ppermute x0 -> x2, waiting for transfers between devices: none -> 13.4 us  [turn(): return lax.ppermute(block, ('c', 'y'), up + down)]
    ppermute x11 -> x7, starting transfers between devices: 38.5 us -> 25.6 us  [shift(): return lax.ppermute(block, 'y', [(y, (y + by) % 4) for y in range(4)])]
    all_to_all x1, waiting for transfers between devices: 13.9 us -> 0.97 us  [layer(): arrived = lax.all_to_all(mine, ('z', 'xh'), 0, 0, tiled=True)]
    all_to_all x1, starting transfers between devices: 5.19 us -> 13.9 us  [layer(): returned = lax.all_to_all(home, ('z', 'xh'), 0, 0, tiled=True)]
    ppermute x11 -> x7, waiting for transfers between devices: 16 us -> 7.77 us  [shift(): return lax.ppermute(block, 'y', [(y, (y + by) % 4) for y in range(4)])]
    ppermute x0 -> x2, starting transfers between devices: none -> 6.31 us  [turn(): return lax.ppermute(block, ('c', 'y'), up + down)]
    unnamed x12 -> x20, local copies, waits for them, and re-layouts: 0.83 us -> 3.24 us
  transfers between devices with their start and end apart: 22 -> 20, of which waited for: 9 -> 10; matrix products, arithmetic and copies ran while one was open for 4% -> 2% of each run, Pallas kernels for 1% -> 2%
where the time goes in v7:
time: 204 us; the launch traced here: 200 us
  waiting for transfers between devices  88.9 us (44%)
  starting transfers between devices  84.6 us (41%)
  Pallas kernels  13 us (6%)
  local copies, waits for them, and re-layouts  7.98 us (4%)
  other arithmetic  2.93 us (1%)
  matrix products  2.17 us (1%)
    ppermute x9, waiting for transfers between devices, swap(): return lax.ppermute(block, axis, SWAP)  44 us
    ppermute x7, starting transfers between devices, shift(): return lax.ppermute(block, 'y', [(y, (y + by) % 4) for y in range(4)])  25.6 us
    all_to_all x1, waiting for transfers between devices, layer(): returned = lax.all_to_all(home, ('z', 'xh'), 0, 0, tiled=True)  22.8 us
    ppermute x9, starting transfers between devices, swap(): return lax.ppermute(block, axis, SWAP)  20.6 us
    all_to_all x1, starting transfers between devices, layer(): arrived = lax.all_to_all(mine, ('z', 'xh'), 0, 0, tiled=True)  18.3 us
    all_to_all x1, starting transfers between devices, layer(): returned = lax.all_to_all(home, ('z', 'xh'), 0, 0, tiled=True)  13.9 us
    ppermute x2, waiting for transfers between devices, turn(): return lax.ppermute(block, ('c', 'y'), up + down)  13.4 us
    pallas_call x1, Pallas kernels, run_experts(): pl.pallas_call(expert_kernel, in_specs=[pl.BlockSpec(memory_space=pltpu.S...  9.65 us
  transfers between devices with their start and end apart: 20, of which 10 were waited for; matrix products, arithmetic and copies ran while one was open for 2% of the time, Pallas kernels for 2%

profile of v7, /device:TPU:6, one launch (start us, length us, event | category | flops | bytes accessed | tf_op | source)
XLA Modules:
  0.0 200.1 jit_solution(15045828331845186521)
XLA Ops:
  0.0 0.8 slice_bitcast_fusion.3
  0.8 1.2 fusion.1
  2.2 0.6 copy-done.9
  2.7 0.5 convolution_convert_fusion
  3.2 0.9 reshape.60
  4.2 18.3 %all-to-all-start = ((bf16[32,48,128]{2,1,0:T(8,128)(2,1)}), bf16[32,48,128]{2,1,0:T(8,128)(2,1)}, u32[]{:S(2)}, u32[]{:S(2)}) async-start(bf16[32,48,128]{2,1,0:T(8,128)(2,1)} %reshape.60), calls=%async_computation | async-start | bytes 786432 | tf_op jit(solution)/shard_map/all_to_all | solution.py:185
  22.6 5.1 %collective-permute-start.9 = (bf16[256,512]{1,0:T(8,128)(2,1)S(1)}, bf16[256,512]{1,0:T(8,128)(2,1)S(1)}, u32[]{:S(2)}, u32[]{:S(2)}) collective-permute-start(bf16[256,512]{1,0:T(8,128)(2,1)S(1)} %get-tuple-element.14), channel_id=1, source_target_pairs={{0,3},{1,0},{2,1},{3,2},{4,7},{5,4},{6,5},{7,6},{8,11},{9,8},{10,9... | collective-permute-start | bytes 786440 | tf_op jit(solution)/shard_map/ppermute | solution.py:26
  27.6 2.5 %collective-permute-start.10 = (bf16[256,512]{1,0:T(8,128)(2,1)S(1)}, bf16[256,512]{1,0:T(8,128)(2,1)S(1)}, u32[]{:S(2)}, u32[]{:S(2)}) collective-permute-start(bf16[256,512]{1,0:T(8,128)(2,1)S(1)} %get-tuple-element.16), channel_id=1, source_target_pairs={{0,2},{1,3},{2,0},{3,1},{4,6},{5,7},{6,4},{7,5},{8,10},{9,11},{10,... | collective-permute-start | bytes 786440 | tf_op jit(solution)/shard_map/ppermute | solution.py:26
  30.2 2.9 %collective-permute-start.11 = (bf16[256,512]{1,0:T(8,128)(2,1)S(1)}, bf16[256,512]{1,0:T(8,128)(2,1)S(1)}, u32[]{:S(2)}, u32[]{:S(2)}) collective-permute-start(bf16[256,512]{1,0:T(8,128)(2,1)S(1)} %get-tuple-element.15), channel_id=1, source_target_pairs={{0,1},{1,2},{2,3},{3,0},{4,5},{5,6},{6,7},{7,4},{8,9},{9,10},{10,1... | collective-permute-start | bytes 786440 | tf_op jit(solution)/shard_map/ppermute | solution.py:26
  33.1 2.7 %collective-permute-start.4 = (bf16[2048,256]{1,0:T(8,128)(2,1)S(1)}, bf16[2048,256]{1,0:T(8,128)(2,1)}, u32[]{:S(2)}, u32[]{:S(2)}) collective-permute-start(bf16[2048,256]{1,0:T(8,128)(2,1)S(1)} %copy-done.4), channel_id=1, source_target_pairs={{0,8},{8,0},{1,9},{9,1},{2,10},{10,2},{3,11},{11,3},{4,12},{12,4},... | collective-permute-start | bytes 3145736 | tf_op jit(solution)/shard_map/ppermute | solution.py:36
  35.8 3.1 %collective-permute-start.7 = (bf16[2048,256]{1,0:T(8,128)(2,1)}, bf16[2048,256]{1,0:T(8,128)(2,1)}, u32[]{:S(2)}, u32[]{:S(2)}) collective-permute-start(bf16[2048,256]{1,0:T(8,128)(2,1)} %refs_8_.1), channel_id=1, source_target_pairs={{0,8},{8,0},{1,9},{9,1},{2,10},{10,2},{3,11},{11,3},{4,12},{12,4},... | collective-permute-start | bytes 3145736 | tf_op jit(solution)/shard_map/ppermute | solution.py:36
  38.9 1.9 collective-permute-start.3
  40.9 3.0 %collective-permute-done.11 = bf16[256,512]{1,0:T(8,128)(2,1)S(1)} collective-permute-done((bf16[256,512]{1,0:T(8,128)(2,1)S(1)}, bf16[256,512]{1,0:T(8,128)(2,1)S(1)}, u32[]{:S(2)}, u32[]{:S(2)}) %collective-permute-start.11) | collective-permute-done | bytes 262176 | tf_op jit(solution)/shard_map/ppermute | solution.py:26
  44.0 2.7 %collective-permute-start.13 = (bf16[4,256,512]{2,1,0:T(8,128)(2,1)S(1)}, bf16[4,256,512]{2,1,0:T(8,128)(2,1)S(1)}, u32[]{:S(2)}, u32[]{:S(2)}) collective-permute-start(bf16[4,256,512]{2,1,0:T(8,128)(2,1)S(1)} %pad_maximum_fusion.refs_12_.refs_0_), channel_id=1, source_target_pairs={{0,8},{8,0},{1,9},{9,1},{2,10},{10,2},{3,11},{11,3},{4,12},{12,4},... | collective-permute-start | bytes 3145736 | tf_op jit(solution)/shard_map/ppermute | solution.py:36
  46.7 1.9 collective-permute-start.6
  48.7 1.0 all-to-all-done
  49.6 1.2 reshape.61.refs_0_
  50.8 11.3 %collective-permute-done.4.refs_6_ = bf16[2048,256]{1,0:T(8,128)(2,1)} collective-permute-done((bf16[2048,256]{1,0:T(8,128)(2,1)S(1)}, bf16[2048,256]{1,0:T(8,128)(2,1)}, u32[]{:S(2)}, u32[]{:S(2)}) %collective-permute-start.4) | collective-permute-done | bytes 1048608 | tf_op jit(solution)/shard_map/ppermute | solution.py:36
  62.1 4.3 %collective-permute-start = (bf16[96,2048]{1,0:T(8,128)(2,1)S(1)}, bf16[96,2048]{1,0:T(8,128)(2,1)S(1)}, u32[]{:S(2)}, u32[]{:S(2)}) collective-permute-start(bf16[96,2048]{1,0:T(8,128)(2,1)S(1)} %reshape.61.refs_0_), channel_id=1, source_target_pairs={{0,3},{1,0},{2,1},{3,2},{4,7},{5,4},{6,5},{7,6},{8,11},{9,8},{10,9... | collective-permute-start | bytes 1179656 | tf_op jit(solution)/shard_map/ppermute | solution.py:26
  66.5 18.1 %collective-permute-done.7.refs_10_ = bf16[2048,256]{1,0:T(8,128)(2,1)} collective-permute-done((bf16[2048,256]{1,0:T(8,128)(2,1)}, bf16[2048,256]{1,0:T(8,128)(2,1)}, u32[]{:S(2)}, u32[]{:S(2)}) %collective-permute-start.7) | collective-permute-done | bytes 1048608 | tf_op jit(solution)/shard_map/ppermute | solution.py:36
  84.6 3.7 %collective-permute-start.1 = (bf16[96,2048]{1,0:T(8,128)(2,1)S(1)}, bf16[96,2048]{1,0:T(8,128)(2,1)S(1)}, u32[]{:S(2)}, u32[]{:S(2)}) collective-permute-start(bf16[96,2048]{1,0:T(8,128)(2,1)S(1)} %reshape.61.refs_0_), channel_id=1, source_target_pairs={{0,1},{1,2},{2,3},{3,0},{4,5},{5,6},{6,7},{7,4},{8,9},{9,10},{10,1... | collective-permute-start | bytes 1179656 | tf_op jit(solution)/shard_map/ppermute | solution.py:26
  88.3 1.9 collective-permute-start.12
  90.3 14.5 %collective-permute-done.13.refs_14_.refs_2_ = bf16[4,256,512]{2,1,0:T(8,128)(2,1)S(1)} collective-permute-done((bf16[4,256,512]{2,1,0:T(8,128)(2,1)S(1)}, bf16[4,256,512]{2,1,0:T(8,128)(2,1)S(1)}, u32[]{:S(2)}, u32[]{:S(2)}) %collective-permute-start.13) | collective-permute-done | bytes 1048608 | tf_op jit(solution)/shard_map/ppermute | solution.py:36
  104.8 1.9 collective-permute-start.5
  106.7 2.4 %collective-permute-start.8 = (bf16[2048,256]{1,0:T(8,128)(2,1)}, bf16[2048,256]{1,0:T(8,128)(2,1)}, u32[]{:S(2)}, u32[]{:S(2)}) collective-permute-start(bf16[2048,256]{1,0:T(8,128)(2,1)} %collective-permute-done.7.refs_10_), channel_id=1, source_target_pairs={{0,4},{4,0},{1,5},{5,1},{2,6},{6,2},{3,7},{7,3},{8,12},{12,8},{9,1... | collective-permute-start | bytes 3145736 | tf_op jit(solution)/shard_map/ppermute | solution.py:36
  109.2 0.8 copy-done.2
  110.0 1.9 collective-permute-start.14
  111.9 1.1 broadcast_select_fusion
  113.0 3.8 %collective-permute-start.2 = (bf16[96,2048]{1,0:T(8,128)(2,1)S(1)}, bf16[96,2048]{1,0:T(8,128)(2,1)S(1)}, u32[]{:S(2)}, u32[]{:S(2)}) collective-permute-start(bf16[96,2048]{1,0:T(8,128)(2,1)S(1)} %broadcast_select_fusion), channel_id=1, source_target_pairs={{0,1},{1,2},{2,3},{3,0},{4,7},{5,4},{6,5},{7,6},{8,9},{9,10},{10,1... | collective-permute-start | bytes 1179656 | tf_op jit(solution)/shard_map/ppermute | solution.py:32
  116.8 7.1 %collective-permute-done.2.refs_2_ = bf16[96,2048]{1,0:T(8,128)(2,1)S(1)} collective-permute-done((bf16[96,2048]{1,0:T(8,128)(2,1)S(1)}, bf16[96,2048]{1,0:T(8,128)(2,1)S(1)}, u32[]{:S(2)}, u32[]{:S(2)}) %collective-permute-start.2) | collective-permute-done | bytes 393248 | tf_op jit(solution)/shard_map/ppermute | solution.py:32
  123.9 1.2 copy-done.5
  125.2 9.6 %experts.1 = (bf16[384,1024]{1,0:T(8,128)(2,1)S(1)}, bf16[384,512]{1,0:T(8,128)(2,1)S(1)}) custom-call(s32[1]{0:T(128)} %bitcast.4.at_ref, bf16[96,2048]{1,0:T(8,128)(2,1)S(1)} %reshape.61.refs_0_, bf16[96,2048]{1,0:T(8,128)(2,1)S(1)} %copy-done.1, bf16[96,2048]{1,0:T(8,128)(2,1)S(1)} %collective-permute-done.2.refs_2_, bf16[96,2048]{1,0:T(8,128)(2,1)S(1)} %copy-done.3, ...), custom_call_target="tpu_custom_call" | custom-call | flops 3221225472 | bytes 8388608 | tf_op jit(solution)/shard_map/experts/pallas_call | solution.py:85
  134.8 2.5 %collective-permute-start.15 = (bf16[384,512]{1,0:T(8,128)(2,1)S(1)}, bf16[384,512]{1,0:T(8,128)(2,1)S(1)}, u32[]{:S(2)}, u32[]{:S(2)}) collective-permute-start(bf16[384,512]{1,0:T(8,128)(2,1)S(1)} %get-tuple-element.11), channel_id=1, source_target_pairs={{0,1},{1,2},{2,3},{3,0},{4,7},{5,4},{6,5},{7,6},{8,9},{9,10},{10,1... | collective-permute-start | bytes 1179656 | tf_op jit(solution)/shard_map/ppermute | solution.py:32
  137.4 2.0 %down.3 = (f32[384,512]{1,0:T(8,128)S(1)}, f32[384,512]{1,0:T(8,128)S(1)}) custom-call(bf16[384,1024]{1,0:T(8,128)(2,1)S(1)} %get-tuple-element.9.hidden_ref, bf16[4,256,512]{2,1,0:T(8,128)(2,1)S(1)} %pad_maximum_fusion.refs_12_.refs_0_, bf16[4,256,512]{2,1,0:T(8,128)(2,1)S(1)} %collective-permute-done.12.refs_13_.refs_1_, ...), custom_call_target="tpu_custom_call" | custom-call | flops 805306368 | bytes 2097152 | tf_op jit(solution)/shard_map/down/pallas_call | solution.py:132
  139.4 6.3 %collective-permute-done.15 = bf16[384,512]{1,0:T(8,128)(2,1)S(1)} collective-permute-done((bf16[384,512]{1,0:T(8,128)(2,1)S(1)}, bf16[384,512]{1,0:T(8,128)(2,1)S(1)}, u32[]{:S(2)}, u32[]{:S(2)}) %collective-permute-start.15) | collective-permute-done | bytes 393248 | tf_op jit(solution)/shard_map/ppermute | solution.py:32
  145.9 1.9 collective-permute-start.16
  147.9 5.1 %collective-permute-start.17 = (bf16[384,512]{1,0:T(8,128)(2,1)S(1)}, bf16[384,512]{1,0:T(8,128)(2,1)S(1)}, u32[]{:S(2)}, u32[]{:S(2)}) collective-permute-start(bf16[384,512]{1,0:T(8,128)(2,1)S(1)} %get-tuple-element.18), channel_id=1, source_target_pairs={{0,3},{1,0},{2,1},{3,2},{4,7},{5,4},{6,5},{7,6},{8,11},{9,8},{10,9... | collective-permute-start | bytes 1179656 | tf_op jit(solution)/shard_map/ppermute | solution.py:26
  153.0 1.3 down.2
  154.3 3.6 %collective-permute-done.16 = bf16[384,512]{1,0:T(8,128)(2,1)S(1)} collective-permute-done((bf16[384,512]{1,0:T(8,128)(2,1)S(1)}, bf16[384,512]{1,0:T(8,128)(2,1)S(1)}, u32[]{:S(2)}, u32[]{:S(2)}) %collective-permute-start.16) | collective-permute-done | bytes 393248 | tf_op jit(solution)/shard_map/ppermute | solution.py:26
  157.9 1.2 collective-permute-done.17
  159.5 0.3 copy.8
  159.8 1.1 reshape.63
  160.9 13.9 %all-to-all-start.1 = ((bf16[32,48,128]{2,1,0:T(8,128)(2,1)}), bf16[32,48,128]{2,1,0:T(8,128)(2,1)S(1)}, u32[]{:S(2)}, u32[]{:S(2)}) async-start(bf16[32,48,128]{2,1,0:T(8,128)(2,1)} %reshape.63), calls=%async_computation.1 | async-start | bytes 786432 | tf_op jit(solution)/shard_map/all_to_all | solution.py:222
  174.8 0.7 copy-done.8
  175.7 0.3 convolution_select_fusion
  176.0 22.8 %all-to-all-done.1 = bf16[32,48,128]{2,1,0:T(8,128)(2,1)S(1)} async-done(((bf16[32,48,128]{2,1,0:T(8,128)(2,1)}), bf16[32,48,128]{2,1,0:T(8,128)(2,1)S(1)}, u32[]{:S(2)}, u32[]{:S(2)}) %all-to-all-start.1) | async-done | bytes 393248 | tf_op jit(solution)/shard_map/all_to_all | solution.py:222
  198.8 0.2 reshape.64
  199.1 1.0 convolution_convert_fusion.1
  (41 shorter events, 1.3 us)
Async XLA Ops:
  0.0 2.2 %copy-start.7 = (bf16[128,2048]{1,0:T(8,128)(2,1)S(1)}, bf16[128,2048]{1,0:T(8,128)(2,1)}, u32[]{:S(2)}) copy-start(bf16[128,2048]{1,0:T(8,128)(2,1)} %param.7) | copy-start | bytes 1572868
  2.0 0.7 copy-start.9
  3.2 19.2 %copy-start.6 = (bf16[1024,512]{1,0:T(8,128)(2,1)S(1)}, bf16[1024,512]{1,0:T(8,128)(2,1)}, u32[]{:S(2)}) copy-start(bf16[1024,512]{1,0:T(8,128)(2,1)} %param.13) | copy-start | bytes 3145732
  4.2 45.4 %all-to-all-start = ((bf16[32,48,128]{2,1,0:T(8,128)(2,1)}), bf16[32,48,128]{2,1,0:T(8,128)(2,1)}, u32[]{:S(2)}, u32[]{:S(2)}) async-start(bf16[32,48,128]{2,1,0:T(8,128)(2,1)} %reshape.60), calls=%async_computation | async-start | bytes 786432 | tf_op jit(solution)/shard_map/all_to_all | solution.py:185
  22.5 10.6 %copy-start.4 = (bf16[2048,256]{1,0:T(8,128)(2,1)S(1)}, bf16[2048,256]{1,0:T(8,128)(2,1)}, u32[]{:S(2)}) copy-start(bf16[2048,256]{1,0:T(8,128)(2,1)} %refs_4_.1) | copy-start | bytes 3145732
  22.6 16.4 %collective-permute-start.9 = (bf16[256,512]{1,0:T(8,128)(2,1)S(1)}, bf16[256,512]{1,0:T(8,128)(2,1)S(1)}, u32[]{:S(2)}, u32[]{:S(2)}) collective-permute-start(bf16[256,512]{1,0:T(8,128)(2,1)S(1)} %get-tuple-element.14), channel_id=1, source_target_pairs={{0,3},{1,0},{2,1},{3,2},{4,7},{5,4},{6,5},{7,6},{8,11},{9,8},{10,9... | collective-permute-start | bytes 786440 | tf_op jit(solution)/shard_map/ppermute | solution.py:26
  27.6 13.2 %collective-permute-start.10 = (bf16[256,512]{1,0:T(8,128)(2,1)S(1)}, bf16[256,512]{1,0:T(8,128)(2,1)S(1)}, u32[]{:S(2)}, u32[]{:S(2)}) collective-permute-start(bf16[256,512]{1,0:T(8,128)(2,1)S(1)} %get-tuple-element.16), channel_id=1, source_target_pairs={{0,2},{1,3},{2,0},{3,1},{4,6},{5,7},{6,4},{7,5},{8,10},{9,11},{10,... | collective-permute-start | bytes 786440 | tf_op jit(solution)/shard_map/ppermute | solution.py:26
  30.2 13.7 %collective-permute-start.11 = (bf16[256,512]{1,0:T(8,128)(2,1)S(1)}, bf16[256,512]{1,0:T(8,128)(2,1)S(1)}, u32[]{:S(2)}, u32[]{:S(2)}) collective-permute-start(bf16[256,512]{1,0:T(8,128)(2,1)S(1)} %get-tuple-element.15), channel_id=1, source_target_pairs={{0,1},{1,2},{2,3},{3,0},{4,5},{5,6},{6,7},{7,4},{8,9},{9,10},{10,1... | collective-permute-start | bytes 786440 | tf_op jit(solution)/shard_map/ppermute | solution.py:26
  33.1 29.1 %collective-permute-start.4 = (bf16[2048,256]{1,0:T(8,128)(2,1)S(1)}, bf16[2048,256]{1,0:T(8,128)(2,1)}, u32[]{:S(2)}, u32[]{:S(2)}) collective-permute-start(bf16[2048,256]{1,0:T(8,128)(2,1)S(1)} %copy-done.4), channel_id=1, source_target_pairs={{0,8},{8,0},{1,9},{9,1},{2,10},{10,2},{3,11},{11,3},{4,12},{12,4},... | collective-permute-start | bytes 3145736 | tf_op jit(solution)/shard_map/ppermute | solution.py:36
  35.8 48.8 %collective-permute-start.7 = (bf16[2048,256]{1,0:T(8,128)(2,1)}, bf16[2048,256]{1,0:T(8,128)(2,1)}, u32[]{:S(2)}, u32[]{:S(2)}) collective-permute-start(bf16[2048,256]{1,0:T(8,128)(2,1)} %refs_8_.1), channel_id=1, source_target_pairs={{0,8},{8,0},{1,9},{9,1},{2,10},{10,2},{3,11},{11,3},{4,12},{12,4},... | collective-permute-start | bytes 3145736 | tf_op jit(solution)/shard_map/ppermute | solution.py:36
  38.9 49.4 %collective-permute-start.3 = (bf16[2048,256]{1,0:T(8,128)(2,1)S(1)}, bf16[2048,256]{1,0:T(8,128)(2,1)}, u32[]{:S(2)}, u32[]{:S(2)}) collective-permute-start(bf16[2048,256]{1,0:T(8,128)(2,1)S(1)} %copy-done.4), channel_id=1, source_target_pairs={{0,4},{4,0},{1,5},{5,1},{2,6},{6,2},{3,7},{7,3},{8,12},{12,8},{9,1... | collective-permute-start | bytes 3145736 | tf_op jit(solution)/shard_map/ppermute | solution.py:36
  44.0 60.8 %collective-permute-start.13 = (bf16[4,256,512]{2,1,0:T(8,128)(2,1)S(1)}, bf16[4,256,512]{2,1,0:T(8,128)(2,1)S(1)}, u32[]{:S(2)}, u32[]{:S(2)}) collective-permute-start(bf16[4,256,512]{2,1,0:T(8,128)(2,1)S(1)} %pad_maximum_fusion.refs_12_.refs_0_), channel_id=1, source_target_pairs={{0,8},{8,0},{1,9},{9,1},{2,10},{10,2},{3,11},{11,3},{4,12},{12,4},... | collective-permute-start | bytes 3145736 | tf_op jit(solution)/shard_map/ppermute | solution.py:36
  46.7 66.3 %collective-permute-start.6 = (bf16[2048,256]{1,0:T(8,128)(2,1)}, bf16[2048,256]{1,0:T(8,128)(2,1)}, u32[]{:S(2)}, u32[]{:S(2)}) collective-permute-start(bf16[2048,256]{1,0:T(8,128)(2,1)} %refs_8_.1), channel_id=1, source_target_pairs={{0,4},{4,0},{1,5},{5,1},{2,6},{6,2},{3,7},{7,3},{8,12},{12,8},{9,1... | collective-permute-start | bytes 3145736 | tf_op jit(solution)/shard_map/ppermute | solution.py:36
  62.1 44.6 %collective-permute-start = (bf16[96,2048]{1,0:T(8,128)(2,1)S(1)}, bf16[96,2048]{1,0:T(8,128)(2,1)S(1)}, u32[]{:S(2)}, u32[]{:S(2)}) collective-permute-start(bf16[96,2048]{1,0:T(8,128)(2,1)S(1)} %reshape.61.refs_0_), channel_id=1, source_target_pairs={{0,3},{1,0},{2,1},{3,2},{4,7},{5,4},{6,5},{7,6},{8,11},{9,8},{10,9... | collective-permute-start | bytes 1179656 | tf_op jit(solution)/shard_map/ppermute | solution.py:26
  84.6 24.6 %collective-permute-start.1 = (bf16[96,2048]{1,0:T(8,128)(2,1)S(1)}, bf16[96,2048]{1,0:T(8,128)(2,1)S(1)}, u32[]{:S(2)}, u32[]{:S(2)}) collective-permute-start(bf16[96,2048]{1,0:T(8,128)(2,1)S(1)} %reshape.61.refs_0_), channel_id=1, source_target_pairs={{0,1},{1,2},{2,3},{3,0},{4,5},{5,6},{6,7},{7,4},{8,9},{9,10},{10,1... | collective-permute-start | bytes 1179656 | tf_op jit(solution)/shard_map/ppermute | solution.py:26
  88.3 28.5 %collective-permute-start.12 = (bf16[4,256,512]{2,1,0:T(8,128)(2,1)S(1)}, bf16[4,256,512]{2,1,0:T(8,128)(2,1)S(1)}, u32[]{:S(2)}, u32[]{:S(2)}) collective-permute-start(bf16[4,256,512]{2,1,0:T(8,128)(2,1)S(1)} %pad_maximum_fusion.refs_12_.refs_0_), channel_id=1, source_target_pairs={{0,4},{4,0},{1,5},{5,1},{2,6},{6,2},{3,7},{7,3},{8,12},{12,8},{9,1... | collective-permute-start | bytes 3145736 | tf_op jit(solution)/shard_map/ppermute | solution.py:36
  104.8 12.0 %collective-permute-start.5 = (bf16[2048,256]{1,0:T(8,128)(2,1)}, bf16[2048,256]{1,0:T(8,128)(2,1)}, u32[]{:S(2)}, u32[]{:S(2)}) collective-permute-start(bf16[2048,256]{1,0:T(8,128)(2,1)} %collective-permute-done.4.refs_6_), channel_id=1, source_target_pairs={{0,4},{4,0},{1,5},{5,1},{2,6},{6,2},{3,7},{7,3},{8,12},{12,8},{9,1... | collective-permute-start | bytes 3145736 | tf_op jit(solution)/shard_map/ppermute | solution.py:36
  106.7 2.4 %copy-start = (bf16[96,2048]{1,0:T(8,128)(2,1)}, bf16[96,2048]{1,0:T(8,128)(2,1)S(1)}, u32[]{:S(2)}) copy-start(bf16[96,2048]{1,0:T(8,128)(2,1)S(1)} %collective-permute-done.refs_1_) | copy-start | bytes 1179652
  106.7 10.1 %collective-permute-start.8 = (bf16[2048,256]{1,0:T(8,128)(2,1)}, bf16[2048,256]{1,0:T(8,128)(2,1)}, u32[]{:S(2)}, u32[]{:S(2)}) collective-permute-start(bf16[2048,256]{1,0:T(8,128)(2,1)} %collective-permute-done.7.refs_10_), channel_id=1, source_target_pairs={{0,4},{4,0},{1,5},{5,1},{2,6},{6,2},{3,7},{7,3},{8,12},{12,8},{9,1... | collective-permute-start | bytes 3145736 | tf_op jit(solution)/shard_map/ppermute | solution.py:36
  109.2 0.8 copy-start.2
  110.0 14.0 %collective-permute-start.14 = (bf16[4,256,512]{2,1,0:T(8,128)(2,1)S(1)}, bf16[4,256,512]{2,1,0:T(8,128)(2,1)}, u32[]{:S(2)}, u32[]{:S(2)}) collective-permute-start(bf16[4,256,512]{2,1,0:T(8,128)(2,1)S(1)} %collective-permute-done.13.refs_14_.refs_2_), channel_id=1, source_target_pairs={{0,4},{4,0},{1,5},{5,1},{2,6},{6,2},{3,7},{7,3},{8,12},{12,8},{9,1... | collective-permute-start | bytes 3145736 | tf_op jit(solution)/shard_map/ppermute | solution.py:36
  111.9 12.0 %copy-start.1 = (bf16[96,2048]{1,0:T(8,128)(2,1)S(1)}, bf16[96,2048]{1,0:T(8,128)(2,1)}, u32[]{:S(2)}) copy-start(bf16[96,2048]{1,0:T(8,128)(2,1)} %copy-done) | copy-start | bytes 1179652
  111.9 12.0 %copy-start.3 = (bf16[96,2048]{1,0:T(8,128)(2,1)S(1)}, bf16[96,2048]{1,0:T(8,128)(2,1)}, u32[]{:S(2)}) copy-start(bf16[96,2048]{1,0:T(8,128)(2,1)} %copy-done.2) | copy-start | bytes 1179652
  113.0 10.9 %collective-permute-start.2 = (bf16[96,2048]{1,0:T(8,128)(2,1)S(1)}, bf16[96,2048]{1,0:T(8,128)(2,1)S(1)}, u32[]{:S(2)}, u32[]{:S(2)}) collective-permute-start(bf16[96,2048]{1,0:T(8,128)(2,1)S(1)} %broadcast_select_fusion), channel_id=1, source_target_pairs={{0,1},{1,2},{2,3},{3,0},{4,7},{5,4},{6,5},{7,6},{8,9},{9,10},{10,1... | collective-permute-start | bytes 1179656 | tf_op jit(solution)/shard_map/ppermute | solution.py:32
  123.9 1.2 copy-start.5
  134.8 10.9 %collective-permute-start.15 = (bf16[384,512]{1,0:T(8,128)(2,1)S(1)}, bf16[384,512]{1,0:T(8,128)(2,1)S(1)}, u32[]{:S(2)}, u32[]{:S(2)}) collective-permute-start(bf16[384,512]{1,0:T(8,128)(2,1)S(1)} %get-tuple-element.11), channel_id=1, source_target_pairs={{0,1},{1,2},{2,3},{3,0},{4,7},{5,4},{6,5},{7,6},{8,9},{9,10},{10,1... | collective-permute-start | bytes 1179656 | tf_op jit(solution)/shard_map/ppermute | solution.py:32
  145.9 12.0 %collective-permute-start.16 = (bf16[384,512]{1,0:T(8,128)(2,1)S(1)}, bf16[384,512]{1,0:T(8,128)(2,1)S(1)}, u32[]{:S(2)}, u32[]{:S(2)}) collective-permute-start(bf16[384,512]{1,0:T(8,128)(2,1)S(1)} %get-tuple-element.17), channel_id=1, source_target_pairs={{0,1},{1,2},{2,3},{3,0},{4,5},{5,6},{6,7},{7,4},{8,9},{9,10},{10,1... | collective-permute-start | bytes 1179656 | tf_op jit(solution)/shard_map/ppermute | solution.py:26
  147.9 11.3 %collective-permute-start.17 = (bf16[384,512]{1,0:T(8,128)(2,1)S(1)}, bf16[384,512]{1,0:T(8,128)(2,1)S(1)}, u32[]{:S(2)}, u32[]{:S(2)}) collective-permute-start(bf16[384,512]{1,0:T(8,128)(2,1)S(1)} %get-tuple-element.18), channel_id=1, source_target_pairs={{0,3},{1,0},{2,1},{3,2},{4,7},{5,4},{6,5},{7,6},{8,11},{9,8},{10,9... | collective-permute-start | bytes 1179656 | tf_op jit(solution)/shard_map/ppermute | solution.py:26
  160.9 38.0 %all-to-all-start.1 = ((bf16[32,48,128]{2,1,0:T(8,128)(2,1)}), bf16[32,48,128]{2,1,0:T(8,128)(2,1)S(1)}, u32[]{:S(2)}, u32[]{:S(2)}) async-start(bf16[32,48,128]{2,1,0:T(8,128)(2,1)} %reshape.63), calls=%async_computation.1 | async-start | bytes 786432 | tf_op jit(solution)/shard_map/all_to_all | solution.py:222
  174.8 0.7 copy-start.8

commit v8 on v7

--- a/solution.py
+++ b/solution.py
@@ -60,7 +60,7 @@
     for i in range(4):
         copies.append(pltpu.make_async_copy(gates[i], wide.at[2 * i], sems.at[3 * i]))
         copies.append(pltpu.make_async_copy(uppers[i], wide.at[2 * i + 1], sems.at[3 * i + 1]))
-        copies.append(pltpu.make_async_copy(downs[i].at[2], tall.at[i], sems.at[3 * i + 2]))
+        copies.append(pltpu.make_async_copy(downs[i], tall.at[i], sems.at[3 * i + 2]))
     for copy in moves + copies:
         copy.start()
     for move in moves:
@@ -81,7 +81,7 @@
 def run_experts(at, blocks, gates, uppers, downs):
     count, width = 4 * blocks[0].shape[0], blocks[0].shape[1]
     depth = gates[0].shape[1]
-    _, _, out_width = downs[0].shape
+    out_width = downs[0].shape[1]
     return pl.pallas_call(
         expert_kernel,
         in_specs=[pl.BlockSpec(memory_space=pltpu.SMEM)]
@@ -189,16 +189,17 @@
     for k in range(4):
         start = ((y - k) & 3) * depth
         cut.append(lax.dynamic_slice_in_dim(w_down, start, depth, 0))
-    for k in (1, 2, 3):
+    for k in (2, 1, 3):
         cut[k] = shift(cut[k], -k)
-    down_o = jnp.stack(cut)
-    down_x = swap(down_o, "xl")
     gate_c = swap(w_gate, "c")
     up_c = swap(w_up, "c")
-    down_c = swap(down_o, "c")
+    leads = [cut[2], swap(cut[2], "c"), swap(cut[2], "xl")]
+    leads.append(swap(leads[2], "c"))
+    rest = jnp.stack([cut[1], cut[3], cut[0]])
+    rests = [rest, swap(rest, "c"), swap(rest, "xl")]
+    rests.append(swap(rests[2], "c"))
     gate_d = swap(gate_x, "c")
     up_d = swap(up_x, "c")
-    down_d = swap(down_x, "c")
 
     lower_core = lax.axis_index("c") == 0
     below = shift(near, 1)
@@ -206,15 +207,14 @@
     across = turn(jnp.where(lower_core, below, above))
     blocks = (near, above, across, below)
     gates, uppers = (w_gate, gate_c, gate_x, gate_d), (w_up, up_c, up_x, up_d)
-    downs = (down_o, down_c, down_x, down_d)
-    hidden, away = run_experts(y[None].astype(jnp.int32), blocks, gates, uppers, downs)
+    hidden, away = run_experts(y[None].astype(jnp.int32), blocks, gates, uppers, leads)
     middle = turn(away).astype(jnp.float32)
-    upward, downward = run_down(hidden, downs, (1, 3))
+    upward, downward = run_down(hidden, rests, (0, 1))
     upward += jnp.where(lower_core, middle, 0.0)
     downward += jnp.where(lower_core, 0.0, middle)
     first = shift(upward.astype(jnp.bfloat16), 1)
     second = shift(downward.astype(jnp.bfloat16), -1)
-    (total,) = run_down(hidden, downs, (0,))
+    (total,) = run_down(hidden, rests, (2,))
     total = total + first.astype(jnp.float32) + second.astype(jnp.float32)
     home = total.astype(jnp.bfloat16)
     home = home.reshape(4, expert_count, share, out_width).transpose(1, 0, 2, 3)

time: 204 us -> 206 us (level); the launches traced: 200 us -> 205 us
  starting transfers between devices: 84.6 us -> 91.3 us
  local copies, waits for them, and re-layouts: 7.98 us -> 5.7 us
    ppermute x9 -> x12, starting transfers between devices: 20.6 us -> 27.7 us  [swap(): return lax.ppermute(block, axis, SWAP)]
    ppermute x7, waiting for transfers between devices: 7.77 us -> 13.9 us  [shift(): return lax.ppermute(block, 'y', [(y, (y + by) % 4) for y in range(4)])]
    ppermute x2, waiting for transfers between devices: 13.4 us -> 7.29 us  [turn(): return lax.ppermute(block, ('c', 'y'), up + down)]
    ppermute x2, starting transfers between devices: 6.31 us -> 3.84 us  [turn(): return lax.ppermute(block, ('c', 'y'), up + down)]
    ppermute x7, starting transfers between devices: 25.6 us -> 27.7 us  [shift(): return lax.ppermute(block, 'y', [(y, (y + by) % 4) for y in range(4)])]
    ppermute x9 -> x12, waiting for transfers between devices: 44 us -> 45.4 us  [swap(): return lax.ppermute(block, axis, SWAP)]
  transfers between devices with their start and end apart: 20 -> 23, of which waited for: 10 -> 8; matrix products, arithmetic and copies ran while one was open for 2% -> 0% of each run, Pallas kernels for 2% -> 6%
where the time goes in v8:
time: 206 us; the launch traced here: 205 us
  starting transfers between devices  91.3 us (44%)
  waiting for transfers between devices  90 us (44%)
  Pallas kernels  13 us (6%)
  local copies, waits for them, and re-layouts  5.7 us (3%)
  matrix products  2.17 us (1%)
    ppermute x12, waiting for transfers between devices, swap(): return lax.ppermute(block, axis, SWAP)  45.4 us
    ppermute x7, starting transfers between devices, shift(): return lax.ppermute(block, 'y', [(y, (y + by) % 4) for y in range(4)])  27.7 us
    ppermute x12, starting transfers between devices, swap(): return lax.ppermute(block, axis, SWAP)  27.7 us
    all_to_all x1, waiting for transfers between devices, layer(): returned = lax.all_to_all(home, ('z', 'xh'), 0, 0, tiled=True)  23.3 us
    all_to_all x1, starting transfers between devices, layer(): arrived = lax.all_to_all(mine, ('z', 'xh'), 0, 0, tiled=True)  18.2 us
    all_to_all x1, starting transfers between devices, layer(): returned = lax.all_to_all(home, ('z', 'xh'), 0, 0, tiled=True)  13.9 us
    ppermute x7, waiting for transfers between devices, shift(): return lax.ppermute(block, 'y', [(y, (y + by) % 4) for y in range(4)])  13.9 us
    pallas_call x1, Pallas kernels, run_experts(): pl.pallas_call(expert_kernel, in_specs=[pl.BlockSpec(memory_space=pltpu.S...  10.6 us
  transfers between devices with their start and end apart: 23, of which 8 were waited for; matrix products, arithmetic and copies ran while one was open for 0% of the time, Pallas kernels for 6%

profile of v8, /device:TPU:6, one launch (start us, length us, event | category | flops | bytes accessed | tf_op | source)
XLA Modules:
  0.0 204.5 jit_solution(15390018606777332988)
XLA Ops:
  0.0 0.8 slice_bitcast_fusion.3
  0.8 1.2 fusion.1
  2.2 0.6 copy-done.5
  2.7 0.5 convolution_convert_fusion
  3.2 0.9 reshape.60
  4.2 18.2 %all-to-all-start = ((bf16[32,48,128]{2,1,0:T(8,128)(2,1)}), bf16[32,48,128]{2,1,0:T(8,128)(2,1)S(1)}, u32[]{:S(2)}, u32[]{:S(2)}) async-start(bf16[32,48,128]{2,1,0:T(8,128)(2,1)} %reshape.60), calls=%async_computation | async-start | bytes 786432 | tf_op jit(solution)/shard_map/all_to_all | solution.py:185
  22.4 2.7 %collective-permute-start.4 = (bf16[2048,256]{1,0:T(8,128)(2,1)}, bf16[2048,256]{1,0:T(8,128)(2,1)}, u32[]{:S(2)}, u32[]{:S(2)}) collective-permute-start(bf16[2048,256]{1,0:T(8,128)(2,1)} %refs_4_.1), channel_id=1, source_target_pairs={{0,8},{8,0},{1,9},{9,1},{2,10},{10,2},{3,11},{11,3},{4,12},{12,4},... | collective-permute-start | bytes 3145736 | tf_op jit(solution)/shard_map/ppermute | solution.py:36
  25.2 3.1 %collective-permute-start.7 = (bf16[2048,256]{1,0:T(8,128)(2,1)}, bf16[2048,256]{1,0:T(8,128)(2,1)}, u32[]{:S(2)}, u32[]{:S(2)}) collective-permute-start(bf16[2048,256]{1,0:T(8,128)(2,1)} %refs_8_.1), channel_id=1, source_target_pairs={{0,8},{8,0},{1,9},{9,1},{2,10},{10,2},{3,11},{11,3},{4,12},{12,4},... | collective-permute-start | bytes 3145736 | tf_op jit(solution)/shard_map/ppermute | solution.py:36
  28.4 5.1 %collective-permute-start.9 = (bf16[256,512]{1,0:T(8,128)(2,1)S(1)}, bf16[256,512]{1,0:T(8,128)(2,1)S(1)}, u32[]{:S(2)}, u32[]{:S(2)}) collective-permute-start(bf16[256,512]{1,0:T(8,128)(2,1)S(1)} %get-tuple-element.14), channel_id=1, source_target_pairs={{0,2},{1,3},{2,0},{3,1},{4,6},{5,7},{6,4},{7,5},{8,10},{9,11},{10,... | collective-permute-start | bytes 786440 | tf_op jit(solution)/shard_map/ppermute | solution.py:26
  33.5 3.0 %collective-permute-start.13 = (bf16[256,512]{1,0:T(8,128)(2,1)S(1)}, bf16[256,512]{1,0:T(8,128)(2,1)S(1)}, u32[]{:S(2)}, u32[]{:S(2)}) collective-permute-start(bf16[256,512]{1,0:T(8,128)(2,1)S(1)} %get-tuple-element.13), channel_id=1, source_target_pairs={{0,3},{1,0},{2,1},{3,2},{4,7},{5,4},{6,5},{7,6},{8,11},{9,8},{10,9... | collective-permute-start | bytes 786440 | tf_op jit(solution)/shard_map/ppermute | solution.py:26
  36.5 2.2 %collective-permute-done.9.refs_12_ = bf16[256,512]{1,0:T(8,128)(2,1)S(1)} collective-permute-done((bf16[256,512]{1,0:T(8,128)(2,1)S(1)}, bf16[256,512]{1,0:T(8,128)(2,1)S(1)}, u32[]{:S(2)}, u32[]{:S(2)}) %collective-permute-start.9) | collective-permute-done | bytes 262176 | tf_op jit(solution)/shard_map/ppermute | solution.py:26
  38.7 2.7 %collective-permute-start.11 = (bf16[256,512]{1,0:T(8,128)(2,1)S(1)}, bf16[256,512]{1,0:T(8,128)(2,1)S(1)}, u32[]{:S(2)}, u32[]{:S(2)}) collective-permute-start(bf16[256,512]{1,0:T(8,128)(2,1)S(1)} %collective-permute-done.9.refs_12_), channel_id=1, source_target_pairs={{0,8},{8,0},{1,9},{9,1},{2,10},{10,2},{3,11},{11,3},{4,12},{12,4},... | collective-permute-start | bytes 786440 | tf_op jit(solution)/shard_map/ppermute | solution.py:36
  41.4 5.7 %collective-permute-start.14 = (bf16[256,512]{1,0:T(8,128)(2,1)S(1)}, bf16[256,512]{1,0:T(8,128)(2,1)S(1)}, u32[]{:S(2)}, u32[]{:S(2)}) collective-permute-start(bf16[256,512]{1,0:T(8,128)(2,1)S(1)} %get-tuple-element.16), channel_id=1, source_target_pairs={{0,1},{1,2},{2,3},{3,0},{4,5},{5,6},{6,7},{7,4},{8,9},{9,10},{10,1... | collective-permute-start | bytes 786440 | tf_op jit(solution)/shard_map/ppermute | solution.py:26
  47.2 1.9 collective-permute-start.10
  49.1 31.4 %collective-permute-done.11.refs_14_ = bf16[256,512]{1,0:T(8,128)(2,1)S(1)} collective-permute-done((bf16[256,512]{1,0:T(8,128)(2,1)S(1)}, bf16[256,512]{1,0:T(8,128)(2,1)S(1)}, u32[]{:S(2)}, u32[]{:S(2)}) %collective-permute-start.11) | collective-permute-done | bytes 262176 | tf_op jit(solution)/shard_map/ppermute | solution.py:36
  80.5 1.9 collective-permute-start.12
  82.6 4.9 %collective-permute-start = (bf16[96,2048]{1,0:T(8,128)(2,1)S(1)}, bf16[96,2048]{1,0:T(8,128)(2,1)S(1)}, u32[]{:S(2)}, u32[]{:S(2)}) collective-permute-start(bf16[96,2048]{1,0:T(8,128)(2,1)S(1)} %reshape.61.refs_0_), channel_id=1, source_target_pairs={{0,3},{1,0},{2,1},{3,2},{4,7},{5,4},{6,5},{7,6},{8,11},{9,8},{10,9... | collective-permute-start | bytes 1179656 | tf_op jit(solution)/shard_map/ppermute | solution.py:26
  87.6 2.1 %collective-permute-start.3 = (bf16[2048,256]{1,0:T(8,128)(2,1)}, bf16[2048,256]{1,0:T(8,128)(2,1)}, u32[]{:S(2)}, u32[]{:S(2)}) collective-permute-start(bf16[2048,256]{1,0:T(8,128)(2,1)} %refs_4_.1), channel_id=1, source_target_pairs={{0,4},{4,0},{1,5},{5,1},{2,6},{6,2},{3,7},{7,3},{8,12},{12,8},{9,1... | collective-permute-start | bytes 3145736 | tf_op jit(solution)/shard_map/ppermute | solution.py:36
  89.7 0.7 copy-done
  90.4 1.9 collective-permute-start.1
  92.3 2.2 %collective-permute-start.6 = (bf16[2048,256]{1,0:T(8,128)(2,1)}, bf16[2048,256]{1,0:T(8,128)(2,1)}, u32[]{:S(2)}, u32[]{:S(2)}) collective-permute-start(bf16[2048,256]{1,0:T(8,128)(2,1)} %refs_8_.1), channel_id=1, source_target_pairs={{0,4},{4,0},{1,5},{5,1},{2,6},{6,2},{3,7},{7,3},{8,12},{12,8},{9,1... | collective-permute-start | bytes 3145736 | tf_op jit(solution)/shard_map/ppermute | solution.py:36
  94.6 2.1 %collective-permute-start.5 = (bf16[2048,256]{1,0:T(8,128)(2,1)}, bf16[2048,256]{1,0:T(8,128)(2,1)}, u32[]{:S(2)}, u32[]{:S(2)}) collective-permute-start(bf16[2048,256]{1,0:T(8,128)(2,1)} %collective-permute-done.4.refs_6_), channel_id=1, source_target_pairs={{0,4},{4,0},{1,5},{5,1},{2,6},{6,2},{3,7},{7,3},{8,12},{12,8},{9,1... | collective-permute-start | bytes 3145736 | tf_op jit(solution)/shard_map/ppermute | solution.py:36
  96.7 2.2 %collective-permute-start.8 = (bf16[2048,256]{1,0:T(8,128)(2,1)}, bf16[2048,256]{1,0:T(8,128)(2,1)}, u32[]{:S(2)}, u32[]{:S(2)}) collective-permute-start(bf16[2048,256]{1,0:T(8,128)(2,1)} %collective-permute-done.7.refs_10_), channel_id=1, source_target_pairs={{0,4},{4,0},{1,5},{5,1},{2,6},{6,2},{3,7},{7,3},{8,12},{12,8},{9,1... | collective-permute-start | bytes 3145736 | tf_op jit(solution)/shard_map/ppermute | solution.py:36
  99.0 5.8 %collective-permute-done.1.refs_3_ = bf16[96,2048]{1,0:T(8,128)(2,1)S(1)} collective-permute-done((bf16[96,2048]{1,0:T(8,128)(2,1)S(1)}, bf16[96,2048]{1,0:T(8,128)(2,1)S(1)}, u32[]{:S(2)}, u32[]{:S(2)}) %collective-permute-start.1) | collective-permute-done | bytes 393248 | tf_op jit(solution)/shard_map/ppermute | solution.py:26
  104.8 2.8 %collective-permute-start.16 = (bf16[3,256,512]{2,1,0:T(8,128)(2,1)S(1)}, bf16[3,256,512]{2,1,0:T(8,128)(2,1)S(1)}, u32[]{:S(2)}, u32[]{:S(2)}) collective-permute-start(bf16[3,256,512]{2,1,0:T(8,128)(2,1)S(1)} %pad_maximum_fusion.refs_0_), channel_id=1, source_target_pairs={{0,8},{8,0},{1,9},{9,1},{2,10},{10,2},{3,11},{11,3},{4,12},{12,4},... | collective-permute-start | bytes 2359304 | tf_op jit(solution)/shard_map/ppermute | solution.py:36
  107.7 1.9 collective-permute-start.2
  109.6 1.9 collective-permute-start.15
  111.5 14.0 %collective-permute-done.16.refs_2_ = bf16[3,256,512]{2,1,0:T(8,128)(2,1)S(1)} collective-permute-done((bf16[3,256,512]{2,1,0:T(8,128)(2,1)S(1)}, bf16[3,256,512]{2,1,0:T(8,128)(2,1)S(1)}, u32[]{:S(2)}, u32[]{:S(2)}) %collective-permute-start.16) | collective-permute-done | bytes 786464 | tf_op jit(solution)/shard_map/ppermute | solution.py:36
  125.6 1.9 collective-permute-start.17
  127.5 10.6 %experts.1 = (bf16[384,1024]{1,0:T(8,128)(2,1)S(1)}, bf16[384,512]{1,0:T(8,128)(2,1)S(1)}) custom-call(s32[1]{0:T(128)} %bitcast.4.at_ref, bf16[96,2048]{1,0:T(8,128)(2,1)S(1)} %reshape.61.refs_0_, bf16[96,2048]{1,0:T(8,128)(2,1)S(1)} %collective-permute-done.refs_1_, bf16[96,2048]{1,0:T(8,128)(2,1)S(1)} %collective-permute-done.2.refs_2_, ...), custom_call_target="tpu_custom_call" | custom-call | flops 3221225472 | bytes 8388608 | tf_op jit(solution)/shard_map/experts/pallas_call | solution.py:85
  138.1 1.9 collective-permute-start.18
  140.1 1.6 down.3
  141.7 7.3 %collective-permute-done.18 = bf16[384,512]{1,0:T(8,128)(2,1)S(1)} collective-permute-done((bf16[384,512]{1,0:T(8,128)(2,1)S(1)}, bf16[384,512]{1,0:T(8,128)(2,1)S(1)}, u32[]{:S(2)}, u32[]{:S(2)}) %collective-permute-start.18) | collective-permute-done | bytes 393248 | tf_op jit(solution)/shard_map/ppermute | solution.py:32
  149.0 0.2 fusion.5
  149.2 1.9 collective-permute-start.19
  151.2 5.1 %collective-permute-start.20 = (bf16[384,512]{1,0:T(8,128)(2,1)S(1)}, bf16[384,512]{1,0:T(8,128)(2,1)S(1)}, u32[]{:S(2)}, u32[]{:S(2)}) collective-permute-start(bf16[384,512]{1,0:T(8,128)(2,1)S(1)} %get-tuple-element.18), channel_id=1, source_target_pairs={{0,3},{1,0},{2,1},{3,2},{4,7},{5,4},{6,5},{7,6},{8,11},{9,8},{10,9... | collective-permute-start | bytes 1179656 | tf_op jit(solution)/shard_map/ppermute | solution.py:26
  156.3 0.8 down.2
  157.1 4.7 %collective-permute-done.19 = bf16[384,512]{1,0:T(8,128)(2,1)S(1)} collective-permute-done((bf16[384,512]{1,0:T(8,128)(2,1)S(1)}, bf16[384,512]{1,0:T(8,128)(2,1)S(1)}, u32[]{:S(2)}, u32[]{:S(2)}) %collective-permute-start.19) | collective-permute-done | bytes 393248 | tf_op jit(solution)/shard_map/ppermute | solution.py:26
  161.8 1.2 collective-permute-done.20
  163.1 0.2 reshape.62
  163.4 0.3 copy.8
  163.6 1.1 reshape.63
  164.7 13.9 %all-to-all-start.1 = ((bf16[32,48,128]{2,1,0:T(8,128)(2,1)}), bf16[32,48,128]{2,1,0:T(8,128)(2,1)S(1)}, u32[]{:S(2)}, u32[]{:S(2)}) async-start(bf16[32,48,128]{2,1,0:T(8,128)(2,1)} %reshape.63), calls=%async_computation.1 | async-start | bytes 786432 | tf_op jit(solution)/shard_map/all_to_all | solution.py:222
  178.7 0.7 copy-done.4
  179.6 0.3 convolution_select_fusion
  179.9 23.3 %all-to-all-done.1 = bf16[32,48,128]{2,1,0:T(8,128)(2,1)S(1)} async-done(((bf16[32,48,128]{2,1,0:T(8,128)(2,1)}), bf16[32,48,128]{2,1,0:T(8,128)(2,1)S(1)}, u32[]{:S(2)}, u32[]{:S(2)}) %all-to-all-start.1) | async-done | bytes 393248 | tf_op jit(solution)/shard_map/all_to_all | solution.py:222
  203.2 0.2 reshape.64
  203.5 1.0 convolution_convert_fusion.1
  (39 shorter events, 1.0 us)
Async XLA Ops:
  0.0 2.2 %copy-start.3 = (bf16[128,2048]{1,0:T(8,128)(2,1)S(1)}, bf16[128,2048]{1,0:T(8,128)(2,1)}, u32[]{:S(2)}) copy-start(bf16[128,2048]{1,0:T(8,128)(2,1)} %param.7) | copy-start | bytes 1572868
  2.0 0.7 copy-start.5
  3.2 25.1 %copy-start.2 = (bf16[1024,512]{1,0:T(8,128)(2,1)S(1)}, bf16[1024,512]{1,0:T(8,128)(2,1)}, u32[]{:S(2)}) copy-start(bf16[1024,512]{1,0:T(8,128)(2,1)} %param.13) | copy-start | bytes 3145732
  4.2 78.2 %all-to-all-start = ((bf16[32,48,128]{2,1,0:T(8,128)(2,1)}), bf16[32,48,128]{2,1,0:T(8,128)(2,1)S(1)}, u32[]{:S(2)}, u32[]{:S(2)}) async-start(bf16[32,48,128]{2,1,0:T(8,128)(2,1)} %reshape.60), calls=%async_computation | async-start | bytes 786432 | tf_op jit(solution)/shard_map/all_to_all | solution.py:185
  22.4 69.9 %collective-permute-start.4 = (bf16[2048,256]{1,0:T(8,128)(2,1)}, bf16[2048,256]{1,0:T(8,128)(2,1)}, u32[]{:S(2)}, u32[]{:S(2)}) collective-permute-start(bf16[2048,256]{1,0:T(8,128)(2,1)} %refs_4_.1), channel_id=1, source_target_pairs={{0,8},{8,0},{1,9},{9,1},{2,10},{10,2},{3,11},{11,3},{4,12},{12,4},... | collective-permute-start | bytes 3145736 | tf_op jit(solution)/shard_map/ppermute | solution.py:36
  25.2 69.4 %collective-permute-start.7 = (bf16[2048,256]{1,0:T(8,128)(2,1)}, bf16[2048,256]{1,0:T(8,128)(2,1)}, u32[]{:S(2)}, u32[]{:S(2)}) collective-permute-start(bf16[2048,256]{1,0:T(8,128)(2,1)} %refs_8_.1), channel_id=1, source_target_pairs={{0,8},{8,0},{1,9},{9,1},{2,10},{10,2},{3,11},{11,3},{4,12},{12,4},... | collective-permute-start | bytes 3145736 | tf_op jit(solution)/shard_map/ppermute | solution.py:36
  28.4 10.3 %collective-permute-start.9 = (bf16[256,512]{1,0:T(8,128)(2,1)S(1)}, bf16[256,512]{1,0:T(8,128)(2,1)S(1)}, u32[]{:S(2)}, u32[]{:S(2)}) collective-permute-start(bf16[256,512]{1,0:T(8,128)(2,1)S(1)} %get-tuple-element.14), channel_id=1, source_target_pairs={{0,2},{1,3},{2,0},{3,1},{4,6},{5,7},{6,4},{7,5},{8,10},{9,11},{10,... | collective-permute-start | bytes 786440 | tf_op jit(solution)/shard_map/ppermute | solution.py:26
  33.5 13.7 %collective-permute-start.13 = (bf16[256,512]{1,0:T(8,128)(2,1)S(1)}, bf16[256,512]{1,0:T(8,128)(2,1)S(1)}, u32[]{:S(2)}, u32[]{:S(2)}) collective-permute-start(bf16[256,512]{1,0:T(8,128)(2,1)S(1)} %get-tuple-element.13), channel_id=1, source_target_pairs={{0,3},{1,0},{2,1},{3,2},{4,7},{5,4},{6,5},{7,6},{8,11},{9,8},{10,9... | collective-permute-start | bytes 786440 | tf_op jit(solution)/shard_map/ppermute | solution.py:26
  38.7 41.8 %collective-permute-start.11 = (bf16[256,512]{1,0:T(8,128)(2,1)S(1)}, bf16[256,512]{1,0:T(8,128)(2,1)S(1)}, u32[]{:S(2)}, u32[]{:S(2)}) collective-permute-start(bf16[256,512]{1,0:T(8,128)(2,1)S(1)} %collective-permute-done.9.refs_12_), channel_id=1, source_target_pairs={{0,8},{8,0},{1,9},{9,1},{2,10},{10,2},{3,11},{11,3},{4,12},{12,4},... | collective-permute-start | bytes 786440 | tf_op jit(solution)/shard_map/ppermute | solution.py:36
  41.4 41.2 %collective-permute-start.14 = (bf16[256,512]{1,0:T(8,128)(2,1)S(1)}, bf16[256,512]{1,0:T(8,128)(2,1)S(1)}, u32[]{:S(2)}, u32[]{:S(2)}) collective-permute-start(bf16[256,512]{1,0:T(8,128)(2,1)S(1)} %get-tuple-element.16), channel_id=1, source_target_pairs={{0,1},{1,2},{2,3},{3,0},{4,5},{5,6},{6,7},{7,4},{8,9},{9,10},{10,1... | collective-permute-start | bytes 786440 | tf_op jit(solution)/shard_map/ppermute | solution.py:26
  47.2 40.3 %collective-permute-start.10 = (bf16[256,512]{1,0:T(8,128)(2,1)S(1)}, bf16[256,512]{1,0:T(8,128)(2,1)S(1)}, u32[]{:S(2)}, u32[]{:S(2)}) collective-permute-start(bf16[256,512]{1,0:T(8,128)(2,1)S(1)} %collective-permute-done.9.refs_12_), channel_id=1, source_target_pairs={{0,4},{4,0},{1,5},{5,1},{2,6},{6,2},{3,7},{7,3},{8,12},{12,8},{9,1... | collective-permute-start | bytes 786440 | tf_op jit(solution)/shard_map/ppermute | solution.py:36
  80.5 9.2 %collective-permute-start.12 = (bf16[256,512]{1,0:T(8,128)(2,1)S(1)}, bf16[256,512]{1,0:T(8,128)(2,1)S(1)}, u32[]{:S(2)}, u32[]{:S(2)}) collective-permute-start(bf16[256,512]{1,0:T(8,128)(2,1)S(1)} %collective-permute-done.11.refs_14_), channel_id=1, source_target_pairs={{0,4},{4,0},{1,5},{5,1},{2,6},{6,2},{3,7},{7,3},{8,12},{12,8},{9,1... | collective-permute-start | bytes 786440 | tf_op jit(solution)/shard_map/ppermute | solution.py:36
  82.6 14.1 %collective-permute-start = (bf16[96,2048]{1,0:T(8,128)(2,1)S(1)}, bf16[96,2048]{1,0:T(8,128)(2,1)S(1)}, u32[]{:S(2)}, u32[]{:S(2)}) collective-permute-start(bf16[96,2048]{1,0:T(8,128)(2,1)S(1)} %reshape.61.refs_0_), channel_id=1, source_target_pairs={{0,3},{1,0},{2,1},{3,2},{4,7},{5,4},{6,5},{7,6},{8,11},{9,8},{10,9... | collective-permute-start | bytes 1179656 | tf_op jit(solution)/shard_map/ppermute | solution.py:26
  87.6 20.1 %collective-permute-start.3 = (bf16[2048,256]{1,0:T(8,128)(2,1)}, bf16[2048,256]{1,0:T(8,128)(2,1)}, u32[]{:S(2)}, u32[]{:S(2)}) collective-permute-start(bf16[2048,256]{1,0:T(8,128)(2,1)} %refs_4_.1), channel_id=1, source_target_pairs={{0,4},{4,0},{1,5},{5,1},{2,6},{6,2},{3,7},{7,3},{8,12},{12,8},{9,1... | collective-permute-start | bytes 3145736 | tf_op jit(solution)/shard_map/ppermute | solution.py:36
  89.7 0.7 copy-start
  90.4 14.4 %collective-permute-start.1 = (bf16[96,2048]{1,0:T(8,128)(2,1)S(1)}, bf16[96,2048]{1,0:T(8,128)(2,1)S(1)}, u32[]{:S(2)}, u32[]{:S(2)}) collective-permute-start(bf16[96,2048]{1,0:T(8,128)(2,1)S(1)} %reshape.61.refs_0_), channel_id=1, source_target_pairs={{0,1},{1,2},{2,3},{3,0},{4,5},{5,6},{6,7},{7,4},{8,9},{9,10},{10,1... | collective-permute-start | bytes 1179656 | tf_op jit(solution)/shard_map/ppermute | solution.py:26
  92.3 17.3 %collective-permute-start.6 = (bf16[2048,256]{1,0:T(8,128)(2,1)}, bf16[2048,256]{1,0:T(8,128)(2,1)}, u32[]{:S(2)}, u32[]{:S(2)}) collective-permute-start(bf16[2048,256]{1,0:T(8,128)(2,1)} %refs_8_.1), channel_id=1, source_target_pairs={{0,4},{4,0},{1,5},{5,1},{2,6},{6,2},{3,7},{7,3},{8,12},{12,8},{9,1... | collective-permute-start | bytes 3145736 | tf_op jit(solution)/shard_map/ppermute | solution.py:36
  94.6 32.9 %collective-permute-start.5 = (bf16[2048,256]{1,0:T(8,128)(2,1)}, bf16[2048,256]{1,0:T(8,128)(2,1)}, u32[]{:S(2)}, u32[]{:S(2)}) collective-permute-start(bf16[2048,256]{1,0:T(8,128)(2,1)} %collective-permute-done.4.refs_6_), channel_id=1, source_target_pairs={{0,4},{4,0},{1,5},{5,1},{2,6},{6,2},{3,7},{7,3},{8,12},{12,8},{9,1... | collective-permute-start | bytes 3145736 | tf_op jit(solution)/shard_map/ppermute | solution.py:36
  96.7 30.8 %collective-permute-start.8 = (bf16[2048,256]{1,0:T(8,128)(2,1)}, bf16[2048,256]{1,0:T(8,128)(2,1)}, u32[]{:S(2)}, u32[]{:S(2)}) collective-permute-start(bf16[2048,256]{1,0:T(8,128)(2,1)} %collective-permute-done.7.refs_10_), channel_id=1, source_target_pairs={{0,4},{4,0},{1,5},{5,1},{2,6},{6,2},{3,7},{7,3},{8,12},{12,8},{9,1... | collective-permute-start | bytes 3145736 | tf_op jit(solution)/shard_map/ppermute | solution.py:36
  104.8 20.8 %collective-permute-start.16 = (bf16[3,256,512]{2,1,0:T(8,128)(2,1)S(1)}, bf16[3,256,512]{2,1,0:T(8,128)(2,1)S(1)}, u32[]{:S(2)}, u32[]{:S(2)}) collective-permute-start(bf16[3,256,512]{2,1,0:T(8,128)(2,1)S(1)} %pad_maximum_fusion.refs_0_), channel_id=1, source_target_pairs={{0,8},{8,0},{1,9},{9,1},{2,10},{10,2},{3,11},{11,3},{4,12},{12,4},... | collective-permute-start | bytes 2359304 | tf_op jit(solution)/shard_map/ppermute | solution.py:36
  107.6 19.9 %copy-start.1 = (bf16[256,512]{1,0:T(8,128)(2,1)S(1)}, bf16[256,512]{1,0:T(8,128)(2,1)}, u32[]{:S(2)}) copy-start(bf16[256,512]{1,0:T(8,128)(2,1)} %copy-done) | copy-start | bytes 786436
  107.7 19.8 %collective-permute-start.2 = (bf16[96,2048]{1,0:T(8,128)(2,1)S(1)}, bf16[96,2048]{1,0:T(8,128)(2,1)S(1)}, u32[]{:S(2)}, u32[]{:S(2)}) collective-permute-start(bf16[96,2048]{1,0:T(8,128)(2,1)S(1)} %broadcast_select_fusion), channel_id=1, source_target_pairs={{0,1},{1,2},{2,3},{3,0},{4,7},{5,4},{6,5},{7,6},{8,9},{9,10},{10,1... | collective-permute-start | bytes 1179656 | tf_op jit(solution)/shard_map/ppermute | solution.py:32
  109.6 30.4 %collective-permute-start.15 = (bf16[3,256,512]{2,1,0:T(8,128)(2,1)S(1)}, bf16[3,256,512]{2,1,0:T(8,128)(2,1)S(1)}, u32[]{:S(2)}, u32[]{:S(2)}) collective-permute-start(bf16[3,256,512]{2,1,0:T(8,128)(2,1)S(1)} %pad_maximum_fusion.refs_0_), channel_id=1, source_target_pairs={{0,4},{4,0},{1,5},{5,1},{2,6},{6,2},{3,7},{7,3},{8,12},{12,8},{9,1... | collective-permute-start | bytes 2359304 | tf_op jit(solution)/shard_map/ppermute | solution.py:36
  125.6 14.5 %collective-permute-start.17 = (bf16[3,256,512]{2,1,0:T(8,128)(2,1)S(1)}, bf16[3,256,512]{2,1,0:T(8,128)(2,1)S(1)}, u32[]{:S(2)}, u32[]{:S(2)}) collective-permute-start(bf16[3,256,512]{2,1,0:T(8,128)(2,1)S(1)} %collective-permute-done.16.refs_2_), channel_id=1, source_target_pairs={{0,4},{4,0},{1,5},{5,1},{2,6},{6,2},{3,7},{7,3},{8,12},{12,8},{9,1... | collective-permute-start | bytes 2359304 | tf_op jit(solution)/shard_map/ppermute | solution.py:36
  138.1 10.9 %collective-permute-start.18 = (bf16[384,512]{1,0:T(8,128)(2,1)S(1)}, bf16[384,512]{1,0:T(8,128)(2,1)S(1)}, u32[]{:S(2)}, u32[]{:S(2)}) collective-permute-start(bf16[384,512]{1,0:T(8,128)(2,1)S(1)} %get-tuple-element.11), channel_id=1, source_target_pairs={{0,1},{1,2},{2,3},{3,0},{4,7},{5,4},{6,5},{7,6},{8,9},{9,10},{10,1... | collective-permute-start | bytes 1179656 | tf_op jit(solution)/shard_map/ppermute | solution.py:32
  149.2 12.6 %collective-permute-start.19 = (bf16[384,512]{1,0:T(8,128)(2,1)S(1)}, bf16[384,512]{1,0:T(8,128)(2,1)S(1)}, u32[]{:S(2)}, u32[]{:S(2)}) collective-permute-start(bf16[384,512]{1,0:T(8,128)(2,1)S(1)} %get-tuple-element.17), channel_id=1, source_target_pairs={{0,1},{1,2},{2,3},{3,0},{4,5},{5,6},{6,7},{7,4},{8,9},{9,10},{10,1... | collective-permute-start | bytes 1179656 | tf_op jit(solution)/shard_map/ppermute | solution.py:26
  151.2 11.8 %collective-permute-start.20 = (bf16[384,512]{1,0:T(8,128)(2,1)S(1)}, bf16[384,512]{1,0:T(8,128)(2,1)S(1)}, u32[]{:S(2)}, u32[]{:S(2)}) collective-permute-start(bf16[384,512]{1,0:T(8,128)(2,1)S(1)} %get-tuple-element.18), channel_id=1, source_target_pairs={{0,3},{1,0},{2,1},{3,2},{4,7},{5,4},{6,5},{7,6},{8,11},{9,8},{10,9... | collective-permute-start | bytes 1179656 | tf_op jit(solution)/shard_map/ppermute | solution.py:26
  164.7 38.5 %all-to-all-start.1 = ((bf16[32,48,128]{2,1,0:T(8,128)(2,1)}), bf16[32,48,128]{2,1,0:T(8,128)(2,1)S(1)}, u32[]{:S(2)}, u32[]{:S(2)}) async-start(bf16[32,48,128]{2,1,0:T(8,128)(2,1)} %reshape.63), calls=%async_computation.1 | async-start | bytes 786432 | tf_op jit(solution)/shard_map/all_to_all | solution.py:222
  178.7 0.7 copy-start.4

commit v9 on v8

--- a/solution.py
+++ b/solution.py
@@ -51,15 +51,16 @@
 def expert_kernel(at_ref, *refs):
     blocks, gates, uppers, downs = refs[0:4], refs[4:8], refs[8:12], refs[12:16]
     hidden_ref, part_ref, rows, wide, tall, sems, row_sems = refs[16:]
-    depth = wide.shape[2]
+    depth = wide.shape[2] // 2
     count = blocks[0].shape[0]
     moves, copies = [], []
     for i in range(4):
         place = pl.ds(pl.multiple_of(((at_ref[0] + i) & 3) * count, 16), count)
         moves.append(pltpu.make_async_copy(blocks[i], rows.at[place], row_sems.at[i]))
     for i in range(4):
-        copies.append(pltpu.make_async_copy(gates[i], wide.at[2 * i], sems.at[3 * i]))
-        copies.append(pltpu.make_async_copy(uppers[i], wide.at[2 * i + 1], sems.at[3 * i + 1]))
+        gate_at, up_at = wide.at[i, :, pl.ds(0, depth)], wide.at[i, :, pl.ds(depth, depth)]
+        copies.append(pltpu.make_async_copy(gates[i], gate_at, sems.at[3 * i]))
+        copies.append(pltpu.make_async_copy(uppers[i], up_at, sems.at[3 * i + 1]))
         copies.append(pltpu.make_async_copy(downs[i], tall.at[i], sems.at[3 * i + 2]))
     for copy in moves + copies:
         copy.start()
@@ -68,10 +69,9 @@
     total = jnp.zeros(part_ref.shape, jnp.float32)
     for i in range(4):
         copies[3 * i].wait()
-        gate_proj = dot32(rows[...], wide[2 * i])
         copies[3 * i + 1].wait()
-        upper = dot32(rows[...], wide[2 * i + 1])
-        piece = (jax.nn.silu(gate_proj) * upper).astype(jnp.bfloat16)
+        both = dot32(rows[...], wide[i])
+        piece = (jax.nn.silu(both[:, :depth]) * both[:, depth:]).astype(jnp.bfloat16)
         hidden_ref[:, i * depth : (i + 1) * depth] = piece
         copies[3 * i + 2].wait()
         total += dot32(piece, tall[i])
@@ -93,7 +93,7 @@
         ],
         scratch_shapes=[
             pltpu.VMEM((count, width), jnp.bfloat16),
-            pltpu.VMEM((8, width, depth), jnp.bfloat16),
+            pltpu.VMEM((4, width, 2 * depth), jnp.bfloat16),
             pltpu.VMEM((4, depth, out_width), jnp.bfloat16),
             pltpu.SemaphoreType.DMA((12,)),
             pltpu.SemaphoreType.DMA((4,)),

time: 206 us -> 203 us (0.985)
  Pallas kernels: 13 us -> 9.57 us
    pallas_call x1, Pallas kernels: 10.6 us -> 7.15 us  [run_experts(): pl.pallas_call(expert_kernel, in_specs=[pl.BlockSpec(memory_space=pltpu.S...]
  transfers between devices with their start and end apart: 23 -> 23, of which waited for: 8 -> 8; matrix products, arithmetic and copies ran while one was open for 0% -> 0% of each run, Pallas kernels for 6% -> 5%
where the time goes in v9:
time: 203 us; the launch traced here: 201 us
  starting transfers between devices  91.4 us (45%)
  waiting for transfers between devices  90 us (44%)
  Pallas kernels  9.57 us (5%)
  local copies, waits for them, and re-layouts  5.7 us (3%)
  matrix products  2.17 us (1%)
    ppermute x12, waiting for transfers between devices, swap(): return lax.ppermute(block, axis, SWAP)  45.4 us
    ppermute x7, starting transfers between devices, shift(): return lax.ppermute(block, 'y', [(y, (y + by) % 4) for y in range(4)])  27.7 us
    ppermute x12, starting transfers between devices, swap(): return lax.ppermute(block, axis, SWAP)  27.7 us
    all_to_all x1, waiting for transfers between devices, layer(): returned = lax.all_to_all(home, ('z', 'xh'), 0, 0, tiled=True)  23.4 us
    all_to_all x1, starting transfers between devices, layer(): arrived = lax.all_to_all(mine, ('z', 'xh'), 0, 0, tiled=True)  18.2 us
    all_to_all x1, starting transfers between devices, layer(): returned = lax.all_to_all(home, ('z', 'xh'), 0, 0, tiled=True)  14 us
    ppermute x7, waiting for transfers between devices, shift(): return lax.ppermute(block, 'y', [(y, (y + by) % 4) for y in range(4)])  13.9 us
    ppermute x2, waiting for transfers between devices, turn(): return lax.ppermute(block, ('c', 'y'), up + down)  7.32 us
  transfers between devices with their start and end apart: 23, of which 8 were waited for; matrix products, arithmetic and copies ran while one was open for 0% of the time, Pallas kernels for 5%

profile of v9, /device:TPU:6, one launch (start us, length us, event | category | flops | bytes accessed | tf_op | source)
XLA Modules:
  0.0 201.1 jit_solution(7970109533102006458)
XLA Ops:
  0.0 0.8 slice_bitcast_fusion.3
  0.8 1.2 fusion.1
  2.2 0.6 copy-done.5
  2.7 0.5 convolution_convert_fusion
  3.2 0.9 reshape.60
  4.2 18.2 %all-to-all-start = ((bf16[32,48,128]{2,1,0:T(8,128)(2,1)}), bf16[32,48,128]{2,1,0:T(8,128)(2,1)S(1)}, u32[]{:S(2)}, u32[]{:S(2)}) async-start(bf16[32,48,128]{2,1,0:T(8,128)(2,1)} %reshape.60), calls=%async_computation | async-start | bytes 786432 | tf_op jit(solution)/shard_map/all_to_all | solution.py:185
  22.4 2.7 %collective-permute-start.4 = (bf16[2048,256]{1,0:T(8,128)(2,1)}, bf16[2048,256]{1,0:T(8,128)(2,1)}, u32[]{:S(2)}, u32[]{:S(2)}) collective-permute-start(bf16[2048,256]{1,0:T(8,128)(2,1)} %refs_4_.1), channel_id=1, source_target_pairs={{0,8},{8,0},{1,9},{9,1},{2,10},{10,2},{3,11},{11,3},{4,12},{12,4},... | collective-permute-start | bytes 3145736 | tf_op jit(solution)/shard_map/ppermute | solution.py:36
  25.2 3.1 %collective-permute-start.7 = (bf16[2048,256]{1,0:T(8,128)(2,1)}, bf16[2048,256]{1,0:T(8,128)(2,1)}, u32[]{:S(2)}, u32[]{:S(2)}) collective-permute-start(bf16[2048,256]{1,0:T(8,128)(2,1)} %refs_8_.1), channel_id=1, source_target_pairs={{0,8},{8,0},{1,9},{9,1},{2,10},{10,2},{3,11},{11,3},{4,12},{12,4},... | collective-permute-start | bytes 3145736 | tf_op jit(solution)/shard_map/ppermute | solution.py:36
  28.4 5.1 %collective-permute-start.9 = (bf16[256,512]{1,0:T(8,128)(2,1)S(1)}, bf16[256,512]{1,0:T(8,128)(2,1)S(1)}, u32[]{:S(2)}, u32[]{:S(2)}) collective-permute-start(bf16[256,512]{1,0:T(8,128)(2,1)S(1)} %get-tuple-element.14), channel_id=1, source_target_pairs={{0,2},{1,3},{2,0},{3,1},{4,6},{5,7},{6,4},{7,5},{8,10},{9,11},{10,... | collective-permute-start | bytes 786440 | tf_op jit(solution)/shard_map/ppermute | solution.py:26
  33.5 3.0 %collective-permute-start.13 = (bf16[256,512]{1,0:T(8,128)(2,1)S(1)}, bf16[256,512]{1,0:T(8,128)(2,1)S(1)}, u32[]{:S(2)}, u32[]{:S(2)}) collective-permute-start(bf16[256,512]{1,0:T(8,128)(2,1)S(1)} %get-tuple-element.13), channel_id=1, source_target_pairs={{0,3},{1,0},{2,1},{3,2},{4,7},{5,4},{6,5},{7,6},{8,11},{9,8},{10,9... | collective-permute-start | bytes 786440 | tf_op jit(solution)/shard_map/ppermute | solution.py:26
  36.5 2.2 %collective-permute-done.9.refs_12_ = bf16[256,512]{1,0:T(8,128)(2,1)S(1)} collective-permute-done((bf16[256,512]{1,0:T(8,128)(2,1)S(1)}, bf16[256,512]{1,0:T(8,128)(2,1)S(1)}, u32[]{:S(2)}, u32[]{:S(2)}) %collective-permute-start.9) | collective-permute-done | bytes 262176 | tf_op jit(solution)/shard_map/ppermute | solution.py:26
  38.7 2.7 %collective-permute-start.11 = (bf16[256,512]{1,0:T(8,128)(2,1)S(1)}, bf16[256,512]{1,0:T(8,128)(2,1)S(1)}, u32[]{:S(2)}, u32[]{:S(2)}) collective-permute-start(bf16[256,512]{1,0:T(8,128)(2,1)S(1)} %collective-permute-done.9.refs_12_), channel_id=1, source_target_pairs={{0,8},{8,0},{1,9},{9,1},{2,10},{10,2},{3,11},{11,3},{4,12},{12,4},... | collective-permute-start | bytes 786440 | tf_op jit(solution)/shard_map/ppermute | solution.py:36
  41.4 5.7 %collective-permute-start.14 = (bf16[256,512]{1,0:T(8,128)(2,1)S(1)}, bf16[256,512]{1,0:T(8,128)(2,1)S(1)}, u32[]{:S(2)}, u32[]{:S(2)}) collective-permute-start(bf16[256,512]{1,0:T(8,128)(2,1)S(1)} %get-tuple-element.16), channel_id=1, source_target_pairs={{0,1},{1,2},{2,3},{3,0},{4,5},{5,6},{6,7},{7,4},{8,9},{9,10},{10,1... | collective-permute-start | bytes 786440 | tf_op jit(solution)/shard_map/ppermute | solution.py:26
  47.2 1.9 collective-permute-start.10
  49.1 31.4 %collective-permute-done.11.refs_14_ = bf16[256,512]{1,0:T(8,128)(2,1)S(1)} collective-permute-done((bf16[256,512]{1,0:T(8,128)(2,1)S(1)}, bf16[256,512]{1,0:T(8,128)(2,1)S(1)}, u32[]{:S(2)}, u32[]{:S(2)}) %collective-permute-start.11) | collective-permute-done | bytes 262176 | tf_op jit(solution)/shard_map/ppermute | solution.py:36
  80.5 1.9 collective-permute-start.12
  82.6 4.9 %collective-permute-start = (bf16[96,2048]{1,0:T(8,128)(2,1)S(1)}, bf16[96,2048]{1,0:T(8,128)(2,1)S(1)}, u32[]{:S(2)}, u32[]{:S(2)}) collective-permute-start(bf16[96,2048]{1,0:T(8,128)(2,1)S(1)} %reshape.61.refs_0_), channel_id=1, source_target_pairs={{0,3},{1,0},{2,1},{3,2},{4,7},{5,4},{6,5},{7,6},{8,11},{9,8},{10,9... | collective-permute-start | bytes 1179656 | tf_op jit(solution)/shard_map/ppermute | solution.py:26
  87.6 2.1 %collective-permute-start.3 = (bf16[2048,256]{1,0:T(8,128)(2,1)}, bf16[2048,256]{1,0:T(8,128)(2,1)}, u32[]{:S(2)}, u32[]{:S(2)}) collective-permute-start(bf16[2048,256]{1,0:T(8,128)(2,1)} %refs_4_.1), channel_id=1, source_target_pairs={{0,4},{4,0},{1,5},{5,1},{2,6},{6,2},{3,7},{7,3},{8,12},{12,8},{9,1... | collective-permute-start | bytes 3145736 | tf_op jit(solution)/shard_map/ppermute | solution.py:36
  89.7 0.7 copy-done
  90.4 1.9 collective-permute-start.1
  92.3 2.2 %collective-permute-start.6 = (bf16[2048,256]{1,0:T(8,128)(2,1)}, bf16[2048,256]{1,0:T(8,128)(2,1)}, u32[]{:S(2)}, u32[]{:S(2)}) collective-permute-start(bf16[2048,256]{1,0:T(8,128)(2,1)} %refs_8_.1), channel_id=1, source_target_pairs={{0,4},{4,0},{1,5},{5,1},{2,6},{6,2},{3,7},{7,3},{8,12},{12,8},{9,1... | collective-permute-start | bytes 3145736 | tf_op jit(solution)/shard_map/ppermute | solution.py:36
  94.6 2.1 %collective-permute-start.5 = (bf16[2048,256]{1,0:T(8,128)(2,1)}, bf16[2048,256]{1,0:T(8,128)(2,1)}, u32[]{:S(2)}, u32[]{:S(2)}) collective-permute-start(bf16[2048,256]{1,0:T(8,128)(2,1)} %collective-permute-done.4.refs_6_), channel_id=1, source_target_pairs={{0,4},{4,0},{1,5},{5,1},{2,6},{6,2},{3,7},{7,3},{8,12},{12,8},{9,1... | collective-permute-start | bytes 3145736 | tf_op jit(solution)/shard_map/ppermute | solution.py:36
  96.7 2.2 %collective-permute-start.8 = (bf16[2048,256]{1,0:T(8,128)(2,1)}, bf16[2048,256]{1,0:T(8,128)(2,1)}, u32[]{:S(2)}, u32[]{:S(2)}) collective-permute-start(bf16[2048,256]{1,0:T(8,128)(2,1)} %collective-permute-done.7.refs_10_), channel_id=1, source_target_pairs={{0,4},{4,0},{1,5},{5,1},{2,6},{6,2},{3,7},{7,3},{8,12},{12,8},{9,1... | collective-permute-start | bytes 3145736 | tf_op jit(solution)/shard_map/ppermute | solution.py:36
  99.0 5.8 %collective-permute-done.1.refs_3_ = bf16[96,2048]{1,0:T(8,128)(2,1)S(1)} collective-permute-done((bf16[96,2048]{1,0:T(8,128)(2,1)S(1)}, bf16[96,2048]{1,0:T(8,128)(2,1)S(1)}, u32[]{:S(2)}, u32[]{:S(2)}) %collective-permute-start.1) | collective-permute-done | bytes 393248 | tf_op jit(solution)/shard_map/ppermute | solution.py:26
  104.8 2.8 %collective-permute-start.16 = (bf16[3,256,512]{2,1,0:T(8,128)(2,1)S(1)}, bf16[3,256,512]{2,1,0:T(8,128)(2,1)S(1)}, u32[]{:S(2)}, u32[]{:S(2)}) collective-permute-start(bf16[3,256,512]{2,1,0:T(8,128)(2,1)S(1)} %pad_maximum_fusion.refs_0_), channel_id=1, source_target_pairs={{0,8},{8,0},{1,9},{9,1},{2,10},{10,2},{3,11},{11,3},{4,12},{12,4},... | collective-permute-start | bytes 2359304 | tf_op jit(solution)/shard_map/ppermute | solution.py:36
  107.7 1.9 collective-permute-start.2
  109.6 1.9 collective-permute-start.15
  111.5 14.0 %collective-permute-done.16.refs_2_ = bf16[3,256,512]{2,1,0:T(8,128)(2,1)S(1)} collective-permute-done((bf16[3,256,512]{2,1,0:T(8,128)(2,1)S(1)}, bf16[3,256,512]{2,1,0:T(8,128)(2,1)S(1)}, u32[]{:S(2)}, u32[]{:S(2)}) %collective-permute-start.16) | collective-permute-done | bytes 786464 | tf_op jit(solution)/shard_map/ppermute | solution.py:36
  125.6 1.9 collective-permute-start.17
  127.5 7.1 %experts.1 = (bf16[384,1024]{1,0:T(8,128)(2,1)S(1)}, bf16[384,512]{1,0:T(8,128)(2,1)S(1)}) custom-call(s32[1]{0:T(128)} %bitcast.4.at_ref, bf16[96,2048]{1,0:T(8,128)(2,1)S(1)} %reshape.61.refs_0_, bf16[96,2048]{1,0:T(8,128)(2,1)S(1)} %collective-permute-done.refs_1_, bf16[96,2048]{1,0:T(8,128)(2,1)S(1)} %collective-permute-done.2.refs_2_, ...), custom_call_target="tpu_custom_call" | custom-call | flops 3221225472 | bytes 8388608 | tf_op jit(solution)/shard_map/experts/pallas_call | solution.py:85
  134.7 1.9 collective-permute-start.18
  136.6 1.6 down.3
  138.3 7.3 %collective-permute-done.18 = bf16[384,512]{1,0:T(8,128)(2,1)S(1)} collective-permute-done((bf16[384,512]{1,0:T(8,128)(2,1)S(1)}, bf16[384,512]{1,0:T(8,128)(2,1)S(1)}, u32[]{:S(2)}, u32[]{:S(2)}) %collective-permute-start.18) | collective-permute-done | bytes 393248 | tf_op jit(solution)/shard_map/ppermute | solution.py:32
  145.6 0.2 fusion.5
  145.8 1.9 collective-permute-start.19
  147.7 5.1 %collective-permute-start.20 = (bf16[384,512]{1,0:T(8,128)(2,1)S(1)}, bf16[384,512]{1,0:T(8,128)(2,1)S(1)}, u32[]{:S(2)}, u32[]{:S(2)}) collective-permute-start(bf16[384,512]{1,0:T(8,128)(2,1)S(1)} %get-tuple-element.18), channel_id=1, source_target_pairs={{0,3},{1,0},{2,1},{3,2},{4,7},{5,4},{6,5},{7,6},{8,11},{9,8},{10,9... | collective-permute-start | bytes 1179656 | tf_op jit(solution)/shard_map/ppermute | solution.py:26
  152.9 0.8 down.2
  153.7 4.7 %collective-permute-done.19 = bf16[384,512]{1,0:T(8,128)(2,1)S(1)} collective-permute-done((bf16[384,512]{1,0:T(8,128)(2,1)S(1)}, bf16[384,512]{1,0:T(8,128)(2,1)S(1)}, u32[]{:S(2)}, u32[]{:S(2)}) %collective-permute-start.19) | collective-permute-done | bytes 393248 | tf_op jit(solution)/shard_map/ppermute | solution.py:26
  158.4 1.2 collective-permute-done.20
  159.7 0.2 reshape.62
  159.9 0.3 copy.8
  160.2 1.1 reshape.63
  161.3 14.0 %all-to-all-start.1 = ((bf16[32,48,128]{2,1,0:T(8,128)(2,1)}), bf16[32,48,128]{2,1,0:T(8,128)(2,1)S(1)}, u32[]{:S(2)}, u32[]{:S(2)}) async-start(bf16[32,48,128]{2,1,0:T(8,128)(2,1)} %reshape.63), calls=%async_computation.1 | async-start | bytes 786432 | tf_op jit(solution)/shard_map/all_to_all | solution.py:222
  175.3 0.7 copy-done.4
  176.2 0.3 convolution_select_fusion
  176.5 23.4 %all-to-all-done.1 = bf16[32,48,128]{2,1,0:T(8,128)(2,1)S(1)} async-done(((bf16[32,48,128]{2,1,0:T(8,128)(2,1)}), bf16[32,48,128]{2,1,0:T(8,128)(2,1)S(1)}, u32[]{:S(2)}, u32[]{:S(2)}) %all-to-all-start.1) | async-done | bytes 393248 | tf_op jit(solution)/shard_map/all_to_all | solution.py:222
  199.8 0.2 reshape.64
  200.1 1.0 convolution_convert_fusion.1
  (39 shorter events, 1.0 us)
Async XLA Ops:
  0.0 2.2 %copy-start.3 = (bf16[128,2048]{1,0:T(8,128)(2,1)S(1)}, bf16[128,2048]{1,0:T(8,128)(2,1)}, u32[]{:S(2)}) copy-start(bf16[128,2048]{1,0:T(8,128)(2,1)} %param.7) | copy-start | bytes 1572868
  2.0 0.7 copy-start.5
  3.2 25.1 %copy-start.2 = (bf16[1024,512]{1,0:T(8,128)(2,1)S(1)}, bf16[1024,512]{1,0:T(8,128)(2,1)}, u32[]{:S(2)}) copy-start(bf16[1024,512]{1,0:T(8,128)(2,1)} %param.13) | copy-start | bytes 3145732
  4.2 78.2 %all-to-all-start = ((bf16[32,48,128]{2,1,0:T(8,128)(2,1)}), bf16[32,48,128]{2,1,0:T(8,128)(2,1)S(1)}, u32[]{:S(2)}, u32[]{:S(2)}) async-start(bf16[32,48,128]{2,1,0:T(8,128)(2,1)} %reshape.60), calls=%async_computation | async-start | bytes 786432 | tf_op jit(solution)/shard_map/all_to_all | solution.py:185
  22.4 69.9 %collective-permute-start.4 = (bf16[2048,256]{1,0:T(8,128)(2,1)}, bf16[2048,256]{1,0:T(8,128)(2,1)}, u32[]{:S(2)}, u32[]{:S(2)}) collective-permute-start(bf16[2048,256]{1,0:T(8,128)(2,1)} %refs_4_.1), channel_id=1, source_target_pairs={{0,8},{8,0},{1,9},{9,1},{2,10},{10,2},{3,11},{11,3},{4,12},{12,4},... | collective-permute-start | bytes 3145736 | tf_op jit(solution)/shard_map/ppermute | solution.py:36
  25.2 69.4 %collective-permute-start.7 = (bf16[2048,256]{1,0:T(8,128)(2,1)}, bf16[2048,256]{1,0:T(8,128)(2,1)}, u32[]{:S(2)}, u32[]{:S(2)}) collective-permute-start(bf16[2048,256]{1,0:T(8,128)(2,1)} %refs_8_.1), channel_id=1, source_target_pairs={{0,8},{8,0},{1,9},{9,1},{2,10},{10,2},{3,11},{11,3},{4,12},{12,4},... | collective-permute-start | bytes 3145736 | tf_op jit(solution)/shard_map/ppermute | solution.py:36
  28.4 10.3 %collective-permute-start.9 = (bf16[256,512]{1,0:T(8,128)(2,1)S(1)}, bf16[256,512]{1,0:T(8,128)(2,1)S(1)}, u32[]{:S(2)}, u32[]{:S(2)}) collective-permute-start(bf16[256,512]{1,0:T(8,128)(2,1)S(1)} %get-tuple-element.14), channel_id=1, source_target_pairs={{0,2},{1,3},{2,0},{3,1},{4,6},{5,7},{6,4},{7,5},{8,10},{9,11},{10,... | collective-permute-start | bytes 786440 | tf_op jit(solution)/shard_map/ppermute | solution.py:26
  33.5 13.7 %collective-permute-start.13 = (bf16[256,512]{1,0:T(8,128)(2,1)S(1)}, bf16[256,512]{1,0:T(8,128)(2,1)S(1)}, u32[]{:S(2)}, u32[]{:S(2)}) collective-permute-start(bf16[256,512]{1,0:T(8,128)(2,1)S(1)} %get-tuple-element.13), channel_id=1, source_target_pairs={{0,3},{1,0},{2,1},{3,2},{4,7},{5,4},{6,5},{7,6},{8,11},{9,8},{10,9... | collective-permute-start | bytes 786440 | tf_op jit(solution)/shard_map/ppermute | solution.py:26
  38.7 41.8 %collective-permute-start.11 = (bf16[256,512]{1,0:T(8,128)(2,1)S(1)}, bf16[256,512]{1,0:T(8,128)(2,1)S(1)}, u32[]{:S(2)}, u32[]{:S(2)}) collective-permute-start(bf16[256,512]{1,0:T(8,128)(2,1)S(1)} %collective-permute-done.9.refs_12_), channel_id=1, source_target_pairs={{0,8},{8,0},{1,9},{9,1},{2,10},{10,2},{3,11},{11,3},{4,12},{12,4},... | collective-permute-start | bytes 786440 | tf_op jit(solution)/shard_map/ppermute | solution.py:36
  41.4 41.2 %collective-permute-start.14 = (bf16[256,512]{1,0:T(8,128)(2,1)S(1)}, bf16[256,512]{1,0:T(8,128)(2,1)S(1)}, u32[]{:S(2)}, u32[]{:S(2)}) collective-permute-start(bf16[256,512]{1,0:T(8,128)(2,1)S(1)} %get-tuple-element.16), channel_id=1, source_target_pairs={{0,1},{1,2},{2,3},{3,0},{4,5},{5,6},{6,7},{7,4},{8,9},{9,10},{10,1... | collective-permute-start | bytes 786440 | tf_op jit(solution)/shard_map/ppermute | solution.py:26
  47.2 40.3 %collective-permute-start.10 = (bf16[256,512]{1,0:T(8,128)(2,1)S(1)}, bf16[256,512]{1,0:T(8,128)(2,1)S(1)}, u32[]{:S(2)}, u32[]{:S(2)}) collective-permute-start(bf16[256,512]{1,0:T(8,128)(2,1)S(1)} %collective-permute-done.9.refs_12_), channel_id=1, source_target_pairs={{0,4},{4,0},{1,5},{5,1},{2,6},{6,2},{3,7},{7,3},{8,12},{12,8},{9,1... | collective-permute-start | bytes 786440 | tf_op jit(solution)/shard_map/ppermute | solution.py:36
  80.5 9.2 %collective-permute-start.12 = (bf16[256,512]{1,0:T(8,128)(2,1)S(1)}, bf16[256,512]{1,0:T(8,128)(2,1)S(1)}, u32[]{:S(2)}, u32[]{:S(2)}) collective-permute-start(bf16[256,512]{1,0:T(8,128)(2,1)S(1)} %collective-permute-done.11.refs_14_), channel_id=1, source_target_pairs={{0,4},{4,0},{1,5},{5,1},{2,6},{6,2},{3,7},{7,3},{8,12},{12,8},{9,1... | collective-permute-start | bytes 786440 | tf_op jit(solution)/shard_map/ppermute | solution.py:36
  82.6 14.1 %collective-permute-start = (bf16[96,2048]{1,0:T(8,128)(2,1)S(1)}, bf16[96,2048]{1,0:T(8,128)(2,1)S(1)}, u32[]{:S(2)}, u32[]{:S(2)}) collective-permute-start(bf16[96,2048]{1,0:T(8,128)(2,1)S(1)} %reshape.61.refs_0_), channel_id=1, source_target_pairs={{0,3},{1,0},{2,1},{3,2},{4,7},{5,4},{6,5},{7,6},{8,11},{9,8},{10,9... | collective-permute-start | bytes 1179656 | tf_op jit(solution)/shard_map/ppermute | solution.py:26
  87.6 20.1 %collective-permute-start.3 = (bf16[2048,256]{1,0:T(8,128)(2,1)}, bf16[2048,256]{1,0:T(8,128)(2,1)}, u32[]{:S(2)}, u32[]{:S(2)}) collective-permute-start(bf16[2048,256]{1,0:T(8,128)(2,1)} %refs_4_.1), channel_id=1, source_target_pairs={{0,4},{4,0},{1,5},{5,1},{2,6},{6,2},{3,7},{7,3},{8,12},{12,8},{9,1... | collective-permute-start | bytes 3145736 | tf_op jit(solution)/shard_map/ppermute | solution.py:36
  89.7 0.7 copy-start
  90.4 14.4 %collective-permute-start.1 = (bf16[96,2048]{1,0:T(8,128)(2,1)S(1)}, bf16[96,2048]{1,0:T(8,128)(2,1)S(1)}, u32[]{:S(2)}, u32[]{:S(2)}) collective-permute-start(bf16[96,2048]{1,0:T(8,128)(2,1)S(1)} %reshape.61.refs_0_), channel_id=1, source_target_pairs={{0,1},{1,2},{2,3},{3,0},{4,5},{5,6},{6,7},{7,4},{8,9},{9,10},{10,1... | collective-permute-start | bytes 1179656 | tf_op jit(solution)/shard_map/ppermute | solution.py:26
  92.3 17.3 %collective-permute-start.6 = (bf16[2048,256]{1,0:T(8,128)(2,1)}, bf16[2048,256]{1,0:T(8,128)(2,1)}, u32[]{:S(2)}, u32[]{:S(2)}) collective-permute-start(bf16[2048,256]{1,0:T(8,128)(2,1)} %refs_8_.1), channel_id=1, source_target_pairs={{0,4},{4,0},{1,5},{5,1},{2,6},{6,2},{3,7},{7,3},{8,12},{12,8},{9,1... | collective-permute-start | bytes 3145736 | tf_op jit(solution)/shard_map/ppermute | solution.py:36
  94.6 32.9 %collective-permute-start.5 = (bf16[2048,256]{1,0:T(8,128)(2,1)}, bf16[2048,256]{1,0:T(8,128)(2,1)}, u32[]{:S(2)}, u32[]{:S(2)}) collective-permute-start(bf16[2048,256]{1,0:T(8,128)(2,1)} %collective-permute-done.4.refs_6_), channel_id=1, source_target_pairs={{0,4},{4,0},{1,5},{5,1},{2,6},{6,2},{3,7},{7,3},{8,12},{12,8},{9,1... | collective-permute-start | bytes 3145736 | tf_op jit(solution)/shard_map/ppermute | solution.py:36
  96.7 30.8 %collective-permute-start.8 = (bf16[2048,256]{1,0:T(8,128)(2,1)}, bf16[2048,256]{1,0:T(8,128)(2,1)}, u32[]{:S(2)}, u32[]{:S(2)}) collective-permute-start(bf16[2048,256]{1,0:T(8,128)(2,1)} %collective-permute-done.7.refs_10_), channel_id=1, source_target_pairs={{0,4},{4,0},{1,5},{5,1},{2,6},{6,2},{3,7},{7,3},{8,12},{12,8},{9,1... | collective-permute-start | bytes 3145736 | tf_op jit(solution)/shard_map/ppermute | solution.py:36
  104.8 20.8 %collective-permute-start.16 = (bf16[3,256,512]{2,1,0:T(8,128)(2,1)S(1)}, bf16[3,256,512]{2,1,0:T(8,128)(2,1)S(1)}, u32[]{:S(2)}, u32[]{:S(2)}) collective-permute-start(bf16[3,256,512]{2,1,0:T(8,128)(2,1)S(1)} %pad_maximum_fusion.refs_0_), channel_id=1, source_target_pairs={{0,8},{8,0},{1,9},{9,1},{2,10},{10,2},{3,11},{11,3},{4,12},{12,4},... | collective-permute-start | bytes 2359304 | tf_op jit(solution)/shard_map/ppermute | solution.py:36
  107.6 19.9 %copy-start.1 = (bf16[256,512]{1,0:T(8,128)(2,1)S(1)}, bf16[256,512]{1,0:T(8,128)(2,1)}, u32[]{:S(2)}) copy-start(bf16[256,512]{1,0:T(8,128)(2,1)} %copy-done) | copy-start | bytes 786436
  107.7 19.8 %collective-permute-start.2 = (bf16[96,2048]{1,0:T(8,128)(2,1)S(1)}, bf16[96,2048]{1,0:T(8,128)(2,1)S(1)}, u32[]{:S(2)}, u32[]{:S(2)}) collective-permute-start(bf16[96,2048]{1,0:T(8,128)(2,1)S(1)} %broadcast_select_fusion), channel_id=1, source_target_pairs={{0,1},{1,2},{2,3},{3,0},{4,7},{5,4},{6,5},{7,6},{8,9},{9,10},{10,1... | collective-permute-start | bytes 1179656 | tf_op jit(solution)/shard_map/ppermute | solution.py:32
  109.6 27.0 %collective-permute-start.15 = (bf16[3,256,512]{2,1,0:T(8,128)(2,1)S(1)}, bf16[3,256,512]{2,1,0:T(8,128)(2,1)S(1)}, u32[]{:S(2)}, u32[]{:S(2)}) collective-permute-start(bf16[3,256,512]{2,1,0:T(8,128)(2,1)S(1)} %pad_maximum_fusion.refs_0_), channel_id=1, source_target_pairs={{0,4},{4,0},{1,5},{5,1},{2,6},{6,2},{3,7},{7,3},{8,12},{12,8},{9,1... | collective-permute-start | bytes 2359304 | tf_op jit(solution)/shard_map/ppermute | solution.py:36
  125.6 11.1 %collective-permute-start.17 = (bf16[3,256,512]{2,1,0:T(8,128)(2,1)S(1)}, bf16[3,256,512]{2,1,0:T(8,128)(2,1)S(1)}, u32[]{:S(2)}, u32[]{:S(2)}) collective-permute-start(bf16[3,256,512]{2,1,0:T(8,128)(2,1)S(1)} %collective-permute-done.16.refs_2_), channel_id=1, source_target_pairs={{0,4},{4,0},{1,5},{5,1},{2,6},{6,2},{3,7},{7,3},{8,12},{12,8},{9,1... | collective-permute-start | bytes 2359304 | tf_op jit(solution)/shard_map/ppermute | solution.py:36
  134.7 10.9 %collective-permute-start.18 = (bf16[384,512]{1,0:T(8,128)(2,1)S(1)}, bf16[384,512]{1,0:T(8,128)(2,1)S(1)}, u32[]{:S(2)}, u32[]{:S(2)}) collective-permute-start(bf16[384,512]{1,0:T(8,128)(2,1)S(1)} %get-tuple-element.11), channel_id=1, source_target_pairs={{0,1},{1,2},{2,3},{3,0},{4,7},{5,4},{6,5},{7,6},{8,9},{9,10},{10,1... | collective-permute-start | bytes 1179656 | tf_op jit(solution)/shard_map/ppermute | solution.py:32
  145.8 12.5 %collective-permute-start.19 = (bf16[384,512]{1,0:T(8,128)(2,1)S(1)}, bf16[384,512]{1,0:T(8,128)(2,1)S(1)}, u32[]{:S(2)}, u32[]{:S(2)}) collective-permute-start(bf16[384,512]{1,0:T(8,128)(2,1)S(1)} %get-tuple-element.17), channel_id=1, source_target_pairs={{0,1},{1,2},{2,3},{3,0},{4,5},{5,6},{6,7},{7,4},{8,9},{9,10},{10,1... | collective-permute-start | bytes 1179656 | tf_op jit(solution)/shard_map/ppermute | solution.py:26
  147.7 11.8 %collective-permute-start.20 = (bf16[384,512]{1,0:T(8,128)(2,1)S(1)}, bf16[384,512]{1,0:T(8,128)(2,1)S(1)}, u32[]{:S(2)}, u32[]{:S(2)}) collective-permute-start(bf16[384,512]{1,0:T(8,128)(2,1)S(1)} %get-tuple-element.18), channel_id=1, source_target_pairs={{0,3},{1,0},{2,1},{3,2},{4,7},{5,4},{6,5},{7,6},{8,11},{9,8},{10,9... | collective-permute-start | bytes 1179656 | tf_op jit(solution)/shard_map/ppermute | solution.py:26
  161.3 38.6 %all-to-all-start.1 = ((bf16[32,48,128]{2,1,0:T(8,128)(2,1)}), bf16[32,48,128]{2,1,0:T(8,128)(2,1)S(1)}, u32[]{:S(2)}, u32[]{:S(2)}) async-start(bf16[32,48,128]{2,1,0:T(8,128)(2,1)} %reshape.63), calls=%async_computation.1 | async-start | bytes 786432 | tf_op jit(solution)/shard_map/all_to_all | solution.py:222
  175.3 0.7 copy-start.4

commit v10 on v9

--- a/solution.py
+++ b/solution.py
@@ -1,5 +1,3 @@
-import functools
-
 import jax
 import jax.numpy as jnp
 from jax import lax
@@ -26,10 +24,9 @@
     return lax.ppermute(block, "y", [(y, (y + by) % 4) for y in range(4)])
 
 
-def turn(block):
-    up = [(y, (y + 1) % 4) for y in range(4)]
-    down = [(4 + y, 4 + (y - 1) % 4) for y in range(4)]
-    return lax.ppermute(block, ("c", "y"), up + down)
+def around(block, by):
+    pairs = [(y, (y + by) % 4) for y in range(4)] + [(4 + y, 4 + (y - by) % 4) for y in range(4)]
+    return lax.ppermute(block, ("c", "y"), pairs)
 
 
 def swap(block, axis):
@@ -54,8 +51,8 @@
     depth = wide.shape[2] // 2
     count = blocks[0].shape[0]
     moves, copies = [], []
-    for i in range(4):
-        place = pl.ds(pl.multiple_of(((at_ref[0] + i) & 3) * count, 16), count)
+    for i, ahead in enumerate((0, -at_ref[1], 2, at_ref[1])):
+        place = pl.ds(pl.multiple_of(((at_ref[0] + ahead) & 3) * count, 16), count)
         moves.append(pltpu.make_async_copy(blocks[i], rows.at[place], row_sems.at[i]))
     for i in range(4):
         gate_at, up_at = wide.at[i, :, pl.ds(0, depth)], wide.at[i, :, pl.ds(depth, depth)]
@@ -108,12 +105,12 @@
     )(at, *blocks, *gates, *uppers, *downs)
 
 
-def down_kernel(picks, hidden_ref, *refs):
-    downs, outs, (tall, sems) = refs[:4], refs[4 : 4 + len(picks)], refs[4 + len(picks) :]
+def down_kernel(pick_ref, hidden_ref, *refs):
+    downs, outs, (tall, sems) = refs[:4], refs[4:-2], refs[-2:]
     depth = tall.shape[1]
     copies = [
-        pltpu.make_async_copy(downs[i].at[k], tall.at[4 * n + i], sems.at[4 * n + i])
-        for n, k in enumerate(picks)
+        pltpu.make_async_copy(downs[i].at[pick_ref[n]], tall.at[4 * n + i], sems.at[4 * n + i])
+        for n in range(len(outs))
         for i in range(4)
     ]
     for copy in copies:
@@ -123,29 +120,30 @@
         for i in range(4):
             copies[4 * n + i].wait()
             total += dot32(hidden_ref[:, i * depth : (i + 1) * depth], tall[4 * n + i])
-        out[...] = total
-
-
-def run_down(hidden, downs, picks):
-    count = hidden.shape[0]
+        out[...] = total.astype(out.dtype)
+
+
+def run_down(picks, hidden, downs, dtypes):
+    count, parts = hidden.shape[0], len(dtypes)
     _, depth, out_width = downs[0].shape
     return pl.pallas_call(
-        functools.partial(down_kernel, picks),
-        in_specs=[pl.BlockSpec(memory_space=pltpu.VMEM)] + [pl.BlockSpec(memory_space=pl.ANY)] * 4,
-        out_specs=[pl.BlockSpec(memory_space=pltpu.VMEM)] * len(picks),
-        out_shape=[jax.ShapeDtypeStruct((count, out_width), jnp.float32)] * len(picks),
+        down_kernel,
+        in_specs=[pl.BlockSpec(memory_space=pltpu.SMEM), pl.BlockSpec(memory_space=pltpu.VMEM)]
+        + [pl.BlockSpec(memory_space=pl.ANY)] * 4,
+        out_specs=[pl.BlockSpec(memory_space=pltpu.VMEM)] * parts,
+        out_shape=[jax.ShapeDtypeStruct((count, out_width), dtype) for dtype in dtypes],
         scratch_shapes=[
-            pltpu.VMEM((4 * len(picks), depth, out_width), jnp.bfloat16),
-            pltpu.SemaphoreType.DMA((4 * len(picks),)),
+            pltpu.VMEM((4 * parts, depth, out_width), jnp.bfloat16),
+            pltpu.SemaphoreType.DMA((4 * parts,)),
         ],
         cost_estimate=pl.CostEstimate(
-            flops=8 * len(picks) * count * depth * out_width,
-            bytes_accessed=8 * len(picks) * depth * out_width,
+            flops=8 * parts * count * depth * out_width,
+            bytes_accessed=8 * parts * depth * out_width,
             transcendentals=0,
         ),
         compiler_params=pltpu.CompilerParams(vmem_limit_bytes=12 << 20),
         name="down",
-    )(hidden, *downs)
+    )(picks, hidden, *downs)
 
 
 def layer(tokens, norm_gain, expert_ids, gate_weights, w_gate, w_up, w_down):
@@ -201,20 +199,21 @@
     gate_d = swap(gate_x, "c")
     up_d = swap(up_x, "c")
 
-    lower_core = lax.axis_index("c") == 0
-    below = shift(near, 1)
-    above = shift(near, -1)
-    across = turn(jnp.where(lower_core, below, above))
-    blocks = (near, above, across, below)
+    core = lax.axis_index("c").astype(jnp.int32)
+    ahead = around(near, 1)
+    behind = around(near, -1)
+    across = around(ahead, 1)
+    blocks = (near, ahead, across, behind)
     gates, uppers = (w_gate, gate_c, gate_x, gate_d), (w_up, up_c, up_x, up_d)
-    hidden, away = run_experts(y[None].astype(jnp.int32), blocks, gates, uppers, leads)
-    middle = turn(away).astype(jnp.float32)
-    upward, downward = run_down(hidden, rests, (0, 1))
-    upward += jnp.where(lower_core, middle, 0.0)
-    downward += jnp.where(lower_core, 0.0, middle)
-    first = shift(upward.astype(jnp.bfloat16), 1)
-    second = shift(downward.astype(jnp.bfloat16), -1)
-    (total,) = run_down(hidden, rests, (2,))
+    at = jnp.stack([y.astype(jnp.int32), 1 - 2 * core])
+    hidden, away = run_experts(at, blocks, gates, uppers, leads)
+    middle = around(away, 1)
+    against, along = run_down(
+        jnp.stack([1 - core, core]), hidden, rests, (jnp.bfloat16, jnp.float32)
+    )
+    first = around(against, -1)
+    second = around((along + middle.astype(jnp.float32)).astype(jnp.bfloat16), 1)
+    (total,) = run_down(jnp.full((1,), 2, jnp.int32), hidden, rests, (jnp.float32,))
     total = total + first.astype(jnp.float32) + second.astype(jnp.float32)
     home = total.astype(jnp.bfloat16)
     home = home.reshape(4, expert_count, share, out_width).transpose(1, 0, 2, 3)

time: 203 us -> 201 us (level)
  waiting for transfers between devices: 90 us -> 75.9 us
  local copies, waits for them, and re-layouts: 5.7 us -> 16.7 us
    ppermute x7 -> x3, starting transfers between devices: 27.7 us -> 10.9 us  [shift(): return lax.ppermute(block, 'y', [(y, (y + by) % 4) for y in range(4)])]
    ppermute x2 -> x6, starting transfers between devices: 3.84 us -> 20.3 us  [around(): return lax.ppermute(block, ('c', 'y'), pairs)]
    unnamed x12 -> x38, local copies, waits for them, and re-layouts: 1.93 us -> 12.9 us
    ppermute x7 -> x3, waiting for transfers between devices: 13.9 us -> 3.38 us  [shift(): return lax.ppermute(block, 'y', [(y, (y + by) % 4) for y in range(4)])]
    ppermute x12, waiting for transfers between devices: 45.4 us -> 35 us  [swap(): return lax.ppermute(block, axis, SWAP)]
    ppermute x2 -> x6, waiting for transfers between devices: 7.32 us -> 12.7 us  [around(): return lax.ppermute(block, ('c', 'y'), pairs)]
  transfers between devices with their start and end apart: 23 -> 23, of which waited for: 8 -> 9; matrix products, arithmetic and copies ran while one was open for 0% -> 1% of each run, Pallas kernels for 5% -> 5%
where the time goes in v10:
time: 201 us; the launch traced here: 199 us
  starting transfers between devices  91.4 us (45%)
  waiting for transfers between devices  75.9 us (38%)
  local copies, waits for them, and re-layouts  16.7 us (8%)
  Pallas kernels  10.8 us (5%)
  matrix products  2.16 us (1%)
    ppermute x12, waiting for transfers between devices, swap(): return lax.ppermute(block, axis, SWAP)  35 us
    ppermute x12, starting transfers between devices, swap(): return lax.ppermute(block, axis, SWAP)  27.9 us
    all_to_all x1, waiting for transfers between devices, layer(): returned = lax.all_to_all(home, ('z', 'xh'), 0, 0, tiled=True)  24.7 us
    ppermute x6, starting transfers between devices, around(): return lax.ppermute(block, ('c', 'y'), pairs)  20.3 us
    all_to_all x1, starting transfers between devices, layer(): arrived = lax.all_to_all(mine, ('z', 'xh'), 0, 0, tiled=True)  18.2 us
    all_to_all x1, starting transfers between devices, layer(): returned = lax.all_to_all(home, ('z', 'xh'), 0, 0, tiled=True)  14 us
    unnamed x38, local copies, waits for them, and re-layouts  12.9 us
    ppermute x6, waiting for transfers between devices, around(): return lax.ppermute(block, ('c', 'y'), pairs)  12.7 us
  transfers between devices with their start and end apart: 23, of which 9 were waited for; matrix products, arithmetic and copies ran while one was open for 1% of the time, Pallas kernels for 5%

profile of v10, /device:TPU:6, one launch (start us, length us, event | category | flops | bytes accessed | tf_op | source)
XLA Modules:
  0.0 199.3 jit_solution(12532144974872878637)
XLA Ops:
  0.0 0.8 slice_bitcast_fusion.3
  0.8 1.2 fusion.1
  3.2 0.9 reshape.60
  4.2 18.2 %all-to-all-start = ((bf16[32,48,128]{2,1,0:T(8,128)(2,1)}), bf16[32,48,128]{2,1,0:T(8,128)(2,1)S(1)}, u32[]{:S(2)}, u32[]{:S(2)}) async-start(bf16[32,48,128]{2,1,0:T(8,128)(2,1)} %reshape.60), calls=%async_computation | async-start | bytes 786432 | tf_op jit(solution)/shard_map/all_to_all | solution.py:183
  22.4 2.7 %collective-permute-start.4 = (bf16[2048,256]{1,0:T(8,128)(2,1)S(1)}, bf16[2048,256]{1,0:T(8,128)(2,1)}, u32[]{:S(2)}, u32[]{:S(2)}) collective-permute-start(bf16[2048,256]{1,0:T(8,128)(2,1)S(1)} %copy-done.3), channel_id=1, source_target_pairs={{0,8},{8,0},{1,9},{9,1},{2,10},{10,2},{3,11},{11,3},{4,12},{12,4},... | collective-permute-start | bytes 3145736 | tf_op jit(solution)/shard_map/ppermute | solution.py:33
  25.2 3.1 %collective-permute-start.7 = (bf16[2048,256]{1,0:T(8,128)(2,1)}, bf16[2048,256]{1,0:T(8,128)(2,1)}, u32[]{:S(2)}, u32[]{:S(2)}) collective-permute-start(bf16[2048,256]{1,0:T(8,128)(2,1)} %refs_8_.1), channel_id=1, source_target_pairs={{0,8},{8,0},{1,9},{9,1},{2,10},{10,2},{3,11},{11,3},{4,12},{12,4},... | collective-permute-start | bytes 3145736 | tf_op jit(solution)/shard_map/ppermute | solution.py:33
  28.4 5.1 %collective-permute-start.9 = (bf16[256,512]{1,0:T(8,128)(2,1)S(1)}, bf16[256,512]{1,0:T(8,128)(2,1)S(1)}, u32[]{:S(2)}, u32[]{:S(2)}) collective-permute-start(bf16[256,512]{1,0:T(8,128)(2,1)S(1)} %get-tuple-element.14), channel_id=1, source_target_pairs={{0,2},{1,3},{2,0},{3,1},{4,6},{5,7},{6,4},{7,5},{8,10},{9,11},{10,... | collective-permute-start | bytes 786440 | tf_op jit(solution)/shard_map/ppermute | solution.py:24
  33.5 3.0 %collective-permute-start.13 = (bf16[256,512]{1,0:T(8,128)(2,1)S(1)}, bf16[256,512]{1,0:T(8,128)(2,1)S(1)}, u32[]{:S(2)}, u32[]{:S(2)}) collective-permute-start(bf16[256,512]{1,0:T(8,128)(2,1)S(1)} %get-tuple-element.13), channel_id=1, source_target_pairs={{0,3},{1,0},{2,1},{3,2},{4,7},{5,4},{6,5},{7,6},{8,11},{9,8},{10,9... | collective-permute-start | bytes 786440 | tf_op jit(solution)/shard_map/ppermute | solution.py:24
  36.5 2.9 %collective-permute-start.14 = (bf16[256,512]{1,0:T(8,128)(2,1)S(1)}, bf16[256,512]{1,0:T(8,128)(2,1)S(1)}, u32[]{:S(2)}, u32[]{:S(2)}) collective-permute-start(bf16[256,512]{1,0:T(8,128)(2,1)S(1)} %get-tuple-element.16), channel_id=1, source_target_pairs={{0,1},{1,2},{2,3},{3,0},{4,5},{5,6},{6,7},{7,4},{8,9},{9,10},{10,1... | collective-permute-start | bytes 786440 | tf_op jit(solution)/shard_map/ppermute | solution.py:24
  39.4 1.9 collective-permute-start.3
  41.3 3.4 %collective-permute-done.13 = bf16[256,512]{1,0:T(8,128)(2,1)S(1)} collective-permute-done((bf16[256,512]{1,0:T(8,128)(2,1)S(1)}, bf16[256,512]{1,0:T(8,128)(2,1)S(1)}, u32[]{:S(2)}, u32[]{:S(2)}) %collective-permute-start.13) | collective-permute-done | bytes 262176 | tf_op jit(solution)/shard_map/ppermute | solution.py:24
  44.7 2.7 %collective-permute-start.11 = (bf16[256,512]{1,0:T(8,128)(2,1)S(1)}, bf16[256,512]{1,0:T(8,128)(2,1)S(1)}, u32[]{:S(2)}, u32[]{:S(2)}) collective-permute-start(bf16[256,512]{1,0:T(8,128)(2,1)S(1)} %collective-permute-done.9.refs_12_), channel_id=1, source_target_pairs={{0,8},{8,0},{1,9},{9,1},{2,10},{10,2},{3,11},{11,3},{4,12},{12,4},... | collective-permute-start | bytes 786440 | tf_op jit(solution)/shard_map/ppermute | solution.py:33
  47.4 1.9 collective-permute-start.6
  49.4 30.9 %collective-permute-done.11.refs_14_ = bf16[256,512]{1,0:T(8,128)(2,1)S(1)} collective-permute-done((bf16[256,512]{1,0:T(8,128)(2,1)S(1)}, bf16[256,512]{1,0:T(8,128)(2,1)S(1)}, u32[]{:S(2)}, u32[]{:S(2)}) %collective-permute-start.11) | collective-permute-done | bytes 262176 | tf_op jit(solution)/shard_map/ppermute | solution.py:33
  80.3 1.9 collective-permute-start.10
  82.9 0.8 collective-permute-done.10.refs_13_
  83.7 0.8 copy-done.11
  84.5 2.0 %collective-permute-start.12 = (bf16[256,512]{1,0:T(8,128)(2,1)S(1)}, bf16[256,512]{1,0:T(8,128)(2,1)S(1)}, u32[]{:S(2)}, u32[]{:S(2)}) collective-permute-start(bf16[256,512]{1,0:T(8,128)(2,1)S(1)} %collective-permute-done.11.refs_14_), channel_id=1, source_target_pairs={{0,4},{4,0},{1,5},{5,1},{2,6},{6,2},{3,7},{7,3},{8,12},{12,8},{9,1... | collective-permute-start | bytes 786440 | tf_op jit(solution)/shard_map/ppermute | solution.py:33
  87.2 2.3 %collective-permute-start.5 = (bf16[2048,256]{1,0:T(8,128)(2,1)}, bf16[2048,256]{1,0:T(8,128)(2,1)}, u32[]{:S(2)}, u32[]{:S(2)}) collective-permute-start(bf16[2048,256]{1,0:T(8,128)(2,1)} %collective-permute-done.4.refs_6_), channel_id=1, source_target_pairs={{0,4},{4,0},{1,5},{5,1},{2,6},{6,2},{3,7},{7,3},{8,12},{12,8},{9,1... | collective-permute-start | bytes 3145736 | tf_op jit(solution)/shard_map/ppermute | solution.py:33
  89.5 2.0 %collective-permute-start.8 = (bf16[2048,256]{1,0:T(8,128)(2,1)}, bf16[2048,256]{1,0:T(8,128)(2,1)}, u32[]{:S(2)}, u32[]{:S(2)}) collective-permute-start(bf16[2048,256]{1,0:T(8,128)(2,1)} %collective-permute-done.7.refs_10_), channel_id=1, source_target_pairs={{0,4},{4,0},{1,5},{5,1},{2,6},{6,2},{3,7},{7,3},{8,12},{12,8},{9,1... | collective-permute-start | bytes 3145736 | tf_op jit(solution)/shard_map/ppermute | solution.py:33
  92.4 2.9 %collective-permute-start.16 = (bf16[3,256,512]{2,1,0:T(8,128)(2,1)S(1)}, bf16[3,256,512]{2,1,0:T(8,128)(2,1)S(1)}, u32[]{:S(2)}, u32[]{:S(2)}) collective-permute-start(bf16[3,256,512]{2,1,0:T(8,128)(2,1)S(1)} %pad_maximum_fusion.refs_0_), channel_id=1, source_target_pairs={{0,8},{8,0},{1,9},{9,1},{2,10},{10,2},{3,11},{11,3},{4,12},{12,4},... | collective-permute-start | bytes 2359304 | tf_op jit(solution)/shard_map/ppermute | solution.py:33
  95.6 3.5 %collective-permute-start = (bf16[96,2048]{1,0:T(8,128)(2,1)S(1)}, bf16[96,2048]{1,0:T(8,128)(2,1)}, u32[]{:S(2)}, u32[]{:S(2)}) collective-permute-start(bf16[96,2048]{1,0:T(8,128)(2,1)S(1)} %reshape.61.refs_0_), channel_id=1, source_target_pairs={{0,1},{1,2},{2,3},{3,0},{4,7},{5,4},{6,5},{7,6},{8,9},{9,10},{10,1... | collective-permute-start | bytes 1179656 | tf_op jit(solution)/shard_map/ppermute | solution.py:29
  99.1 3.6 %collective-permute-start.2 = (bf16[96,2048]{1,0:T(8,128)(2,1)S(1)}, bf16[96,2048]{1,0:T(8,128)(2,1)S(1)}, u32[]{:S(2)}, u32[]{:S(2)}) collective-permute-start(bf16[96,2048]{1,0:T(8,128)(2,1)S(1)} %reshape.61.refs_0_), channel_id=1, source_target_pairs={{0,3},{1,0},{2,1},{3,2},{4,5},{5,6},{6,7},{7,4},{8,11},{9,8},{10,9... | collective-permute-start | bytes 1179656 | tf_op jit(solution)/shard_map/ppermute | solution.py:29
  102.7 4.3 %collective-permute-done.refs_1_ = bf16[96,2048]{1,0:T(8,128)(2,1)} collective-permute-done((bf16[96,2048]{1,0:T(8,128)(2,1)S(1)}, bf16[96,2048]{1,0:T(8,128)(2,1)}, u32[]{:S(2)}, u32[]{:S(2)}) %collective-permute-start) | collective-permute-done | bytes 393248 | tf_op jit(solution)/shard_map/ppermute | solution.py:29
  107.0 3.8 %collective-permute-start.1 = (bf16[96,2048]{1,0:T(8,128)(2,1)}, bf16[96,2048]{1,0:T(8,128)(2,1)}, u32[]{:S(2)}, u32[]{:S(2)}) collective-permute-start(bf16[96,2048]{1,0:T(8,128)(2,1)} %collective-permute-done.refs_1_), channel_id=1, source_target_pairs={{0,1},{1,2},{2,3},{3,0},{4,7},{5,4},{6,5},{7,6},{8,9},{9,10},{10,1... | collective-permute-start | bytes 1179656 | tf_op jit(solution)/shard_map/ppermute | solution.py:29
  110.8 3.3 %collective-permute-done.16.refs_2_ = bf16[3,256,512]{2,1,0:T(8,128)(2,1)S(1)} collective-permute-done((bf16[3,256,512]{2,1,0:T(8,128)(2,1)S(1)}, bf16[3,256,512]{2,1,0:T(8,128)(2,1)S(1)}, u32[]{:S(2)}, u32[]{:S(2)}) %collective-permute-start.16) | collective-permute-done | bytes 786464 | tf_op jit(solution)/shard_map/ppermute | solution.py:33
  114.1 1.9 collective-permute-start.15
  116.8 2.4 %collective-permute-start.17 = (bf16[3,256,512]{2,1,0:T(8,128)(2,1)S(1)}, bf16[3,256,512]{2,1,0:T(8,128)(2,1)S(1)}, u32[]{:S(2)}, u32[]{:S(2)}) collective-permute-start(bf16[3,256,512]{2,1,0:T(8,128)(2,1)S(1)} %collective-permute-done.16.refs_2_), channel_id=1, source_target_pairs={{0,4},{4,0},{1,5},{5,1},{2,6},{6,2},{3,7},{7,3},{8,12},{12,8},{9,1... | collective-permute-start | bytes 2359304 | tf_op jit(solution)/shard_map/ppermute | solution.py:33
  119.3 1.2 copy-done.4
  120.5 1.0 copy-done.6
  121.5 0.9 copy-done.8
  122.5 0.9 copy-done.10
  123.4 0.9 copy-done.12
  124.4 0.9 copy-done.14
  125.3 7.8 %experts.1 = (bf16[384,1024]{1,0:T(8,128)(2,1)S(1)}, bf16[384,512]{1,0:T(8,128)(2,1)}) custom-call(s32[2]{0:T(128)S(1)} %pad_add_fusion.at_ref, bf16[96,2048]{1,0:T(8,128)(2,1)S(1)} %reshape.61.refs_0_, bf16[96,2048]{1,0:T(8,128)(2,1)} %collective-permute-done.refs_1_, bf16[96,2048]{1,0:T(8,128)(2,1)} %collective-permute-done.1.refs_2_, ...), custom_call_target="tpu_custom_call" | custom-call | flops 3221225472 | bytes 8388608 | tf_op jit(solution)/shard_map/experts/pallas_call | solution.py:82
  133.2 0.9 copy-done
  134.1 3.5 %collective-permute-start.19 = (bf16[384,512]{1,0:T(8,128)(2,1)}, bf16[384,512]{1,0:T(8,128)(2,1)S(1)}, u32[]{:S(2)}, u32[]{:S(2)}) collective-permute-start(bf16[384,512]{1,0:T(8,128)(2,1)} %get-tuple-element.12), channel_id=1, source_target_pairs={{0,1},{1,2},{2,3},{3,0},{4,7},{5,4},{6,5},{7,6},{8,9},{9,10},{10,1... | collective-permute-start | bytes 1179656 | tf_op jit(solution)/shard_map/ppermute | solution.py:29
  137.7 1.1 copy-done.1
  138.8 2.2 %down.3 = (bf16[384,512]{1,0:T(8,128)(2,1)S(1)}, f32[384,512]{1,0:T(8,128)S(1)}) custom-call(s32[2]{0:T(128)S(1)} %pad_add_fusion.1.pick_ref, bf16[384,1024]{1,0:T(8,128)(2,1)S(1)} %copy-done.1, bf16[3,256,512]{2,1,0:T(8,128)(2,1)S(1)} %pad_maximum_fusion.refs_0_, bf16[3,256,512]{2,1,0:T(8,128)(2,1)S(1)} %collective-permute-done.15.refs_1_, ...), custom_call_target="tpu_custom_call" | custom-call | flops 805306368 | bytes 2097152 | tf_op jit(solution)/shard_map/down/pallas_call | solution.py:129
  141.0 3.6 %collective-permute-start.18 = (bf16[384,512]{1,0:T(8,128)(2,1)S(1)}, bf16[384,512]{1,0:T(8,128)(2,1)S(1)}, u32[]{:S(2)}, u32[]{:S(2)}) collective-permute-start(bf16[384,512]{1,0:T(8,128)(2,1)S(1)} %get-tuple-element.10), channel_id=1, source_target_pairs={{0,3},{1,0},{2,1},{3,2},{4,5},{5,6},{6,7},{7,4},{8,11},{9,8},{10,9... | collective-permute-start | bytes 1179656 | tf_op jit(solution)/shard_map/ppermute | solution.py:29
  145.3 2.4 %collective-permute-start.20 = (bf16[384,512]{1,0:T(8,128)(2,1)S(1)}, bf16[384,512]{1,0:T(8,128)(2,1)S(1)}, u32[]{:S(2)}, u32[]{:S(2)}) collective-permute-start(bf16[384,512]{1,0:T(8,128)(2,1)S(1)} %add_convert_fusion.1), channel_id=1, source_target_pairs={{0,1},{1,2},{2,3},{3,0},{4,7},{5,4},{6,5},{7,6},{8,9},{9,10},{10,1... | collective-permute-start | bytes 1179656 | tf_op jit(solution)/shard_map/ppermute | solution.py:29
  147.7 0.8 down.2
  148.5 3.9 %collective-permute-done.18 = bf16[384,512]{1,0:T(8,128)(2,1)S(1)} collective-permute-done((bf16[384,512]{1,0:T(8,128)(2,1)S(1)}, bf16[384,512]{1,0:T(8,128)(2,1)S(1)}, u32[]{:S(2)}, u32[]{:S(2)}) %collective-permute-start.18) | collective-permute-done | bytes 393248 | tf_op jit(solution)/shard_map/ppermute | solution.py:29
  152.4 3.9 %collective-permute-done.20 = bf16[384,512]{1,0:T(8,128)(2,1)S(1)} collective-permute-done((bf16[384,512]{1,0:T(8,128)(2,1)S(1)}, bf16[384,512]{1,0:T(8,128)(2,1)S(1)}, u32[]{:S(2)}, u32[]{:S(2)}) %collective-permute-start.20) | collective-permute-done | bytes 393248 | tf_op jit(solution)/shard_map/ppermute | solution.py:29
  157.0 1.1 reshape.63
  158.1 14.0 %all-to-all-start.1 = ((bf16[32,48,128]{2,1,0:T(8,128)(2,1)}), bf16[32,48,128]{2,1,0:T(8,128)(2,1)S(1)}, u32[]{:S(2)}, u32[]{:S(2)}) async-start(bf16[32,48,128]{2,1,0:T(8,128)(2,1)} %reshape.63), calls=%async_computation.1 | async-start | bytes 786432 | tf_op jit(solution)/shard_map/all_to_all | solution.py:221
  173.3 24.7 %all-to-all-done.1 = bf16[32,48,128]{2,1,0:T(8,128)(2,1)S(1)} async-done(((bf16[32,48,128]{2,1,0:T(8,128)(2,1)}), bf16[32,48,128]{2,1,0:T(8,128)(2,1)S(1)}, u32[]{:S(2)}, u32[]{:S(2)}) %all-to-all-start.1) | async-done | bytes 393248 | tf_op jit(solution)/shard_map/all_to_all | solution.py:221
  198.2 1.0 convolution_convert_fusion.1
  (66 shorter events, 7.5 us)
Async XLA Ops:
  0.0 2.2 %copy-start.16 = (bf16[128,2048]{1,0:T(8,128)(2,1)S(1)}, bf16[128,2048]{1,0:T(8,128)(2,1)}, u32[]{:S(2)}) copy-start(bf16[128,2048]{1,0:T(8,128)(2,1)} %param.7) | copy-start | bytes 1572868
  2.0 0.7 copy-start.18
  2.7 19.7 %copy-start.3 = (bf16[2048,256]{1,0:T(8,128)(2,1)S(1)}, bf16[2048,256]{1,0:T(8,128)(2,1)}, u32[]{:S(2)}) copy-start(bf16[2048,256]{1,0:T(8,128)(2,1)} %refs_4_.1) | copy-start | bytes 3145732
  3.2 25.1 %copy-start.15 = (bf16[1024,512]{1,0:T(8,128)(2,1)S(1)}, bf16[1024,512]{1,0:T(8,128)(2,1)}, u32[]{:S(2)}) copy-start(bf16[1024,512]{1,0:T(8,128)(2,1)} %param.13) | copy-start | bytes 3145732
  4.2 91.2 %all-to-all-start = ((bf16[32,48,128]{2,1,0:T(8,128)(2,1)}), bf16[32,48,128]{2,1,0:T(8,128)(2,1)S(1)}, u32[]{:S(2)}, u32[]{:S(2)}) async-start(bf16[32,48,128]{2,1,0:T(8,128)(2,1)} %reshape.60), calls=%async_computation | async-start | bytes 786432 | tf_op jit(solution)/shard_map/all_to_all | solution.py:183
  22.4 64.8 %collective-permute-start.4 = (bf16[2048,256]{1,0:T(8,128)(2,1)S(1)}, bf16[2048,256]{1,0:T(8,128)(2,1)}, u32[]{:S(2)}, u32[]{:S(2)}) collective-permute-start(bf16[2048,256]{1,0:T(8,128)(2,1)S(1)} %copy-done.3), channel_id=1, source_target_pairs={{0,8},{8,0},{1,9},{9,1},{2,10},{10,2},{3,11},{11,3},{4,12},{12,4},... | collective-permute-start | bytes 3145736 | tf_op jit(solution)/shard_map/ppermute | solution.py:33
  25.2 64.3 %collective-permute-start.7 = (bf16[2048,256]{1,0:T(8,128)(2,1)}, bf16[2048,256]{1,0:T(8,128)(2,1)}, u32[]{:S(2)}, u32[]{:S(2)}) collective-permute-start(bf16[2048,256]{1,0:T(8,128)(2,1)} %refs_8_.1), channel_id=1, source_target_pairs={{0,8},{8,0},{1,9},{9,1},{2,10},{10,2},{3,11},{11,3},{4,12},{12,4},... | collective-permute-start | bytes 3145736 | tf_op jit(solution)/shard_map/ppermute | solution.py:33
  28.4 11.0 %collective-permute-start.9 = (bf16[256,512]{1,0:T(8,128)(2,1)S(1)}, bf16[256,512]{1,0:T(8,128)(2,1)S(1)}, u32[]{:S(2)}, u32[]{:S(2)}) collective-permute-start(bf16[256,512]{1,0:T(8,128)(2,1)S(1)} %get-tuple-element.14), channel_id=1, source_target_pairs={{0,2},{1,3},{2,0},{3,1},{4,6},{5,7},{6,4},{7,5},{8,10},{9,11},{10,... | collective-permute-start | bytes 786440 | tf_op jit(solution)/shard_map/ppermute | solution.py:24
  33.5 11.2 %collective-permute-start.13 = (bf16[256,512]{1,0:T(8,128)(2,1)S(1)}, bf16[256,512]{1,0:T(8,128)(2,1)S(1)}, u32[]{:S(2)}, u32[]{:S(2)}) collective-permute-start(bf16[256,512]{1,0:T(8,128)(2,1)S(1)} %get-tuple-element.13), channel_id=1, source_target_pairs={{0,3},{1,0},{2,1},{3,2},{4,7},{5,4},{6,5},{7,6},{8,11},{9,8},{10,9... | collective-permute-start | bytes 786440 | tf_op jit(solution)/shard_map/ppermute | solution.py:24
  36.5 10.9 %collective-permute-start.14 = (bf16[256,512]{1,0:T(8,128)(2,1)S(1)}, bf16[256,512]{1,0:T(8,128)(2,1)S(1)}, u32[]{:S(2)}, u32[]{:S(2)}) collective-permute-start(bf16[256,512]{1,0:T(8,128)(2,1)S(1)} %get-tuple-element.16), channel_id=1, source_target_pairs={{0,1},{1,2},{2,3},{3,0},{4,5},{5,6},{6,7},{7,4},{8,9},{9,10},{10,1... | collective-permute-start | bytes 786440 | tf_op jit(solution)/shard_map/ppermute | solution.py:24
  39.4 56.2 %collective-permute-start.3 = (bf16[2048,256]{1,0:T(8,128)(2,1)S(1)}, bf16[2048,256]{1,0:T(8,128)(2,1)}, u32[]{:S(2)}, u32[]{:S(2)}) collective-permute-start(bf16[2048,256]{1,0:T(8,128)(2,1)S(1)} %copy-done.3), channel_id=1, source_target_pairs={{0,4},{4,0},{1,5},{5,1},{2,6},{6,2},{3,7},{7,3},{8,12},{12,8},{9,1... | collective-permute-start | bytes 3145736 | tf_op jit(solution)/shard_map/ppermute | solution.py:33
  44.7 35.6 %collective-permute-start.11 = (bf16[256,512]{1,0:T(8,128)(2,1)S(1)}, bf16[256,512]{1,0:T(8,128)(2,1)S(1)}, u32[]{:S(2)}, u32[]{:S(2)}) collective-permute-start(bf16[256,512]{1,0:T(8,128)(2,1)S(1)} %collective-permute-done.9.refs_12_), channel_id=1, source_target_pairs={{0,8},{8,0},{1,9},{9,1},{2,10},{10,2},{3,11},{11,3},{4,12},{12,4},... | collective-permute-start | bytes 786440 | tf_op jit(solution)/shard_map/ppermute | solution.py:33
  47.4 51.6 %collective-permute-start.6 = (bf16[2048,256]{1,0:T(8,128)(2,1)}, bf16[2048,256]{1,0:T(8,128)(2,1)}, u32[]{:S(2)}, u32[]{:S(2)}) collective-permute-start(bf16[2048,256]{1,0:T(8,128)(2,1)} %refs_8_.1), channel_id=1, source_target_pairs={{0,4},{4,0},{1,5},{5,1},{2,6},{6,2},{3,7},{7,3},{8,12},{12,8},{9,1... | collective-permute-start | bytes 3145736 | tf_op jit(solution)/shard_map/ppermute | solution.py:33
  80.3 3.4 %collective-permute-start.10 = (bf16[256,512]{1,0:T(8,128)(2,1)S(1)}, bf16[256,512]{1,0:T(8,128)(2,1)S(1)}, u32[]{:S(2)}, u32[]{:S(2)}) collective-permute-start(bf16[256,512]{1,0:T(8,128)(2,1)S(1)} %collective-permute-done.9.refs_12_), channel_id=1, source_target_pairs={{0,4},{4,0},{1,5},{5,1},{2,6},{6,2},{3,7},{7,3},{8,12},{12,8},{9,1... | collective-permute-start | bytes 786440 | tf_op jit(solution)/shard_map/ppermute | solution.py:33
  82.2 0.7 copy-start.7
  83.7 0.8 copy-start.11
  84.5 7.2 %collective-permute-start.12 = (bf16[256,512]{1,0:T(8,128)(2,1)S(1)}, bf16[256,512]{1,0:T(8,128)(2,1)S(1)}, u32[]{:S(2)}, u32[]{:S(2)}) collective-permute-start(bf16[256,512]{1,0:T(8,128)(2,1)S(1)} %collective-permute-done.11.refs_14_), channel_id=1, source_target_pairs={{0,4},{4,0},{1,5},{5,1},{2,6},{6,2},{3,7},{7,3},{8,12},{12,8},{9,1... | collective-permute-start | bytes 786440 | tf_op jit(solution)/shard_map/ppermute | solution.py:33
  86.5 0.7 copy-start.9
  87.2 32.1 %collective-permute-start.5 = (bf16[2048,256]{1,0:T(8,128)(2,1)}, bf16[2048,256]{1,0:T(8,128)(2,1)}, u32[]{:S(2)}, u32[]{:S(2)}) collective-permute-start(bf16[2048,256]{1,0:T(8,128)(2,1)} %collective-permute-done.4.refs_6_), channel_id=1, source_target_pairs={{0,4},{4,0},{1,5},{5,1},{2,6},{6,2},{3,7},{7,3},{8,12},{12,8},{9,1... | collective-permute-start | bytes 3145736 | tf_op jit(solution)/shard_map/ppermute | solution.py:33
  89.5 29.8 %collective-permute-start.8 = (bf16[2048,256]{1,0:T(8,128)(2,1)}, bf16[2048,256]{1,0:T(8,128)(2,1)}, u32[]{:S(2)}, u32[]{:S(2)}) collective-permute-start(bf16[2048,256]{1,0:T(8,128)(2,1)} %collective-permute-done.7.refs_10_), channel_id=1, source_target_pairs={{0,4},{4,0},{1,5},{5,1},{2,6},{6,2},{3,7},{7,3},{8,12},{12,8},{9,1... | collective-permute-start | bytes 3145736 | tf_op jit(solution)/shard_map/ppermute | solution.py:33
  91.7 0.7 copy-start.13
  92.4 21.7 %collective-permute-start.16 = (bf16[3,256,512]{2,1,0:T(8,128)(2,1)S(1)}, bf16[3,256,512]{2,1,0:T(8,128)(2,1)S(1)}, u32[]{:S(2)}, u32[]{:S(2)}) collective-permute-start(bf16[3,256,512]{2,1,0:T(8,128)(2,1)S(1)} %pad_maximum_fusion.refs_0_), channel_id=1, source_target_pairs={{0,8},{8,0},{1,9},{9,1},{2,10},{10,2},{3,11},{11,3},{4,12},{12,4},... | collective-permute-start | bytes 2359304 | tf_op jit(solution)/shard_map/ppermute | solution.py:33
  95.6 11.4 %collective-permute-start = (bf16[96,2048]{1,0:T(8,128)(2,1)S(1)}, bf16[96,2048]{1,0:T(8,128)(2,1)}, u32[]{:S(2)}, u32[]{:S(2)}) collective-permute-start(bf16[96,2048]{1,0:T(8,128)(2,1)S(1)} %reshape.61.refs_0_), channel_id=1, source_target_pairs={{0,1},{1,2},{2,3},{3,0},{4,7},{5,4},{6,5},{7,6},{8,9},{9,10},{10,1... | collective-permute-start | bytes 1179656 | tf_op jit(solution)/shard_map/ppermute | solution.py:29
  99.1 17.0 %collective-permute-start.2 = (bf16[96,2048]{1,0:T(8,128)(2,1)S(1)}, bf16[96,2048]{1,0:T(8,128)(2,1)S(1)}, u32[]{:S(2)}, u32[]{:S(2)}) collective-permute-start(bf16[96,2048]{1,0:T(8,128)(2,1)S(1)} %reshape.61.refs_0_), channel_id=1, source_target_pairs={{0,3},{1,0},{2,1},{3,2},{4,5},{5,6},{6,7},{7,4},{8,11},{9,8},{10,9... | collective-permute-start | bytes 1179656 | tf_op jit(solution)/shard_map/ppermute | solution.py:29
  107.0 12.3 %collective-permute-start.1 = (bf16[96,2048]{1,0:T(8,128)(2,1)}, bf16[96,2048]{1,0:T(8,128)(2,1)}, u32[]{:S(2)}, u32[]{:S(2)}) collective-permute-start(bf16[96,2048]{1,0:T(8,128)(2,1)} %collective-permute-done.refs_1_), channel_id=1, source_target_pairs={{0,1},{1,2},{2,3},{3,0},{4,7},{5,4},{6,5},{7,6},{8,9},{9,10},{10,1... | collective-permute-start | bytes 1179656 | tf_op jit(solution)/shard_map/ppermute | solution.py:29
  114.1 23.5 %collective-permute-start.15 = (bf16[3,256,512]{2,1,0:T(8,128)(2,1)S(1)}, bf16[3,256,512]{2,1,0:T(8,128)(2,1)S(1)}, u32[]{:S(2)}, u32[]{:S(2)}) collective-permute-start(bf16[3,256,512]{2,1,0:T(8,128)(2,1)S(1)} %pad_maximum_fusion.refs_0_), channel_id=1, source_target_pairs={{0,4},{4,0},{1,5},{5,1},{2,6},{6,2},{3,7},{7,3},{8,12},{12,8},{9,1... | collective-permute-start | bytes 2359304 | tf_op jit(solution)/shard_map/ppermute | solution.py:33
  116.0 0.8 copy-start.5
  116.8 20.8 %collective-permute-start.17 = (bf16[3,256,512]{2,1,0:T(8,128)(2,1)S(1)}, bf16[3,256,512]{2,1,0:T(8,128)(2,1)S(1)}, u32[]{:S(2)}, u32[]{:S(2)}) collective-permute-start(bf16[3,256,512]{2,1,0:T(8,128)(2,1)S(1)} %collective-permute-done.16.refs_2_), channel_id=1, source_target_pairs={{0,4},{4,0},{1,5},{5,1},{2,6},{6,2},{3,7},{7,3},{8,12},{12,8},{9,1... | collective-permute-start | bytes 2359304 | tf_op jit(solution)/shard_map/ppermute | solution.py:33
  119.3 1.2 copy-start.4
  120.5 1.0 copy-start.6
  121.5 0.9 copy-start.8
  122.5 0.9 copy-start.10
  123.4 0.9 copy-start.12
  124.4 0.9 copy-start.14
  133.2 0.9 copy-start
  134.1 11.1 %collective-permute-start.19 = (bf16[384,512]{1,0:T(8,128)(2,1)}, bf16[384,512]{1,0:T(8,128)(2,1)S(1)}, u32[]{:S(2)}, u32[]{:S(2)}) collective-permute-start(bf16[384,512]{1,0:T(8,128)(2,1)} %get-tuple-element.12), channel_id=1, source_target_pairs={{0,1},{1,2},{2,3},{3,0},{4,7},{5,4},{6,5},{7,6},{8,9},{9,10},{10,1... | collective-permute-start | bytes 1179656 | tf_op jit(solution)/shard_map/ppermute | solution.py:29
  137.6 1.1 copy-start.1
  141.0 11.5 %collective-permute-start.18 = (bf16[384,512]{1,0:T(8,128)(2,1)S(1)}, bf16[384,512]{1,0:T(8,128)(2,1)S(1)}, u32[]{:S(2)}, u32[]{:S(2)}) collective-permute-start(bf16[384,512]{1,0:T(8,128)(2,1)S(1)} %get-tuple-element.10), channel_id=1, source_target_pairs={{0,3},{1,0},{2,1},{3,2},{4,5},{5,6},{6,7},{7,4},{8,11},{9,8},{10,9... | collective-permute-start | bytes 1179656 | tf_op jit(solution)/shard_map/ppermute | solution.py:29
  145.2 2.5 %copy-start.2 = (bf16[384,1024]{1,0:T(8,128)(2,1)S(1)}, bf16[384,1024]{1,0:T(8,128)(2,1)}, u32[]{:S(2)}) copy-start(bf16[384,1024]{1,0:T(8,128)(2,1)} %copy-done) | copy-start | bytes 2359300
  145.3 11.0 %collective-permute-start.20 = (bf16[384,512]{1,0:T(8,128)(2,1)S(1)}, bf16[384,512]{1,0:T(8,128)(2,1)S(1)}, u32[]{:S(2)}, u32[]{:S(2)}) collective-permute-start(bf16[384,512]{1,0:T(8,128)(2,1)S(1)} %add_convert_fusion.1), channel_id=1, source_target_pairs={{0,1},{1,2},{2,3},{3,0},{4,7},{5,4},{6,5},{7,6},{8,9},{9,10},{10,1... | collective-permute-start | bytes 1179656 | tf_op jit(solution)/shard_map/ppermute | solution.py:29
  158.1 39.9 %all-to-all-start.1 = ((bf16[32,48,128]{2,1,0:T(8,128)(2,1)}), bf16[32,48,128]{2,1,0:T(8,128)(2,1)S(1)}, u32[]{:S(2)}, u32[]{:S(2)}) async-start(bf16[32,48,128]{2,1,0:T(8,128)(2,1)} %reshape.63), calls=%async_computation.1 | async-start | bytes 786432 | tf_op jit(solution)/shard_map/all_to_all | solution.py:221
  172.1 0.7 copy-start.17

commit v11 on v10

--- a/solution.py
+++ b/solution.py
@@ -1,3 +1,5 @@
+import functools
+
 import jax
 import jax.numpy as jnp
 from jax import lax
@@ -51,8 +53,8 @@
     depth = wide.shape[2] // 2
     count = blocks[0].shape[0]
     moves, copies = [], []
-    for i, ahead in enumerate((0, -at_ref[1], 2, at_ref[1])):
-        place = pl.ds(pl.multiple_of(((at_ref[0] + ahead) & 3) * count, 16), count)
+    for i in range(4):
+        place = pl.ds(pl.multiple_of(((at_ref[0] + i) & 3) * count, 16), count)
         moves.append(pltpu.make_async_copy(blocks[i], rows.at[place], row_sems.at[i]))
     for i in range(4):
         gate_at, up_at = wide.at[i, :, pl.ds(0, depth)], wide.at[i, :, pl.ds(depth, depth)]
@@ -105,11 +107,12 @@
     )(at, *blocks, *gates, *uppers, *downs)
 
 
-def down_kernel(pick_ref, hidden_ref, *refs):
+def down_kernel(fixed, core_ref, hidden_ref, *refs):
     downs, outs, (tall, sems) = refs[:4], refs[4:-2], refs[-2:]
     depth = tall.shape[1]
+    picks = fixed or (1 - core_ref[0], core_ref[0])
     copies = [
-        pltpu.make_async_copy(downs[i].at[pick_ref[n]], tall.at[4 * n + i], sems.at[4 * n + i])
+        pltpu.make_async_copy(downs[i].at[picks[n]], tall.at[4 * n + i], sems.at[4 * n + i])
         for n in range(len(outs))
         for i in range(4)
     ]
@@ -123,11 +126,11 @@
         out[...] = total.astype(out.dtype)
 
 
-def run_down(picks, hidden, downs, dtypes):
+def run_down(fixed, core, hidden, downs, dtypes):
     count, parts = hidden.shape[0], len(dtypes)
     _, depth, out_width = downs[0].shape
     return pl.pallas_call(
-        down_kernel,
+        functools.partial(down_kernel, fixed),
         in_specs=[pl.BlockSpec(memory_space=pltpu.SMEM), pl.BlockSpec(memory_space=pltpu.VMEM)]
         + [pl.BlockSpec(memory_space=pl.ANY)] * 4,
         out_specs=[pl.BlockSpec(memory_space=pltpu.VMEM)] * parts,
@@ -143,7 +146,7 @@
         ),
         compiler_params=pltpu.CompilerParams(vmem_limit_bytes=12 << 20),
         name="down",
-    )(picks, hidden, *downs)
+    )(core, hidden, *downs)
 
 
 def layer(tokens, norm_gain, expert_ids, gate_weights, w_gate, w_up, w_down):
@@ -199,21 +202,19 @@
     gate_d = swap(gate_x, "c")
     up_d = swap(up_x, "c")
 
-    core = lax.axis_index("c").astype(jnp.int32)
-    ahead = around(near, 1)
-    behind = around(near, -1)
-    across = around(ahead, 1)
-    blocks = (near, ahead, across, behind)
+    lower_core = lax.axis_index("c") == 0
+    below = shift(near, 1)
+    above = shift(near, -1)
+    across = around(jnp.where(lower_core, below, above), 1)
+    blocks = (near, above, across, below)
     gates, uppers = (w_gate, gate_c, gate_x, gate_d), (w_up, up_c, up_x, up_d)
-    at = jnp.stack([y.astype(jnp.int32), 1 - 2 * core])
-    hidden, away = run_experts(at, blocks, gates, uppers, leads)
+    hidden, away = run_experts(y[None].astype(jnp.int32), blocks, gates, uppers, leads)
     middle = around(away, 1)
-    against, along = run_down(
-        jnp.stack([1 - core, core]), hidden, rests, (jnp.bfloat16, jnp.float32)
-    )
+    core = lax.axis_index("c").astype(jnp.int32)[None]
+    against, along = run_down((), core, hidden, rests, (jnp.bfloat16, jnp.float32))
     first = around(against, -1)
     second = around((along + middle.astype(jnp.float32)).astype(jnp.bfloat16), 1)
-    (total,) = run_down(jnp.full((1,), 2, jnp.int32), hidden, rests, (jnp.float32,))
+    (total,) = run_down((2,), core, hidden, rests, (jnp.float32,))
     total = total + first.astype(jnp.float32) + second.astype(jnp.float32)
     home = total.astype(jnp.bfloat16)
     home = home.reshape(4, expert_count, share, out_width).transpose(1, 0, 2, 3)

time: 201 us -> 199 us (0.990)
  local copies, waits for them, and re-layouts: 16.7 us -> 5.7 us
  waiting for transfers between devices: 75.9 us -> 86.3 us
    unnamed x38 -> x12, local copies, waits for them, and re-layouts: 12.9 us -> 1.93 us
    ppermute x12, waiting for transfers between devices: 35 us -> 45.4 us  [swap(): return lax.ppermute(block, axis, SWAP)]
    ppermute x3 -> x5, starting transfers between devices: 10.9 us -> 20.6 us  [shift(): return lax.ppermute(block, 'y', [(y, (y + by) % 4) for y in range(4)])]
    ppermute x6 -> x4, starting transfers between devices: 20.3 us -> 10.9 us  [around(): return lax.ppermute(block, ('c', 'y'), pairs)]
    ppermute x3 -> x5, waiting for transfers between devices: 3.38 us -> 8.05 us  [shift(): return lax.ppermute(block, 'y', [(y, (y + by) % 4) for y in range(4)])]
    all_to_all x1, waiting for transfers between devices: 24.7 us -> 21.4 us  [layer(): returned = lax.all_to_all(home, ('z', 'xh'), 0, 0, tiled=True)]
    ppermute x6 -> x4, waiting for transfers between devices: 12.7 us -> 11.4 us  [around(): return lax.ppermute(block, ('c', 'y'), pairs)]
  transfers between devices with their start and end apart: 23 -> 23, of which waited for: 9 -> 8; matrix products, arithmetic and copies ran while one was open for 1% -> 1% of each run, Pallas kernels for 5% -> 5%
where the time goes in v11:
time: 199 us; the launch traced here: 197 us
  starting transfers between devices  91.3 us (46%)
  waiting for transfers between devices  86.3 us (43%)
  Pallas kernels  9.61 us (5%)
  local copies, waits for them, and re-layouts  5.7 us (3%)
  matrix products  2.17 us (1%)
    ppermute x12, waiting for transfers between devices, swap(): return lax.ppermute(block, axis, SWAP)  45.4 us
    ppermute x12, starting transfers between devices, swap(): return lax.ppermute(block, axis, SWAP)  27.7 us
    all_to_all x1, waiting for transfers between devices, layer(): returned = lax.all_to_all(home, ('z', 'xh'), 0, 0, tiled=True)  21.4 us
    ppermute x5, starting transfers between devices, shift(): return lax.ppermute(block, 'y', [(y, (y + by) % 4) for y in range(4)])  20.6 us
    all_to_all x1, starting transfers between devices, layer(): arrived = lax.all_to_all(mine, ('z', 'xh'), 0, 0, tiled=True)  18.2 us
    all_to_all x1, starting transfers between devices, layer(): returned = lax.all_to_all(home, ('z', 'xh'), 0, 0, tiled=True)  13.9 us
    ppermute x4, waiting for transfers between devices, around(): return lax.ppermute(block, ('c', 'y'), pairs)  11.4 us
    ppermute x4, starting transfers between devices, around(): return lax.ppermute(block, ('c', 'y'), pairs)  10.9 us
  transfers between devices with their start and end apart: 23, of which 8 were waited for; matrix products, arithmetic and copies ran while one was open for 1% of the time, Pallas kernels for 5%

profile of v11, /device:TPU:6, one launch (start us, length us, event | category | flops | bytes accessed | tf_op | source)
XLA Modules:
  0.0 197.3 jit_solution(13849432015031990414)
XLA Ops:
  0.0 0.8 slice_bitcast_fusion.3
  0.8 1.2 fusion.1
  2.2 0.6 copy-done.5
  2.7 0.5 convolution_convert_fusion
  3.2 0.9 reshape.60
  4.2 18.2 %all-to-all-start = ((bf16[32,48,128]{2,1,0:T(8,128)(2,1)}), bf16[32,48,128]{2,1,0:T(8,128)(2,1)S(1)}, u32[]{:S(2)}, u32[]{:S(2)}) async-start(bf16[32,48,128]{2,1,0:T(8,128)(2,1)} %reshape.60), calls=%async_computation | async-start | bytes 786432 | tf_op jit(solution)/shard_map/all_to_all | solution.py:186
  22.4 2.7 %collective-permute-start.4 = (bf16[2048,256]{1,0:T(8,128)(2,1)}, bf16[2048,256]{1,0:T(8,128)(2,1)}, u32[]{:S(2)}, u32[]{:S(2)}) collective-permute-start(bf16[2048,256]{1,0:T(8,128)(2,1)} %refs_4_.1), channel_id=1, source_target_pairs={{0,8},{8,0},{1,9},{9,1},{2,10},{10,2},{3,11},{11,3},{4,12},{12,4},... | collective-permute-start | bytes 3145736 | tf_op jit(solution)/shard_map/ppermute | solution.py:35
  25.2 3.1 %collective-permute-start.7 = (bf16[2048,256]{1,0:T(8,128)(2,1)}, bf16[2048,256]{1,0:T(8,128)(2,1)}, u32[]{:S(2)}, u32[]{:S(2)}) collective-permute-start(bf16[2048,256]{1,0:T(8,128)(2,1)} %refs_8_.1), channel_id=1, source_target_pairs={{0,8},{8,0},{1,9},{9,1},{2,10},{10,2},{3,11},{11,3},{4,12},{12,4},... | collective-permute-start | bytes 3145736 | tf_op jit(solution)/shard_map/ppermute | solution.py:35
  28.4 5.1 %collective-permute-start.9 = (bf16[256,512]{1,0:T(8,128)(2,1)S(1)}, bf16[256,512]{1,0:T(8,128)(2,1)S(1)}, u32[]{:S(2)}, u32[]{:S(2)}) collective-permute-start(bf16[256,512]{1,0:T(8,128)(2,1)S(1)} %get-tuple-element.14), channel_id=1, source_target_pairs={{0,2},{1,3},{2,0},{3,1},{4,6},{5,7},{6,4},{7,5},{8,10},{9,11},{10,... | collective-permute-start | bytes 786440 | tf_op jit(solution)/shard_map/ppermute | solution.py:26
  33.5 3.0 %collective-permute-start.13 = (bf16[256,512]{1,0:T(8,128)(2,1)S(1)}, bf16[256,512]{1,0:T(8,128)(2,1)S(1)}, u32[]{:S(2)}, u32[]{:S(2)}) collective-permute-start(bf16[256,512]{1,0:T(8,128)(2,1)S(1)} %get-tuple-element.13), channel_id=1, source_target_pairs={{0,3},{1,0},{2,1},{3,2},{4,7},{5,4},{6,5},{7,6},{8,11},{9,8},{10,9... | collective-permute-start | bytes 786440 | tf_op jit(solution)/shard_map/ppermute | solution.py:26
  36.5 2.2 %collective-permute-done.9.refs_12_ = bf16[256,512]{1,0:T(8,128)(2,1)S(1)} collective-permute-done((bf16[256,512]{1,0:T(8,128)(2,1)S(1)}, bf16[256,512]{1,0:T(8,128)(2,1)S(1)}, u32[]{:S(2)}, u32[]{:S(2)}) %collective-permute-start.9) | collective-permute-done | bytes 262176 | tf_op jit(solution)/shard_map/ppermute | solution.py:26
  38.7 2.7 %collective-permute-start.11 = (bf16[256,512]{1,0:T(8,128)(2,1)S(1)}, bf16[256,512]{1,0:T(8,128)(2,1)S(1)}, u32[]{:S(2)}, u32[]{:S(2)}) collective-permute-start(bf16[256,512]{1,0:T(8,128)(2,1)S(1)} %collective-permute-done.9.refs_12_), channel_id=1, source_target_pairs={{0,8},{8,0},{1,9},{9,1},{2,10},{10,2},{3,11},{11,3},{4,12},{12,4},... | collective-permute-start | bytes 786440 | tf_op jit(solution)/shard_map/ppermute | solution.py:35
  41.4 5.7 %collective-permute-start.14 = (bf16[256,512]{1,0:T(8,128)(2,1)S(1)}, bf16[256,512]{1,0:T(8,128)(2,1)S(1)}, u32[]{:S(2)}, u32[]{:S(2)}) collective-permute-start(bf16[256,512]{1,0:T(8,128)(2,1)S(1)} %get-tuple-element.16), channel_id=1, source_target_pairs={{0,1},{1,2},{2,3},{3,0},{4,5},{5,6},{6,7},{7,4},{8,9},{9,10},{10,1... | collective-permute-start | bytes 786440 | tf_op jit(solution)/shard_map/ppermute | solution.py:26
  47.2 1.9 collective-permute-start.10
  49.1 31.4 %collective-permute-done.11.refs_14_ = bf16[256,512]{1,0:T(8,128)(2,1)S(1)} collective-permute-done((bf16[256,512]{1,0:T(8,128)(2,1)S(1)}, bf16[256,512]{1,0:T(8,128)(2,1)S(1)}, u32[]{:S(2)}, u32[]{:S(2)}) %collective-permute-start.11) | collective-permute-done | bytes 262176 | tf_op jit(solution)/shard_map/ppermute | solution.py:35
  80.5 1.9 collective-permute-start.12
  82.6 4.9 %collective-permute-start = (bf16[96,2048]{1,0:T(8,128)(2,1)S(1)}, bf16[96,2048]{1,0:T(8,128)(2,1)S(1)}, u32[]{:S(2)}, u32[]{:S(2)}) collective-permute-start(bf16[96,2048]{1,0:T(8,128)(2,1)S(1)} %reshape.61.refs_0_), channel_id=1, source_target_pairs={{0,3},{1,0},{2,1},{3,2},{4,7},{5,4},{6,5},{7,6},{8,11},{9,8},{10,9... | collective-permute-start | bytes 1179656 | tf_op jit(solution)/shard_map/ppermute | solution.py:26
  87.5 2.1 %collective-permute-start.3 = (bf16[2048,256]{1,0:T(8,128)(2,1)}, bf16[2048,256]{1,0:T(8,128)(2,1)}, u32[]{:S(2)}, u32[]{:S(2)}) collective-permute-start(bf16[2048,256]{1,0:T(8,128)(2,1)} %refs_4_.1), channel_id=1, source_target_pairs={{0,4},{4,0},{1,5},{5,1},{2,6},{6,2},{3,7},{7,3},{8,12},{12,8},{9,1... | collective-permute-start | bytes 3145736 | tf_op jit(solution)/shard_map/ppermute | solution.py:35
  89.7 0.7 copy-done
  90.4 1.9 collective-permute-start.1
  92.3 2.2 %collective-permute-start.6 = (bf16[2048,256]{1,0:T(8,128)(2,1)}, bf16[2048,256]{1,0:T(8,128)(2,1)}, u32[]{:S(2)}, u32[]{:S(2)}) collective-permute-start(bf16[2048,256]{1,0:T(8,128)(2,1)} %refs_8_.1), channel_id=1, source_target_pairs={{0,4},{4,0},{1,5},{5,1},{2,6},{6,2},{3,7},{7,3},{8,12},{12,8},{9,1... | collective-permute-start | bytes 3145736 | tf_op jit(solution)/shard_map/ppermute | solution.py:35
  94.6 2.1 %collective-permute-start.5 = (bf16[2048,256]{1,0:T(8,128)(2,1)}, bf16[2048,256]{1,0:T(8,128)(2,1)}, u32[]{:S(2)}, u32[]{:S(2)}) collective-permute-start(bf16[2048,256]{1,0:T(8,128)(2,1)} %collective-permute-done.4.refs_6_), channel_id=1, source_target_pairs={{0,4},{4,0},{1,5},{5,1},{2,6},{6,2},{3,7},{7,3},{8,12},{12,8},{9,1... | collective-permute-start | bytes 3145736 | tf_op jit(solution)/shard_map/ppermute | solution.py:35
  96.7 2.2 %collective-permute-start.8 = (bf16[2048,256]{1,0:T(8,128)(2,1)}, bf16[2048,256]{1,0:T(8,128)(2,1)}, u32[]{:S(2)}, u32[]{:S(2)}) collective-permute-start(bf16[2048,256]{1,0:T(8,128)(2,1)} %collective-permute-done.7.refs_10_), channel_id=1, source_target_pairs={{0,4},{4,0},{1,5},{5,1},{2,6},{6,2},{3,7},{7,3},{8,12},{12,8},{9,1... | collective-permute-start | bytes 3145736 | tf_op jit(solution)/shard_map/ppermute | solution.py:35
  99.0 5.8 %collective-permute-done.1.refs_3_ = bf16[96,2048]{1,0:T(8,128)(2,1)S(1)} collective-permute-done((bf16[96,2048]{1,0:T(8,128)(2,1)S(1)}, bf16[96,2048]{1,0:T(8,128)(2,1)S(1)}, u32[]{:S(2)}, u32[]{:S(2)}) %collective-permute-start.1) | collective-permute-done | bytes 393248 | tf_op jit(solution)/shard_map/ppermute | solution.py:26
  104.8 2.8 %collective-permute-start.16 = (bf16[3,256,512]{2,1,0:T(8,128)(2,1)S(1)}, bf16[3,256,512]{2,1,0:T(8,128)(2,1)S(1)}, u32[]{:S(2)}, u32[]{:S(2)}) collective-permute-start(bf16[3,256,512]{2,1,0:T(8,128)(2,1)S(1)} %pad_maximum_fusion.refs_0_), channel_id=1, source_target_pairs={{0,8},{8,0},{1,9},{9,1},{2,10},{10,2},{3,11},{11,3},{4,12},{12,4},... | collective-permute-start | bytes 2359304 | tf_op jit(solution)/shard_map/ppermute | solution.py:35
  107.7 1.9 collective-permute-start.2
  109.6 1.9 collective-permute-start.15
  111.5 14.0 %collective-permute-done.16.refs_2_ = bf16[3,256,512]{2,1,0:T(8,128)(2,1)S(1)} collective-permute-done((bf16[3,256,512]{2,1,0:T(8,128)(2,1)S(1)}, bf16[3,256,512]{2,1,0:T(8,128)(2,1)S(1)}, u32[]{:S(2)}, u32[]{:S(2)}) %collective-permute-start.16) | collective-permute-done | bytes 786464 | tf_op jit(solution)/shard_map/ppermute | solution.py:35
  125.6 1.9 collective-permute-start.17
  127.5 7.1 %experts.1 = (bf16[384,1024]{1,0:T(8,128)(2,1)S(1)}, bf16[384,512]{1,0:T(8,128)(2,1)S(1)}) custom-call(s32[1]{0:T(128)} %bitcast.5.at_ref, bf16[96,2048]{1,0:T(8,128)(2,1)S(1)} %reshape.61.refs_0_, bf16[96,2048]{1,0:T(8,128)(2,1)S(1)} %collective-permute-done.refs_1_, bf16[96,2048]{1,0:T(8,128)(2,1)S(1)} %collective-permute-done.2.refs_2_, ...), custom_call_target="tpu_custom_call" | custom-call | flops 3221225472 | bytes 8388608 | tf_op jit(solution)/shard_map/experts/pallas_call | solution.py:84
  134.7 1.9 collective-permute-start.19
  136.6 1.6 down.3
  138.3 5.1 %collective-permute-start.18 = (bf16[384,512]{1,0:T(8,128)(2,1)S(1)}, bf16[384,512]{1,0:T(8,128)(2,1)S(1)}, u32[]{:S(2)}, u32[]{:S(2)}) collective-permute-start(bf16[384,512]{1,0:T(8,128)(2,1)S(1)} %get-tuple-element.10), channel_id=1, source_target_pairs={{0,3},{1,0},{2,1},{3,2},{4,5},{5,6},{6,7},{7,4},{8,11},{9,8},{10,9... | collective-permute-start | bytes 1179656 | tf_op jit(solution)/shard_map/ppermute | solution.py:31
  143.4 3.3 %collective-permute-done.19 = bf16[384,512]{1,0:T(8,128)(2,1)S(1)} collective-permute-done((bf16[384,512]{1,0:T(8,128)(2,1)S(1)}, bf16[384,512]{1,0:T(8,128)(2,1)S(1)}, u32[]{:S(2)}, u32[]{:S(2)}) %collective-permute-start.19) | collective-permute-done | bytes 393248 | tf_op jit(solution)/shard_map/ppermute | solution.py:31
  146.8 1.9 collective-permute-start.20
  148.7 0.8 down.2
  149.6 0.5 collective-permute-done.18
  150.0 7.6 %collective-permute-done.20 = bf16[384,512]{1,0:T(8,128)(2,1)S(1)} collective-permute-done((bf16[384,512]{1,0:T(8,128)(2,1)S(1)}, bf16[384,512]{1,0:T(8,128)(2,1)S(1)}, u32[]{:S(2)}, u32[]{:S(2)}) %collective-permute-start.20) | collective-permute-done | bytes 393248 | tf_op jit(solution)/shard_map/ppermute | solution.py:31
  157.8 0.2 reshape.62
  158.1 0.3 copy.8
  158.3 1.1 reshape.63
  159.4 13.9 %all-to-all-start.1 = ((bf16[32,48,128]{2,1,0:T(8,128)(2,1)}), bf16[32,48,128]{2,1,0:T(8,128)(2,1)S(1)}, u32[]{:S(2)}, u32[]{:S(2)}) async-start(bf16[32,48,128]{2,1,0:T(8,128)(2,1)} %reshape.63), calls=%async_computation.1 | async-start | bytes 786432 | tf_op jit(solution)/shard_map/all_to_all | solution.py:222
  173.4 0.7 copy-done.4
  174.1 0.2 convolution_compare_fusion
  174.3 0.3 convolution_select_fusion
  174.6 21.4 %all-to-all-done.1 = bf16[32,48,128]{2,1,0:T(8,128)(2,1)S(1)} async-done(((bf16[32,48,128]{2,1,0:T(8,128)(2,1)}), bf16[32,48,128]{2,1,0:T(8,128)(2,1)S(1)}, u32[]{:S(2)}, u32[]{:S(2)}) %all-to-all-start.1) | async-done | bytes 393248 | tf_op jit(solution)/shard_map/all_to_all | solution.py:222
  196.0 0.2 reshape.64
  196.3 1.0 convolution_convert_fusion.1
  (39 shorter events, 0.9 us)
Async XLA Ops:
  0.0 2.2 %copy-start.3 = (bf16[128,2048]{1,0:T(8,128)(2,1)S(1)}, bf16[128,2048]{1,0:T(8,128)(2,1)}, u32[]{:S(2)}) copy-start(bf16[128,2048]{1,0:T(8,128)(2,1)} %param.7) | copy-start | bytes 1572868
  2.0 0.7 copy-start.5
  3.2 25.1 %copy-start.2 = (bf16[1024,512]{1,0:T(8,128)(2,1)S(1)}, bf16[1024,512]{1,0:T(8,128)(2,1)}, u32[]{:S(2)}) copy-start(bf16[1024,512]{1,0:T(8,128)(2,1)} %param.13) | copy-start | bytes 3145732
  4.2 78.2 %all-to-all-start = ((bf16[32,48,128]{2,1,0:T(8,128)(2,1)}), bf16[32,48,128]{2,1,0:T(8,128)(2,1)S(1)}, u32[]{:S(2)}, u32[]{:S(2)}) async-start(bf16[32,48,128]{2,1,0:T(8,128)(2,1)} %reshape.60), calls=%async_computation | async-start | bytes 786432 | tf_op jit(solution)/shard_map/all_to_all | solution.py:186
  22.4 69.9 %collective-permute-start.4 = (bf16[2048,256]{1,0:T(8,128)(2,1)}, bf16[2048,256]{1,0:T(8,128)(2,1)}, u32[]{:S(2)}, u32[]{:S(2)}) collective-permute-start(bf16[2048,256]{1,0:T(8,128)(2,1)} %refs_4_.1), channel_id=1, source_target_pairs={{0,8},{8,0},{1,9},{9,1},{2,10},{10,2},{3,11},{11,3},{4,12},{12,4},... | collective-permute-start | bytes 3145736 | tf_op jit(solution)/shard_map/ppermute | solution.py:35
  25.2 69.4 %collective-permute-start.7 = (bf16[2048,256]{1,0:T(8,128)(2,1)}, bf16[2048,256]{1,0:T(8,128)(2,1)}, u32[]{:S(2)}, u32[]{:S(2)}) collective-permute-start(bf16[2048,256]{1,0:T(8,128)(2,1)} %refs_8_.1), channel_id=1, source_target_pairs={{0,8},{8,0},{1,9},{9,1},{2,10},{10,2},{3,11},{11,3},{4,12},{12,4},... | collective-permute-start | bytes 3145736 | tf_op jit(solution)/shard_map/ppermute | solution.py:35
  28.4 10.3 %collective-permute-start.9 = (bf16[256,512]{1,0:T(8,128)(2,1)S(1)}, bf16[256,512]{1,0:T(8,128)(2,1)S(1)}, u32[]{:S(2)}, u32[]{:S(2)}) collective-permute-start(bf16[256,512]{1,0:T(8,128)(2,1)S(1)} %get-tuple-element.14), channel_id=1, source_target_pairs={{0,2},{1,3},{2,0},{3,1},{4,6},{5,7},{6,4},{7,5},{8,10},{9,11},{10,... | collective-permute-start | bytes 786440 | tf_op jit(solution)/shard_map/ppermute | solution.py:26
  33.5 13.7 %collective-permute-start.13 = (bf16[256,512]{1,0:T(8,128)(2,1)S(1)}, bf16[256,512]{1,0:T(8,128)(2,1)S(1)}, u32[]{:S(2)}, u32[]{:S(2)}) collective-permute-start(bf16[256,512]{1,0:T(8,128)(2,1)S(1)} %get-tuple-element.13), channel_id=1, source_target_pairs={{0,3},{1,0},{2,1},{3,2},{4,7},{5,4},{6,5},{7,6},{8,11},{9,8},{10,9... | collective-permute-start | bytes 786440 | tf_op jit(solution)/shard_map/ppermute | solution.py:26
  38.7 41.8 %collective-permute-start.11 = (bf16[256,512]{1,0:T(8,128)(2,1)S(1)}, bf16[256,512]{1,0:T(8,128)(2,1)S(1)}, u32[]{:S(2)}, u32[]{:S(2)}) collective-permute-start(bf16[256,512]{1,0:T(8,128)(2,1)S(1)} %collective-permute-done.9.refs_12_), channel_id=1, source_target_pairs={{0,8},{8,0},{1,9},{9,1},{2,10},{10,2},{3,11},{11,3},{4,12},{12,4},... | collective-permute-start | bytes 786440 | tf_op jit(solution)/shard_map/ppermute | solution.py:35
  41.4 41.2 %collective-permute-start.14 = (bf16[256,512]{1,0:T(8,128)(2,1)S(1)}, bf16[256,512]{1,0:T(8,128)(2,1)S(1)}, u32[]{:S(2)}, u32[]{:S(2)}) collective-permute-start(bf16[256,512]{1,0:T(8,128)(2,1)S(1)} %get-tuple-element.16), channel_id=1, source_target_pairs={{0,1},{1,2},{2,3},{3,0},{4,5},{5,6},{6,7},{7,4},{8,9},{9,10},{10,1... | collective-permute-start | bytes 786440 | tf_op jit(solution)/shard_map/ppermute | solution.py:26
  47.2 40.3 %collective-permute-start.10 = (bf16[256,512]{1,0:T(8,128)(2,1)S(1)}, bf16[256,512]{1,0:T(8,128)(2,1)S(1)}, u32[]{:S(2)}, u32[]{:S(2)}) collective-permute-start(bf16[256,512]{1,0:T(8,128)(2,1)S(1)} %collective-permute-done.9.refs_12_), channel_id=1, source_target_pairs={{0,4},{4,0},{1,5},{5,1},{2,6},{6,2},{3,7},{7,3},{8,12},{12,8},{9,1... | collective-permute-start | bytes 786440 | tf_op jit(solution)/shard_map/ppermute | solution.py:35
  80.5 9.2 %collective-permute-start.12 = (bf16[256,512]{1,0:T(8,128)(2,1)S(1)}, bf16[256,512]{1,0:T(8,128)(2,1)S(1)}, u32[]{:S(2)}, u32[]{:S(2)}) collective-permute-start(bf16[256,512]{1,0:T(8,128)(2,1)S(1)} %collective-permute-done.11.refs_14_), channel_id=1, source_target_pairs={{0,4},{4,0},{1,5},{5,1},{2,6},{6,2},{3,7},{7,3},{8,12},{12,8},{9,1... | collective-permute-start | bytes 786440 | tf_op jit(solution)/shard_map/ppermute | solution.py:35
  82.6 14.1 %collective-permute-start = (bf16[96,2048]{1,0:T(8,128)(2,1)S(1)}, bf16[96,2048]{1,0:T(8,128)(2,1)S(1)}, u32[]{:S(2)}, u32[]{:S(2)}) collective-permute-start(bf16[96,2048]{1,0:T(8,128)(2,1)S(1)} %reshape.61.refs_0_), channel_id=1, source_target_pairs={{0,3},{1,0},{2,1},{3,2},{4,7},{5,4},{6,5},{7,6},{8,11},{9,8},{10,9... | collective-permute-start | bytes 1179656 | tf_op jit(solution)/shard_map/ppermute | solution.py:26
  87.5 20.1 %collective-permute-start.3 = (bf16[2048,256]{1,0:T(8,128)(2,1)}, bf16[2048,256]{1,0:T(8,128)(2,1)}, u32[]{:S(2)}, u32[]{:S(2)}) collective-permute-start(bf16[2048,256]{1,0:T(8,128)(2,1)} %refs_4_.1), channel_id=1, source_target_pairs={{0,4},{4,0},{1,5},{5,1},{2,6},{6,2},{3,7},{7,3},{8,12},{12,8},{9,1... | collective-permute-start | bytes 3145736 | tf_op jit(solution)/shard_map/ppermute | solution.py:35
  89.7 0.7 copy-start
  90.4 14.4 %collective-permute-start.1 = (bf16[96,2048]{1,0:T(8,128)(2,1)S(1)}, bf16[96,2048]{1,0:T(8,128)(2,1)S(1)}, u32[]{:S(2)}, u32[]{:S(2)}) collective-permute-start(bf16[96,2048]{1,0:T(8,128)(2,1)S(1)} %reshape.61.refs_0_), channel_id=1, source_target_pairs={{0,1},{1,2},{2,3},{3,0},{4,5},{5,6},{6,7},{7,4},{8,9},{9,10},{10,1... | collective-permute-start | bytes 1179656 | tf_op jit(solution)/shard_map/ppermute | solution.py:26
  92.3 17.3 %collective-permute-start.6 = (bf16[2048,256]{1,0:T(8,128)(2,1)}, bf16[2048,256]{1,0:T(8,128)(2,1)}, u32[]{:S(2)}, u32[]{:S(2)}) collective-permute-start(bf16[2048,256]{1,0:T(8,128)(2,1)} %refs_8_.1), channel_id=1, source_target_pairs={{0,4},{4,0},{1,5},{5,1},{2,6},{6,2},{3,7},{7,3},{8,12},{12,8},{9,1... | collective-permute-start | bytes 3145736 | tf_op jit(solution)/shard_map/ppermute | solution.py:35
  94.6 32.9 %collective-permute-start.5 = (bf16[2048,256]{1,0:T(8,128)(2,1)}, bf16[2048,256]{1,0:T(8,128)(2,1)}, u32[]{:S(2)}, u32[]{:S(2)}) collective-permute-start(bf16[2048,256]{1,0:T(8,128)(2,1)} %collective-permute-done.4.refs_6_), channel_id=1, source_target_pairs={{0,4},{4,0},{1,5},{5,1},{2,6},{6,2},{3,7},{7,3},{8,12},{12,8},{9,1... | collective-permute-start | bytes 3145736 | tf_op jit(solution)/shard_map/ppermute | solution.py:35
  96.7 30.8 %collective-permute-start.8 = (bf16[2048,256]{1,0:T(8,128)(2,1)}, bf16[2048,256]{1,0:T(8,128)(2,1)}, u32[]{:S(2)}, u32[]{:S(2)}) collective-permute-start(bf16[2048,256]{1,0:T(8,128)(2,1)} %collective-permute-done.7.refs_10_), channel_id=1, source_target_pairs={{0,4},{4,0},{1,5},{5,1},{2,6},{6,2},{3,7},{7,3},{8,12},{12,8},{9,1... | collective-permute-start | bytes 3145736 | tf_op jit(solution)/shard_map/ppermute | solution.py:35
  104.8 20.8 %collective-permute-start.16 = (bf16[3,256,512]{2,1,0:T(8,128)(2,1)S(1)}, bf16[3,256,512]{2,1,0:T(8,128)(2,1)S(1)}, u32[]{:S(2)}, u32[]{:S(2)}) collective-permute-start(bf16[3,256,512]{2,1,0:T(8,128)(2,1)S(1)} %pad_maximum_fusion.refs_0_), channel_id=1, source_target_pairs={{0,8},{8,0},{1,9},{9,1},{2,10},{10,2},{3,11},{11,3},{4,12},{12,4},... | collective-permute-start | bytes 2359304 | tf_op jit(solution)/shard_map/ppermute | solution.py:35
  107.6 19.9 %copy-start.1 = (bf16[256,512]{1,0:T(8,128)(2,1)S(1)}, bf16[256,512]{1,0:T(8,128)(2,1)}, u32[]{:S(2)}) copy-start(bf16[256,512]{1,0:T(8,128)(2,1)} %copy-done) | copy-start | bytes 786436
  107.7 19.8 %collective-permute-start.2 = (bf16[96,2048]{1,0:T(8,128)(2,1)S(1)}, bf16[96,2048]{1,0:T(8,128)(2,1)S(1)}, u32[]{:S(2)}, u32[]{:S(2)}) collective-permute-start(bf16[96,2048]{1,0:T(8,128)(2,1)S(1)} %broadcast_select_fusion), channel_id=1, source_target_pairs={{0,1},{1,2},{2,3},{3,0},{4,7},{5,4},{6,5},{7,6},{8,9},{9,10},{10,1... | collective-permute-start | bytes 1179656 | tf_op jit(solution)/shard_map/ppermute | solution.py:31
  109.6 27.0 %collective-permute-start.15 = (bf16[3,256,512]{2,1,0:T(8,128)(2,1)S(1)}, bf16[3,256,512]{2,1,0:T(8,128)(2,1)S(1)}, u32[]{:S(2)}, u32[]{:S(2)}) collective-permute-start(bf16[3,256,512]{2,1,0:T(8,128)(2,1)S(1)} %pad_maximum_fusion.refs_0_), channel_id=1, source_target_pairs={{0,4},{4,0},{1,5},{5,1},{2,6},{6,2},{3,7},{7,3},{8,12},{12,8},{9,1... | collective-permute-start | bytes 2359304 | tf_op jit(solution)/shard_map/ppermute | solution.py:35
  125.6 11.1 %collective-permute-start.17 = (bf16[3,256,512]{2,1,0:T(8,128)(2,1)S(1)}, bf16[3,256,512]{2,1,0:T(8,128)(2,1)S(1)}, u32[]{:S(2)}, u32[]{:S(2)}) collective-permute-start(bf16[3,256,512]{2,1,0:T(8,128)(2,1)S(1)} %collective-permute-done.16.refs_2_), channel_id=1, source_target_pairs={{0,4},{4,0},{1,5},{5,1},{2,6},{6,2},{3,7},{7,3},{8,12},{12,8},{9,1... | collective-permute-start | bytes 2359304 | tf_op jit(solution)/shard_map/ppermute | solution.py:35
  134.7 12.0 %collective-permute-start.19 = (bf16[384,512]{1,0:T(8,128)(2,1)S(1)}, bf16[384,512]{1,0:T(8,128)(2,1)S(1)}, u32[]{:S(2)}, u32[]{:S(2)}) collective-permute-start(bf16[384,512]{1,0:T(8,128)(2,1)S(1)} %get-tuple-element.12), channel_id=1, source_target_pairs={{0,1},{1,2},{2,3},{3,0},{4,7},{5,4},{6,5},{7,6},{8,9},{9,10},{10,1... | collective-permute-start | bytes 1179656 | tf_op jit(solution)/shard_map/ppermute | solution.py:31
  138.3 11.8 %collective-permute-start.18 = (bf16[384,512]{1,0:T(8,128)(2,1)S(1)}, bf16[384,512]{1,0:T(8,128)(2,1)S(1)}, u32[]{:S(2)}, u32[]{:S(2)}) collective-permute-start(bf16[384,512]{1,0:T(8,128)(2,1)S(1)} %get-tuple-element.10), channel_id=1, source_target_pairs={{0,3},{1,0},{2,1},{3,2},{4,5},{5,6},{6,7},{7,4},{8,11},{9,8},{10,9... | collective-permute-start | bytes 1179656 | tf_op jit(solution)/shard_map/ppermute | solution.py:31
  146.8 10.9 %collective-permute-start.20 = (bf16[384,512]{1,0:T(8,128)(2,1)S(1)}, bf16[384,512]{1,0:T(8,128)(2,1)S(1)}, u32[]{:S(2)}, u32[]{:S(2)}) collective-permute-start(bf16[384,512]{1,0:T(8,128)(2,1)S(1)} %add_convert_fusion.1), channel_id=1, source_target_pairs={{0,1},{1,2},{2,3},{3,0},{4,7},{5,4},{6,5},{7,6},{8,9},{9,10},{10,1... | collective-permute-start | bytes 1179656 | tf_op jit(solution)/shard_map/ppermute | solution.py:31
  159.4 36.6 %all-to-all-start.1 = ((bf16[32,48,128]{2,1,0:T(8,128)(2,1)}), bf16[32,48,128]{2,1,0:T(8,128)(2,1)S(1)}, u32[]{:S(2)}, u32[]{:S(2)}) async-start(bf16[32,48,128]{2,1,0:T(8,128)(2,1)} %reshape.63), calls=%async_computation.1 | async-start | bytes 786432 | tf_op jit(solution)/shard_map/all_to_all | solution.py:222
  173.4 0.7 copy-start.4
